TPU v7x, 128 devices: a whole 4x4x4 slice. The times are simulated.
128 devices in a mesh: kv: 16 (over z, x), tp: 8 (over y, core).
Axes of the slice: x: 4, y: 4, z: 4, core: 2. Of those that a mesh axis runs over, the one named last changes fastest.
Arguments:
- tokens: bfloat16 [64, 2048], P(None, 'kv'), may hold values from -6 to 6
- token_gain: float32 [2048], P('kv'), may hold values from 0.1 to 1.9
- w_query: bfloat16 [2048, 1536], P('kv', 'tp'), may hold values from -0.125 to 0.125
- w_down_kv: bfloat16 [2048, 512], P('kv'), may hold values from -0.125 to 0.125
- w_rope_key: bfloat16 [2048, 64], P('kv'), may hold values from -0.125 to 0.125
- latent_gain: float32 [512], replicated, may hold values from 0.1 to 1.9
- w_key_up: bfloat16 [8, 512, 128], P('tp'), may hold values from -0.25 to 0.25
- w_value_up: bfloat16 [8, 512, 128], P('tp'), may hold values from -0.25 to 0.25
- w_out: bfloat16 [1024, 2048], P('tp', 'kv'), may hold values from -0.1875 to 0.1875
- out_gain: float32 [2048], P('kv'), may hold values from 0.1 to 1.9
- cache_latent: bfloat16 [64, 8192, 512], P('tp', 'kv'), may hold values from -6 to 6
- cache_rope: bfloat16 [64, 8192, 64], P('tp', 'kv'), may hold values from -6 to 6
- lengths: int32 [64], replicated, may hold values from 1 to 8191, as said below
Outputs:
- mixed: bfloat16 [64, 2048], P(None, 'kv')
Inputs may be any that keep to these rules, and one draw needn't show every extreme that they name: `lengths`: each of the 64 sequences has 1 to 8191 cached positions; some sequence has exactly 8191 and some exactly 1.
All inputs are finite; a program needn't handle non-finite values.
Results may differ from a plain program's by a relative error of at most 0.015.
Values may be sent and summed in bfloat16 or wider, within the bound.
No kernel may reach another device: no remote copies, remote signals or barrier semaphores. Data moves between devices by JAX's collectives and lax.ppermute only.
A program may use at most 64 MiB of HBM per device.

v0:
```python
import functools

import jax
import jax.numpy as jnp
from jax import lax
from jax.sharding import Mesh
from jax.sharding import PartitionSpec as P

KV = ("kv_0", "kv_1")


EPSILON = 1e-06
NEGATIVE = -1e30


def over_pieces(value, axis):
    parts = lax.all_gather(value, axis)
    return parts.sum(axis=0)


def by_axis(value, axes):
    return functools.reduce(lax.pmax, axes, value)


def over_axes(value, axes):
    for axis in axes:
        value = lax.psum(value, axis)
    return value


def rotate_half(values, cosine, sine_table):
    half_width = values.shape[-1] // 2
    lower_half = values[..., :half_width]
    upper_half = values[..., half_width:]
    return jnp.concatenate(
        [
            lower_half * cosine - upper_half * sine_table,
            upper_half * cosine + lower_half * sine_table,
        ],
        axis=-1,
    )


def angle_tables(lengths, rope_width):
    inverse_freq = 1.0 / 10000.0 ** (jnp.arange(0, rope_width, 2, dtype=jnp.float32) / rope_width)
    angles = lengths.astype(jnp.float32)[:, None] * inverse_freq[None, :]
    return (jnp.cos(angles), jnp.sin(angles))


def on_device(
    tokens,
    token_gain,
    w_query,
    w_down_kv,
    w_rope_key,
    latent_gain,
    w_key_up,
    w_value_up,
    w_out,
    out_gain,
    cache_latent,
    cache_rope,
    lengths,
):
    model_width = tokens.shape[1] * lax.axis_size(KV)
    seq_count = tokens.shape[0]
    local_heads, latent_width, nope_width = w_key_up.shape
    rope_width = w_rope_key.shape[1]
    head_width = nope_width + rope_width
    factor = head_width ** (-0.5)
    token_values = tokens.astype(jnp.float32)
    scaled = (token_values * token_gain).astype(jnp.bfloat16)
    query_part = jnp.dot(scaled, w_query, preferred_element_type=jnp.float32)
    latent_part = jnp.dot(scaled, w_down_kv, preferred_element_type=jnp.float32)
    rope_part = jnp.dot(scaled, w_rope_key, preferred_element_type=jnp.float32)
    query_raw, latent_raw, rope_raw = (
        over_pieces(query_part, KV),
        over_pieces(latent_part, KV),
        over_pieces(rope_part, KV),
    )
    query_heads = query_raw.astype(jnp.bfloat16).reshape(seq_count, local_heads, head_width)
    latent = (
        latent_raw
        * lax.rsqrt(jnp.mean(latent_raw * latent_raw, axis=1, keepdims=True) + EPSILON)
        * latent_gain
    ).astype(jnp.bfloat16)
    cosine, sine_table = angle_tables(lengths, rope_width)
    new_rope = rotate_half(rope_raw, cosine, sine_table).astype(jnp.bfloat16)
    query_nope = query_heads[..., :nope_width]
    query_rope = rotate_half(
        query_heads[..., nope_width:].astype(jnp.float32),
        cosine[:, None, :],
        sine_table[:, None, :],
    ).astype(jnp.bfloat16)
    query_latent = jnp.einsum(
        "bhn,hcn->bhc", query_nope, w_key_up, preferred_element_type=jnp.float32
    ).astype(jnp.bfloat16)
    seq_latent, seq_rope = (
        lax.all_to_all(query_latent, "tp", split_axis=0, concat_axis=1, tiled=True),
        lax.all_to_all(query_rope, "tp", split_axis=0, concat_axis=1, tiled=True),
    )
    local_seqs = cache_latent.shape[0]
    local_pos = cache_latent.shape[1]
    first_row = lax.axis_index("tp") * local_seqs
    own_latent = lax.dynamic_slice_in_dim(latent, first_row, local_seqs, 0)
    own_rope = lax.dynamic_slice_in_dim(new_rope, first_row, local_seqs, 0)
    own_length = lax.dynamic_slice_in_dim(lengths, first_row, local_seqs, 0)
    first_pos = lax.axis_index(KV) * local_pos
    positions = first_pos + jnp.arange(local_pos, dtype=jnp.int32)
    scores = (
        jnp.einsum("bhc,blc->bhl", seq_latent, cache_latent, preferred_element_type=jnp.float32)
        + jnp.einsum("bhr,blr->bhl", seq_rope, cache_rope, preferred_element_type=jnp.float32)
    ) * factor
    visible = positions[None, None, :] < own_length[:, None, None]
    new_score = (
        jnp.einsum("bhc,bc->bh", seq_latent, own_latent, preferred_element_type=jnp.float32)
        + jnp.einsum("bhr,br->bh", seq_rope, own_rope, preferred_element_type=jnp.float32)
    ) * factor
    holder = ((own_length >= first_pos) & (own_length < first_pos + local_pos))[:, None]
    local_max = jnp.maximum(
        jnp.max(jnp.where(visible, scores, NEGATIVE), axis=2),
        jnp.where(holder, new_score, NEGATIVE),
    )
    weights = jnp.where(visible, jnp.exp(scores - local_max[..., None]), 0.0)
    new_weight = jnp.where(holder, jnp.exp(new_score - local_max), 0.0)
    weight_sum = jnp.sum(weights, axis=2) + new_weight
    rounded_new = lax.optimization_barrier(new_weight.astype(jnp.bfloat16)).astype(jnp.float32)
    weighted = (
        jnp.einsum(
            "bhl,blc->bhc",
            weights.astype(jnp.bfloat16),
            cache_latent,
            preferred_element_type=jnp.float32,
        )
        + rounded_new[..., None] * own_latent.astype(jnp.float32)[:, None, :]
    )
    global_max = by_axis(local_max, KV)
    rescale = jnp.exp(local_max - global_max)
    weight_sum, weighted = (
        over_pieces(weight_sum * rescale, KV),
        over_pieces(weighted * rescale[..., None], KV),
    )
    head_latent = (weighted / weight_sum[..., None]).astype(jnp.bfloat16)
    batch_latent = lax.all_to_all(head_latent, "tp", split_axis=1, concat_axis=0, tiled=True)
    head_out = (
        jnp.einsum("bhc,hcv->bhv", batch_latent, w_value_up, preferred_element_type=jnp.float32)
        .astype(jnp.bfloat16)
        .reshape(seq_count, -1)
    )
    mixed_sum = over_pieces(jnp.dot(head_out, w_out, preferred_element_type=jnp.float32), "tp")
    out_squares = over_axes(jnp.sum(mixed_sum * mixed_sum, axis=1), KV)
    return (mixed_sum * lax.rsqrt(out_squares / model_width + EPSILON)[:, None] * out_gain).astype(
        jnp.bfloat16
    )


def solution(mesh):
    finer = Mesh(mesh.devices.reshape(4, 4, mesh.shape["tp"]), ("kv_0", "kv_1", "tp"))
    return jax.shard_map(
        on_device,
        mesh=finer,
        in_specs=(
            P(None, KV),
            P(KV),
            P(KV, "tp"),
            P(KV, None),
            P(KV, None),
            P(),
            P("tp", None, None),
            P("tp", None, None),
            P("tp", KV),
            P(KV),
            P("tp", KV, None),
            P("tp", KV, None),
            P(),
        ),
        out_specs=P(None, KV),
        check_vma=False,
    )
```

profile of v0, /device:TPU:0, one launch (start us, length us, event | category | flops | bytes accessed | tf_op | source)
XLA Modules:
  0.0 201.2 jit_solution(11221222304284880200)
XLA Ops:
  6.5 0.0 copy-start
  6.5 0.0 all-gather.9.cloned.1.call-start
  6.5 1.8 fusion.47
  8.4 0.0 all-gather.9.cloned.1.call-update
  8.4 0.7 convert_element_type.83
  9.0 1.0 fusion.48
  10.0 27.6 %all-gather = f32[1024,192]{1,0:T(8,128)S(1)} all-gather(f32[64,192]{1,0:T(8,128)S(1)} %fusion.48), channel_id=2, replica_groups=mesh['kv_0'=4,'kv_1'=4,'tp'=8] {'kv_0','kv_1'}, dimensions={0}, use_global_device_ids=true | all-gather | bytes 835584 | tf_op jit(solution)/shard_map/all_gather | solution.py:17
  37.6 0.1 reduce_sum.81
  37.7 0.1 copy.50
  37.8 0.2 fusion.34
  38.0 0.6 broadcast.112
  38.5 0.7 reduce.1
  39.2 0.1 copy.78
  39.3 0.7 reshape.207
  40.0 4.3 %all-to-all-start.1 = ((bf16[8,2,256]{2,1,0:T(2,128)(2,1)}), bf16[8,2,256]{2,1,0:T(2,128)(2,1)S(1)}, u32[]{:S(2)}, u32[]{:S(2)}) async-start(bf16[8,2,256]{2,1,0:T(2,128)(2,1)} %reshape.207), calls=%async_computation.1 | async-start | bytes 16384 | tf_op jit(solution)/shard_map/all_to_all | solution.py:100
  44.4 0.9 fusion.46
  45.2 23.5 %all-gather.2 = f32[1024,64]{1,0:T(8,128)S(1)} all-gather(f32[64,64]{1,0:T(8,128)S(1)} %fusion.46), channel_id=4, replica_groups=mesh['kv_0'=4,'kv_1'=4,'tp'=8] {'kv_0','kv_1'}, dimensions={0}, use_global_device_ids=true | all-gather | bytes 278528 | tf_op jit(solution)/shard_map/all_gather | solution.py:17
  68.8 0.1 fusion.52
  68.9 0.1 copy.52
  69.0 0.1 copy.51
  69.1 0.0 copy-done.6
  69.1 0.1 compare_and_fusion
  69.2 0.2 fusion.2
  69.3 0.1 broadcast_compare_fusion
  69.4 0.1 fusion.30
  69.6 0.1 fusion.37
  69.6 0.1 copy.46
  69.7 0.7 reduce
  70.4 0.0 copy-start.4
  70.4 0.6 reshape.205
  71.1 0.0 all-to-all-done.1
  71.1 4.6 %all-to-all-start = ((bf16[8,2,2048]{2,1,0:T(2,128)(2,1)}), bf16[8,2,2048]{2,1,0:T(2,128)(2,1)S(1)}, u32[]{:S(2)}, u32[]{:S(2)}) async-start(bf16[8,2,2048]{2,1,0:T(2,128)(2,1)} %reshape.205), calls=%async_computation | async-start | bytes 131072 | tf_op jit(solution)/shard_map/all_to_all | solution.py:99
  75.7 0.0 all-gather.11.cloned.1.call-start
  75.7 0.1 reshape.208
  75.8 0.1 fusion.40
  76.0 5.4 %all-to-all-done = bf16[8,2,2048]{2,1,0:T(2,128)(2,1)S(1)} async-done(((bf16[8,2,2048]{2,1,0:T(2,128)(2,1)}), bf16[8,2,2048]{2,1,0:T(2,128)(2,1)S(1)}, u32[]{:S(2)}, u32[]{:S(2)}) %all-to-all-start) | async-done | bytes 65568 | tf_op jit(solution)/shard_map/all_to_all | solution.py:99
  81.3 0.1 reshape.206
  81.4 3.4 %fusion.14 = f32[8,8,512]{2,1,0:T(8,128)S(1)} fusion(bf16[8,512,512]{2,1,0:T(8,128)(2,1)} %param.23, bf16[8,8,1,512]{3,1,0,2:T(8,128)(2,1)S(1)} %bitcast.77), kind=kOutput, calls=%fused_computation.21 | convolution fusion | flops 33554432 | bytes 4390912 | tf_op jit(solution)/shard_map/bhc,blc->bhl/dot_general | solution.py:111
  84.8 0.3 select_reduce_fusion
  85.0 1.8 reduce_sum.82
  86.8 0.0 copy-start.1
  86.8 0.0 copy-start.3
  86.8 0.1 multiply_reduce_fusion
  87.0 0.1 dynamic-slice
  87.0 0.1 fusion.51
  87.1 0.1 fusion.12
  87.3 0.1 select_maximum_fusion
  87.3 8.8 %pmax.14 = f32[8,8]{1,0:T(8,128)S(1)} all-reduce(f32[8,8]{1,0:T(8,128)S(1)} %select_maximum_fusion), channel_id=1, replica_groups=mesh['kv_0'=4,'kv_1'=4,'tp'=8] {'kv_0'}, use_global_device_ids=true, to_apply=%region_5.6 | all-reduce | flops 64 | bytes 512 | tf_op jit(solution)/shard_map/pmax | solution.py:22
  96.2 0.2 fusion.7
  96.3 9.9 %pmax.15 = f32[8,8]{1,0:T(8,128)S(1)} all-reduce(f32[8,8]{1,0:T(8,128)S(1)} %pmax.14), channel_id=1, replica_groups=mesh['kv_0'=4,'kv_1'=4,'tp'=8] {'kv_1'}, use_global_device_ids=true, to_apply=%region_6.7 | all-reduce | flops 64 | bytes 512 | tf_op jit(solution)/shard_map/pmax | solution.py:22
  106.2 0.1 add_multiply_fusion
  106.3 3.5 %fusion.1 = f32[8,8,512]{2,1,0:T(8,128)} fusion(bf16[8,512,512]{2,1,0:T(8,128)(2,1)} %param.23, f32[8,8,512]{2,1,0:T(8,128)S(1)} %get-tuple-element.19, f32[8,8]{1,0:T(8,128)S(1)} %get-tuple-element.7, f32[8,512]{1,0:T(8,128)S(1)} %get-tuple-element.10, f32[8,8]{1,0:T(8,128)S(1)} %convert_element_type.87, f32[8,8]{1,0:T(8,128)S(1)} %select_maximum_fusion, ...), kind=kOutput, calls=%fused_computation.3 | convolution fusion | flops 33751040 | bytes 4477696 | tf_op jit(solution)/shard_map/bhl,blc->bhc/dot_general | solution.py:129
  109.8 0.0 all-gather.11.cloned.1.call-update
  109.8 20.5 %all-gather.4 = f32[128,8]{1,0:T(8,128)S(1)} all-gather(f32[8,8]{1,0:T(8,128)S(1)} %get-tuple-element.5), channel_id=6, replica_groups=mesh['kv_0'=4,'kv_1'=4,'tp'=8] {'kv_0','kv_1'}, dimensions={0}, use_global_device_ids=true | all-gather | bytes 4352 | tf_op jit(solution)/shard_map/all_gather | solution.py:17
  130.4 19.7 %all-gather.11.cloned.1.call-done = f32[128,8,512]{2,1,0:T(8,128)} async-done(((f32[8,8,512]{2,1,0:T(8,128)}), f32[128,8,512]{2,1,0:T(8,128)}) %all-gather.11.cloned.1.call-update) | async-done | bytes 2097168 | tf_op jit(solution)/shard_map/all_gather | solution.py:17
  150.1 1.8 reduce_sum.85
  151.9 0.1 divide_convert_fusion
  152.0 9.7 %all_to_all.51 = bf16[8,8,512]{2,0,1:T(8,128)(2,1)S(1)} all-to-all(bf16[8,8,512]{2,0,1:T(8,128)(2,1)S(1)} %copy.43), channel_id=1, replica_groups=mesh['kv_0'=4,'kv_1'=4,'tp'=8] {'tp'}, dimensions={1} | all-to-all | bytes 131072 | tf_op jit(solution)/shard_map/all_to_all | solution.py:144
  161.7 0.3 fusion.3
  162.0 12.8 %all-gather.5 = f32[512,128]{1,0:T(8,128)S(1)} all-gather(f32[64,128]{1,0:T(8,128)S(1)} %fusion.3), channel_id=7, replica_groups=mesh['kv_0'=4,'kv_1'=4,'tp'=8] {'tp'}, dimensions={0}, use_global_device_ids=true | all-gather | bytes 294912 | tf_op jit(solution)/shard_map/all_gather | solution.py:17
  174.8 0.1 multiply_reduce_fusion.1
  174.9 10.1 %psum.14 = f32[64]{0:T(128)S(1)} all-reduce(f32[64]{0:T(128)S(1)} %multiply_reduce_fusion.1), channel_id=1, replica_groups=mesh['kv_0'=4,'kv_1'=4,'tp'=8] {'kv_0'}, use_global_device_ids=true, to_apply=%region_12.13 | all-reduce | flops 64 | bytes 512 | tf_op jit(solution)/shard_map/psum | solution.py:27
  185.0 8.6 %psum.15 = f32[64]{0:T(128)S(1)} all-reduce(f32[64]{0:T(128)S(1)} %psum.14), channel_id=1, replica_groups=mesh['kv_0'=4,'kv_1'=4,'tp'=8] {'kv_1'}, use_global_device_ids=true, to_apply=%region_13.14 | all-reduce | flops 64 | bytes 512 | tf_op jit(solution)/shard_map/psum | solution.py:27
  193.6 0.7 multiply_convert_fusion
  (24 shorter events, 0.2 us)
Async XLA Ops:
  6.5 78.2 %copy-start = (bf16[8,512,64]{1,2,0:T(8,128)(2,1)S(1)}, bf16[8,512,64]{1,2,0:T(8,128)(2,1)}, u32[]{:S(2)}) copy-start(bf16[8,512,64]{1,2,0:T(8,128)(2,1)} %param.24) | copy-start | bytes 1572868
  6.5 62.5 %copy-start.6 = (s32[64]{0:T(128)S(1)}, s32[64]{0:T(128)}, u32[]{:S(2)}) copy-start(s32[64]{0:T(128)} %param.25) | copy-start | bytes 772
  6.5 62.6 %copy-start.2 = (bf16[1,512,128]{2,1,0:T(8,128)(2,1)S(1)}, bf16[1,512,128]{2,1,0:T(8,128)(2,1)}, u32[]{:S(2)}) copy-start(bf16[1,512,128]{2,1,0:T(8,128)(2,1)} %param.19) | copy-start | bytes 393220
  6.5 78.5 %all-gather.9.cloned.1.call-start = ((), (), s32[]{:S(2)}) async-start(), calls=%async_computation.3 | async-start | bytes 2228224 | tf_op jit(solution)/shard_map/all_gather | solution.py:17
  40.0 31.1 %all-to-all-start.1 = ((bf16[8,2,256]{2,1,0:T(2,128)(2,1)}), bf16[8,2,256]{2,1,0:T(2,128)(2,1)S(1)}, u32[]{:S(2)}, u32[]{:S(2)}) async-start(bf16[8,2,256]{2,1,0:T(2,128)(2,1)} %reshape.207), calls=%async_computation.1 | async-start | bytes 16384 | tf_op jit(solution)/shard_map/all_to_all | solution.py:100
  70.4 16.6 %copy-start.4 = (f32[512]{0:T(512)S(1)}, f32[512]{0:T(512)}, u32[]{:S(2)}) copy-start(f32[512]{0:T(512)} %param.18) | copy-start | bytes 6148
  71.1 10.2 %all-to-all-start = ((bf16[8,2,2048]{2,1,0:T(2,128)(2,1)}), bf16[8,2,2048]{2,1,0:T(2,128)(2,1)S(1)}, u32[]{:S(2)}, u32[]{:S(2)}) async-start(bf16[8,2,2048]{2,1,0:T(2,128)(2,1)} %reshape.205), calls=%async_computation | async-start | bytes 131072 | tf_op jit(solution)/shard_map/all_to_all | solution.py:99
  75.7 74.4 %all-gather.11.cloned.1.call-start = ((), (), s32[]{:S(2)}) async-start(), calls=%async_computation.4 | async-start | bytes 2228224 | tf_op jit(solution)/shard_map/all_gather | solution.py:17
  86.8 74.9 %copy-start.1 = (bf16[1,512,128]{2,1,0:T(8,128)(2,1)S(1)}, bf16[1,512,128]{2,1,0:T(8,128)(2,1)}, u32[]{:S(2)}) copy-start(bf16[1,512,128]{2,1,0:T(8,128)(2,1)} %param.20) | copy-start | bytes 393220
  86.8 74.9 %copy-start.3 = (bf16[128,128]{1,0:T(8,128)(2,1)S(1)}, bf16[128,128]{1,0:T(8,128)(2,1)}, u32[]{:S(2)}) copy-start(bf16[128,128]{1,0:T(8,128)(2,1)} %param.21) | copy-start | bytes 98308
  106.2 87.4 %copy-start.5 = (f32[128]{0:T(128)S(1)}, f32[128]{0:T(128)}, u32[]{:S(2)}) copy-start(f32[128]{0:T(128)} %param.22) | copy-start | bytes 1540
Sparse Core Ops, SparseCore 0:
  9.5 47.9 all-gather.8
  110.0 40.0 all-gather.10
where the time goes:
time: 202 us; the launch traced here: 201 us
  blocking collectives  132 us (65%)
  waiting for transfers between devices  25.1 us (12%)
  between operations  13.5 us (7%)
  matrix products  11.5 us (6%)
  starting transfers between devices  8.97 us (4%)
  other arithmetic  7.72 us (4%)
  local copies, waits for them, and re-layouts  2.73 us (1%)
    all_gather x4, blocking collectives, over_pieces(): parts = lax.all_gather(value, axis)  84.4 us
    all_gather x2, waiting for transfers between devices, over_pieces(): parts = lax.all_gather(value, axis)  19.7 us
    pmax x2, blocking collectives, by_axis(): return functools.reduce(lax.pmax, axes, value)  18.7 us
    psum x2, blocking collectives, over_axes(): value = lax.psum(value, axis)  18.7 us
    all_to_all x1, blocking collectives, on_device(): lax.all_to_all(head_latent, 'tp', split_axis=1, concat_axis=0, tiled=True)  9.71 us
    all_to_all x1, waiting for transfers between devices, on_device(): lax.all_to_all(query_latent, 'tp', split_axis=0, concat_axis=1, tiled=True)  5.36 us
    all_to_all x1, starting transfers between devices, on_device(): lax.all_to_all(query_latent, 'tp', split_axis=0, concat_axis=1, tiled=True)  4.59 us
    all_to_all x1, starting transfers between devices, on_device(): lax.all_to_all(query_rope, 'tp', split_axis=0, concat_axis=1, tiled=True)  4.34 us
  transfers between devices with their start and end apart: 4, of which 2 were waited for; matrix products, arithmetic and copies ran while one was open for 6% of the time, Pallas kernels for 0%

commit v1 on v0

v1 whole, which is shorter than its diff:
```python
import jax
import jax.numpy as jnp
from jax import lax
from jax.sharding import Mesh
from jax.sharding import PartitionSpec as P

KV = ("kv_0", "kv_1")
ALL = ("kv_0", "kv_1", "tp")
EPSILON = 1e-06
NEGATIVE = -1e30


def rotate_half(values, cosine, sine_table):
    half_width = values.shape[-1] // 2
    lower_half = values[..., :half_width]
    upper_half = values[..., half_width:]
    return jnp.concatenate(
        [
            lower_half * cosine - upper_half * sine_table,
            upper_half * cosine + lower_half * sine_table,
        ],
        axis=-1,
    )


def angle_tables(lengths, rope_width):
    inverse_freq = 1.0 / 10000.0 ** (jnp.arange(0, rope_width, 2, dtype=jnp.float32) / rope_width)
    angles = lengths.astype(jnp.float32)[:, None] * inverse_freq[None, :]
    return (jnp.cos(angles), jnp.sin(angles))


def exchange(value, axes):
    return lax.all_to_all(value, axes, split_axis=0, concat_axis=0, tiled=True)


def flip_pairs(value, index, bits):
    for bit in range(bits):
        width = 1 << bit
        shape = value.shape
        pairs = value.reshape((shape[0] // (2 * width), 2, width) + shape[1:])
        value = jnp.where((index >> bit) & 1 == 1, pairs[:, ::-1], pairs).reshape(shape)
    return value


def three_parts(value):
    high = lax.reduce_precision(value, 8, 7)
    middle = lax.reduce_precision(value - high, 8, 7)
    low = lax.reduce_precision(value - high - middle, 8, 7)
    return [part.astype(jnp.bfloat16) for part in (high, middle, low)]


def on_device(
    tokens,
    token_gain,
    w_query,
    w_down_kv,
    w_rope_key,
    latent_gain,
    w_key_up,
    w_value_up,
    w_out,
    out_gain,
    cache_latent,
    cache_rope,
    lengths,
):
    kv_size = lax.axis_size(KV)
    tp_size = lax.axis_size("tp")
    kv_index = lax.axis_index(KV)
    tp_index = lax.axis_index("tp")
    model_width = tokens.shape[1] * kv_size
    seqs = tokens.shape[0]
    local_seqs, local_pos, latent_width = cache_latent.shape
    rope_width = cache_rope.shape[2]
    nope = w_key_up.shape[2]
    value_width = w_value_up.shape[2]
    head_width = nope + rope_width
    factor = head_width ** (-0.5)

    weights = jnp.concatenate([w_key_up[0], w_value_up[0], w_out], axis=0)[None]
    for mask in (2, 6, 1):
        other = lax.ppermute(weights, "tp", [(i, i ^ mask) for i in range(tp_size)])
        weights = jnp.concatenate([weights, other], axis=0)
    order = (0, 2, 6, 4, 1, 3, 7, 5)

    scaled = (tokens.astype(jnp.float32) * token_gain).astype(jnp.bfloat16)
    query_part = jnp.dot(scaled, w_query, preferred_element_type=jnp.float32).astype(jnp.bfloat16)
    chunk = latent_width // tp_size
    rope_chunk = rope_width // tp_size
    down = lax.dynamic_slice_in_dim(w_down_kv, tp_index * chunk, chunk, 1)
    down_rope = lax.dynamic_slice_in_dim(w_rope_key, tp_index * rope_chunk, rope_chunk, 1)
    key_part = jnp.dot(
        scaled, jnp.concatenate([down, down_rope], axis=1), preferred_element_type=jnp.float32
    ).astype(jnp.bfloat16)
    key_part = key_part.reshape(tp_size, local_seqs, chunk + rope_chunk).transpose(1, 0, 2)
    key_part = jnp.tile(key_part, (kv_size // local_seqs, 1, 1))
    query_part = jnp.broadcast_to(
        query_part.reshape(1, tp_size, local_seqs * head_width),
        (kv_size, tp_size, local_seqs * head_width),
    )
    used = local_seqs * head_width + chunk + rope_chunk
    filled = -(-used // 128) * 128
    sent = jnp.concatenate(
        [query_part, key_part, jnp.zeros((kv_size, tp_size, filled - used), jnp.bfloat16)], axis=2
    ).reshape(kv_size * tp_size, filled)
    got = exchange(sent, ALL).reshape(kv_size, tp_size, filled).astype(jnp.float32).sum(axis=0)

    query = got[:, : local_seqs * head_width].reshape(tp_size, local_seqs, head_width)
    query = flip_pairs(query, tp_index, 3).astype(jnp.bfloat16)
    query = jnp.stack([query[i] for i in order])
    latent_raw = got[:, used - chunk - rope_chunk : used - rope_chunk].reshape(1, latent_width)
    rope_raw = got[:, used - rope_chunk : used].reshape(1, rope_width)
    latent = (
        latent_raw
        * lax.rsqrt(jnp.mean(latent_raw * latent_raw, axis=1, keepdims=True) + EPSILON)
        * latent_gain
    ).astype(jnp.bfloat16)
    own_length = lax.dynamic_slice_in_dim(lengths, tp_index * local_seqs, local_seqs, 0)
    cosine, sine_table = angle_tables(own_length, rope_width)
    new_seq = kv_index % local_seqs
    is_new = (jnp.arange(local_seqs) == new_seq) & (kv_index < local_seqs)
    new_rope = rotate_half(
        rope_raw,
        lax.dynamic_slice_in_dim(cosine, new_seq, 1, 0),
        lax.dynamic_slice_in_dim(sine_table, new_seq, 1, 0),
    ).astype(jnp.bfloat16)
    query_rope = rotate_half(query[..., nope:].astype(jnp.float32), cosine, sine_table).astype(
        jnp.bfloat16
    )
    query_latent = jnp.einsum(
        "hsn,hcn->shc",
        query[..., :nope],
        weights[:, :latent_width],
        preferred_element_type=jnp.float32,
    ).astype(jnp.bfloat16)
    query_rope = query_rope.transpose(1, 0, 2)

    positions = kv_index * local_pos + jnp.arange(local_pos, dtype=jnp.int32)
    scores = (
        jnp.einsum("bhc,blc->bhl", query_latent, cache_latent, preferred_element_type=jnp.float32)
        + jnp.einsum("bhr,blr->bhl", query_rope, cache_rope, preferred_element_type=jnp.float32)
    ) * factor
    visible = positions[None, None, :] < own_length[:, None, None]
    new_score = (
        jnp.einsum("bhc,c->bh", query_latent, latent[0], preferred_element_type=jnp.float32)
        + jnp.einsum("bhr,r->bh", query_rope, new_rope[0], preferred_element_type=jnp.float32)
    ) * factor
    holder = is_new[:, None]
    local_max = jnp.maximum(
        jnp.max(jnp.where(visible, scores, NEGATIVE), axis=2),
        jnp.where(holder, new_score, NEGATIVE),
    )
    weight = jnp.where(visible, jnp.exp(scores - local_max[..., None]), 0.0)
    new_weight = jnp.where(holder, jnp.exp(new_score - local_max), 0.0)
    weight_sum = jnp.sum(weight, axis=2) + new_weight
    weighted = (
        jnp.einsum(
            "bhl,blc->bhc",
            weight.astype(jnp.bfloat16),
            cache_latent,
            preferred_element_type=jnp.float32,
        )
        + new_weight[..., None] * latent.astype(jnp.float32)[:, None, :]
    )
    some = weight_sum > 0.0
    safe_sum = jnp.where(some, weight_sum, 1.0)
    log_sum = jnp.where(some, local_max + jnp.log(safe_sum), NEGATIVE)
    mean_latent = (weighted / safe_sum[..., None]).astype(jnp.bfloat16)
    part = jnp.einsum(
        "shc,hcv->shv",
        mean_latent,
        weights[:, latent_width : 2 * latent_width],
        preferred_element_type=jnp.float32,
    ).astype(jnp.bfloat16)

    heads = tp_size
    pairs = local_seqs * heads
    block = jnp.concatenate(
        [part.reshape(1, pairs * value_width)]
        + [x.reshape(1, pairs) for x in three_parts(log_sum)]
        + [jnp.zeros((1, pairs), jnp.bfloat16)],
        axis=1,
    )
    got = exchange(jnp.broadcast_to(block, (kv_size, block.shape[1])), KV)
    logs = got[:, pairs * value_width :].astype(jnp.float32).reshape(kv_size, 4, pairs)
    logs = logs[:, 0] + logs[:, 1] + logs[:, 2]
    share = jnp.exp(logs - jnp.max(logs, axis=0, keepdims=True))
    share = share / jnp.sum(share, axis=0, keepdims=True)
    parts = got[:, : pairs * value_width].reshape(kv_size, pairs, value_width)
    head_out = jnp.sum(parts.astype(jnp.float32) * share[..., None], axis=0)
    head_out = head_out.astype(jnp.bfloat16).reshape(local_seqs, heads * value_width)
    mixed = jnp.dot(
        head_out,
        weights[:, 2 * latent_width :].reshape(heads * value_width, -1),
        preferred_element_type=jnp.float32,
    ).astype(jnp.bfloat16)

    everyone = kv_size * tp_size
    got = exchange(jnp.broadcast_to(mixed[None], (everyone,) + mixed.shape), ALL)
    got = got.reshape(kv_size, seqs, mixed.shape[1])
    squares = jnp.sum(jnp.square(got.astype(jnp.float32)), axis=(0, 2))
    own = lax.dynamic_index_in_dim(got, kv_index, 0, keepdims=False).astype(jnp.float32)
    return (own * lax.rsqrt(squares / model_width + EPSILON)[:, None] * out_gain).astype(
        jnp.bfloat16
    )


def solution(mesh):
    finer = Mesh(mesh.devices.reshape(4, 4, mesh.shape["tp"]), ("kv_0", "kv_1", "tp"))
    return jax.shard_map(
        on_device,
        mesh=finer,
        in_specs=(
            P(None, KV),
            P(KV),
            P(KV, "tp"),
            P(KV, None),
            P(KV, None),
            P(),
            P("tp", None, None),
            P("tp", None, None),
            P("tp", KV),
            P(KV),
            P("tp", KV, None),
            P("tp", KV, None),
            P(),
        ),
        out_specs=P(None, KV),
        check_vma=False,
    )
```

time: 202 us -> 102 us (0.50)
  blocking collectives: 132 us -> 0 us
  waiting for transfers between devices: 25.1 us -> 44.3 us
  starting transfers between devices: 8.97 us -> 26.7 us
  between operations: 13.5 us -> 1 us
  local copies, waits for them, and re-layouts: 2.73 us -> 10 us
  matrix products: 11.5 us -> 8.86 us
  other arithmetic: 7.72 us -> 9.97 us
    all_gather x4 -> x0, blocking collectives: 84.4 us -> none  [over_pieces(): parts = lax.all_gather(value, axis)]
    ppermute x0 -> x3, waiting for transfers between devices: none -> 24.5 us  [on_device(): other = lax.ppermute(weights, 'tp', [(i, i ^ mask) for i in range(tp_size)])]
    all_gather x2 -> x0, waiting for transfers between devices: 19.7 us -> none  [over_pieces(): parts = lax.all_gather(value, axis)]
    pmax x2 -> x0, blocking collectives: 18.7 us -> none  [by_axis(): return functools.reduce(lax.pmax, axes, value)]
    psum x2 -> x0, blocking collectives: 18.7 us -> none  [over_axes(): value = lax.psum(value, axis)]
    all_to_all x2 -> x3, starting transfers between devices: 8.93 us -> 23.6 us  [exchange(): return lax.all_to_all(value, axes, split_axis=0, concat_axis=0, tiled=True)]
    all_to_all x2 -> x3, waiting for transfers between devices: 5.36 us -> 19.7 us  [exchange(): return lax.all_to_all(value, axes, split_axis=0, concat_axis=0, tiled=True)]
    all_to_all x1 -> x0, blocking collectives: 9.71 us -> none  [on_device(): lax.all_to_all(head_latent, 'tp', split_axis=1, concat_axis=0, tiled=True)]
  transfers between devices with their start and end apart: 4 -> 6, of which waited for: 2 -> 5; matrix products, arithmetic and copies ran while one was open for 6% -> 4% of each run, Pallas kernels for 0% -> 0%
where the time goes in v1:
time: 102 us; the launch traced here: 101 us
  waiting for transfers between devices  44.3 us (43%)
  starting transfers between devices  26.7 us (26%)
  local copies, waits for them, and re-layouts  10 us (10%)
  other arithmetic  9.97 us (10%)
  matrix products  8.86 us (9%)
    ppermute x3, waiting for transfers between devices, on_device(): other = lax.ppermute(weights, 'tp', [(i, i ^ mask) for i in range(tp_size)])  24.5 us
    all_to_all x3, starting transfers between devices, exchange(): return lax.all_to_all(value, axes, split_axis=0, concat_axis=0, tiled=True)  23.6 us
    all_to_all x3, waiting for transfers between devices, exchange(): return lax.all_to_all(value, axes, split_axis=0, concat_axis=0, tiled=True)  19.7 us
    unnamed x30, local copies, waits for them, and re-layouts  5.22 us
    dot_general x1, matrix products, on_device(): jnp.einsum('bhc,blc->bhl', query_latent, cache_latent, preferred_element_...  3.53 us
    ppermute x3, starting transfers between devices, on_device(): other = lax.ppermute(weights, 'tp', [(i, i ^ mask) for i in range(tp_size)])  3.16 us
    broadcast_in_dim x1, other arithmetic, on_device(): got = exchange(jnp.broadcast_to(block, (kv_size, block.shape[1])), KV)  2.93 us
    concatenate x3, other arithmetic, on_device(): weights = jnp.concatenate([weights, other], axis=0)  2.22 us
  transfers between devices with their start and end apart: 6, of which 5 were waited for; matrix products, arithmetic and copies ran while one was open for 4% of the time, Pallas kernels for 0%

profile of v1, /device:TPU:0, one launch (start us, length us, event | category | flops | bytes accessed | tf_op | source)
XLA Modules:
  0.0 100.8 jit_solution(3092843155420183951)
XLA Ops:
  0.0 0.8 constant_dynamic-slice_fusion.2
  0.8 0.1 copy.33
  0.9 0.8 constant_dynamic-slice_fusion.3
  1.7 0.9 fusion.4
  2.7 1.0 convolution_convert_fusion.1
  3.6 0.1 broadcast_in_dim.91
  3.9 0.1 concatenate.52
  4.0 0.5 broadcast.122
  4.5 0.9 reduce.6
  5.4 1.2 %reshape.274 = bf16[128,2,832]{2,1,0:T(2,128)(2,1)} reshape(bf16[128,1664]{1,0:T(8,128)(2,1)S(1)} %reduce.6) | data formatting | bytes 851968
  6.6 11.2 %all-to-all-start = ((bf16[128,2,832]{2,1,0:T(2,128)(2,1)}), bf16[128,2,832]{2,1,0:T(2,128)(2,1)S(1)}, u32[]{:S(2)}, u32[]{:S(2)}) async-start(bf16[128,2,832]{2,1,0:T(2,128)(2,1)} %reshape.274), calls=%async_computation | async-start | bytes 917504 | tf_op jit(solution)/shard_map/all_to_all | solution.py:33
  17.9 1.0 %collective-permute-start = (bf16[1,1152,128]{2,1,0:T(8,128)(2,1)S(1)}, bf16[1,1152,128]{2,1,0:T(8,128)(2,1)S(1)}, u32[]{:S(2)}, u32[]{:S(2)}) collective-permute-start(bf16[1,1152,128]{2,1,0:T(8,128)(2,1)S(1)} %maximum_bitcast_fusion), channel_id=1, source_target_pairs={{0,2},{1,3},{2,0},{3,1},{4,6},{5,7},{6,4},{7,5},{8,10},{9,11},{10,... | collective-permute-start | bytes 884744 | tf_op jit(solution)/shard_map/ppermute | solution.py:82
  18.9 0.1 fusion.39
  19.0 0.1 multiply_cosine_fusion
  19.1 0.1 broadcast_compare_fusion
  19.2 10.9 %collective-permute-done = bf16[1,1152,128]{2,1,0:T(8,128)(2,1)S(1)} collective-permute-done((bf16[1,1152,128]{2,1,0:T(8,128)(2,1)S(1)}, bf16[1,1152,128]{2,1,0:T(8,128)(2,1)S(1)}, u32[]{:S(2)}, u32[]{:S(2)}) %collective-permute-start) | collective-permute-done | bytes 294944 | tf_op jit(solution)/shard_map/ppermute | solution.py:82
  30.1 0.9 pad_maximum_fusion.2
  31.0 2.1 %collective-permute-start.1 = (bf16[2,1152,128]{2,1,0:T(8,128)(2,1)}, bf16[2,1152,128]{2,1,0:T(8,128)(2,1)S(1)}, u32[]{:S(2)}, u32[]{:S(2)}) collective-permute-start(bf16[2,1152,128]{2,1,0:T(8,128)(2,1)} %pad_maximum_fusion.2), channel_id=1, source_target_pairs={{0,6},{1,7},{2,4},{3,5},{4,2},{5,3},{6,0},{7,1},{8,14},{9,15},{10,... | collective-permute-start | bytes 1769480 | tf_op jit(solution)/shard_map/ppermute | solution.py:82
  33.1 0.6 reshape.275
  33.7 0.9 convert_element_type.136
  34.7 0.6 multiply_reduce_fusion.1
  35.3 0.1 reshape_reshape.9
  36.1 0.1 mul.178
  36.2 0.1 reshape.255
  36.3 11.0 %collective-permute-done.1 = bf16[2,1152,128]{2,1,0:T(8,128)(2,1)S(1)} collective-permute-done((bf16[2,1152,128]{2,1,0:T(8,128)(2,1)}, bf16[2,1152,128]{2,1,0:T(8,128)(2,1)S(1)}, u32[]{:S(2)}, u32[]{:S(2)}) %collective-permute-start.1) | collective-permute-done | bytes 589856 | tf_op jit(solution)/shard_map/ppermute | solution.py:82
  47.4 1.1 %pad_maximum_fusion.1 = bf16[4,1152,128]{2,1,0:T(8,128)(2,1)} fusion(bf16[2,1152,128]{2,1,0:T(8,128)(2,1)S(1)} %collective-permute-done.1, bf16[1,1152,128]{2,1,0:T(8,128)(2,1)S(1)} %collective-permute-done, bf16[1,1152,128]{2,1,0:T(8,128)(2,1)S(1)} %maximum_bitcast_fusion), kind=kLoop, calls=%fused_computation.1 | loop fusion | flops 1179648 | bytes 2359296 | tf_op jit(solution)/shard_map/concatenate | solution.py:83
  48.5 0.1 subtract_convert_fusion
  48.6 0.1 maximum_bitcast_fusion.1
  48.7 0.1 convert_bitcast_fusion.1
  48.8 0.2 fusion.31
  49.0 0.1 copy.41
  49.0 2.5 %collective-permute-done.2 = bf16[4,1152,128]{2,1,0:T(8,128)(2,1)S(1)} collective-permute-done((bf16[4,1152,128]{2,1,0:T(8,128)(2,1)}, bf16[4,1152,128]{2,1,0:T(8,128)(2,1)S(1)}, u32[]{:S(2)}, u32[]{:S(2)}) %collective-permute-start.2) | collective-permute-done | bytes 1179680 | tf_op jit(solution)/shard_map/ppermute | solution.py:82
  51.6 0.2 pad_maximum_fusion
  51.8 1.4 %copy-done.2 = bf16[8,1152,128]{2,1,0:T(8,128)(2,1)} copy-done((bf16[8,1152,128]{2,1,0:T(8,128)(2,1)}, bf16[8,1152,128]{2,1,0:T(8,128)(2,1)S(1)}, u32[]{:S(2)}) %copy-start.2) | copy-done | bytes 2359320
  53.2 0.4 fusion.3
  53.6 0.3 fusion.40
  53.9 3.5 %fusion.14 = f32[8,8,512]{2,1,0:T(8,128)S(1)} fusion(bf16[8,512,512]{2,1,0:T(8,128)(2,1)} %param.23, bf16[8,8,512]{2,0,1:T(8,128)(2,1)S(1)} %fusion.3), kind=kOutput, calls=%fused_computation.35 | convolution fusion | flops 33554432 | bytes 4390912 | tf_op jit(solution)/shard_map/bhc,blc->bhl/dot_general | solution.py:140
  57.4 0.3 select_reduce_fusion
  57.7 0.1 select_maximum_fusion
  57.8 0.2 fusion.9
  58.0 0.1 fusion.29
  58.1 0.7 fusion.2
  58.8 1.5 %fusion.5 = bf16[8,8,128]{2,0,1:T(8,128)(2,1)S(1)} fusion(bf16[8,1152,128]{2,1,0:T(8,128)(2,1)} %copy-done.2, bf16[8,8,512]{2,1,0:T(8,128)(2,1)S(1)} %fusion.2), kind=kOutput, calls=%fused_computation.13 | convolution fusion | flops 8396800 | bytes 1130496 | tf_op jit(solution)/shard_map/shc,hcv->shv/dot_general | solution.py:169
  60.3 0.1 reshape.257
  60.4 0.1 reshape.258
  60.5 0.1 reshape.259
  60.6 0.1 concatenate.57
  60.7 0.1 reduce.5
  60.8 0.3 broadcast_in_dim.101
  61.1 2.9 %reduce.7 = bf16[16,8448]{1,0:T(8,128)(2,1)} reduce(bf16[16,1,8448]{2,1,0:T(2,128)(2,1)S(1)} %broadcast_in_dim.101, bf16[]{:T(256)} %broadcast.122), dimensions={1}, to_apply=%broadcast_in_dim.101.reduce_sub_computation | reduce | bytes 540674 | tf_op jit(solution)/shard_map/broadcast_in_dim | solution.py:184
  64.0 1.7 %reshape.276 = bf16[16,2,4224]{2,1,0:T(2,128)(2,1)} reshape(bf16[16,8448]{1,0:T(8,128)(2,1)} %reduce.7) | data formatting | bytes 540672
  65.7 7.3 %all-to-all-start.1 = ((bf16[16,2,4224]{2,1,0:T(2,128)(2,1)}), bf16[16,2,4224]{2,1,0:T(2,128)(2,1)S(1)}, u32[]{:S(2)}, u32[]{:S(2)}) async-start(bf16[16,2,4224]{2,1,0:T(2,128)(2,1)} %reshape.276), calls=%async_computation.1 | async-start | bytes 540672 | tf_op jit(solution)/shard_map/all_to_all | solution.py:33
  73.1 9.0 %all-to-all-done.1 = bf16[16,2,4224]{2,1,0:T(2,128)(2,1)S(1)} async-done(((bf16[16,2,4224]{2,1,0:T(2,128)(2,1)}), bf16[16,2,4224]{2,1,0:T(2,128)(2,1)S(1)}, u32[]{:S(2)}, u32[]{:S(2)}) %all-to-all-start.1) | async-done | bytes 270368 | tf_op jit(solution)/shard_map/all_to_all | solution.py:33
  82.1 0.2 reshape.277
  82.4 0.1 reshape.266
  82.6 0.2 mul.189
  82.8 0.4 fusion.8
  83.2 0.1 convolution_convert_fusion.4
  83.3 0.7 broadcast_in_dim.102
  84.1 5.0 %all-to-all-start.2 = ((bf16[128,8,128]{2,1,0:T(8,128)(2,1)}), bf16[128,8,128]{2,1,0:T(8,128)(2,1)S(1)}, u32[]{:S(2)}, u32[]{:S(2)}) async-start(bf16[128,8,128]{2,1,0:T(8,128)(2,1)} %broadcast_in_dim.102), calls=%async_computation.2 | async-start | bytes 524288 | tf_op jit(solution)/shard_map/all_to_all | solution.py:33
  89.1 10.7 %all-to-all-done.2 = bf16[128,8,128]{2,1,0:T(8,128)(2,1)S(1)} async-done(((bf16[128,8,128]{2,1,0:T(8,128)(2,1)}), bf16[128,8,128]{2,1,0:T(8,128)(2,1)S(1)}, u32[]{:S(2)}, u32[]{:S(2)}) %all-to-all-start.2) | async-done | bytes 262176 | tf_op jit(solution)/shard_map/all_to_all | solution.py:33
  99.8 0.2 multiply_reduce_fusion
  100.0 0.1 reduce_sum.67
  100.1 0.7 fusion.23
  (59 shorter events, 0.6 us)
Async XLA Ops:
  0.0 57.4 %copy-start = (bf16[8,512,64]{1,2,0:T(8,128)(2,1)S(1)}, bf16[8,512,64]{1,2,0:T(8,128)(2,1)}, u32[]{:S(2)}) copy-start(bf16[8,512,64]{1,2,0:T(8,128)(2,1)} %param.24) | copy-start | bytes 1572868
  0.0 17.8 %copy-start.4 = (bf16[1,512,128]{2,1,0:T(8,128)(2,1)S(1)}, bf16[1,512,128]{2,1,0:T(8,128)(2,1)}, u32[]{:S(2)}) copy-start(bf16[1,512,128]{2,1,0:T(8,128)(2,1)} %param.19) | copy-start | bytes 393220
  0.0 17.8 %copy-start.3 = (bf16[1,512,128]{2,1,0:T(8,128)(2,1)S(1)}, bf16[1,512,128]{2,1,0:T(8,128)(2,1)}, u32[]{:S(2)}) copy-start(bf16[1,512,128]{2,1,0:T(8,128)(2,1)} %param.20) | copy-start | bytes 393220
  0.0 17.8 %copy-start.5 = (bf16[128,128]{1,0:T(8,128)(2,1)S(1)}, bf16[128,128]{1,0:T(8,128)(2,1)}, u32[]{:S(2)}) copy-start(bf16[128,128]{1,0:T(8,128)(2,1)} %param.21) | copy-start | bytes 98308
  3.8 15.1 %copy-start.8 = (s32[64]{0:T(128)S(1)}, s32[64]{0:T(128)}, u32[]{:S(2)}) copy-start(s32[64]{0:T(128)} %param.25) | copy-start | bytes 772
  6.6 26.5 %all-to-all-start = ((bf16[128,2,832]{2,1,0:T(2,128)(2,1)}), bf16[128,2,832]{2,1,0:T(2,128)(2,1)S(1)}, u32[]{:S(2)}, u32[]{:S(2)}) async-start(bf16[128,2,832]{2,1,0:T(2,128)(2,1)} %reshape.274), calls=%async_computation | async-start | bytes 917504 | tf_op jit(solution)/shard_map/all_to_all | solution.py:33
  17.9 12.3 %collective-permute-start = (bf16[1,1152,128]{2,1,0:T(8,128)(2,1)S(1)}, bf16[1,1152,128]{2,1,0:T(8,128)(2,1)S(1)}, u32[]{:S(2)}, u32[]{:S(2)}) collective-permute-start(bf16[1,1152,128]{2,1,0:T(8,128)(2,1)S(1)} %maximum_bitcast_fusion), channel_id=1, source_target_pairs={{0,2},{1,3},{2,0},{3,1},{4,6},{5,7},{6,4},{7,5},{8,10},{9,11},{10,... | collective-permute-start | bytes 884744 | tf_op jit(solution)/shard_map/ppermute | solution.py:82
  31.0 5.2 %copy-start.6 = (f32[512]{0:T(512)S(1)}, f32[512]{0:T(512)}, u32[]{:S(2)}) copy-start(f32[512]{0:T(512)} %param.18) | copy-start | bytes 6148
  31.0 16.4 %collective-permute-start.1 = (bf16[2,1152,128]{2,1,0:T(8,128)(2,1)}, bf16[2,1152,128]{2,1,0:T(8,128)(2,1)S(1)}, u32[]{:S(2)}, u32[]{:S(2)}) collective-permute-start(bf16[2,1152,128]{2,1,0:T(8,128)(2,1)} %pad_maximum_fusion.2), channel_id=1, source_target_pairs={{0,6},{1,7},{2,4},{3,5},{4,2},{5,3},{6,0},{7,1},{8,14},{9,15},{10,... | collective-permute-start | bytes 1769480 | tf_op jit(solution)/shard_map/ppermute | solution.py:82
  48.5 3.1 %collective-permute-start.2 = (bf16[4,1152,128]{2,1,0:T(8,128)(2,1)}, bf16[4,1152,128]{2,1,0:T(8,128)(2,1)S(1)}, u32[]{:S(2)}, u32[]{:S(2)}) collective-permute-start(bf16[4,1152,128]{2,1,0:T(8,128)(2,1)} %pad_maximum_fusion.1), channel_id=1, source_target_pairs={{0,1},{1,0},{2,3},{3,2},{4,5},{5,4},{6,7},{7,6},{8,9},{9,8},{10,11... | collective-permute-start | bytes 3538952 | tf_op jit(solution)/shard_map/ppermute | solution.py:82
  51.8 1.4 %copy-start.2 = (bf16[8,1152,128]{2,1,0:T(8,128)(2,1)}, bf16[8,1152,128]{2,1,0:T(8,128)(2,1)S(1)}, u32[]{:S(2)}) copy-start(bf16[8,1152,128]{2,1,0:T(8,128)(2,1)S(1)} %pad_maximum_fusion) | copy-start | bytes 7077892
  53.9 4.2 %copy-start.1 = (bf16[8,512,512]{2,1,0:T(8,128)(2,1)S(1)}, bf16[8,512,512]{2,1,0:T(8,128)(2,1)}, u32[]{:S(2)}) copy-start(bf16[8,512,512]{2,1,0:T(8,128)(2,1)} %param.23) | copy-start | bytes 12582916
  65.7 16.4 %all-to-all-start.1 = ((bf16[16,2,4224]{2,1,0:T(2,128)(2,1)}), bf16[16,2,4224]{2,1,0:T(2,128)(2,1)S(1)}, u32[]{:S(2)}, u32[]{:S(2)}) async-start(bf16[16,2,4224]{2,1,0:T(2,128)(2,1)} %reshape.276), calls=%async_computation.1 | async-start | bytes 540672 | tf_op jit(solution)/shard_map/all_to_all | solution.py:33
  73.1 27.0 %copy-start.7 = (f32[128]{0:T(128)S(1)}, f32[128]{0:T(128)}, u32[]{:S(2)}) copy-start(f32[128]{0:T(128)} %param.22) | copy-start | bytes 1540
  84.1 15.7 %all-to-all-start.2 = ((bf16[128,8,128]{2,1,0:T(8,128)(2,1)}), bf16[128,8,128]{2,1,0:T(8,128)(2,1)S(1)}, u32[]{:S(2)}, u32[]{:S(2)}) async-start(bf16[128,8,128]{2,1,0:T(8,128)(2,1)} %broadcast_in_dim.102), calls=%async_computation.2 | async-start | bytes 524288 | tf_op jit(solution)/shard_map/all_to_all | solution.py:33

commit v2 on v0

v2 whole, which is shorter than its diff:
```python
import functools

import jax
import jax.numpy as jnp
from jax import lax
from jax.experimental import pallas as pl
from jax.experimental.pallas import tpu as pltpu
from jax.sharding import Mesh
from jax.sharding import PartitionSpec as P


KV = ("kv_0", "kv_1")
ALL = ("kv_0", "kv_1", "tp")
EPSILON = 1e-06
NEGATIVE = -1e30
F32 = jnp.float32
BF16 = jnp.bfloat16

NT = (((1,), (1,)), ((), ()))
NN = (((1,), (0,)), ((), ()))


def dot(a, b, dims):
    return lax.dot_general(a, b, dims, preferred_element_type=F32)


def params(mib):
    return pltpu.CompilerParams(vmem_limit_bytes=mib * 1024 * 1024)


def in_vmem():
    return pl.BlockSpec(memory_space=pltpu.VMEM)


def in_smem():
    return pl.BlockSpec(memory_space=pltpu.SMEM)


def lanes(shape):
    return lax.broadcasted_iota(jnp.int32, shape, 1)


def rows(shape):
    return lax.broadcasted_iota(jnp.int32, shape, 0)


def project_kernel(index, tokens, gain, wq, wd, wr, out, *, groups, local, copies):
    tp = index[1]
    scaled = (tokens[...].astype(F32) * gain[...]).astype(BF16)
    query = dot(scaled, wq[...], NT)
    latent = dot(scaled, wd[...], NN)
    rope = dot(scaled, wr[...], NT)
    seqs = scaled.shape[0]
    chunk = latent.shape[1] // groups
    own = jnp.zeros((seqs, chunk), F32)
    for g in range(groups):
        own = jnp.where(tp == g, latent[:, g * chunk : (g + 1) * chunk], own)
    width = rope.shape[1]
    rope = jnp.where(lanes(rope.shape) // (width // groups) == tp, rope, 0.0)
    blank = jnp.zeros((seqs, 128 - width), F32)
    own = jnp.concatenate([blank, own], axis=1)
    rope = jnp.concatenate([blank, rope], axis=1)
    first = query[:, :128].astype(BF16)
    second = jnp.concatenate([query[:, 128:], blank], axis=1)
    row = rows((local, 128))
    for t in range(groups):
        top = first[t * local : (t + 1) * local]
        low = second[t * local : (t + 1) * local]
        for j in range(local):
            r = t * local + j
            new = jnp.where(row == 0, own[r : r + 1], 0.0) + jnp.where(row == 1, rope[r : r + 1], 0.0)
            tile = (low + new).astype(BF16)
            for c in range(copies // local):
                b = (c * local + j) * groups + t
                out[b, :, :128] = top
                out[b, :, 128:] = tile


def rotate(values, cosine, sine):
    half = values.shape[1] // 2
    swapped = jnp.concatenate([values[:, half:], values[:, :half]], axis=1)
    return values * cosine + swapped * sine


def attend_kernel(
    index, lengths, got, near, far, gain, cosine, sine, latents, ropes,
    out, cache, cache_rope, sums, lifted, turned, means, sems,
    *, kv_size, groups, local, factor, nope,
):
    kv = index[0]
    tp = index[1]
    copies = []
    for s in range(local):
        a = pltpu.make_async_copy(latents.at[s], cache.at[s], sems.at[s])
        b = pltpu.make_async_copy(ropes.at[s], cache_rope.at[s], sems.at[local + s])
        a.start()
        b.start()
        copies.append((a, b))
    width = cache_rope.shape[1]
    latent_width = cache.shape[2]
    positions = cache.shape[1]
    for h in range(groups):
        total = got[h].astype(F32)
        for k in range(1, kv_size):
            total = total + got[k * groups + h].astype(F32)
        sums[h] = total
    raw = jnp.concatenate([sums[h][0:1, nope + width :] for h in range(groups)], axis=1)
    rope_raw = sums[0][1:2, nope + width :]
    for h in range(1, groups):
        rope_raw = rope_raw + sums[h][1:2, nope + width :]
    square = jnp.sum(raw * raw, axis=1, keepdims=True) / latent_width
    new_latent = (raw * lax.rsqrt(square + EPSILON) * gain[...]).astype(BF16).astype(F32)
    new_seq = lax.rem(kv, local)
    new_rope = rotate(rope_raw, cosine[pl.ds(new_seq, 1), :], sine[pl.ds(new_seq, 1), :])
    new_rope = new_rope.astype(BF16).astype(F32)
    half = groups // 2
    y = tp // 2
    core = lax.rem(tp, 2)
    for i in range(groups):
        step = (0, half - 1, 1, 2)[i % half]
        head = 2 * lax.rem(y + step, half) + (core if i < half else 1 - core)
        q = sums[head]
        w = near if i < half else far
        lifted[i] = dot(q[:, :nope].astype(BF16), w[i % half, :latent_width, :], NT)
        turned[i] = rotate(
            q[:, nope : nope + width].astype(BF16).astype(F32), cosine[...], sine[...]
        )
    position = kv * positions + lanes((groups, positions))
    lane = lanes((groups, 128))
    logs = jnp.full((groups, 128), NEGATIVE, F32)
    for s in range(local):
        q = lifted[:, s, :].astype(BF16)
        qr = turned[:, s, :].astype(BF16)
        for copy in copies[s]:
            copy.wait()
        c = cache[s]
        scores = (dot(q, c, NT) + dot(qr, cache_rope[s], NN)) * factor
        new = (
            jnp.sum(q.astype(F32) * new_latent, axis=1, keepdims=True)
            + jnp.sum(qr.astype(F32) * new_rope, axis=1, keepdims=True)
        ) * factor
        is_new = jnp.logical_and(new_seq == s, kv < local)
        new = jnp.where(is_new, new, NEGATIVE)
        visible = position < lengths[tp * local + s]
        top = jnp.max(jnp.where(visible, scores, NEGATIVE), axis=1, keepdims=True)
        top = jnp.maximum(top, new)
        weight = jnp.where(visible, jnp.exp(scores - top), 0.0)
        new_weight = jnp.where(is_new, jnp.exp(new - top), 0.0)
        total = jnp.sum(weight, axis=1, keepdims=True) + new_weight
        mixed = dot(weight.astype(BF16), c, NN)
        mixed = mixed + new_weight.astype(BF16).astype(F32) * new_latent
        some = total > 0.0
        safe = jnp.where(some, total, 1.0)
        means[s] = mixed / safe
        logs = jnp.where(lane == s, jnp.where(some, top + jnp.log(safe), NEGATIVE), logs)
    for i in range(groups):
        w = near if i < half else far
        x = means[:, i, :].astype(BF16)
        up = dot(x, w[i % half, latent_width : 2 * latent_width, :], NN).astype(BF16)
        for k in range(kv_size):
            out[k, i * local : (i + 1) * local, :] = up
    square = jnp.concatenate([logs, jnp.zeros((128 - groups, 128), F32)], axis=0)
    turned_logs = jnp.transpose(square)[:local]
    high = turned_logs.astype(BF16).astype(F32)
    rest = turned_logs - high
    middle = rest.astype(BF16).astype(F32)
    low = (rest - middle).astype(BF16).astype(F32)
    packed = jnp.where(
        lane < groups,
        high,
        jnp.where(
            lane < 2 * groups,
            pltpu.roll(middle, groups, 1),
            jnp.where(lane < 3 * groups, pltpu.roll(low, 2 * groups, 1), 0.0),
        ),
    ).astype(BF16)
    for k in range(kv_size):
        out[k, groups * local :, :] = packed


def combine_kernel(got, near, far, out, *, kv_size, groups, local, first):
    logs = []
    for k in range(kv_size):
        x = got[k, groups * local :, :].astype(F32)
        logs.append(x + pltpu.roll(x, 128 - groups, 1) + pltpu.roll(x, 128 - 2 * groups, 1))
    top = functools.reduce(jnp.maximum, logs)
    shares = [jnp.exp(x - top) for x in logs]
    total = functools.reduce(jnp.add, shares)
    inverse = 1.0 / total
    shares = [x * inverse for x in shares]
    half = groups // 2
    mixed = jnp.zeros((local, out.shape[2]), F32)
    for i in range(groups):
        head = jnp.zeros((local, 128), F32)
        for k in range(kv_size):
            part = got[k, i * local : (i + 1) * local, :].astype(F32)
            head = head + part * shares[k][:, i : i + 1]
        w = near if i < half else far
        mixed = mixed + dot(head.astype(BF16), w[i % half, first:, :], NN)
    mixed = mixed.astype(BF16)
    for d in range(out.shape[0]):
        out[d] = mixed


def finish_kernel(index, got, gain, out, *, kv_size, groups, local):
    kv = index[0]
    width = got.shape[2]
    for t in range(groups):
        squares = jnp.zeros((local, width), F32)
        for k in range(kv_size):
            x = got[k * groups + t].astype(F32)
            squares = squares + x * x
        mean = jnp.sum(squares, axis=1, keepdims=True) / (width * kv_size)
        own = got[kv * groups + t].astype(F32)
        out[t * local : (t + 1) * local, :] = (
            own * lax.rsqrt(mean + EPSILON) * gain[...]
        ).astype(BF16)


def exchange(value, axes):
    return lax.all_to_all(value, axes, split_axis=0, concat_axis=0, tiled=True)


def on_device(
    tokens,
    token_gain,
    w_query,
    w_down_kv,
    w_rope_key,
    latent_gain,
    w_key_up,
    w_value_up,
    w_out,
    out_gain,
    cache_latent,
    cache_rope,
    lengths,
):
    kv_size = lax.axis_size(KV)
    groups = lax.axis_size("tp")
    everyone = kv_size * groups
    index = jnp.stack([lax.axis_index(KV), lax.axis_index("tp")]).astype(jnp.int32)
    seqs = tokens.shape[0]
    local, positions, latent_width = cache_latent.shape
    rope = cache_rope.shape[2]
    nope = w_key_up.shape[2]
    value = w_value_up.shape[2]
    factor = (nope + rope) ** (-0.5)

    own = jnp.concatenate([w_key_up[0], w_value_up[0], w_out], axis=0)
    cut = own.shape[0] // 2
    up = [(i, (i + 2) % groups) for i in range(groups)]
    down = [(i, (i - 2) % groups) for i in range(groups)]
    before = lax.ppermute(own, "tp", up)
    after = lax.ppermute(own, "tp", down)
    far_low = lax.ppermute(before[:cut], "tp", up)
    far_high = lax.ppermute(after[cut:], "tp", down)
    near = jnp.concatenate([own, before, after, far_low, far_high], axis=0)
    near = near.reshape(4, own.shape[0], own.shape[1])
    far = lax.ppermute(near, "tp", [(i, i ^ 1) for i in range(groups)])

    sent = pl.pallas_call(
        functools.partial(project_kernel, groups=groups, local=local, copies=kv_size),
        out_shape=jax.ShapeDtypeStruct((everyone, local, 256), BF16),
        in_specs=[in_smem()] + [in_vmem()] * 5,
        out_specs=in_vmem(),
        compiler_params=params(8),
        name="project",
    )(index, tokens, token_gain[None], w_query.T, w_down_kv, w_rope_key.T)
    got = exchange(sent, ALL)

    own_length = lax.dynamic_slice_in_dim(
        lengths, lax.axis_index("tp") * local, local, 0
    ).astype(F32)
    inverse_freq = 1.0 / 10000.0 ** (jnp.arange(0, rope, 2, dtype=F32) / rope)
    angles = own_length[:, None] * jnp.concatenate([inverse_freq, inverse_freq])[None, :]
    cosine = jnp.cos(angles)
    sine = jnp.sin(angles) * jnp.where(jnp.arange(rope) < rope // 2, -1.0, 1.0)[None, :]

    sent = pl.pallas_call(
        functools.partial(
            attend_kernel,
            kv_size=kv_size,
            groups=groups,
            local=local,
            factor=factor,
            nope=nope,
        ),
        out_shape=jax.ShapeDtypeStruct((kv_size, groups * local + local, value), BF16),
        in_specs=[in_smem(), in_smem()]
        + [in_vmem()] * 6
        + [pl.BlockSpec(memory_space=pl.ANY)] * 2,
        out_specs=in_vmem(),
        scratch_shapes=[
            pltpu.VMEM((local, positions, latent_width), BF16),
            pltpu.VMEM((local, rope, positions), BF16),
            pltpu.VMEM((groups, local, 256), F32),
            pltpu.VMEM((groups, local, latent_width), F32),
            pltpu.VMEM((groups, local, rope), F32),
            pltpu.VMEM((local, groups, latent_width), F32),
            pltpu.SemaphoreType.DMA((2 * local,)),
        ],
        compiler_params=params(24),
        name="attend",
    )(
        index,
        lengths,
        got,
        near,
        far,
        latent_gain[None],
        cosine,
        sine,
        cache_latent,
        cache_rope.transpose(0, 2, 1),
    )
    got = exchange(sent, KV)

    sent = pl.pallas_call(
        functools.partial(
            combine_kernel,
            kv_size=kv_size,
            groups=groups,
            local=local,
            first=2 * latent_width,
        ),
        out_shape=jax.ShapeDtypeStruct((everyone, local, w_out.shape[1]), BF16),
        in_specs=[in_vmem()] * 3,
        out_specs=in_vmem(),
        compiler_params=params(8),
        name="combine",
    )(got, near, far)
    got = exchange(sent, ALL)
    return pl.pallas_call(
        functools.partial(finish_kernel, kv_size=kv_size, groups=groups, local=local),
        out_shape=jax.ShapeDtypeStruct((seqs, w_out.shape[1]), BF16),
        in_specs=[in_smem(), in_vmem(), in_vmem()],
        out_specs=in_vmem(),
        compiler_params=params(8),
        name="finish",
    )(index, got, out_gain[None])


def solution(mesh):
    finer = Mesh(mesh.devices.reshape(4, 4, mesh.shape["tp"]), ("kv_0", "kv_1", "tp"))

    return jax.shard_map(
        on_device,
        mesh=finer,
        in_specs=(
            P(None, KV),
            P(KV),
            P(KV, "tp"),
            P(KV, None),
            P(KV, None),
            P(),
            P("tp", None, None),
            P("tp", None, None),
            P("tp", KV),
            P(KV),
            P("tp", KV, None),
            P("tp", KV, None),
            P(),
        ),
        out_specs=P(None, KV),
        check_vma=False,
    )
```

time: 202 us -> 83.1 us (0.41)
  blocking collectives: 132 us -> 26.9 us
  between operations: 13.5 us -> 0.18 us
  matrix products: 11.5 us -> 0 us
  Pallas kernels: 0 us -> 10.2 us
  starting transfers between devices: 8.97 us -> 18 us
  other arithmetic: 7.72 us -> 1.36 us
  waiting for transfers between devices: 25.1 us -> 20.3 us
  local copies, waits for them, and re-layouts: 2.73 us -> 4.98 us
    all_gather x4 -> x0, blocking collectives: 84.4 us -> none  [over_pieces(): parts = lax.all_gather(value, axis)]
    all_gather x2 -> x0, waiting for transfers between devices: 19.7 us -> none  [over_pieces(): parts = lax.all_gather(value, axis)]
    pmax x2 -> x0, blocking collectives: 18.7 us -> none  [by_axis(): return functools.reduce(lax.pmax, axes, value)]
    psum x2 -> x0, blocking collectives: 18.7 us -> none  [over_axes(): value = lax.psum(value, axis)]
    all_to_all x1 -> x2, blocking collectives: 9.71 us -> 26.9 us  [exchange(): return lax.all_to_all(value, axes, split_axis=0, concat_axis=0, tiled=True)]
    dot_general x10 -> x0, matrix products: 11.5 us -> none  [the longest x1 3.54 us: on_device(): jnp.einsum('bhl,blc->bhc', weights.astype(jnp.bfloat16), cache_latent, pr...]
    pallas_call x0 -> x4, Pallas kernels: none -> 10.2 us  [the longest x1 6.45 us: on_device(): pl.pallas_call(functools.partial(attend_kernel, kv_size=kv_size, groups=g...]
    all_to_all x2 -> x1, waiting for transfers between devices: 5.36 us -> 13.2 us  [exchange(): return lax.all_to_all(value, axes, split_axis=0, concat_axis=0, tiled=True)]
  transfers between devices with their start and end apart: 4 -> 6, of which waited for: 2 -> 3; matrix products, arithmetic and copies ran while one was open for 6% -> 4% of each run, Pallas kernels for 0% -> 2%
where the time goes in v2:
time: 83.1 us; the launch traced here: 82 us
  blocking collectives  26.9 us (32%)
  waiting for transfers between devices  20.3 us (24%)
  starting transfers between devices  18 us (22%)
  Pallas kernels  10.2 us (12%)
  local copies, waits for them, and re-layouts  4.98 us (6%)
  other arithmetic  1.36 us (2%)
    all_to_all x2, blocking collectives, exchange(): return lax.all_to_all(value, axes, split_axis=0, concat_axis=0, tiled=True)  26.9 us
    all_to_all x1, waiting for transfers between devices, exchange(): return lax.all_to_all(value, axes, split_axis=0, concat_axis=0, tiled=True)  13.2 us
    all_to_all x1, starting transfers between devices, exchange(): return lax.all_to_all(value, axes, split_axis=0, concat_axis=0, tiled=True)  11.2 us
    pallas_call x1, Pallas kernels, on_device(): pl.pallas_call(functools.partial(attend_kernel, kv_size=kv_size, groups=g...  6.45 us
    unnamed x26, local copies, waits for them, and re-layouts  4.94 us
    ppermute x1, waiting for transfers between devices, on_device(): before = lax.ppermute(own, 'tp', up)  4.24 us
    ppermute x1, starting transfers between devices, on_device(): far_high = lax.ppermute(after[cut:], 'tp', down)  3 us
    ppermute x1, waiting for transfers between devices, on_device(): far_low = lax.ppermute(before[:cut], 'tp', up)  2.9 us
  transfers between devices with their start and end apart: 6, of which 3 were waited for; matrix products, arithmetic and copies ran while one was open for 4% of the time, Pallas kernels for 2%

profile of v2, /device:TPU:0, one launch (start us, length us, event | category | flops | bytes accessed | tf_op | source)
XLA Modules:
  0.0 82.0 jit_solution(7640527106815544663)
XLA Ops:
  0.0 1.0 %pad_maximum_fusion = bf16[1152,128]{1,0:T(8,128)(2,1)S(1)} fusion(bf16[128,128]{1,0:T(8,128)(2,1)} %param.21, bf16[512,128]{1,0:T(8,128)(2,1)} %bitcast.23, bf16[512,128]{1,0:T(8,128)(2,1)} %bitcast.22), kind=kLoop, calls=%fused_computation | loop fusion | flops 884736 | bytes 589824 | tf_op jit(solution)/shard_map/concatenate | solution.py:250
  1.0 1.8 %collective-permute-start = (bf16[1152,128]{1,0:T(8,128)(2,1)S(1)}, bf16[1152,128]{1,0:T(8,128)(2,1)S(1)}, u32[]{:S(2)}, u32[]{:S(2)}) collective-permute-start(bf16[1152,128]{1,0:T(8,128)(2,1)S(1)} %pad_maximum_fusion), channel_id=1, source_target_pairs={{0,2},{1,3},{2,4},{3,5},{4,6},{5,7},{6,0},{7,1},{8,10},{9,11},{10,... | collective-permute-start | bytes 884744 | tf_op jit(solution)/shard_map/ppermute | solution.py:254
  2.8 1.5 %collective-permute-start.1 = (bf16[1152,128]{1,0:T(8,128)(2,1)S(1)}, bf16[1152,128]{1,0:T(8,128)(2,1)S(1)}, u32[]{:S(2)}, u32[]{:S(2)}) collective-permute-start(bf16[1152,128]{1,0:T(8,128)(2,1)S(1)} %pad_maximum_fusion), channel_id=1, source_target_pairs={{0,6},{1,7},{2,0},{3,1},{4,2},{5,3},{6,4},{7,5},{8,14},{9,15},{10,... | collective-permute-start | bytes 884744 | tf_op jit(solution)/shard_map/ppermute | solution.py:255
  4.3 0.9 %constant_dynamic-update-slice_fusion.6 = bf16[4608,128]{1,0:T(8,128)(2,1)S(1)} fusion(bf16[1,512,128]{2,1,0:T(8,128)(2,1)} %param.19), kind=kLoop, calls=%fused_computation.7 | loop fusion | bytes 262144
  5.2 0.9 %constant_dynamic-update-slice_fusion.5 = bf16[4608,128]{1,0:T(8,128)(2,1)S(1)} fusion(bf16[4608,128]{1,0:T(8,128)(2,1)S(1)} %constant_dynamic-update-slice_fusion.6, bf16[1,512,128]{2,1,0:T(8,128)(2,1)} %param.20), kind=kLoop, calls=%fused_computation.6 | loop fusion | bytes 262144
  6.2 0.8 constant_dynamic-update-slice_fusion.4
  6.9 0.0 copy-start.2
  6.9 0.0 copy-start.3
  6.9 0.0 copy-start.4
  6.9 0.0 copy-start.5
  7.0 0.0 copy-start.9
  7.0 4.2 %collective-permute-done = bf16[1152,128]{1,0:T(8,128)(2,1)S(1)} collective-permute-done((bf16[1152,128]{1,0:T(8,128)(2,1)S(1)}, bf16[1152,128]{1,0:T(8,128)(2,1)S(1)}, u32[]{:S(2)}, u32[]{:S(2)}) %collective-permute-start) | collective-permute-done | bytes 294944 | tf_op jit(solution)/shard_map/ppermute | solution.py:254
  11.2 0.4 collective-permute-start.2
  11.6 0.0 collective-permute-done.1
  11.6 3.0 %collective-permute-start.3 = (bf16[576,128]{1,0:T(8,128)(2,1)S(1)}, bf16[576,128]{1,0:T(8,128)(2,1)S(1)}, u32[]{:S(2)}, u32[]{:S(2)}) collective-permute-start(bf16[576,128]{1,0:T(8,128)(2,1)S(1)} %slice.9), channel_id=1, source_target_pairs={{0,6},{1,7},{2,0},{3,1},{4,2},{5,3},{6,4},{7,5},{8,14},{9,15},{10,... | collective-permute-start | bytes 442376 | tf_op jit(solution)/shard_map/ppermute | solution.py:257
  14.7 0.0 copy-start.7
  14.7 0.0 copy-start.1
  14.7 0.0 copy-start.6
  14.7 2.9 %collective-permute-done.2 = bf16[576,128]{1,0:T(8,128)(2,1)S(1)} collective-permute-done((bf16[576,128]{1,0:T(8,128)(2,1)S(1)}, bf16[576,128]{1,0:T(8,128)(2,1)S(1)}, u32[]{:S(2)}, u32[]{:S(2)}) %collective-permute-start.2) | collective-permute-done | bytes 147488 | tf_op jit(solution)/shard_map/ppermute | solution.py:256
  17.7 0.0 collective-permute-done.3
  17.7 0.1 collective-permute-start.4
  17.8 0.1 pad_add_fusion.index
  17.9 0.0 copy-done.2
  17.9 0.0 copy-done.3
  17.9 0.0 copy-done.4
  17.9 0.0 copy-done.5
  17.9 0.0 copy-done.9
  17.9 2.0 %project.1 = bf16[128,8,256]{2,1,0:T(8,128)(2,1)} custom-call(s32[2]{0:T(128)S(1)} %pad_add_fusion.index, bf16[64,128]{1,0:T(8,128)(2,1)S(1)} %copy-done.4, f32[1,128]{1,0:T(1,128)S(1)} %bitcast.21, bf16[192,128]{1,0:T(8,128)(2,1)S(1)} %bitcast.17, bf16[128,512]{1,0:T(8,128)(2,1)S(1)} %copy-done.2, bf16[64,128]{1,0:T(8,128)(2,1)S(1)} %bitcast.18), custom_call_target="tpu_custom_call" | custom-call | tf_op jit(solution)/shard_map/project/pallas_call | solution.py:262
  19.9 11.2 %all-to-all-start = ((bf16[128,8,256]{2,1,0:T(8,128)(2,1)}), bf16[128,8,256]{2,1,0:T(8,128)(2,1)S(1)}, u32[]{:S(2)}, u32[]{:S(2)}) async-start(bf16[128,8,256]{2,1,0:T(8,128)(2,1)} %project.1), calls=%async_computation | async-start | bytes 1048576 | tf_op jit(solution)/shard_map/all_to_all | solution.py:221
  31.2 0.0 copy-done.7
  31.2 0.1 dynamic-slice_convert_fusion
  31.3 0.1 compare_select_fusion
  31.4 0.1 fusion
  31.5 13.2 %all-to-all-done.got = bf16[128,8,256]{2,1,0:T(8,128)(2,1)S(1)} async-done(((bf16[128,8,256]{2,1,0:T(8,128)(2,1)}), bf16[128,8,256]{2,1,0:T(8,128)(2,1)S(1)}, u32[]{:S(2)}, u32[]{:S(2)}) %all-to-all-start) | async-done | bytes 524320 | tf_op jit(solution)/shard_map/all_to_all | solution.py:221
  44.7 0.0 collective-permute-done.4.far
  44.7 0.0 copy-done.1
  44.7 0.0 copy-done.6
  44.7 0.0 copy-start
  44.7 2.2 %copy-done = bf16[8,512,512]{2,1,0:T(8,128)(2,1)S(1)} copy-done((bf16[8,512,512]{2,1,0:T(8,128)(2,1)S(1)}, bf16[8,512,512]{2,1,0:T(8,128)(2,1)}, u32[]{:S(2)}) %copy-start) | copy-done | bytes 4194328
  46.9 6.5 %attend.1 = bf16[16,72,128]{2,1,0:T(8,128)(2,1)S(1)} custom-call(s32[2]{0:T(128)S(1)} %pad_add_fusion.index, s32[64]{0:T(128)S(1)} %copy-done.7, bf16[128,8,256]{2,1,0:T(8,128)(2,1)S(1)} %all-to-all-done.got, bf16[4,1152,128]{2,1,0:T(8,128)(2,1)S(1)} %bitcast.14, bf16[4,1152,128]{2,1,0:T(8,128)(2,1)S(1)} %collective-permute-done.4.far, ...), custom_call_target="tpu_custom_call" | custom-call | tf_op jit(solution)/shard_map/attend/pallas_call | solution.py:280
  53.3 11.7 %all_to_all.15.got = bf16[16,72,128]{2,1,0:T(8,128)(2,1)S(1)} all-to-all(bf16[16,72,128]{2,1,0:T(8,128)(2,1)S(1)} %attend.1), channel_id=1, replica_groups=mesh['kv_0'=4,'kv_1'=4,'tp'=8] {'kv_0','kv_1'}, dimensions={0} | all-to-all | bytes 589824 | tf_op jit(solution)/shard_map/all_to_all | solution.py:221
  65.0 0.0 copy-start.8
  65.1 0.5 combine.1
  65.5 15.2 %all_to_all.16.got = bf16[128,8,128]{2,1,0:T(8,128)(2,1)S(1)} all-to-all(bf16[128,8,128]{2,1,0:T(8,128)(2,1)S(1)} %combine.1), channel_id=1, replica_groups=mesh['kv_0'=4,'kv_1'=4,'tp'=8] {'kv_0','kv_1','tp'}, dimensions={0} | all-to-all | bytes 524288 | tf_op jit(solution)/shard_map/all_to_all | solution.py:221
  80.7 0.0 copy-done.8
  80.7 1.3 %finish.1 = bf16[64,128]{1,0:T(8,128)(2,1)} custom-call(s32[2]{0:T(128)S(1)} %pad_add_fusion.index, bf16[128,8,128]{2,1,0:T(8,128)(2,1)S(1)} %all_to_all.16.got, f32[1,128]{1,0:T(1,128)S(1)} %bitcast.20), custom_call_target="tpu_custom_call" | custom-call | tf_op jit(solution)/shard_map/finish/pallas_call | solution.py:334
  (7 shorter events, 0.2 us)
Async XLA Ops:
  1.0 10.2 %collective-permute-start = (bf16[1152,128]{1,0:T(8,128)(2,1)S(1)}, bf16[1152,128]{1,0:T(8,128)(2,1)S(1)}, u32[]{:S(2)}, u32[]{:S(2)}) collective-permute-start(bf16[1152,128]{1,0:T(8,128)(2,1)S(1)} %pad_maximum_fusion), channel_id=1, source_target_pairs={{0,2},{1,3},{2,4},{3,5},{4,6},{5,7},{6,0},{7,1},{8,10},{9,11},{10,... | collective-permute-start | bytes 884744 | tf_op jit(solution)/shard_map/ppermute | solution.py:254
  2.8 8.8 %collective-permute-start.1 = (bf16[1152,128]{1,0:T(8,128)(2,1)S(1)}, bf16[1152,128]{1,0:T(8,128)(2,1)S(1)}, u32[]{:S(2)}, u32[]{:S(2)}) collective-permute-start(bf16[1152,128]{1,0:T(8,128)(2,1)S(1)} %pad_maximum_fusion), channel_id=1, source_target_pairs={{0,6},{1,7},{2,0},{3,1},{4,2},{5,3},{6,4},{7,5},{8,14},{9,15},{10,... | collective-permute-start | bytes 884744 | tf_op jit(solution)/shard_map/ppermute | solution.py:255
  6.9 11.0 %copy-start.2 = (bf16[128,512]{1,0:T(8,128)(2,1)S(1)}, bf16[128,512]{1,0:T(8,128)(2,1)}, u32[]{:S(2)}) copy-start(bf16[128,512]{1,0:T(8,128)(2,1)} %wd.1) | copy-start | bytes 393220
  6.9 11.0 %copy-start.3 = (bf16[128,192]{0,1:T(8,128)(2,1)S(1)}, bf16[128,192]{0,1:T(8,128)(2,1)}, u32[]{:S(2)}) copy-start(bf16[128,192]{0,1:T(8,128)(2,1)} %param.15) | copy-start | bytes 147460
  6.9 11.0 %copy-start.4 = (bf16[64,128]{1,0:T(8,128)(2,1)S(1)}, bf16[64,128]{1,0:T(8,128)(2,1)}, u32[]{:S(2)}) copy-start(bf16[64,128]{1,0:T(8,128)(2,1)} %tokens.1) | copy-start | bytes 49156
  6.9 11.0 %copy-start.5 = (bf16[128,64]{0,1:T(8,128)(2,1)S(1)}, bf16[128,64]{0,1:T(8,128)(2,1)}, u32[]{:S(2)}) copy-start(bf16[128,64]{0,1:T(8,128)(2,1)} %param.17) | copy-start | bytes 49156
  7.0 10.9 %copy-start.9 = (f32[128]{0:T(128)S(1)}, f32[128]{0:T(128)}, u32[]{:S(2)}) copy-start(f32[128]{0:T(128)} %param.14) | copy-start | bytes 1540
  11.2 6.4 %collective-permute-start.2 = (bf16[576,128]{1,0:T(8,128)(2,1)S(1)}, bf16[576,128]{1,0:T(8,128)(2,1)S(1)}, u32[]{:S(2)}, u32[]{:S(2)}) collective-permute-start(bf16[576,128]{1,0:T(8,128)(2,1)S(1)} %slice.8), channel_id=1, source_target_pairs={{0,2},{1,3},{2,4},{3,5},{4,6},{5,7},{6,0},{7,1},{8,10},{9,11},{10,... | collective-permute-start | bytes 442376 | tf_op jit(solution)/shard_map/ppermute | solution.py:256
  11.6 6.1 %collective-permute-start.3 = (bf16[576,128]{1,0:T(8,128)(2,1)S(1)}, bf16[576,128]{1,0:T(8,128)(2,1)S(1)}, u32[]{:S(2)}, u32[]{:S(2)}) collective-permute-start(bf16[576,128]{1,0:T(8,128)(2,1)S(1)} %slice.9), channel_id=1, source_target_pairs={{0,6},{1,7},{2,0},{3,1},{4,2},{5,3},{6,4},{7,5},{8,14},{9,15},{10,... | collective-permute-start | bytes 442376 | tf_op jit(solution)/shard_map/ppermute | solution.py:257
  14.7 16.5 %copy-start.7 = (s32[64]{0:T(128)S(1)}, s32[64]{0:T(128)}, u32[]{:S(2)}) copy-start(s32[64]{0:T(128)} %lengths.1) | copy-start | bytes 772
  14.7 30.0 %copy-start.1 = (bf16[8,512,64]{1,2,0:T(8,128)(2,1)S(1)}, bf16[8,512,64]{1,2,0:T(8,128)(2,1)}, u32[]{:S(2)}) copy-start(bf16[8,512,64]{1,2,0:T(8,128)(2,1)} %param.24) | copy-start | bytes 1572868
  14.7 29.9 %copy-start.6 = (f32[512]{0:T(512)S(1)}, f32[512]{0:T(512)}, u32[]{:S(2)}) copy-start(f32[512]{0:T(512)} %param.18) | copy-start | bytes 6148
  17.7 27.0 %collective-permute-start.4 = (bf16[4,1152,128]{2,1,0:T(8,128)(2,1)S(1)}, bf16[4,1152,128]{2,1,0:T(8,128)(2,1)S(1)}, u32[]{:S(2)}, u32[]{:S(2)}) collective-permute-start(bf16[4,1152,128]{2,1,0:T(8,128)(2,1)S(1)} %bitcast.13), channel_id=1, source_target_pairs={{0,1},{1,0},{2,3},{3,2},{4,5},{5,4},{6,7},{7,6},{8,9},{9,8},{10,11... | collective-permute-start | bytes 3538952 | tf_op jit(solution)/shard_map/ppermute | solution.py:260
  19.9 24.7 %all-to-all-start = ((bf16[128,8,256]{2,1,0:T(8,128)(2,1)}), bf16[128,8,256]{2,1,0:T(8,128)(2,1)S(1)}, u32[]{:S(2)}, u32[]{:S(2)}) async-start(bf16[128,8,256]{2,1,0:T(8,128)(2,1)} %project.1), calls=%async_computation | async-start | bytes 1048576 | tf_op jit(solution)/shard_map/all_to_all | solution.py:221
  44.7 2.2 %copy-start = (bf16[8,512,512]{2,1,0:T(8,128)(2,1)S(1)}, bf16[8,512,512]{2,1,0:T(8,128)(2,1)}, u32[]{:S(2)}) copy-start(bf16[8,512,512]{2,1,0:T(8,128)(2,1)} %latents.1) | copy-start | bytes 12582916
  65.0 15.6 %copy-start.8 = (f32[128]{0:T(128)S(1)}, f32[128]{0:T(128)}, u32[]{:S(2)}) copy-start(f32[128]{0:T(128)} %param.22) | copy-start | bytes 1540

commit v3 on v2

v3 whole, which is shorter than its diff:
```python
import functools

import jax
import jax.numpy as jnp
from jax import lax
from jax.experimental import pallas as pl
from jax.experimental.pallas import tpu as pltpu
from jax.sharding import Mesh
from jax.sharding import PartitionSpec as P


KV = ("kv_0", "kv_1")
ALL = ("kv_0", "kv_1", "tp")
EPSILON = 1e-06
NEGATIVE = -1e30
F32 = jnp.float32
BF16 = jnp.bfloat16

NT = (((1,), (1,)), ((), ()))
NN = (((1,), (0,)), ((), ()))


def dot(a, b, dims):
    return lax.dot_general(a, b, dims, preferred_element_type=F32)


def params(mib):
    return pltpu.CompilerParams(vmem_limit_bytes=mib * 1024 * 1024)


def in_vmem():
    return pl.BlockSpec(memory_space=pltpu.VMEM)


def in_hbm():
    return pl.BlockSpec(memory_space=pltpu.HBM)


def lanes(shape):
    return lax.broadcasted_iota(jnp.int32, shape, 1)


def project_kernel(
    tokens, gain, wq, wd, wr, wk, wv, wo, out, key, own, tokens_, gain_, wq_, wd_, wr_, mixed, sems
):
    kv = lax.axis_index(KV)
    tp = lax.axis_index("tp")
    groups = lax.axis_size("tp")
    half_rows = key.shape[0]
    values = wv.shape[1]
    pairs = (
        (tokens, tokens_),
        (gain, gain_),
        (wq, wq_),
        (wd, wd_),
        (wr, wr_),
        (wk.at[0, pl.ds(lax.rem(kv, 2) * half_rows, half_rows)], key),
        (wv.at[0], own.at[pl.ds(0, values)]),
        (wo, own.at[pl.ds(values, wo.shape[0])]),
    )
    copies = [pltpu.make_async_copy(x, y, sems.at[n]) for n, (x, y) in enumerate(pairs)]
    for copy in copies:
        copy.start()
    for copy in copies[:5]:
        copy.wait()
    scaled = (tokens_[...].astype(F32) * gain_[...]).astype(BF16)
    query = dot(scaled, wq_[...], NT)
    latent = dot(scaled, wd_[...], NN)
    rope = dot(scaled, wr_[...], NT)
    chunk = latent.shape[1] // groups
    part = latent[:, :chunk]
    for g in range(1, groups):
        part = jnp.where(tp == g, latent[:, g * chunk : (g + 1) * chunk], part)
    width = rope.shape[1]
    rope = jnp.where(lanes(rope.shape) // (width // groups) == tp, rope, 0.0)
    local = mixed.shape[1]
    tiles = (
        query[:, :128],
        jnp.concatenate([query[:, 128:], part], axis=1),
        jnp.concatenate([rope, jnp.zeros_like(rope)], axis=1),
    )
    for n, tile in enumerate(tiles):
        mixed[:, :, n * 128 : (n + 1) * 128] = tile.reshape(groups, local, 128)
    for s in range(local):
        tile = mixed[:, s, :].astype(BF16)
        out[2 * s] = tile
        out[2 * s + 1] = tile
    for copy in copies[5:]:
        copy.wait()


def lift_kernel(got, key, out, *, nope, rope):
    kv = lax.axis_index(KV)
    kv_size, groups, _ = got.shape
    total = got[0].astype(F32)
    for k in range(1, kv_size):
        total = total + got[k].astype(F32)
    lifted = dot(total[:, :nope].astype(BF16), key[...], NT)
    query_rope = total[:, nope : nope + rope].astype(BF16).astype(F32)
    latent = total[:, nope + rope : 256]
    new_rope = total[:, 256 : 256 + rope]
    last = jnp.concatenate(
        [jnp.where(lax.rem(kv, 2) == 0, query_rope, new_rope), latent], axis=1
    )
    row = jnp.concatenate([lifted, last], axis=1)
    for t in range(groups):
        for k in range(kv_size):
            out[k * groups + t] = row[t : t + 1]


def rotate(values, cosine, sine):
    half = values.shape[1] // 2
    swapped = jnp.concatenate([values[:, half:], values[:, :half]], axis=1)
    return values * cosine + swapped * sine


def slot_head(i):
    tp = lax.axis_index("tp")
    groups = lax.axis_size("tp")
    half = groups // 2
    core = lax.rem(tp, 2)
    step = (0, half - 1, 1, 2)[i % half]
    return 2 * lax.rem(tp // 2 + step, half) + (core if i < half else 1 - core)


def attend_kernel(
    got, lengths, gain, cosine, sine, latents, ropes, means, packed, cache, cache_rope, slots, sems,
    *, factor,
):
    kv = lax.axis_index(KV)
    local, positions, latent_width = cache.shape
    rope = cache_rope.shape[1]
    groups = slots.shape[1]
    copies = []
    for s in range(local):
        a = pltpu.make_async_copy(latents.at[s], cache.at[s], sems.at[s])
        b = pltpu.make_async_copy(ropes.at[s], cache_rope.at[s], sems.at[local + s])
        a.start()
        b.start()
        copies.append((a, b))
    heads = [slot_head(i) for i in range(groups)]
    for i in range(groups):
        for n in range(2 * local):
            slots[n, i : i + 1, :] = got[n * groups + heads[i]]
    new_seq = lax.rem(kv, local)
    first = [got[2 * new_seq * groups + h] for h in range(groups)]
    second = [got[(2 * new_seq + 1) * groups + h] for h in range(groups)]
    raw = jnp.concatenate([x[:, 256 + rope :] for x in first], axis=1)
    rope_raw = functools.reduce(jnp.add, [x[:, 256 : 256 + rope] for x in second])
    square = jnp.sum(raw * raw, axis=1, keepdims=True) / latent_width
    new_latent = (raw * lax.rsqrt(square + EPSILON) * gain[...]).astype(BF16).astype(F32)
    new_rope = rotate(rope_raw, cosine[pl.ds(new_seq, 1), :], sine[pl.ds(new_seq, 1), :])
    new_rope = new_rope.astype(BF16).astype(F32)
    position = kv * positions + lanes((groups, positions))
    lane = lanes((groups, 128))
    logs = jnp.full((groups, 128), NEGATIVE, F32)
    for s in range(local):
        even = slots[2 * s]
        q = jnp.concatenate([even[:, :256], slots[2 * s + 1][:, :256]], axis=1).astype(BF16)
        qr = rotate(even[:, 256 : 256 + rope], cosine[s : s + 1, :], sine[s : s + 1, :])
        qr = qr.astype(BF16)
        for copy in copies[s]:
            copy.wait()
        c = cache[s]
        scores = (dot(q, c, NT) + dot(qr, cache_rope[s], NN)) * factor
        new = (
            jnp.sum(q.astype(F32) * new_latent, axis=1, keepdims=True)
            + jnp.sum(qr.astype(F32) * new_rope, axis=1, keepdims=True)
        ) * factor
        is_new = jnp.logical_and(new_seq == s, kv < local)
        new = jnp.where(is_new, new, NEGATIVE)
        visible = position < lengths[s : s + 1, :1]
        top = jnp.max(jnp.where(visible, scores, NEGATIVE), axis=1, keepdims=True)
        top = jnp.maximum(top, new)
        weight = jnp.where(visible, jnp.exp(scores - top), 0.0)
        new_weight = jnp.where(is_new, jnp.exp(new - top), 0.0)
        total = jnp.sum(weight, axis=1, keepdims=True) + new_weight
        mixed = dot(weight.astype(BF16), c, NN)
        mixed = mixed + new_weight.astype(BF16).astype(F32) * new_latent
        some = total > 0.0
        safe = jnp.where(some, total, 1.0)
        means[s] = mixed / safe
        logs = jnp.where(lane == s, jnp.where(some, top + jnp.log(safe), NEGATIVE), logs)
    square = jnp.concatenate([logs, jnp.zeros((128 - groups, 128), F32)], axis=0)
    turned = jnp.transpose(square)[:local]
    high = turned.astype(BF16).astype(F32)
    rest = turned - high
    middle = rest.astype(BF16).astype(F32)
    low = (rest - middle).astype(BF16).astype(F32)
    packed[...] = jnp.where(
        lane < groups,
        high,
        jnp.where(
            lane < 2 * groups,
            pltpu.roll(middle, groups, 1),
            jnp.where(lane < 3 * groups, pltpu.roll(low, 2 * groups, 1), 0.0),
        ),
    ).astype(BF16)


def up_kernel(means, packed, near, far, out):
    local, groups, latent_width = means.shape
    half = groups // 2
    kv_size = out.shape[0]
    for i in range(groups):
        w = near if i < half else far
        x = means[:, i, :].astype(BF16)
        up = dot(x, w[i % half, :latent_width, :], NN).astype(BF16)
        for k in range(kv_size):
            out[k, i * local : (i + 1) * local, :] = up
    logs = packed[...]
    for k in range(kv_size):
        out[k, groups * local :, :] = logs


def combine_kernel(got, near, far, out, *, kv_size, groups, local, first):
    logs = []
    for k in range(kv_size):
        x = got[k, groups * local :, :].astype(F32)
        logs.append(x + pltpu.roll(x, 128 - groups, 1) + pltpu.roll(x, 128 - 2 * groups, 1))
    top = functools.reduce(jnp.maximum, logs)
    shares = [jnp.exp(x - top) for x in logs]
    total = functools.reduce(jnp.add, shares)
    inverse = 1.0 / total
    shares = [x * inverse for x in shares]
    half = groups // 2
    mixed = jnp.zeros((local, out.shape[2]), F32)
    for i in range(groups):
        head = jnp.zeros((local, 128), F32)
        for k in range(kv_size):
            part = got[k, i * local : (i + 1) * local, :].astype(F32)
            head = head + part * shares[k][:, i : i + 1]
        w = near if i < half else far
        mixed = mixed + dot(head.astype(BF16), w[i % half, first:, :], NN)
    mixed = mixed.astype(BF16)
    for d in range(out.shape[0]):
        out[d] = mixed


def finish_kernel(got, gain, out, *, kv_size, groups, local):
    kv = lax.axis_index(KV)
    width = got.shape[2]
    for t in range(groups):
        squares = jnp.zeros((local, width), F32)
        for k in range(kv_size):
            x = got[k * groups + t].astype(F32)
            squares = squares + x * x
        mean = jnp.sum(squares, axis=1, keepdims=True) / (width * kv_size)
        own = got[kv * groups + t].astype(F32)
        out[t * local : (t + 1) * local, :] = (
            own * lax.rsqrt(mean + EPSILON) * gain[...]
        ).astype(BF16)


def exchange(value, axes):
    return lax.all_to_all(value, axes, split_axis=0, concat_axis=0, tiled=True)


def on_device(
    tokens,
    token_gain,
    w_query,
    w_down_kv,
    w_rope_key,
    latent_gain,
    w_key_up,
    w_value_up,
    w_out,
    out_gain,
    cache_latent,
    cache_rope,
    lengths,
):
    kv_size = lax.axis_size(KV)
    groups = lax.axis_size("tp")
    everyone = kv_size * groups
    seqs, width = tokens.shape
    local, positions, latent_width = cache_latent.shape
    rope = cache_rope.shape[2]
    nope = w_key_up.shape[2]
    value = w_value_up.shape[2]
    factor = (nope + rope) ** (-0.5)

    own_length = lax.dynamic_slice_in_dim(lengths, lax.axis_index("tp") * local, local, 0)
    inverse_freq = 1.0 / 10000.0 ** (jnp.arange(0, rope, 2, dtype=F32) / rope)
    angles = own_length.astype(F32)[:, None] * jnp.concatenate([inverse_freq, inverse_freq])[None]
    cosine = jnp.cos(angles)
    sine = jnp.sin(angles) * jnp.where(jnp.arange(rope) < rope // 2, -1.0, 1.0)[None, :]
    own_length = jnp.broadcast_to(own_length[:, None], (local, 128))

    sent, key, own = pl.pallas_call(
        project_kernel,
        out_shape=(
            jax.ShapeDtypeStruct((kv_size, groups, 384), BF16),
            jax.ShapeDtypeStruct((latent_width // 2, nope), BF16),
            jax.ShapeDtypeStruct((latent_width + value, value), BF16),
        ),
        in_specs=[in_hbm()] * 8,
        out_specs=(in_vmem(),) * 3,
        scratch_shapes=[
            pltpu.VMEM((seqs, width), BF16),
            pltpu.VMEM((1, width), F32),
            pltpu.VMEM((nope + rope, width), BF16),
            pltpu.VMEM((width, latent_width), BF16),
            pltpu.VMEM((rope, width), BF16),
            pltpu.VMEM((groups, local, 384), F32),
            pltpu.SemaphoreType.DMA((8,)),
        ],
        compiler_params=params(8),
        name="project",
    )(
        tokens,
        token_gain[None],
        w_query.T,
        w_down_kv,
        w_rope_key.T,
        w_key_up,
        w_value_up,
        w_out,
    )
    got = exchange(sent, KV)

    cut = own.shape[0] // 2
    up = [(i, (i + 2) % groups) for i in range(groups)]
    down = [(i, (i - 2) % groups) for i in range(groups)]
    before = lax.ppermute(own, "tp", up)
    after = lax.ppermute(own, "tp", down)
    far_low = lax.ppermute(before[:cut], "tp", up)
    far_high = lax.ppermute(after[cut:], "tp", down)
    near = jnp.concatenate([own, before, after, far_low, far_high], axis=0)
    near = near.reshape(4, own.shape[0], own.shape[1])
    far = lax.ppermute(near, "tp", [(i, i ^ 1) for i in range(groups)])

    sent = pl.pallas_call(
        functools.partial(lift_kernel, nope=nope, rope=rope),
        out_shape=jax.ShapeDtypeStruct((everyone, 1, 384), F32),
        in_specs=[in_vmem()] * 2,
        out_specs=in_vmem(),
        compiler_params=params(8),
        name="lift",
    )(got, key)
    got = exchange(sent, ALL)

    means, packed = pl.pallas_call(
        functools.partial(attend_kernel, factor=factor),
        out_shape=(
            jax.ShapeDtypeStruct((local, groups, latent_width), F32),
            jax.ShapeDtypeStruct((local, 128), BF16),
        ),
        in_specs=[in_vmem()] * 5 + [in_hbm()] * 2,
        out_specs=(in_vmem(),) * 2,
        scratch_shapes=[
            pltpu.VMEM((local, positions, latent_width), BF16),
            pltpu.VMEM((local, rope, positions), BF16),
            pltpu.VMEM((2 * local, groups, 384), F32),
            pltpu.SemaphoreType.DMA((2 * local,)),
        ],
        compiler_params=params(24),
        name="attend",
    )(got, own_length, latent_gain[None], cosine, sine, cache_latent, cache_rope.transpose(0, 2, 1))
    sent = pl.pallas_call(
        up_kernel,
        out_shape=jax.ShapeDtypeStruct((kv_size, groups * local + local, value), BF16),
        in_specs=[in_vmem()] * 4,
        out_specs=in_vmem(),
        compiler_params=params(8),
        name="value_up",
    )(means, packed, near, far)
    got = exchange(sent, KV)

    sent = pl.pallas_call(
        functools.partial(
            combine_kernel,
            kv_size=kv_size,
            groups=groups,
            local=local,
            first=latent_width,
        ),
        out_shape=jax.ShapeDtypeStruct((everyone, local, w_out.shape[1]), BF16),
        in_specs=[in_vmem()] * 3,
        out_specs=in_vmem(),
        compiler_params=params(8),
        name="combine",
    )(got, near, far)
    got = exchange(sent, ALL)
    return pl.pallas_call(
        functools.partial(finish_kernel, kv_size=kv_size, groups=groups, local=local),
        out_shape=jax.ShapeDtypeStruct((seqs, w_out.shape[1]), BF16),
        in_specs=[in_vmem(), in_vmem()],
        out_specs=in_vmem(),
        compiler_params=params(8),
        name="finish",
    )(got, out_gain[None])


def solution(mesh):
    finer = Mesh(mesh.devices.reshape(4, 4, mesh.shape["tp"]), ("kv_0", "kv_1", "tp"))

    return jax.shard_map(
        on_device,
        mesh=finer,
        in_specs=(
            P(None, KV),
            P(KV),
            P(KV, "tp"),
            P(KV, None),
            P(KV, None),
            P(),
            P("tp", None, None),
            P("tp", None, None),
            P("tp", KV),
            P(KV),
            P("tp", KV, None),
            P("tp", KV, None),
            P(),
        ),
        out_specs=P(None, KV),
        check_vma=False,
    )
```

time: 83.1 us -> 94.3 us (1.13)
  local copies, waits for them, and re-layouts: 4.98 us -> 10.4 us
  starting transfers between devices: 18 us -> 21.2 us
  waiting for transfers between devices: 20.3 us -> 23.2 us
    unnamed x26 -> x28, local copies, waits for them, and re-layouts: 4.94 us -> 10.3 us
    all_to_all x1 -> x2, waiting for transfers between devices: 13.2 us -> 16.9 us  [exchange(): return lax.all_to_all(value, axes, split_axis=0, concat_axis=0, tiled=True)]
    all_to_all x1 -> x2, starting transfers between devices: 11.2 us -> 14.5 us  [exchange(): return lax.all_to_all(value, axes, split_axis=0, concat_axis=0, tiled=True)]
    concatenate x1 -> x0, other arithmetic: 1.01 us -> none  [on_device(): own = jnp.concatenate([w_key_up[0], w_value_up[0], w_out], axis=0)]
    pallas_call x2 -> x4, Pallas kernels: 8.48 us -> 8.57 us  [the longest x1 5.43 us: on_device(): pl.pallas_call(functools.partial(attend_kernel, factor=factor), out_shape...]
  transfers between devices with their start and end apart: 6 -> 7, of which waited for: 3 -> 4; matrix products, arithmetic and copies ran while one was open for 4% -> 1% of each run, Pallas kernels for 2% -> 7%
where the time goes in v3:
time: 94.3 us; the launch traced here: 92.9 us
  blocking collectives  27.2 us (29%)
  waiting for transfers between devices  23.2 us (25%)
  starting transfers between devices  21.2 us (22%)
  local copies, waits for them, and re-layouts  10.4 us (11%)
  Pallas kernels  9.8 us (10%)
    all_to_all x2, blocking collectives, exchange(): return lax.all_to_all(value, axes, split_axis=0, concat_axis=0, tiled=True)  27.2 us
    all_to_all x2, waiting for transfers between devices, exchange(): return lax.all_to_all(value, axes, split_axis=0, concat_axis=0, tiled=True)  16.9 us
    all_to_all x2, starting transfers between devices, exchange(): return lax.all_to_all(value, axes, split_axis=0, concat_axis=0, tiled=True)  14.5 us
    unnamed x28, local copies, waits for them, and re-layouts  10.3 us
    pallas_call x1, Pallas kernels, on_device(): pl.pallas_call(functools.partial(attend_kernel, factor=factor), out_shape...  5.43 us
    ppermute x1, waiting for transfers between devices, on_device(): before = lax.ppermute(own, 'tp', up)  4.07 us
    ppermute x1, starting transfers between devices, on_device(): far_high = lax.ppermute(after[cut:], 'tp', down)  3 us
    ppermute x1, waiting for transfers between devices, on_device(): far_low = lax.ppermute(before[:cut], 'tp', up)  2.28 us
  transfers between devices with their start and end apart: 7, of which 4 were waited for; matrix products, arithmetic and copies ran while one was open for 1% of the time, Pallas kernels for 7%

profile of v3, /device:TPU:0, one launch (start us, length us, event | category | flops | bytes accessed | tf_op | source)
XLA Modules:
  0.0 92.9 jit_solution(1165462412780569996)
XLA Ops:
  0.0 0.0 copy-start.2
  0.0 0.9 copy-done.2
  0.9 0.0 copy-start.3
  0.9 0.9 copy-done.3
  1.8 0.0 copy-start.4
  1.8 0.9 copy-done.4
  2.7 0.0 copy-start.5
  2.7 0.8 copy-done.5
  3.5 0.0 copy-start.6
  3.5 0.8 copy-done.6
  4.3 0.0 copy-start.7
  4.3 0.7 copy-done.7
  5.0 0.0 copy-start.8
  5.0 0.7 copy-done.8
  5.7 0.0 copy-start.10
  5.7 0.7 copy-done.10
  6.4 2.0 %project.1 = (bf16[16,8,384]{2,1,0:T(8,128)(2,1)}, bf16[256,128]{1,0:T(8,128)(2,1)S(1)}, bf16[640,128]{1,0:T(8,128)(2,1)S(1)}) custom-call(bf16[64,128]{1,0:T(8,128)(2,1)S(1)} %copy-done.7, f32[1,128]{1,0:T(1,128)S(1)} %bitcast.14, bf16[192,128]{1,0:T(8,128)(2,1)S(1)} %bitcast.11, bf16[128,512]{1,0:T(8,128)(2,1)S(1)} %copy-done.2, ...), custom_call_target="tpu_custom_call" | custom-call | tf_op jit(solution)/shard_map/project/pallas_call | solution.py:291
  8.4 1.8 %collective-permute-start = (bf16[640,128]{1,0:T(8,128)(2,1)S(1)}, bf16[640,128]{1,0:T(8,128)(2,1)S(1)}, u32[]{:S(2)}, u32[]{:S(2)}) collective-permute-start(bf16[640,128]{1,0:T(8,128)(2,1)S(1)} %get-tuple-element.14), channel_id=1, source_target_pairs={{0,2},{1,3},{2,4},{3,5},{4,6},{5,7},{6,0},{7,1},{8,10},{9,11},{10,... | collective-permute-start | bytes 491528 | tf_op jit(solution)/shard_map/ppermute | solution.py:326
  10.1 1.5 %collective-permute-start.1 = (bf16[640,128]{1,0:T(8,128)(2,1)S(1)}, bf16[640,128]{1,0:T(8,128)(2,1)S(1)}, u32[]{:S(2)}, u32[]{:S(2)}) collective-permute-start(bf16[640,128]{1,0:T(8,128)(2,1)S(1)} %get-tuple-element.14), channel_id=1, source_target_pairs={{0,6},{1,7},{2,0},{3,1},{4,2},{5,3},{6,4},{7,5},{8,14},{9,15},{10,... | collective-permute-start | bytes 491528 | tf_op jit(solution)/shard_map/ppermute | solution.py:327
  11.7 4.1 %collective-permute-done = bf16[640,128]{1,0:T(8,128)(2,1)S(1)} collective-permute-done((bf16[640,128]{1,0:T(8,128)(2,1)S(1)}, bf16[640,128]{1,0:T(8,128)(2,1)S(1)}, u32[]{:S(2)}, u32[]{:S(2)}) %collective-permute-start) | collective-permute-done | bytes 163872 | tf_op jit(solution)/shard_map/ppermute | solution.py:326
  15.8 0.3 collective-permute-start.2
  16.1 0.0 collective-permute-done.1
  16.1 3.0 %collective-permute-start.3 = (bf16[320,128]{1,0:T(8,128)(2,1)S(1)}, bf16[320,128]{1,0:T(8,128)(2,1)S(1)}, u32[]{:S(2)}, u32[]{:S(2)}) collective-permute-start(bf16[320,128]{1,0:T(8,128)(2,1)S(1)} %slice.9), channel_id=1, source_target_pairs={{0,6},{1,7},{2,0},{3,1},{4,2},{5,3},{6,4},{7,5},{8,14},{9,15},{10,... | collective-permute-start | bytes 245768 | tf_op jit(solution)/shard_map/ppermute | solution.py:329
  19.1 2.3 %collective-permute-done.2 = bf16[320,128]{1,0:T(8,128)(2,1)S(1)} collective-permute-done((bf16[320,128]{1,0:T(8,128)(2,1)S(1)}, bf16[320,128]{1,0:T(8,128)(2,1)S(1)}, u32[]{:S(2)}, u32[]{:S(2)}) %collective-permute-start.2) | collective-permute-done | bytes 81952 | tf_op jit(solution)/shard_map/ppermute | solution.py:328
  21.4 0.0 collective-permute-done.3
  21.5 0.1 collective-permute-start.4
  21.5 7.9 %all-to-all-start = ((bf16[16,8,384]{2,1,0:T(8,128)(2,1)}), bf16[16,8,384]{2,1,0:T(8,128)(2,1)S(1)}, u32[]{:S(2)}, u32[]{:S(2)}) async-start(bf16[16,8,384]{2,1,0:T(8,128)(2,1)} %get-tuple-element.10), calls=%async_computation | async-start | bytes 196608 | tf_op jit(solution)/shard_map/all_to_all | solution.py:256
  29.5 0.1 compare_select_fusion
  29.5 0.7 fusion.1
  30.3 7.0 %all-to-all-done.got = bf16[16,8,384]{2,1,0:T(8,128)(2,1)S(1)} async-done(((bf16[16,8,384]{2,1,0:T(8,128)(2,1)}), bf16[16,8,384]{2,1,0:T(8,128)(2,1)S(1)}, u32[]{:S(2)}, u32[]{:S(2)}) %all-to-all-start) | async-done | bytes 98336 | tf_op jit(solution)/shard_map/all_to_all | solution.py:256
  37.3 0.9 lift.1
  38.1 6.6 %all-to-all-start.1 = ((f32[128,1,384]{2,1,0:T(1,128)}), f32[128,1,384]{2,1,0:T(1,128)S(1)}, u32[]{:S(2)}, u32[]{:S(2)}) async-start(f32[128,1,384]{2,1,0:T(1,128)} %lift.1), calls=%async_computation.1 | async-start | bytes 393216 | tf_op jit(solution)/shard_map/all_to_all | solution.py:256
  44.7 0.1 fusion
  44.8 9.9 %all-to-all-done.1.got = f32[128,1,384]{2,1,0:T(1,128)S(1)} async-done(((f32[128,1,384]{2,1,0:T(1,128)}), f32[128,1,384]{2,1,0:T(1,128)S(1)}, u32[]{:S(2)}, u32[]{:S(2)}) %all-to-all-start.1) | async-done | bytes 196640 | tf_op jit(solution)/shard_map/all_to_all | solution.py:256
  54.7 0.1 broadcast_in_dim.27.lengths
  54.8 0.0 copy-start
  54.8 2.2 %copy-done = bf16[8,512,512]{2,1,0:T(8,128)(2,1)S(1)} copy-done((bf16[8,512,512]{2,1,0:T(8,128)(2,1)S(1)}, bf16[8,512,512]{2,1,0:T(8,128)(2,1)}, u32[]{:S(2)}) %copy-start) | copy-done | bytes 4194328
  57.0 0.0 copy-start.1
  57.0 1.0 %copy-done.1 = bf16[8,512,64]{1,2,0:T(8,128)(2,1)S(1)} copy-done((bf16[8,512,64]{1,2,0:T(8,128)(2,1)S(1)}, bf16[8,512,64]{1,2,0:T(8,128)(2,1)}, u32[]{:S(2)}) %copy-start.1) | copy-done | bytes 524312
  58.0 0.0 copy-start.9
  58.0 0.7 copy-done.9
  58.7 0.0 copy-start.11
  58.7 5.4 %attend.1 = (f32[8,8,512]{2,1,0:T(8,128)S(1)}, bf16[8,128]{1,0:T(8,128)(2,1)S(1)}) custom-call(f32[128,1,384]{2,1,0:T(1,128)S(1)} %all-to-all-done.1.got, s32[8,128]{1,0:T(8,128)S(1)} %broadcast_in_dim.27.lengths, f32[1,512]{1,0:T(1,128)S(1)} %bitcast.13, f32[8,64]{1,0:T(8,128)S(1)} %get-tuple-element.18.cosine, f32[8,64]{1,0:T(8,128)S(1)} %get-tuple-element.17.sine, ...), custom_call_target="tpu_custom_call" | custom-call | tf_op jit(solution)/shard_map/attend/pallas_call | solution.py:344
  64.1 0.0 collective-permute-done.4.far
  64.2 0.3 value_up.1
  64.5 12.0 %all_to_all.20.got = bf16[16,72,128]{2,1,0:T(8,128)(2,1)S(1)} all-to-all(bf16[16,72,128]{2,1,0:T(8,128)(2,1)S(1)} %value_up.1), channel_id=1, replica_groups=mesh['kv_0'=4,'kv_1'=4,'tp'=8] {'kv_0','kv_1'}, dimensions={0} | all-to-all | bytes 589824 | tf_op jit(solution)/shard_map/all_to_all | solution.py:256
  76.5 0.5 combine.1
  77.0 15.2 %all_to_all.21.got = bf16[128,8,128]{2,1,0:T(8,128)(2,1)S(1)} all-to-all(bf16[128,8,128]{2,1,0:T(8,128)(2,1)S(1)} %combine.1), channel_id=1, replica_groups=mesh['kv_0'=4,'kv_1'=4,'tp'=8] {'kv_0','kv_1','tp'}, dimensions={0} | all-to-all | bytes 524288 | tf_op jit(solution)/shard_map/all_to_all | solution.py:256
  92.2 0.0 copy-done.11
  92.2 0.8 finish.1
  (8 shorter events, 0.1 us)
Async XLA Ops:
  0.0 0.9 copy-start.2
  0.9 0.9 copy-start.3
  1.8 0.9 copy-start.4
  2.7 0.8 copy-start.5
  3.5 0.8 copy-start.6
  4.3 0.7 copy-start.7
  5.0 0.7 copy-start.8
  5.7 0.7 copy-start.10
  8.4 7.4 %collective-permute-start = (bf16[640,128]{1,0:T(8,128)(2,1)S(1)}, bf16[640,128]{1,0:T(8,128)(2,1)S(1)}, u32[]{:S(2)}, u32[]{:S(2)}) collective-permute-start(bf16[640,128]{1,0:T(8,128)(2,1)S(1)} %get-tuple-element.14), channel_id=1, source_target_pairs={{0,2},{1,3},{2,4},{3,5},{4,6},{5,7},{6,0},{7,1},{8,10},{9,11},{10,... | collective-permute-start | bytes 491528 | tf_op jit(solution)/shard_map/ppermute | solution.py:326
  10.1 6.0 %collective-permute-start.1 = (bf16[640,128]{1,0:T(8,128)(2,1)S(1)}, bf16[640,128]{1,0:T(8,128)(2,1)S(1)}, u32[]{:S(2)}, u32[]{:S(2)}) collective-permute-start(bf16[640,128]{1,0:T(8,128)(2,1)S(1)} %get-tuple-element.14), channel_id=1, source_target_pairs={{0,6},{1,7},{2,0},{3,1},{4,2},{5,3},{6,4},{7,5},{8,14},{9,15},{10,... | collective-permute-start | bytes 491528 | tf_op jit(solution)/shard_map/ppermute | solution.py:327
  15.8 5.7 %collective-permute-start.2 = (bf16[320,128]{1,0:T(8,128)(2,1)S(1)}, bf16[320,128]{1,0:T(8,128)(2,1)S(1)}, u32[]{:S(2)}, u32[]{:S(2)}) collective-permute-start(bf16[320,128]{1,0:T(8,128)(2,1)S(1)} %slice.8), channel_id=1, source_target_pairs={{0,2},{1,3},{2,4},{3,5},{4,6},{5,7},{6,0},{7,1},{8,10},{9,11},{10,... | collective-permute-start | bytes 245768 | tf_op jit(solution)/shard_map/ppermute | solution.py:328
  16.1 5.4 %collective-permute-start.3 = (bf16[320,128]{1,0:T(8,128)(2,1)S(1)}, bf16[320,128]{1,0:T(8,128)(2,1)S(1)}, u32[]{:S(2)}, u32[]{:S(2)}) collective-permute-start(bf16[320,128]{1,0:T(8,128)(2,1)S(1)} %slice.9), channel_id=1, source_target_pairs={{0,6},{1,7},{2,0},{3,1},{4,2},{5,3},{6,4},{7,5},{8,14},{9,15},{10,... | collective-permute-start | bytes 245768 | tf_op jit(solution)/shard_map/ppermute | solution.py:329
  21.5 42.7 %collective-permute-start.4 = (bf16[4,640,128]{2,1,0:T(8,128)(2,1)S(1)}, bf16[4,640,128]{2,1,0:T(8,128)(2,1)S(1)}, u32[]{:S(2)}, u32[]{:S(2)}) collective-permute-start(bf16[4,640,128]{2,1,0:T(8,128)(2,1)S(1)} %bitcast.7), channel_id=1, source_target_pairs={{0,1},{1,0},{2,3},{3,2},{4,5},{5,4},{6,7},{7,6},{8,9},{9,8},{10,11... | collective-permute-start | bytes 1966088 | tf_op jit(solution)/shard_map/ppermute | solution.py:332
  21.5 15.7 %all-to-all-start = ((bf16[16,8,384]{2,1,0:T(8,128)(2,1)}), bf16[16,8,384]{2,1,0:T(8,128)(2,1)S(1)}, u32[]{:S(2)}, u32[]{:S(2)}) async-start(bf16[16,8,384]{2,1,0:T(8,128)(2,1)} %get-tuple-element.10), calls=%async_computation | async-start | bytes 196608 | tf_op jit(solution)/shard_map/all_to_all | solution.py:256
  38.1 16.6 %all-to-all-start.1 = ((f32[128,1,384]{2,1,0:T(1,128)}), f32[128,1,384]{2,1,0:T(1,128)S(1)}, u32[]{:S(2)}, u32[]{:S(2)}) async-start(f32[128,1,384]{2,1,0:T(1,128)} %lift.1), calls=%async_computation.1 | async-start | bytes 393216 | tf_op jit(solution)/shard_map/all_to_all | solution.py:256
  54.8 2.2 %copy-start = (bf16[8,512,512]{2,1,0:T(8,128)(2,1)S(1)}, bf16[8,512,512]{2,1,0:T(8,128)(2,1)}, u32[]{:S(2)}) copy-start(bf16[8,512,512]{2,1,0:T(8,128)(2,1)} %latents.1) | copy-start | bytes 12582916
  57.0 1.0 %copy-start.1 = (bf16[8,512,64]{1,2,0:T(8,128)(2,1)S(1)}, bf16[8,512,64]{1,2,0:T(8,128)(2,1)}, u32[]{:S(2)}) copy-start(bf16[8,512,64]{1,2,0:T(8,128)(2,1)} %param.24) | copy-start | bytes 1572868
  58.0 0.7 copy-start.9
  58.7 33.4 %copy-start.11 = (f32[128]{0:T(128)S(1)}, f32[128]{0:T(128)}, u32[]{:S(2)}) copy-start(f32[128]{0:T(128)} %param.22) | copy-start | bytes 1540

commit v4 on v2

--- a/solution.py
+++ b/solution.py
@@ -32,8 +32,12 @@
     return pl.BlockSpec(memory_space=pltpu.VMEM)
 
 
-def in_smem():
-    return pl.BlockSpec(memory_space=pltpu.SMEM)
+def in_hbm():
+    return pl.BlockSpec(memory_space=pltpu.HBM)
+
+
+def keep_in_hbm(*arrays):
+    return [pltpu.with_memory_space_constraint(x, pltpu.HBM) for x in arrays]
 
 
 def lanes(shape):
@@ -44,21 +48,42 @@
     return lax.broadcasted_iota(jnp.int32, shape, 0)
 
 
-def project_kernel(index, tokens, gain, wq, wd, wr, out, *, groups, local, copies):
-    tp = index[1]
-    scaled = (tokens[...].astype(F32) * gain[...]).astype(BF16)
-    query = dot(scaled, wq[...], NT)
-    latent = dot(scaled, wd[...], NN)
-    rope = dot(scaled, wr[...], NT)
+def project_kernel(
+    tokens, gain, wq, wd, wr, wk, wv, wo, out, own, tokens_, gain_, wq_, wd_, wr_, sems
+):
+    tp = lax.axis_index("tp")
+    groups = lax.axis_size("tp")
+    kv_size = lax.axis_size(KV)
+    deep = wk.shape[1]
+    pairs = (
+        (tokens, tokens_),
+        (gain, gain_),
+        (wq, wq_),
+        (wd, wd_),
+        (wr, wr_),
+        (wk.at[0], own.at[pl.ds(0, deep)]),
+        (wv.at[0], own.at[pl.ds(deep, deep)]),
+        (wo, own.at[pl.ds(2 * deep, wo.shape[0])]),
+    )
+    copies = [pltpu.make_async_copy(x, y, sems.at[n]) for n, (x, y) in enumerate(pairs)]
+    for copy in copies:
+        copy.start()
+    for copy in copies[:5]:
+        copy.wait()
+    scaled = (tokens_[...].astype(F32) * gain_[...]).astype(BF16)
+    query = dot(scaled, wq_[...], NT)
+    latent = dot(scaled, wd_[...], NN)
+    rope = dot(scaled, wr_[...], NT)
     seqs = scaled.shape[0]
+    local = seqs // groups
     chunk = latent.shape[1] // groups
-    own = jnp.zeros((seqs, chunk), F32)
-    for g in range(groups):
-        own = jnp.where(tp == g, latent[:, g * chunk : (g + 1) * chunk], own)
+    part = latent[:, :chunk]
+    for g in range(1, groups):
+        part = jnp.where(tp == g, latent[:, g * chunk : (g + 1) * chunk], part)
     width = rope.shape[1]
     rope = jnp.where(lanes(rope.shape) // (width // groups) == tp, rope, 0.0)
     blank = jnp.zeros((seqs, 128 - width), F32)
-    own = jnp.concatenate([blank, own], axis=1)
+    part = jnp.concatenate([blank, part], axis=1)
     rope = jnp.concatenate([blank, rope], axis=1)
     first = query[:, :128].astype(BF16)
     second = jnp.concatenate([query[:, 128:], blank], axis=1)
@@ -68,12 +93,14 @@
         low = second[t * local : (t + 1) * local]
         for j in range(local):
             r = t * local + j
-            new = jnp.where(row == 0, own[r : r + 1], 0.0) + jnp.where(row == 1, rope[r : r + 1], 0.0)
+            new = jnp.where(row == 0, part[r : r + 1], 0.0) + jnp.where(row == 1, rope[r : r + 1], 0.0)
             tile = (low + new).astype(BF16)
-            for c in range(copies // local):
+            for c in range(kv_size // local):
                 b = (c * local + j) * groups + t
                 out[b, :, :128] = top
                 out[b, :, 128:] = tile
+    for copy in copies[5:]:
+        copy.wait()
 
 
 def rotate(values, cosine, sine):
@@ -83,12 +110,15 @@
 
 
 def attend_kernel(
-    index, lengths, got, near, far, gain, cosine, sine, latents, ropes,
+    got, lengths, near, far, gain, cosine, sine, latents, ropes,
     out, cache, cache_rope, sums, lifted, turned, means, sems,
-    *, kv_size, groups, local, factor, nope,
+    *, factor, nope,
 ):
-    kv = index[0]
-    tp = index[1]
+    kv = lax.axis_index(KV)
+    tp = lax.axis_index("tp")
+    kv_size = lax.axis_size(KV)
+    groups = lax.axis_size("tp")
+    local = cache.shape[0]
     copies = []
     for s in range(local):
         a = pltpu.make_async_copy(latents.at[s], cache.at[s], sems.at[s])
@@ -141,7 +171,7 @@
         ) * factor
         is_new = jnp.logical_and(new_seq == s, kv < local)
         new = jnp.where(is_new, new, NEGATIVE)
-        visible = position < lengths[tp * local + s]
+        visible = position < lengths[s : s + 1, :1]
         top = jnp.max(jnp.where(visible, scores, NEGATIVE), axis=1, keepdims=True)
         top = jnp.maximum(top, new)
         weight = jnp.where(visible, jnp.exp(scores - top), 0.0)
@@ -202,8 +232,8 @@
         out[d] = mixed
 
 
-def finish_kernel(index, got, gain, out, *, kv_size, groups, local):
-    kv = index[0]
+def finish_kernel(got, gain, out, *, kv_size, groups, local):
+    kv = lax.axis_index(KV)
     width = got.shape[2]
     for t in range(groups):
         squares = jnp.zeros((local, width), F32)
@@ -239,57 +269,64 @@
     kv_size = lax.axis_size(KV)
     groups = lax.axis_size("tp")
     everyone = kv_size * groups
-    index = jnp.stack([lax.axis_index(KV), lax.axis_index("tp")]).astype(jnp.int32)
-    seqs = tokens.shape[0]
+    seqs, width = tokens.shape
     local, positions, latent_width = cache_latent.shape
     rope = cache_rope.shape[2]
     nope = w_key_up.shape[2]
     value = w_value_up.shape[2]
     factor = (nope + rope) ** (-0.5)
 
-    own = jnp.concatenate([w_key_up[0], w_value_up[0], w_out], axis=0)
-    cut = own.shape[0] // 2
-    up = [(i, (i + 2) % groups) for i in range(groups)]
-    down = [(i, (i - 2) % groups) for i in range(groups)]
-    before = lax.ppermute(own, "tp", up)
-    after = lax.ppermute(own, "tp", down)
-    far_low = lax.ppermute(before[:cut], "tp", up)
-    far_high = lax.ppermute(after[cut:], "tp", down)
-    near = jnp.concatenate([own, before, after, far_low, far_high], axis=0)
-    near = near.reshape(4, own.shape[0], own.shape[1])
-    far = lax.ppermute(near, "tp", [(i, i ^ 1) for i in range(groups)])
-
-    sent = pl.pallas_call(
-        functools.partial(project_kernel, groups=groups, local=local, copies=kv_size),
-        out_shape=jax.ShapeDtypeStruct((everyone, local, 256), BF16),
-        in_specs=[in_smem()] + [in_vmem()] * 5,
-        out_specs=in_vmem(),
+    own_length = lax.dynamic_slice_in_dim(lengths, lax.axis_index("tp") * local, local, 0)
+    inverse_freq = 1.0 / 10000.0 ** (jnp.arange(0, rope, 2, dtype=F32) / rope)
+    angles = own_length.astype(F32)[:, None] * jnp.concatenate([inverse_freq, inverse_freq])[None]
+    cosine = jnp.cos(angles)
+    sine = jnp.sin(angles) * jnp.where(jnp.arange(rope) < rope // 2, -1.0, 1.0)[None, :]
+    own_length = jnp.broadcast_to(own_length[:, None], (local, 128))
+
+    sent, own = pl.pallas_call(
+        project_kernel,
+        out_shape=(
+            jax.ShapeDtypeStruct((everyone, local, 256), BF16),
+            jax.ShapeDtypeStruct((2 * latent_width + value, nope), BF16),
+        ),
+        in_specs=[in_hbm()] * 8,
+        out_specs=(in_vmem(),) * 2,
+        scratch_shapes=[
+            pltpu.VMEM((seqs, width), BF16),
+            pltpu.VMEM((1, width), F32),
+            pltpu.VMEM((nope + rope, width), BF16),
+            pltpu.VMEM((width, latent_width), BF16),
+            pltpu.VMEM((rope, width), BF16),
+            pltpu.SemaphoreType.DMA((8,)),
+        ],
         compiler_params=params(8),
         name="project",
-    )(index, tokens, token_gain[None], w_query.T, w_down_kv, w_rope_key.T)
+    )(
+        *keep_in_hbm(
+            tokens,
+            token_gain[None],
+            w_query.T,
+            w_down_kv,
+            w_rope_key.T,
+            w_key_up,
+            w_value_up,
+            w_out,
+        )
+    )
+
+    collected = [own]
+    for step in (1, 3, 2):
+        collected.append(
+            lax.ppermute(own, "tp", [(i, (i + 2 * step) % groups) for i in range(groups)])
+        )
+    near = jnp.stack(collected)
+    far = lax.ppermute(near, "tp", [(i, i ^ 1) for i in range(groups)])
+
     got = exchange(sent, ALL)
-
-    own_length = lax.dynamic_slice_in_dim(
-        lengths, lax.axis_index("tp") * local, local, 0
-    ).astype(F32)
-    inverse_freq = 1.0 / 10000.0 ** (jnp.arange(0, rope, 2, dtype=F32) / rope)
-    angles = own_length[:, None] * jnp.concatenate([inverse_freq, inverse_freq])[None, :]
-    cosine = jnp.cos(angles)
-    sine = jnp.sin(angles) * jnp.where(jnp.arange(rope) < rope // 2, -1.0, 1.0)[None, :]
-
     sent = pl.pallas_call(
-        functools.partial(
-            attend_kernel,
-            kv_size=kv_size,
-            groups=groups,
-            local=local,
-            factor=factor,
-            nope=nope,
-        ),
+        functools.partial(attend_kernel, factor=factor, nope=nope),
         out_shape=jax.ShapeDtypeStruct((kv_size, groups * local + local, value), BF16),
-        in_specs=[in_smem(), in_smem()]
-        + [in_vmem()] * 6
-        + [pl.BlockSpec(memory_space=pl.ANY)] * 2,
+        in_specs=[in_vmem()] * 7 + [in_hbm()] * 2,
         out_specs=in_vmem(),
         scratch_shapes=[
             pltpu.VMEM((local, positions, latent_width), BF16),
@@ -303,16 +340,14 @@
         compiler_params=params(24),
         name="attend",
     )(
-        index,
-        lengths,
         got,
+        own_length,
         near,
         far,
         latent_gain[None],
         cosine,
         sine,
-        cache_latent,
-        cache_rope.transpose(0, 2, 1),
+        *keep_in_hbm(cache_latent, cache_rope.transpose(0, 2, 1)),
     )
     got = exchange(sent, KV)
 
@@ -334,11 +369,11 @@
     return pl.pallas_call(
         functools.partial(finish_kernel, kv_size=kv_size, groups=groups, local=local),
         out_shape=jax.ShapeDtypeStruct((seqs, w_out.shape[1]), BF16),
-        in_specs=[in_smem(), in_vmem(), in_vmem()],
+        in_specs=[in_vmem(), in_vmem()],
         out_specs=in_vmem(),
         compiler_params=params(8),
         name="finish",
-    )(index, got, out_gain[None])
+    )(got, out_gain[None])
 
 
 def solution(mesh):

time: 83.1 us -> 79.3 us (0.954)
  local copies, waits for them, and re-layouts: 4.98 us -> 0.08 us
  waiting for transfers between devices: 20.3 us -> 24.9 us
  starting transfers between devices: 18 us -> 16.3 us
  other arithmetic: 1.36 us -> 0.42 us
    unnamed x26 -> x6, local copies, waits for them, and re-layouts: 4.94 us -> 0.01 us
    ppermute x4 -> x3, waiting for transfers between devices: 7.15 us -> 11.7 us  [on_device(): lax.ppermute(own, 'tp', [(i, (i + 2 * step) % groups) for i in range(grou...]
    ppermute x4 -> x3, starting transfers between devices: 6.68 us -> 5.41 us  [on_device(): lax.ppermute(own, 'tp', [(i, (i + 2 * step) % groups) for i in range(grou...]
    concatenate x1 -> x0, other arithmetic: 1.01 us -> none  [on_device(): own = jnp.concatenate([w_key_up[0], w_value_up[0], w_out], axis=0)]
  transfers between devices with their start and end apart: 6 -> 5, of which waited for: 3 -> 3; matrix products, arithmetic and copies ran while one was open for 4% -> 0% of each run, Pallas kernels for 2% -> 0%
where the time goes in v4:
time: 79.3 us; the launch traced here: 78.3 us
  blocking collectives  26.9 us (34%)
  waiting for transfers between devices  24.9 us (31%)
  starting transfers between devices  16.3 us (21%)
  Pallas kernels  9.63 us (12%)
    all_to_all x2, blocking collectives, exchange(): return lax.all_to_all(value, axes, split_axis=0, concat_axis=0, tiled=True)  26.9 us
    all_to_all x1, waiting for transfers between devices, exchange(): return lax.all_to_all(value, axes, split_axis=0, concat_axis=0, tiled=True)  13.2 us
    ppermute x3, waiting for transfers between devices, on_device(): lax.ppermute(own, 'tp', [(i, (i + 2 * step) % groups) for i in range(grou...  11.7 us
    all_to_all x1, starting transfers between devices, exchange(): return lax.all_to_all(value, axes, split_axis=0, concat_axis=0, tiled=True)  10.8 us
    pallas_call x1, Pallas kernels, on_device(): pl.pallas_call(functools.partial(attend_kernel, factor=factor, nope=nope)...  5.88 us
    ppermute x3, starting transfers between devices, on_device(): lax.ppermute(own, 'tp', [(i, (i + 2 * step) % groups) for i in range(grou...  5.41 us
    pallas_call x1, Pallas kernels, on_device(): pl.pallas_call(project_kernel, out_shape=(jax.ShapeDtypeStruct((everyone,...  2.52 us
  transfers between devices with their start and end apart: 5, of which 3 were waited for; matrix products, arithmetic and copies ran while one was open for 0% of the time, Pallas kernels for 0%

profile of v4, /device:TPU:0, one launch (start us, length us, event | category | flops | bytes accessed | tf_op | source)
XLA Modules:
  0.0 78.3 jit_solution(13746236683572333867)
XLA Ops:
  0.0 2.5 %project.1 = (bf16[128,8,256]{2,1,0:T(8,128)(2,1)}, bf16[1152,128]{1,0:T(8,128)(2,1)S(1)}) custom-call(bf16[64,128]{1,0:T(8,128)(2,1)} %tokens.1, f32[1,128]{1,0:T(1,128)} %bitcast.19, bf16[192,128]{1,0:T(8,128)(2,1)} %bitcast.17, bf16[128,512]{1,0:T(8,128)(2,1)} %wd.1, bf16[64,128]{1,0:T(8,128)(2,1)} %bitcast.18, bf16[1,512,128]{2,1,0:T(8,128)(2,1)} %wk.1, ...), custom_call_target="tpu_custom_call" | custom-call | tf_op jit(solution)/shard_map/project/pallas_call | solution.py:286
  2.5 3.4 %collective-permute-start.2 = (bf16[1152,128]{1,0:T(8,128)(2,1)S(1)}, bf16[1152,128]{1,0:T(8,128)(2,1)S(1)}, u32[]{:S(2)}, u32[]{:S(2)}) collective-permute-start(bf16[1152,128]{1,0:T(8,128)(2,1)S(1)} %get-tuple-element.8), channel_id=1, source_target_pairs={{0,4},{1,5},{2,6},{3,7},{4,0},{5,1},{6,2},{7,3},{8,12},{9,13},{10,... | collective-permute-start | bytes 884744 | tf_op jit(solution)/shard_map/ppermute | solution.py:320
  5.9 1.1 %collective-permute-start.1 = (bf16[1152,128]{1,0:T(8,128)(2,1)S(1)}, bf16[1152,128]{1,0:T(8,128)(2,1)S(1)}, u32[]{:S(2)}, u32[]{:S(2)}) collective-permute-start(bf16[1152,128]{1,0:T(8,128)(2,1)S(1)} %get-tuple-element.8), channel_id=1, source_target_pairs={{0,6},{1,7},{2,0},{3,1},{4,2},{5,3},{6,4},{7,5},{8,14},{9,15},{10,... | collective-permute-start | bytes 884744 | tf_op jit(solution)/shard_map/ppermute | solution.py:320
  7.0 1.0 %collective-permute-start = (bf16[1152,128]{1,0:T(8,128)(2,1)S(1)}, bf16[1152,128]{1,0:T(8,128)(2,1)S(1)}, u32[]{:S(2)}, u32[]{:S(2)}) collective-permute-start(bf16[1152,128]{1,0:T(8,128)(2,1)S(1)} %get-tuple-element.8), channel_id=1, source_target_pairs={{0,2},{1,3},{2,4},{3,5},{4,6},{5,7},{6,0},{7,1},{8,10},{9,11},{10,... | collective-permute-start | bytes 884744 | tf_op jit(solution)/shard_map/ppermute | solution.py:320
  7.9 6.1 %collective-permute-done.2 = bf16[1152,128]{1,0:T(8,128)(2,1)S(1)} collective-permute-done((bf16[1152,128]{1,0:T(8,128)(2,1)S(1)}, bf16[1152,128]{1,0:T(8,128)(2,1)S(1)}, u32[]{:S(2)}, u32[]{:S(2)}) %collective-permute-start.2) | collective-permute-done | bytes 294944 | tf_op jit(solution)/shard_map/ppermute | solution.py:320
  14.0 5.7 %collective-permute-done.1 = bf16[1152,128]{1,0:T(8,128)(2,1)S(1)} collective-permute-done((bf16[1152,128]{1,0:T(8,128)(2,1)S(1)}, bf16[1152,128]{1,0:T(8,128)(2,1)S(1)}, u32[]{:S(2)}, u32[]{:S(2)}) %collective-permute-start.1) | collective-permute-done | bytes 294944 | tf_op jit(solution)/shard_map/ppermute | solution.py:320
  19.7 0.0 collective-permute-done
  19.7 0.0 copy-start.2
  19.7 0.0 copy-start
  19.7 0.1 pad_maximum_fusion.near
  19.8 0.1 collective-permute-start.3
  19.9 10.8 %all-to-all-start = ((bf16[128,8,256]{2,1,0:T(8,128)(2,1)}), bf16[128,8,256]{2,1,0:T(8,128)(2,1)S(1)}, u32[]{:S(2)}, u32[]{:S(2)}) async-start(bf16[128,8,256]{2,1,0:T(8,128)(2,1)} %get-tuple-element.7), calls=%async_computation | async-start | bytes 1048576 | tf_op jit(solution)/shard_map/all_to_all | solution.py:251
  30.7 0.1 compare_select_fusion
  30.8 0.0 copy-done.2
  30.8 0.1 fusion.1
  30.9 0.1 fusion
  31.0 13.2 %all-to-all-done.got = bf16[128,8,256]{2,1,0:T(8,128)(2,1)S(1)} async-done(((bf16[128,8,256]{2,1,0:T(8,128)(2,1)}), bf16[128,8,256]{2,1,0:T(8,128)(2,1)S(1)}, u32[]{:S(2)}, u32[]{:S(2)}) %all-to-all-start) | async-done | bytes 524320 | tf_op jit(solution)/shard_map/all_to_all | solution.py:251
  44.2 0.0 collective-permute-done.3.far
  44.2 0.1 broadcast_in_dim.27.lengths
  44.3 0.0 copy-done
  44.3 5.9 %attend.1 = bf16[16,72,128]{2,1,0:T(8,128)(2,1)S(1)} custom-call(bf16[128,8,256]{2,1,0:T(8,128)(2,1)S(1)} %all-to-all-done.got, s32[8,128]{1,0:T(8,128)S(1)} %broadcast_in_dim.27.lengths, bf16[4,1152,128]{2,1,0:T(8,128)(2,1)S(1)} %pad_maximum_fusion.near, bf16[4,1152,128]{2,1,0:T(8,128)(2,1)S(1)} %collective-permute-done.3.far, f32[1,512]{1,0:T(1,128)S(1)} %bitcast.11, ...), custom_call_target="tpu_custom_call" | custom-call | tf_op jit(solution)/shard_map/attend/pallas_call | solution.py:326
  50.2 11.7 %all_to_all.15.got = bf16[16,72,128]{2,1,0:T(8,128)(2,1)S(1)} all-to-all(bf16[16,72,128]{2,1,0:T(8,128)(2,1)S(1)} %attend.1), channel_id=1, replica_groups=mesh['kv_0'=4,'kv_1'=4,'tp'=8] {'kv_0','kv_1'}, dimensions={0} | all-to-all | bytes 589824 | tf_op jit(solution)/shard_map/all_to_all | solution.py:251
  61.9 0.0 copy-start.1
  61.9 0.5 combine.1
  62.4 15.2 %all_to_all.16.got = bf16[128,8,128]{2,1,0:T(8,128)(2,1)S(1)} all-to-all(bf16[128,8,128]{2,1,0:T(8,128)(2,1)S(1)} %combine.1), channel_id=1, replica_groups=mesh['kv_0'=4,'kv_1'=4,'tp'=8] {'kv_0','kv_1','tp'}, dimensions={0} | all-to-all | bytes 524288 | tf_op jit(solution)/shard_map/all_to_all | solution.py:251
  77.5 0.0 copy-done.1
  77.5 0.8 finish.1
  (1 shorter events, 0.0 us)
Async XLA Ops:
  2.5 11.5 %collective-permute-start.2 = (bf16[1152,128]{1,0:T(8,128)(2,1)S(1)}, bf16[1152,128]{1,0:T(8,128)(2,1)S(1)}, u32[]{:S(2)}, u32[]{:S(2)}) collective-permute-start(bf16[1152,128]{1,0:T(8,128)(2,1)S(1)} %get-tuple-element.8), channel_id=1, source_target_pairs={{0,4},{1,5},{2,6},{3,7},{4,0},{5,1},{6,2},{7,3},{8,12},{9,13},{10,... | collective-permute-start | bytes 884744 | tf_op jit(solution)/shard_map/ppermute | solution.py:320
  5.9 13.8 %collective-permute-start.1 = (bf16[1152,128]{1,0:T(8,128)(2,1)S(1)}, bf16[1152,128]{1,0:T(8,128)(2,1)S(1)}, u32[]{:S(2)}, u32[]{:S(2)}) collective-permute-start(bf16[1152,128]{1,0:T(8,128)(2,1)S(1)} %get-tuple-element.8), channel_id=1, source_target_pairs={{0,6},{1,7},{2,0},{3,1},{4,2},{5,3},{6,4},{7,5},{8,14},{9,15},{10,... | collective-permute-start | bytes 884744 | tf_op jit(solution)/shard_map/ppermute | solution.py:320
  7.0 12.7 %collective-permute-start = (bf16[1152,128]{1,0:T(8,128)(2,1)S(1)}, bf16[1152,128]{1,0:T(8,128)(2,1)S(1)}, u32[]{:S(2)}, u32[]{:S(2)}) collective-permute-start(bf16[1152,128]{1,0:T(8,128)(2,1)S(1)} %get-tuple-element.8), channel_id=1, source_target_pairs={{0,2},{1,3},{2,4},{3,5},{4,6},{5,7},{6,0},{7,1},{8,10},{9,11},{10,... | collective-permute-start | bytes 884744 | tf_op jit(solution)/shard_map/ppermute | solution.py:320
  19.7 11.1 %copy-start.2 = (s32[64]{0:T(128)S(1)}, s32[64]{0:T(128)}, u32[]{:S(2)}) copy-start(s32[64]{0:T(128)} %param.25) | copy-start | bytes 772
  19.7 24.6 %copy-start = (f32[512]{0:T(512)S(1)}, f32[512]{0:T(512)}, u32[]{:S(2)}) copy-start(f32[512]{0:T(512)} %param.18) | copy-start | bytes 6148
  19.8 24.4 %collective-permute-start.3 = (bf16[4,1152,128]{2,1,0:T(8,128)(2,1)S(1)}, bf16[4,1152,128]{2,1,0:T(8,128)(2,1)S(1)}, u32[]{:S(2)}, u32[]{:S(2)}) collective-permute-start(bf16[4,1152,128]{2,1,0:T(8,128)(2,1)S(1)} %pad_maximum_fusion.near), channel_id=1, source_target_pairs={{0,1},{1,0},{2,3},{3,2},{4,5},{5,4},{6,7},{7,6},{8,9},{9,8},{10,11... | collective-permute-start | bytes 3538952 | tf_op jit(solution)/shard_map/ppermute | solution.py:323
  19.9 24.3 %all-to-all-start = ((bf16[128,8,256]{2,1,0:T(8,128)(2,1)}), bf16[128,8,256]{2,1,0:T(8,128)(2,1)S(1)}, u32[]{:S(2)}, u32[]{:S(2)}) async-start(bf16[128,8,256]{2,1,0:T(8,128)(2,1)} %get-tuple-element.7), calls=%async_computation | async-start | bytes 1048576 | tf_op jit(solution)/shard_map/all_to_all | solution.py:251
  61.9 15.6 %copy-start.1 = (f32[128]{0:T(128)S(1)}, f32[128]{0:T(128)}, u32[]{:S(2)}) copy-start(f32[128]{0:T(128)} %param.22) | copy-start | bytes 1540

commit v5 on v4

--- a/solution.py
+++ b/solution.py
@@ -49,21 +49,20 @@
 
 
 def project_kernel(
-    tokens, gain, wq, wd, wr, wk, wv, wo, out, own, tokens_, gain_, wq_, wd_, wr_, sems
+    tokens, gain, wq, wd, wr, wv, wo, out, own, tokens_, gain_, wq_, wd_, wr_, sems
 ):
     tp = lax.axis_index("tp")
     groups = lax.axis_size("tp")
     kv_size = lax.axis_size(KV)
-    deep = wk.shape[1]
+    deep = wv.shape[1]
     pairs = (
         (tokens, tokens_),
         (gain, gain_),
         (wq, wq_),
         (wd, wd_),
         (wr, wr_),
-        (wk.at[0], own.at[pl.ds(0, deep)]),
-        (wv.at[0], own.at[pl.ds(deep, deep)]),
-        (wo, own.at[pl.ds(2 * deep, wo.shape[0])]),
+        (wv.at[0], own.at[pl.ds(0, deep)]),
+        (wo, own.at[pl.ds(deep, wo.shape[0])]),
     )
     copies = [pltpu.make_async_copy(x, y, sems.at[n]) for n, (x, y) in enumerate(pairs)]
     for copy in copies:
@@ -111,7 +110,7 @@
 
 def attend_kernel(
     got, lengths, near, far, gain, cosine, sine, latents, ropes,
-    out, cache, cache_rope, sums, lifted, turned, means, sems,
+    means, packed, cache, cache_rope, sums, lifted, turned, sems,
     *, factor, nope,
 ):
     kv = lax.axis_index(KV)
@@ -151,7 +150,7 @@
         head = 2 * lax.rem(y + step, half) + (core if i < half else 1 - core)
         q = sums[head]
         w = near if i < half else far
-        lifted[i] = dot(q[:, :nope].astype(BF16), w[i % half, :latent_width, :], NT)
+        lifted[i] = dot(q[:, :nope].astype(BF16), w[i % half], NT)
         turned[i] = rotate(
             q[:, nope : nope + width].astype(BF16).astype(F32), cosine[...], sine[...]
         )
@@ -183,19 +182,13 @@
         safe = jnp.where(some, total, 1.0)
         means[s] = mixed / safe
         logs = jnp.where(lane == s, jnp.where(some, top + jnp.log(safe), NEGATIVE), logs)
-    for i in range(groups):
-        w = near if i < half else far
-        x = means[:, i, :].astype(BF16)
-        up = dot(x, w[i % half, latent_width : 2 * latent_width, :], NN).astype(BF16)
-        for k in range(kv_size):
-            out[k, i * local : (i + 1) * local, :] = up
     square = jnp.concatenate([logs, jnp.zeros((128 - groups, 128), F32)], axis=0)
     turned_logs = jnp.transpose(square)[:local]
     high = turned_logs.astype(BF16).astype(F32)
     rest = turned_logs - high
     middle = rest.astype(BF16).astype(F32)
     low = (rest - middle).astype(BF16).astype(F32)
-    packed = jnp.where(
+    packed[...] = jnp.where(
         lane < groups,
         high,
         jnp.where(
@@ -204,8 +197,21 @@
             jnp.where(lane < 3 * groups, pltpu.roll(low, 2 * groups, 1), 0.0),
         ),
     ).astype(BF16)
+
+
+def up_kernel(means, packed, near, far, out):
+    local, groups, latent_width = means.shape
+    half = groups // 2
+    kv_size = out.shape[0]
+    for i in range(groups):
+        w = near if i < half else far
+        x = means[:, i, :].astype(BF16)
+        up = dot(x, w[i % half, :latent_width, :], NN).astype(BF16)
+        for k in range(kv_size):
+            out[k, i * local : (i + 1) * local, :] = up
+    logs = packed[...]
     for k in range(kv_size):
-        out[k, groups * local :, :] = packed
+        out[k, groups * local :, :] = logs
 
 
 def combine_kernel(got, near, far, out, *, kv_size, groups, local, first):
@@ -249,6 +255,22 @@
 
 def exchange(value, axes):
     return lax.all_to_all(value, axes, split_axis=0, concat_axis=0, tiled=True)
+
+
+def swap(value):
+    return lax.ppermute(value, "tp", [(i, i ^ 1) for i in range(lax.axis_size("tp"))])
+
+
+def along(own):
+    groups = lax.axis_size("tp")
+    up = [(i, (i + 2) % groups) for i in range(groups)]
+    down = [(i, (i - 2) % groups) for i in range(groups)]
+    cut = own.shape[0] // 2
+    before = lax.ppermute(own, "tp", up)
+    after = lax.ppermute(own, "tp", down)
+    low = lax.ppermute(before[:cut], "tp", up)
+    high = lax.ppermute(after[cut:], "tp", down)
+    return jnp.concatenate([own, before, after, low, high], axis=0).reshape((4,) + own.shape)
 
 
 def on_device(
@@ -287,9 +309,9 @@
         project_kernel,
         out_shape=(
             jax.ShapeDtypeStruct((everyone, local, 256), BF16),
-            jax.ShapeDtypeStruct((2 * latent_width + value, nope), BF16),
+            jax.ShapeDtypeStruct((latent_width + value, value), BF16),
         ),
-        in_specs=[in_hbm()] * 8,
+        in_specs=[in_hbm()] * 7,
         out_specs=(in_vmem(),) * 2,
         scratch_shapes=[
             pltpu.VMEM((seqs, width), BF16),
@@ -297,7 +319,7 @@
             pltpu.VMEM((nope + rope, width), BF16),
             pltpu.VMEM((width, latent_width), BF16),
             pltpu.VMEM((rope, width), BF16),
-            pltpu.SemaphoreType.DMA((8,)),
+            pltpu.SemaphoreType.DMA((7,)),
         ],
         compiler_params=params(8),
         name="project",
@@ -308,33 +330,31 @@
             w_query.T,
             w_down_kv,
             w_rope_key.T,
-            w_key_up,
             w_value_up,
             w_out,
         )
     )
 
-    collected = [own]
-    for step in (1, 3, 2):
-        collected.append(
-            lax.ppermute(own, "tp", [(i, (i + 2 * step) % groups) for i in range(groups)])
-        )
-    near = jnp.stack(collected)
-    far = lax.ppermute(near, "tp", [(i, i ^ 1) for i in range(groups)])
+    near_key = along(w_key_up[0])
+    far_key = swap(near_key)
+    near = along(own)
+    far = swap(near)
 
     got = exchange(sent, ALL)
-    sent = pl.pallas_call(
+    means, packed = pl.pallas_call(
         functools.partial(attend_kernel, factor=factor, nope=nope),
-        out_shape=jax.ShapeDtypeStruct((kv_size, groups * local + local, value), BF16),
+        out_shape=(
+            jax.ShapeDtypeStruct((local, groups, latent_width), F32),
+            jax.ShapeDtypeStruct((local, 128), BF16),
+        ),
         in_specs=[in_vmem()] * 7 + [in_hbm()] * 2,
-        out_specs=in_vmem(),
+        out_specs=(in_vmem(),) * 2,
         scratch_shapes=[
             pltpu.VMEM((local, positions, latent_width), BF16),
             pltpu.VMEM((local, rope, positions), BF16),
             pltpu.VMEM((groups, local, 256), F32),
             pltpu.VMEM((groups, local, latent_width), F32),
             pltpu.VMEM((groups, local, rope), F32),
-            pltpu.VMEM((local, groups, latent_width), F32),
             pltpu.SemaphoreType.DMA((2 * local,)),
         ],
         compiler_params=params(24),
@@ -342,13 +362,21 @@
     )(
         got,
         own_length,
-        near,
-        far,
+        near_key,
+        far_key,
         latent_gain[None],
         cosine,
         sine,
         *keep_in_hbm(cache_latent, cache_rope.transpose(0, 2, 1)),
     )
+    sent = pl.pallas_call(
+        up_kernel,
+        out_shape=jax.ShapeDtypeStruct((kv_size, groups * local + local, value), BF16),
+        in_specs=[in_vmem()] * 4,
+        out_specs=in_vmem(),
+        compiler_params=params(8),
+        name="value_up",
+    )(means, packed, near, far)
     got = exchange(sent, KV)
 
     sent = pl.pallas_call(
@@ -357,7 +385,7 @@
             kv_size=kv_size,
             groups=groups,
             local=local,
-            first=2 * latent_width,
+            first=latent_width,
         ),
         out_shape=jax.ShapeDtypeStruct((everyone, local, w_out.shape[1]), BF16),
         in_specs=[in_vmem()] * 3,

time: 79.3 us -> 71.9 us (0.907)
  waiting for transfers between devices: 24.9 us -> 5.7 us
  starting transfers between devices: 16.3 us -> 22.7 us
  blocking collectives: 26.9 us -> 31.2 us
  local copies, waits for them, and re-layouts: 0.08 us -> 1.17 us
    all_to_all x1, waiting for transfers between devices: 13.2 us -> 0.87 us  [exchange(): return lax.all_to_all(value, axes, split_axis=0, concat_axis=0, tiled=True)]
    ppermute x4 -> x10, starting transfers between devices: 5.5 us -> 13.9 us  [the longest x2 5.62 us: along(): high = lax.ppermute(after[cut:], 'tp', down)]
    ppermute x4 -> x10, waiting for transfers between devices: 11.7 us -> 4.83 us  [the longest x2 3.72 us: along(): low = lax.ppermute(before[:cut], 'tp', up)]
    all_to_all x2, blocking collectives: 26.9 us -> 31.2 us  [exchange(): return lax.all_to_all(value, axes, split_axis=0, concat_axis=0, tiled=True)]
    all_to_all x1, starting transfers between devices: 10.8 us -> 8.75 us  [exchange(): return lax.all_to_all(value, axes, split_axis=0, concat_axis=0, tiled=True)]
    unnamed x6 -> x14, local copies, waits for them, and re-layouts: 0.01 us -> 1.05 us
  transfers between devices with their start and end apart: 5 -> 11, of which waited for: 3 -> 4; matrix products, arithmetic and copies ran while one was open for 0% -> 2% of each run, Pallas kernels for 0% -> 12%
where the time goes in v5:
time: 71.9 us; the launch traced here: 71 us
  blocking collectives  31.2 us (43%)
  starting transfers between devices  22.7 us (32%)
  Pallas kernels  9.77 us (14%)
  waiting for transfers between devices  5.7 us (8%)
  local copies, waits for them, and re-layouts  1.17 us (2%)
    all_to_all x2, blocking collectives, exchange(): return lax.all_to_all(value, axes, split_axis=0, concat_axis=0, tiled=True)  31.2 us
    all_to_all x1, starting transfers between devices, exchange(): return lax.all_to_all(value, axes, split_axis=0, concat_axis=0, tiled=True)  8.75 us
    pallas_call x1, Pallas kernels, on_device(): pl.pallas_call(functools.partial(attend_kernel, factor=factor, nope=nope)...  5.74 us
    ppermute x2, starting transfers between devices, along(): high = lax.ppermute(after[cut:], 'tp', down)  5.62 us
    ppermute x2, starting transfers between devices, along(): after = lax.ppermute(own, 'tp', down)  4.31 us
    ppermute x2, waiting for transfers between devices, along(): low = lax.ppermute(before[:cut], 'tp', up)  3.72 us
    pallas_call x1, Pallas kernels, on_device(): pl.pallas_call(project_kernel, out_shape=(jax.ShapeDtypeStruct((everyone,...  2.51 us
    ppermute x2, starting transfers between devices, along(): before = lax.ppermute(own, 'tp', up)  2.23 us
  transfers between devices with their start and end apart: 11, of which 4 were waited for; matrix products, arithmetic and copies ran while one was open for 2% of the time, Pallas kernels for 12%

profile of v5, /device:TPU:0, one launch (start us, length us, event | category | flops | bytes accessed | tf_op | source)
XLA Modules:
  0.0 71.0 jit_solution(2041256033144520338)
XLA Ops:
  0.0 0.0 copy-start.2
  0.0 0.0 copy-start
  0.0 1.7 %collective-permute-start = (bf16[512,128]{1,0:T(8,128)(2,1)}, bf16[512,128]{1,0:T(8,128)(2,1)S(1)}, u32[]{:S(2)}, u32[]{:S(2)}) collective-permute-start(bf16[512,128]{1,0:T(8,128)(2,1)} %bitcast.18), channel_id=1, source_target_pairs={{0,2},{1,3},{2,4},{3,5},{4,6},{5,7},{6,0},{7,1},{8,10},{9,11},{10,... | collective-permute-start | bytes 393224 | tf_op jit(solution)/shard_map/ppermute | solution.py:269
  1.7 1.5 %collective-permute-start.1 = (bf16[512,128]{1,0:T(8,128)(2,1)}, bf16[512,128]{1,0:T(8,128)(2,1)S(1)}, u32[]{:S(2)}, u32[]{:S(2)}) collective-permute-start(bf16[512,128]{1,0:T(8,128)(2,1)} %bitcast.19), channel_id=1, source_target_pairs={{0,6},{1,7},{2,0},{3,1},{4,2},{5,3},{6,4},{7,5},{8,14},{9,15},{10,... | collective-permute-start | bytes 393224 | tf_op jit(solution)/shard_map/ppermute | solution.py:270
  3.2 2.5 %project.1 = (bf16[128,8,256]{2,1,0:T(8,128)(2,1)}, bf16[640,128]{1,0:T(8,128)(2,1)S(1)}) custom-call(bf16[64,128]{1,0:T(8,128)(2,1)} %tokens.1, f32[1,128]{1,0:T(1,128)} %bitcast.22, bf16[192,128]{1,0:T(8,128)(2,1)} %bitcast.20, bf16[128,512]{1,0:T(8,128)(2,1)} %wd.1, bf16[64,128]{1,0:T(8,128)(2,1)} %bitcast.21, bf16[1,512,128]{2,1,0:T(8,128)(2,1)} %wv.1, ...), custom_call_target="tpu_custom_call" | custom-call | tf_op jit(solution)/shard_map/project/pallas_call | solution.py:308
  5.8 0.5 collective-permute-start.5
  6.3 2.8 %collective-permute-start.6 = (bf16[640,128]{1,0:T(8,128)(2,1)S(1)}, bf16[640,128]{1,0:T(8,128)(2,1)S(1)}, u32[]{:S(2)}, u32[]{:S(2)}) collective-permute-start(bf16[640,128]{1,0:T(8,128)(2,1)S(1)} %get-tuple-element.12), channel_id=1, source_target_pairs={{0,6},{1,7},{2,0},{3,1},{4,2},{5,3},{6,4},{7,5},{8,14},{9,15},{10,... | collective-permute-start | bytes 491528 | tf_op jit(solution)/shard_map/ppermute | solution.py:270
  9.1 8.7 %all-to-all-start = ((bf16[128,8,256]{2,1,0:T(8,128)(2,1)}), bf16[128,8,256]{2,1,0:T(8,128)(2,1)S(1)}, u32[]{:S(2)}, u32[]{:S(2)}) async-start(bf16[128,8,256]{2,1,0:T(8,128)(2,1)} %get-tuple-element.9), calls=%async_computation | async-start | bytes 1048576 | tf_op jit(solution)/shard_map/all_to_all | solution.py:257
  17.8 0.9 %constant_dynamic-update-slice_fusion.4 = bf16[2048,128]{1,0:T(8,128)(2,1)S(1)} fusion(bf16[1,512,128]{2,1,0:T(8,128)(2,1)} %param.19), kind=kLoop, calls=%fused_computation.4 | loop fusion | bytes 262144
  18.8 0.0 collective-permute-done
  18.8 1.0 %collective-permute-start.2 = (bf16[256,128]{1,0:T(8,128)(2,1)S(1)}, bf16[256,128]{1,0:T(8,128)(2,1)S(1)}, u32[]{:S(2)}, u32[]{:S(2)}) collective-permute-start(bf16[256,128]{1,0:T(8,128)(2,1)S(1)} %slice.16), channel_id=1, source_target_pairs={{0,2},{1,3},{2,4},{3,5},{4,6},{5,7},{6,0},{7,1},{8,10},{9,11},{10,... | collective-permute-start | bytes 196616 | tf_op jit(solution)/shard_map/ppermute | solution.py:271
  19.8 0.0 collective-permute-done.1
  19.8 2.3 %collective-permute-start.3 = (bf16[256,128]{1,0:T(8,128)(2,1)S(1)}, bf16[256,128]{1,0:T(8,128)(2,1)S(1)}, u32[]{:S(2)}, u32[]{:S(2)}) collective-permute-start(bf16[256,128]{1,0:T(8,128)(2,1)S(1)} %slice.17), channel_id=1, source_target_pairs={{0,6},{1,7},{2,0},{3,1},{4,2},{5,3},{6,4},{7,5},{8,14},{9,15},{10,... | collective-permute-start | bytes 196616 | tf_op jit(solution)/shard_map/ppermute | solution.py:272
  22.2 0.0 collective-permute-done.5
  22.2 0.1 collective-permute-start.7
  22.3 0.0 collective-permute-done.6
  22.4 3.3 %collective-permute-start.8 = (bf16[320,128]{1,0:T(8,128)(2,1)S(1)}, bf16[320,128]{1,0:T(8,128)(2,1)S(1)}, u32[]{:S(2)}, u32[]{:S(2)}) collective-permute-start(bf16[320,128]{1,0:T(8,128)(2,1)S(1)} %slice.19), channel_id=1, source_target_pairs={{0,6},{1,7},{2,0},{3,1},{4,2},{5,3},{6,4},{7,5},{8,14},{9,15},{10,... | collective-permute-start | bytes 245768 | tf_op jit(solution)/shard_map/ppermute | solution.py:272
  25.7 2.5 %collective-permute-done.2 = bf16[256,128]{1,0:T(8,128)(2,1)S(1)} collective-permute-done((bf16[256,128]{1,0:T(8,128)(2,1)S(1)}, bf16[256,128]{1,0:T(8,128)(2,1)S(1)}, u32[]{:S(2)}, u32[]{:S(2)}) %collective-permute-start.2) | collective-permute-done | bytes 65568 | tf_op jit(solution)/shard_map/ppermute | solution.py:271
  28.2 1.3 %collective-permute-done.7 = bf16[320,128]{1,0:T(8,128)(2,1)S(1)} collective-permute-done((bf16[320,128]{1,0:T(8,128)(2,1)S(1)}, bf16[320,128]{1,0:T(8,128)(2,1)S(1)}, u32[]{:S(2)}, u32[]{:S(2)}) %collective-permute-start.7) | collective-permute-done | bytes 81952 | tf_op jit(solution)/shard_map/ppermute | solution.py:271
  29.4 0.0 collective-permute-done.8
  29.5 0.1 collective-permute-start.9
  29.6 0.0 collective-permute-done.3
  29.6 0.6 collective-permute-start.4
  30.2 0.1 compare_select_fusion
  30.3 0.0 copy-done.2
  30.3 0.1 fusion.1
  30.3 0.1 fusion
  30.4 0.9 %all-to-all-done.got = bf16[128,8,256]{2,1,0:T(8,128)(2,1)S(1)} async-done(((bf16[128,8,256]{2,1,0:T(8,128)(2,1)}), bf16[128,8,256]{2,1,0:T(8,128)(2,1)S(1)}, u32[]{:S(2)}, u32[]{:S(2)}) %all-to-all-start) | async-done | bytes 524320 | tf_op jit(solution)/shard_map/all_to_all | solution.py:257
  31.3 1.1 %collective-permute-done.4.far = bf16[4,512,128]{2,1,0:T(8,128)(2,1)S(1)} collective-permute-done((bf16[4,512,128]{2,1,0:T(8,128)(2,1)S(1)}, bf16[4,512,128]{2,1,0:T(8,128)(2,1)S(1)}, u32[]{:S(2)}, u32[]{:S(2)}) %collective-permute-start.4) | collective-permute-done | bytes 524320 | tf_op jit(solution)/shard_map/ppermute | solution.py:261
  32.4 0.1 broadcast_in_dim.27.lengths
  32.5 0.0 copy-done
  32.5 0.0 copy-start.1
  32.5 5.7 %attend.1 = (f32[8,8,512]{2,1,0:T(8,128)S(1)}, bf16[8,128]{1,0:T(8,128)(2,1)S(1)}) custom-call(bf16[128,8,256]{2,1,0:T(8,128)(2,1)S(1)} %all-to-all-done.got, s32[8,128]{1,0:T(8,128)S(1)} %broadcast_in_dim.27.lengths, bf16[4,512,128]{2,1,0:T(8,128)(2,1)S(1)} %bitcast.14, bf16[4,512,128]{2,1,0:T(8,128)(2,1)S(1)} %collective-permute-done.4.far, ...), custom_call_target="tpu_custom_call" | custom-call | tf_op jit(solution)/shard_map/attend/pallas_call | solution.py:344
  38.2 0.0 collective-permute-done.9.far
  38.2 0.3 value_up.1
  38.5 16.4 %all_to_all.15.got = bf16[16,72,128]{2,1,0:T(8,128)(2,1)S(1)} all-to-all(bf16[16,72,128]{2,1,0:T(8,128)(2,1)S(1)} %value_up.1), channel_id=1, replica_groups=mesh['kv_0'=4,'kv_1'=4,'tp'=8] {'kv_0','kv_1'}, dimensions={0} | all-to-all | bytes 589824 | tf_op jit(solution)/shard_map/all_to_all | solution.py:257
  54.9 0.5 combine.1
  55.4 14.8 %all_to_all.16.got = bf16[128,8,128]{2,1,0:T(8,128)(2,1)S(1)} all-to-all(bf16[128,8,128]{2,1,0:T(8,128)(2,1)S(1)} %combine.1), channel_id=1, replica_groups=mesh['kv_0'=4,'kv_1'=4,'tp'=8] {'kv_0','kv_1','tp'}, dimensions={0} | all-to-all | bytes 524288 | tf_op jit(solution)/shard_map/all_to_all | solution.py:257
  70.2 0.0 copy-done.1
  70.2 0.8 %finish.1 = bf16[64,128]{1,0:T(8,128)(2,1)} custom-call(bf16[128,8,128]{2,1,0:T(8,128)(2,1)S(1)} %all_to_all.16.got, f32[1,128]{1,0:T(1,128)S(1)} %bitcast.16), custom_call_target="tpu_custom_call" | custom-call | tf_op jit(solution)/shard_map/finish/pallas_call | solution.py:397
  (14 shorter events, 0.2 us)
Async XLA Ops:
  0.0 30.3 %copy-start.2 = (s32[64]{0:T(128)S(1)}, s32[64]{0:T(128)}, u32[]{:S(2)}) copy-start(s32[64]{0:T(128)} %param.25) | copy-start | bytes 772
  0.0 32.5 %copy-start = (f32[512]{0:T(512)S(1)}, f32[512]{0:T(512)}, u32[]{:S(2)}) copy-start(f32[512]{0:T(512)} %param.18) | copy-start | bytes 6148
  0.0 18.8 %collective-permute-start = (bf16[512,128]{1,0:T(8,128)(2,1)}, bf16[512,128]{1,0:T(8,128)(2,1)S(1)}, u32[]{:S(2)}, u32[]{:S(2)}) collective-permute-start(bf16[512,128]{1,0:T(8,128)(2,1)} %bitcast.18), channel_id=1, source_target_pairs={{0,2},{1,3},{2,4},{3,5},{4,6},{5,7},{6,0},{7,1},{8,10},{9,11},{10,... | collective-permute-start | bytes 393224 | tf_op jit(solution)/shard_map/ppermute | solution.py:269
  1.7 18.1 %collective-permute-start.1 = (bf16[512,128]{1,0:T(8,128)(2,1)}, bf16[512,128]{1,0:T(8,128)(2,1)S(1)}, u32[]{:S(2)}, u32[]{:S(2)}) collective-permute-start(bf16[512,128]{1,0:T(8,128)(2,1)} %bitcast.19), channel_id=1, source_target_pairs={{0,6},{1,7},{2,0},{3,1},{4,2},{5,3},{6,4},{7,5},{8,14},{9,15},{10,... | collective-permute-start | bytes 393224 | tf_op jit(solution)/shard_map/ppermute | solution.py:270
  5.8 16.5 %collective-permute-start.5 = (bf16[640,128]{1,0:T(8,128)(2,1)S(1)}, bf16[640,128]{1,0:T(8,128)(2,1)S(1)}, u32[]{:S(2)}, u32[]{:S(2)}) collective-permute-start(bf16[640,128]{1,0:T(8,128)(2,1)S(1)} %get-tuple-element.12), channel_id=1, source_target_pairs={{0,2},{1,3},{2,4},{3,5},{4,6},{5,7},{6,0},{7,1},{8,10},{9,11},{10,... | collective-permute-start | bytes 491528 | tf_op jit(solution)/shard_map/ppermute | solution.py:269
  6.3 16.0 %collective-permute-start.6 = (bf16[640,128]{1,0:T(8,128)(2,1)S(1)}, bf16[640,128]{1,0:T(8,128)(2,1)S(1)}, u32[]{:S(2)}, u32[]{:S(2)}) collective-permute-start(bf16[640,128]{1,0:T(8,128)(2,1)S(1)} %get-tuple-element.12), channel_id=1, source_target_pairs={{0,6},{1,7},{2,0},{3,1},{4,2},{5,3},{6,4},{7,5},{8,14},{9,15},{10,... | collective-permute-start | bytes 491528 | tf_op jit(solution)/shard_map/ppermute | solution.py:270
  9.1 22.2 %all-to-all-start = ((bf16[128,8,256]{2,1,0:T(8,128)(2,1)}), bf16[128,8,256]{2,1,0:T(8,128)(2,1)S(1)}, u32[]{:S(2)}, u32[]{:S(2)}) async-start(bf16[128,8,256]{2,1,0:T(8,128)(2,1)} %get-tuple-element.9), calls=%async_computation | async-start | bytes 1048576 | tf_op jit(solution)/shard_map/all_to_all | solution.py:257
  18.8 9.4 %collective-permute-start.2 = (bf16[256,128]{1,0:T(8,128)(2,1)S(1)}, bf16[256,128]{1,0:T(8,128)(2,1)S(1)}, u32[]{:S(2)}, u32[]{:S(2)}) collective-permute-start(bf16[256,128]{1,0:T(8,128)(2,1)S(1)} %slice.16), channel_id=1, source_target_pairs={{0,2},{1,3},{2,4},{3,5},{4,6},{5,7},{6,0},{7,1},{8,10},{9,11},{10,... | collective-permute-start | bytes 196616 | tf_op jit(solution)/shard_map/ppermute | solution.py:271
  19.8 9.7 %collective-permute-start.3 = (bf16[256,128]{1,0:T(8,128)(2,1)S(1)}, bf16[256,128]{1,0:T(8,128)(2,1)S(1)}, u32[]{:S(2)}, u32[]{:S(2)}) collective-permute-start(bf16[256,128]{1,0:T(8,128)(2,1)S(1)} %slice.17), channel_id=1, source_target_pairs={{0,6},{1,7},{2,0},{3,1},{4,2},{5,3},{6,4},{7,5},{8,14},{9,15},{10,... | collective-permute-start | bytes 196616 | tf_op jit(solution)/shard_map/ppermute | solution.py:272
  22.2 7.2 %collective-permute-start.7 = (bf16[320,128]{1,0:T(8,128)(2,1)S(1)}, bf16[320,128]{1,0:T(8,128)(2,1)S(1)}, u32[]{:S(2)}, u32[]{:S(2)}) collective-permute-start(bf16[320,128]{1,0:T(8,128)(2,1)S(1)} %slice.18), channel_id=1, source_target_pairs={{0,2},{1,3},{2,4},{3,5},{4,6},{5,7},{6,0},{7,1},{8,10},{9,11},{10,... | collective-permute-start | bytes 245768 | tf_op jit(solution)/shard_map/ppermute | solution.py:271
  22.4 7.1 %collective-permute-start.8 = (bf16[320,128]{1,0:T(8,128)(2,1)S(1)}, bf16[320,128]{1,0:T(8,128)(2,1)S(1)}, u32[]{:S(2)}, u32[]{:S(2)}) collective-permute-start(bf16[320,128]{1,0:T(8,128)(2,1)S(1)} %slice.19), channel_id=1, source_target_pairs={{0,6},{1,7},{2,0},{3,1},{4,2},{5,3},{6,4},{7,5},{8,14},{9,15},{10,... | collective-permute-start | bytes 245768 | tf_op jit(solution)/shard_map/ppermute | solution.py:272
  29.5 8.8 %collective-permute-start.9 = (bf16[4,640,128]{2,1,0:T(8,128)(2,1)S(1)}, bf16[4,640,128]{2,1,0:T(8,128)(2,1)S(1)}, u32[]{:S(2)}, u32[]{:S(2)}) collective-permute-start(bf16[4,640,128]{2,1,0:T(8,128)(2,1)S(1)} %bitcast.10), channel_id=1, source_target_pairs={{0,1},{1,0},{2,3},{3,2},{4,5},{5,4},{6,7},{7,6},{8,9},{9,8},{10,11... | collective-permute-start | bytes 1966088 | tf_op jit(solution)/shard_map/ppermute | solution.py:261
  29.6 2.8 %collective-permute-start.4 = (bf16[4,512,128]{2,1,0:T(8,128)(2,1)S(1)}, bf16[4,512,128]{2,1,0:T(8,128)(2,1)S(1)}, u32[]{:S(2)}, u32[]{:S(2)}) collective-permute-start(bf16[4,512,128]{2,1,0:T(8,128)(2,1)S(1)} %bitcast.13), channel_id=1, source_target_pairs={{0,1},{1,0},{2,3},{3,2},{4,5},{5,4},{6,7},{7,6},{8,9},{9,8},{10,11... | collective-permute-start | bytes 1572872 | tf_op jit(solution)/shard_map/ppermute | solution.py:261
  32.5 37.7 %copy-start.1 = (f32[128]{0:T(128)S(1)}, f32[128]{0:T(128)}, u32[]{:S(2)}) copy-start(f32[128]{0:T(128)} %param.22) | copy-start | bytes 1540

commit v6 on v4

--- a/solution.py
+++ b/solution.py
@@ -2,6 +2,7 @@
 
 import jax
 import jax.numpy as jnp
+import numpy as np
 from jax import lax
 from jax.experimental import pallas as pl
 from jax.experimental.pallas import tpu as pltpu
@@ -110,15 +111,16 @@
 
 
 def attend_kernel(
-    got, lengths, near, far, gain, cosine, sine, latents, ropes,
-    out, cache, cache_rope, sums, lifted, turned, means, sems,
+    got, lengths, frequencies, near, far, gain, latents, ropes,
+    out, cache, cache_rope, sums, lifted, turned, scored, weights, means, sems,
     *, factor, nope,
 ):
     kv = lax.axis_index(KV)
     tp = lax.axis_index("tp")
     kv_size = lax.axis_size(KV)
     groups = lax.axis_size("tp")
-    local = cache.shape[0]
+    local, positions, latent_width = cache.shape
+    width = cache_rope.shape[1]
     copies = []
     for s in range(local):
         a = pltpu.make_async_copy(latents.at[s], cache.at[s], sems.at[s])
@@ -126,23 +128,20 @@
         a.start()
         b.start()
         copies.append((a, b))
-    width = cache_rope.shape[1]
-    latent_width = cache.shape[2]
-    positions = cache.shape[1]
     for h in range(groups):
         total = got[h].astype(F32)
         for k in range(1, kv_size):
             total = total + got[k * groups + h].astype(F32)
         sums[h] = total
-    raw = jnp.concatenate([sums[h][0:1, nope + width :] for h in range(groups)], axis=1)
-    rope_raw = sums[0][1:2, nope + width :]
-    for h in range(1, groups):
-        rope_raw = rope_raw + sums[h][1:2, nope + width :]
-    square = jnp.sum(raw * raw, axis=1, keepdims=True) / latent_width
-    new_latent = (raw * lax.rsqrt(square + EPSILON) * gain[...]).astype(BF16).astype(F32)
-    new_seq = lax.rem(kv, local)
-    new_rope = rotate(rope_raw, cosine[pl.ds(new_seq, 1), :], sine[pl.ds(new_seq, 1), :])
-    new_rope = new_rope.astype(BF16).astype(F32)
+    shape = (local, lengths.shape[1])
+    length = jnp.sum(
+        jnp.where(lanes(shape) == rows(shape) + tp * local, lengths[...], 0), axis=1, keepdims=True
+    )
+    lane = lanes((local, width))
+    angles = length.astype(F32) * frequencies[...]
+    cosine = jnp.cos(angles)
+    sine = jnp.sin(angles)
+    sine = jnp.where(lane < width // 2, -sine, sine)
     half = groups // 2
     y = tp // 2
     core = lax.rem(tp, 2)
@@ -152,47 +151,71 @@
         q = sums[head]
         w = near if i < half else far
         lifted[i] = dot(q[:, :nope].astype(BF16), w[i % half, :latent_width, :], NT)
-        turned[i] = rotate(
-            q[:, nope : nope + width].astype(BF16).astype(F32), cosine[...], sine[...]
-        )
-    position = kv * positions + lanes((groups, positions))
-    lane = lanes((groups, 128))
-    logs = jnp.full((groups, 128), NEGATIVE, F32)
+        turned[i] = rotate(q[:, nope : nope + width].astype(BF16).astype(F32), cosine, sine)
+    raw = jnp.concatenate([sums[h][0:1, nope + width :] for h in range(groups)], axis=1)
+    rope_raw = sums[0][1:2, nope + width :]
+    for h in range(1, groups):
+        rope_raw = rope_raw + sums[h][1:2, nope + width :]
+    square = jnp.sum(raw * raw, axis=1, keepdims=True) / latent_width
+    new_latent = (raw * lax.rsqrt(square + EPSILON) * gain[...]).astype(BF16).astype(F32)
+    new_seq = lax.rem(kv, local)
+    mine = rows((local, width)) == new_seq
+    new_rope = rotate(
+        rope_raw,
+        jnp.sum(jnp.where(mine, cosine, 0.0), axis=0, keepdims=True),
+        jnp.sum(jnp.where(mine, sine, 0.0), axis=0, keepdims=True),
+    )
+    new_rope = new_rope.astype(BF16).astype(F32)
+    pairs = local * groups
     for s in range(local):
         q = lifted[:, s, :].astype(BF16)
         qr = turned[:, s, :].astype(BF16)
+        fresh = jnp.sum(q.astype(F32) * new_latent, axis=1, keepdims=True) + jnp.sum(
+            qr.astype(F32) * new_rope, axis=1, keepdims=True
+        )
         for copy in copies[s]:
             copy.wait()
-        c = cache[s]
-        scores = (dot(q, c, NT) + dot(qr, cache_rope[s], NN)) * factor
-        new = (
-            jnp.sum(q.astype(F32) * new_latent, axis=1, keepdims=True)
-            + jnp.sum(qr.astype(F32) * new_rope, axis=1, keepdims=True)
-        ) * factor
-        is_new = jnp.logical_and(new_seq == s, kv < local)
-        new = jnp.where(is_new, new, NEGATIVE)
-        visible = position < lengths[s : s + 1, :1]
-        top = jnp.max(jnp.where(visible, scores, NEGATIVE), axis=1, keepdims=True)
-        top = jnp.maximum(top, new)
-        weight = jnp.where(visible, jnp.exp(scores - top), 0.0)
-        new_weight = jnp.where(is_new, jnp.exp(new - top), 0.0)
-        total = jnp.sum(weight, axis=1, keepdims=True) + new_weight
-        mixed = dot(weight.astype(BF16), c, NN)
-        mixed = mixed + new_weight.astype(BF16).astype(F32) * new_latent
-        some = total > 0.0
-        safe = jnp.where(some, total, 1.0)
-        means[s] = mixed / safe
-        logs = jnp.where(lane == s, jnp.where(some, top + jnp.log(safe), NEGATIVE), logs)
+        r = s * groups
+        scored[r : r + groups, :positions] = dot(q, cache[s], NT) + dot(qr, cache_rope[s], NN)
+        scored[r : r + groups, positions:] = jnp.broadcast_to(fresh, (groups, 128))
+    scores = scored[:, :positions] * factor
+    row = rows((pairs, 1))
+    sequence = row // groups
+    limit = jnp.zeros((pairs, 1), jnp.int32)
+    for s in range(local):
+        limit = jnp.where(sequence == s, length[s : s + 1, :], limit)
+    is_new = jnp.logical_and(sequence == new_seq, kv < local)
+    new = jnp.where(is_new, scored[:, positions : positions + 1] * factor, NEGATIVE)
+    visible = kv * positions + lanes((pairs, positions)) < limit
+    top = jnp.max(jnp.where(visible, scores, NEGATIVE), axis=1, keepdims=True)
+    top = jnp.maximum(top, new)
+    weight = jnp.where(visible, jnp.exp(scores - top), 0.0)
+    new_weight = jnp.where(is_new, jnp.exp(new - top), 0.0)
+    total = jnp.sum(weight, axis=1, keepdims=True) + new_weight
+    weights[...] = weight.astype(BF16)
+    some = total > 0.0
+    safe = jnp.where(some, total, 1.0)
+    inverse = 1.0 / safe
+    logs = jnp.where(some, top + jnp.log(safe), NEGATIVE)
+    rounded = new_weight.astype(BF16).astype(F32)
+    for s in range(local):
+        r = slice(s * groups, (s + 1) * groups)
+        mixed = dot(weights[r, :], cache[s], NN) + rounded[r] * new_latent
+        means[s] = mixed * inverse[r]
     for i in range(groups):
         w = near if i < half else far
         x = means[:, i, :].astype(BF16)
         up = dot(x, w[i % half, latent_width : 2 * latent_width, :], NN).astype(BF16)
         for k in range(kv_size):
             out[k, i * local : (i + 1) * local, :] = up
-    square = jnp.concatenate([logs, jnp.zeros((128 - groups, 128), F32)], axis=0)
-    turned_logs = jnp.transpose(square)[:local]
-    high = turned_logs.astype(BF16).astype(F32)
-    rest = turned_logs - high
+    lane = lanes((local, 128))
+    table = jnp.zeros((groups, 128), F32)
+    for s in range(local):
+        table = jnp.where(lanes((groups, 128)) == s, logs[s * groups : (s + 1) * groups], table)
+    table = jnp.concatenate([table, jnp.zeros((128 - groups, 128), F32)], axis=0)
+    table = jnp.transpose(table)[:local]
+    high = table.astype(BF16).astype(F32)
+    rest = table - high
     middle = rest.astype(BF16).astype(F32)
     low = (rest - middle).astype(BF16).astype(F32)
     packed = jnp.where(
@@ -275,13 +298,6 @@
     nope = w_key_up.shape[2]
     value = w_value_up.shape[2]
     factor = (nope + rope) ** (-0.5)
-
-    own_length = lax.dynamic_slice_in_dim(lengths, lax.axis_index("tp") * local, local, 0)
-    inverse_freq = 1.0 / 10000.0 ** (jnp.arange(0, rope, 2, dtype=F32) / rope)
-    angles = own_length.astype(F32)[:, None] * jnp.concatenate([inverse_freq, inverse_freq])[None]
-    cosine = jnp.cos(angles)
-    sine = jnp.sin(angles) * jnp.where(jnp.arange(rope) < rope // 2, -1.0, 1.0)[None, :]
-    own_length = jnp.broadcast_to(own_length[:, None], (local, 128))
 
     sent, own = pl.pallas_call(
         project_kernel,
@@ -323,10 +339,12 @@
     far = lax.ppermute(near, "tp", [(i, i ^ 1) for i in range(groups)])
 
     got = exchange(sent, ALL)
+    powers = np.arange(0, rope, 2, dtype=np.float64) / rope
+    frequencies = np.tile(1.0 / 10000.0**powers, 2)[None].astype(np.float32)
     sent = pl.pallas_call(
         functools.partial(attend_kernel, factor=factor, nope=nope),
         out_shape=jax.ShapeDtypeStruct((kv_size, groups * local + local, value), BF16),
-        in_specs=[in_vmem()] * 7 + [in_hbm()] * 2,
+        in_specs=[in_vmem()] * 6 + [in_hbm()] * 2,
         out_specs=in_vmem(),
         scratch_shapes=[
             pltpu.VMEM((local, positions, latent_width), BF16),
@@ -334,6 +352,8 @@
             pltpu.VMEM((groups, local, 256), F32),
             pltpu.VMEM((groups, local, latent_width), F32),
             pltpu.VMEM((groups, local, rope), F32),
+            pltpu.VMEM((local * groups, positions + 128), F32),
+            pltpu.VMEM((local * groups, positions), BF16),
             pltpu.VMEM((local, groups, latent_width), F32),
             pltpu.SemaphoreType.DMA((2 * local,)),
         ],
@@ -341,12 +361,11 @@
         name="attend",
     )(
         got,
-        own_length,
+        lengths[None],
+        frequencies,
         near,
         far,
         latent_gain[None],
-        cosine,
-        sine,
         *keep_in_hbm(cache_latent, cache_rope.transpose(0, 2, 1)),
     )
     got = exchange(sent, KV)

time: 79.3 us -> 76.7 us (0.967)
  blocking collectives: 26.9 us -> 50.9 us
  waiting for transfers between devices: 24.9 us -> 11.7 us
  starting transfers between devices: 16.3 us -> 5.5 us
  Pallas kernels: 9.63 us -> 7.35 us
    all_to_all x2 -> x3, blocking collectives: 26.9 us -> 50.9 us  [exchange(): return lax.all_to_all(value, axes, split_axis=0, concat_axis=0, tiled=True)]
    all_to_all x1 -> x0, waiting for transfers between devices: 13.2 us -> none  [exchange(): return lax.all_to_all(value, axes, split_axis=0, concat_axis=0, tiled=True)]
    all_to_all x1 -> x0, starting transfers between devices: 10.8 us -> none  [exchange(): return lax.all_to_all(value, axes, split_axis=0, concat_axis=0, tiled=True)]
    pallas_call x1, Pallas kernels: 5.88 us -> 4.4 us  [on_device(): pl.pallas_call(functools.partial(attend_kernel, factor=factor, nope=nope)...]
    pallas_call x1, Pallas kernels: 2.52 us -> 1.72 us  [on_device(): pl.pallas_call(project_kernel, out_shape=(jax.ShapeDtypeStruct((everyone,...]
  transfers between devices with their start and end apart: 5 -> 4, of which waited for: 3 -> 2; matrix products, arithmetic and copies ran while one was open for 0% -> 0% of each run, Pallas kernels for 0% -> 0%
where the time goes in v6:
time: 76.7 us; the launch traced here: 75.7 us
  blocking collectives  50.9 us (66%)
  waiting for transfers between devices  11.7 us (15%)
  Pallas kernels  7.35 us (10%)
  starting transfers between devices  5.5 us (7%)
    all_to_all x3, blocking collectives, exchange(): return lax.all_to_all(value, axes, split_axis=0, concat_axis=0, tiled=True)  50.9 us
    ppermute x3, waiting for transfers between devices, on_device(): lax.ppermute(own, 'tp', [(i, (i + 2 * step) % groups) for i in range(grou...  11.7 us
    ppermute x3, starting transfers between devices, on_device(): lax.ppermute(own, 'tp', [(i, (i + 2 * step) % groups) for i in range(grou...  5.41 us
    pallas_call x1, Pallas kernels, on_device(): pl.pallas_call(functools.partial(attend_kernel, factor=factor, nope=nope)...  4.4 us
    pallas_call x1, Pallas kernels, on_device(): pl.pallas_call(project_kernel, out_shape=(jax.ShapeDtypeStruct((everyone,...  1.72 us
  transfers between devices with their start and end apart: 4, of which 2 were waited for; matrix products, arithmetic and copies ran while one was open for 0% of the time, Pallas kernels for 0%

profile of v6, /device:TPU:0, one launch (start us, length us, event | category | flops | bytes accessed | tf_op | source)
XLA Modules:
  0.0 75.7 jit_solution(11415129713577169290)
XLA Ops:
  0.0 1.7 %project.1 = (bf16[128,8,256]{2,1,0:T(8,128)(2,1)S(1)}, bf16[1152,128]{1,0:T(8,128)(2,1)S(1)}) custom-call(bf16[64,128]{1,0:T(8,128)(2,1)} %tokens.1, f32[1,128]{1,0:T(1,128)} %bitcast.21, bf16[192,128]{1,0:T(8,128)(2,1)} %bitcast.19, bf16[128,512]{1,0:T(8,128)(2,1)} %wd.1, bf16[64,128]{1,0:T(8,128)(2,1)} %bitcast.20, bf16[1,512,128]{2,1,0:T(8,128)(2,1)} %wk.1, ...), custom_call_target="tpu_custom_call" | custom-call | tf_op jit(solution)/shard_map/project/pallas_call | solution.py:302
  1.7 3.4 %collective-permute-start.2 = (bf16[1152,128]{1,0:T(8,128)(2,1)S(1)}, bf16[1152,128]{1,0:T(8,128)(2,1)S(1)}, u32[]{:S(2)}, u32[]{:S(2)}) collective-permute-start(bf16[1152,128]{1,0:T(8,128)(2,1)S(1)} %get-tuple-element.8), channel_id=1, source_target_pairs={{0,4},{1,5},{2,6},{3,7},{4,0},{5,1},{6,2},{7,3},{8,12},{9,13},{10,... | collective-permute-start | bytes 884744 | tf_op jit(solution)/shard_map/ppermute | solution.py:336
  5.1 1.1 %collective-permute-start.1 = (bf16[1152,128]{1,0:T(8,128)(2,1)S(1)}, bf16[1152,128]{1,0:T(8,128)(2,1)S(1)}, u32[]{:S(2)}, u32[]{:S(2)}) collective-permute-start(bf16[1152,128]{1,0:T(8,128)(2,1)S(1)} %get-tuple-element.8), channel_id=1, source_target_pairs={{0,6},{1,7},{2,0},{3,1},{4,2},{5,3},{6,4},{7,5},{8,14},{9,15},{10,... | collective-permute-start | bytes 884744 | tf_op jit(solution)/shard_map/ppermute | solution.py:336
  6.2 1.0 %collective-permute-start = (bf16[1152,128]{1,0:T(8,128)(2,1)S(1)}, bf16[1152,128]{1,0:T(8,128)(2,1)S(1)}, u32[]{:S(2)}, u32[]{:S(2)}) collective-permute-start(bf16[1152,128]{1,0:T(8,128)(2,1)S(1)} %get-tuple-element.8), channel_id=1, source_target_pairs={{0,2},{1,3},{2,4},{3,5},{4,6},{5,7},{6,0},{7,1},{8,10},{9,11},{10,... | collective-permute-start | bytes 884744 | tf_op jit(solution)/shard_map/ppermute | solution.py:336
  7.1 6.1 %collective-permute-done.2 = bf16[1152,128]{1,0:T(8,128)(2,1)S(1)} collective-permute-done((bf16[1152,128]{1,0:T(8,128)(2,1)S(1)}, bf16[1152,128]{1,0:T(8,128)(2,1)S(1)}, u32[]{:S(2)}, u32[]{:S(2)}) %collective-permute-start.2) | collective-permute-done | bytes 294944 | tf_op jit(solution)/shard_map/ppermute | solution.py:336
  13.2 5.7 %collective-permute-done.1 = bf16[1152,128]{1,0:T(8,128)(2,1)S(1)} collective-permute-done((bf16[1152,128]{1,0:T(8,128)(2,1)S(1)}, bf16[1152,128]{1,0:T(8,128)(2,1)S(1)}, u32[]{:S(2)}, u32[]{:S(2)}) %collective-permute-start.1) | collective-permute-done | bytes 294944 | tf_op jit(solution)/shard_map/ppermute | solution.py:336
  18.9 0.0 collective-permute-done
  18.9 0.0 copy-start
  18.9 0.0 copy-start.1
  18.9 0.0 copy-start.3
  18.9 0.2 pad_maximum_fusion.near
  19.0 0.1 collective-permute-start.3
  19.1 24.0 %all_to_all.15.got = bf16[128,8,256]{2,1,0:T(8,128)(2,1)S(1)} all-to-all(bf16[128,8,256]{2,1,0:T(8,128)(2,1)S(1)} %get-tuple-element.7), channel_id=1, replica_groups=mesh['kv_0'=4,'kv_1'=4,'tp'=8] {'kv_0','kv_1','tp'}, dimensions={0} | all-to-all | bytes 1048576 | tf_op jit(solution)/shard_map/all_to_all | solution.py:274
  43.2 0.0 collective-permute-done.3.far
  43.2 0.0 copy-done
  43.2 0.0 copy-done.1
  43.2 0.0 copy-done.3
  43.2 4.4 %attend.1 = bf16[16,72,128]{2,1,0:T(8,128)(2,1)S(1)} custom-call(bf16[128,8,256]{2,1,0:T(8,128)(2,1)S(1)} %all_to_all.15.got, s32[1,64]{1,0:T(1,128)S(1)} %bitcast.13, f32[1,64]{1,0:T(1,128)S(1)} %copy-done.3, bf16[4,1152,128]{2,1,0:T(8,128)(2,1)S(1)} %pad_maximum_fusion.near, bf16[4,1152,128]{2,1,0:T(8,128)(2,1)S(1)} %collective-permute-done.3.far, ...), custom_call_target="tpu_custom_call" | custom-call | tf_op jit(solution)/shard_map/attend/pallas_call | solution.py:344
  47.6 11.7 %all_to_all.16.got = bf16[16,72,128]{2,1,0:T(8,128)(2,1)S(1)} all-to-all(bf16[16,72,128]{2,1,0:T(8,128)(2,1)S(1)} %attend.1), channel_id=1, replica_groups=mesh['kv_0'=4,'kv_1'=4,'tp'=8] {'kv_0','kv_1'}, dimensions={0} | all-to-all | bytes 589824 | tf_op jit(solution)/shard_map/all_to_all | solution.py:274
  59.3 0.0 copy-start.2
  59.3 0.5 combine.1
  59.8 15.2 %all_to_all.17.got = bf16[128,8,128]{2,1,0:T(8,128)(2,1)S(1)} all-to-all(bf16[128,8,128]{2,1,0:T(8,128)(2,1)S(1)} %combine.1), channel_id=1, replica_groups=mesh['kv_0'=4,'kv_1'=4,'tp'=8] {'kv_0','kv_1','tp'}, dimensions={0} | all-to-all | bytes 524288 | tf_op jit(solution)/shard_map/all_to_all | solution.py:274
  75.0 0.0 copy-done.2
  75.0 0.8 finish.1
Async XLA Ops:
  1.7 11.5 %collective-permute-start.2 = (bf16[1152,128]{1,0:T(8,128)(2,1)S(1)}, bf16[1152,128]{1,0:T(8,128)(2,1)S(1)}, u32[]{:S(2)}, u32[]{:S(2)}) collective-permute-start(bf16[1152,128]{1,0:T(8,128)(2,1)S(1)} %get-tuple-element.8), channel_id=1, source_target_pairs={{0,4},{1,5},{2,6},{3,7},{4,0},{5,1},{6,2},{7,3},{8,12},{9,13},{10,... | collective-permute-start | bytes 884744 | tf_op jit(solution)/shard_map/ppermute | solution.py:336
  5.1 13.8 %collective-permute-start.1 = (bf16[1152,128]{1,0:T(8,128)(2,1)S(1)}, bf16[1152,128]{1,0:T(8,128)(2,1)S(1)}, u32[]{:S(2)}, u32[]{:S(2)}) collective-permute-start(bf16[1152,128]{1,0:T(8,128)(2,1)S(1)} %get-tuple-element.8), channel_id=1, source_target_pairs={{0,6},{1,7},{2,0},{3,1},{4,2},{5,3},{6,4},{7,5},{8,14},{9,15},{10,... | collective-permute-start | bytes 884744 | tf_op jit(solution)/shard_map/ppermute | solution.py:336
  6.2 12.7 %collective-permute-start = (bf16[1152,128]{1,0:T(8,128)(2,1)S(1)}, bf16[1152,128]{1,0:T(8,128)(2,1)S(1)}, u32[]{:S(2)}, u32[]{:S(2)}) collective-permute-start(bf16[1152,128]{1,0:T(8,128)(2,1)S(1)} %get-tuple-element.8), channel_id=1, source_target_pairs={{0,2},{1,3},{2,4},{3,5},{4,6},{5,7},{6,0},{7,1},{8,10},{9,11},{10,... | collective-permute-start | bytes 884744 | tf_op jit(solution)/shard_map/ppermute | solution.py:336
  18.9 24.3 %copy-start = (f32[512]{0:T(512)S(1)}, f32[512]{0:T(512)}, u32[]{:S(2)}) copy-start(f32[512]{0:T(512)} %param.19) | copy-start | bytes 6148
  18.9 24.3 %copy-start.1 = (s32[64]{0:T(128)S(1)}, s32[64]{0:T(128)}, u32[]{:S(2)}) copy-start(s32[64]{0:T(128)} %param.26) | copy-start | bytes 772
  18.9 24.3 %copy-start.3 = (f32[1,64]{1,0:T(1,128)S(1)}, f32[1,64]{1,0:T(1,128)}, u32[]{:S(2)}) copy-start(f32[1,64]{1,0:T(1,128)} %constant.2.clone.frequencies) | copy-start | bytes 772
  19.0 24.1 %collective-permute-start.3 = (bf16[4,1152,128]{2,1,0:T(8,128)(2,1)S(1)}, bf16[4,1152,128]{2,1,0:T(8,128)(2,1)S(1)}, u32[]{:S(2)}, u32[]{:S(2)}) collective-permute-start(bf16[4,1152,128]{2,1,0:T(8,128)(2,1)S(1)} %pad_maximum_fusion.near), channel_id=1, source_target_pairs={{0,1},{1,0},{2,3},{3,2},{4,5},{5,4},{6,7},{7,6},{8,9},{9,8},{10,11... | collective-permute-start | bytes 3538952 | tf_op jit(solution)/shard_map/ppermute | solution.py:339
  59.3 15.6 %copy-start.2 = (f32[128]{0:T(128)S(1)}, f32[128]{0:T(128)}, u32[]{:S(2)}) copy-start(f32[128]{0:T(128)} %param.23) | copy-start | bytes 1540

commit v7 on v6

--- a/solution.py
+++ b/solution.py
@@ -12,6 +12,7 @@
 
 KV = ("kv_0", "kv_1")
 ALL = ("kv_0", "kv_1", "tp")
+LAST = ("kv_1", "tp")
 EPSILON = 1e-06
 NEGATIVE = -1e30
 F32 = jnp.float32
@@ -50,7 +51,7 @@
 
 
 def project_kernel(
-    tokens, gain, wq, wd, wr, wk, wv, wo, out, own, tokens_, gain_, wq_, wd_, wr_, sems
+    tokens, gain, wq, wd, wr, wk, wv, out, own, tokens_, gain_, wq_, wd_, wr_, sems
 ):
     tp = lax.axis_index("tp")
     groups = lax.axis_size("tp")
@@ -64,7 +65,6 @@
         (wr, wr_),
         (wk.at[0], own.at[pl.ds(0, deep)]),
         (wv.at[0], own.at[pl.ds(deep, deep)]),
-        (wo, own.at[pl.ds(2 * deep, wo.shape[0])]),
     )
     copies = [pltpu.make_async_copy(x, y, sems.at[n]) for n, (x, y) in enumerate(pairs)]
     for copy in copies:
@@ -111,8 +111,9 @@
 
 
 def attend_kernel(
-    got, lengths, frequencies, near, far, gain, latents, ropes,
-    out, cache, cache_rope, sums, lifted, turned, scored, weights, means, sems,
+    got, near, far, lengths_, frequencies_, gain_, latents, ropes,
+    out, lengths, frequencies, gain, cache, cache_rope,
+    sums, lifted, turned, scored, weights, means, sems,
     *, factor, nope,
 ):
     kv = lax.axis_index(KV)
@@ -121,6 +122,12 @@
     groups = lax.axis_size("tp")
     local, positions, latent_width = cache.shape
     width = cache_rope.shape[1]
+    small = []
+    for n, (a, b) in enumerate(
+        ((lengths_, lengths), (frequencies_, frequencies), (gain_, gain))
+    ):
+        small.append(pltpu.make_async_copy(a, b, sems.at[2 * local + n]))
+        small[n].start()
     copies = []
     for s in range(local):
         a = pltpu.make_async_copy(latents.at[s], cache.at[s], sems.at[s])
@@ -133,6 +140,8 @@
         for k in range(1, kv_size):
             total = total + got[k * groups + h].astype(F32)
         sums[h] = total
+    for copy in small:
+        copy.wait()
     shape = (local, lengths.shape[1])
     length = jnp.sum(
         jnp.where(lanes(shape) == rows(shape) + tp * local, lengths[...], 0), axis=1, keepdims=True
@@ -231,7 +240,15 @@
         out[k, groups * local :, :] = packed
 
 
-def combine_kernel(got, near, far, out, *, kv_size, groups, local, first):
+def three_parts(value):
+    high = value.astype(BF16).astype(F32)
+    rest = value - high
+    middle = rest.astype(BF16).astype(F32)
+    low = (rest - middle).astype(BF16).astype(F32)
+    return high, middle, low
+
+
+def combine_kernel(got, near, far, out, *, kv_size, groups, local):
     logs = []
     for k in range(kv_size):
         x = got[k, groups * local :, :].astype(F32)
@@ -242,29 +259,39 @@
     inverse = 1.0 / total
     shares = [x * inverse for x in shares]
     half = groups // 2
-    mixed = jnp.zeros((local, out.shape[2]), F32)
+    blocks = near.shape[1]
+    mixed = [jnp.zeros((local, out.shape[2]), F32) for _ in range(blocks)]
     for i in range(groups):
         head = jnp.zeros((local, 128), F32)
         for k in range(kv_size):
             part = got[k, i * local : (i + 1) * local, :].astype(F32)
             head = head + part * shares[k][:, i : i + 1]
+        head = head.astype(BF16)
         w = near if i < half else far
-        mixed = mixed + dot(head.astype(BF16), w[i % half, first:, :], NN)
-    mixed = mixed.astype(BF16)
+        for n in range(blocks):
+            mixed[n] = mixed[n] + dot(head, w[i % half, n], NN)
+    squares = functools.reduce(jnp.add, [x * x for x in mixed])
+    squares = jnp.sum(squares, axis=1, keepdims=True)
+    high, middle, low = three_parts(squares)
+    lane = lanes((local, out.shape[2]))
+    parts = jnp.where(
+        lane == 0, high, jnp.where(lane == 1, middle, jnp.where(lane == 2, low, 0.0))
+    ).astype(BF16)
+    own = mixed[0].astype(BF16)
     for d in range(out.shape[0]):
-        out[d] = mixed
-
-
-def finish_kernel(got, gain, out, *, kv_size, groups, local):
-    kv = lax.axis_index(KV)
-    width = got.shape[2]
+        out[d, :local, :] = own
+        out[d, local:, :] = parts
+
+
+def finish_kernel(got, gain, out, *, groups, local, model_width):
+    place = lax.axis_index(KV[1])
+    places = got.shape[0] // groups
     for t in range(groups):
-        squares = jnp.zeros((local, width), F32)
-        for k in range(kv_size):
-            x = got[k * groups + t].astype(F32)
-            squares = squares + x * x
-        mean = jnp.sum(squares, axis=1, keepdims=True) / (width * kv_size)
-        own = got[kv * groups + t].astype(F32)
+        parts = functools.reduce(
+            jnp.add, [got[n * groups + t, local:, :].astype(F32) for n in range(places)]
+        )
+        mean = jnp.sum(parts, axis=1, keepdims=True) / model_width
+        own = got[place * groups + t, :local, :].astype(F32)
         out[t * local : (t + 1) * local, :] = (
             own * lax.rsqrt(mean + EPSILON) * gain[...]
         ).astype(BF16)
@@ -272,6 +299,19 @@
 
 def exchange(value, axes):
     return lax.all_to_all(value, axes, split_axis=0, concat_axis=0, tiled=True)
+
+
+def swap(value):
+    return lax.ppermute(value, "tp", [(i, i ^ 1) for i in range(lax.axis_size("tp"))])
+
+
+def along(own, axis, stride):
+    size = lax.axis_size(axis)
+    collected = [own]
+    for step in (1, 3, 2):
+        pairs = [(i, (i + stride * step) % size) for i in range(size)]
+        collected.append(lax.ppermute(own, axis, pairs))
+    return jnp.stack(collected)
 
 
 def on_device(
@@ -303,9 +343,9 @@
         project_kernel,
         out_shape=(
             jax.ShapeDtypeStruct((everyone, local, 256), BF16),
-            jax.ShapeDtypeStruct((2 * latent_width + value, nope), BF16),
+            jax.ShapeDtypeStruct((2 * latent_width, nope), BF16),
         ),
-        in_specs=[in_hbm()] * 8,
+        in_specs=[in_hbm()] * 7,
         out_specs=(in_vmem(),) * 2,
         scratch_shapes=[
             pltpu.VMEM((seqs, width), BF16),
@@ -313,7 +353,7 @@
             pltpu.VMEM((nope + rope, width), BF16),
             pltpu.VMEM((width, latent_width), BF16),
             pltpu.VMEM((rope, width), BF16),
-            pltpu.SemaphoreType.DMA((8,)),
+            pltpu.SemaphoreType.DMA((7,)),
         ],
         compiler_params=params(8),
         name="project",
@@ -326,17 +366,14 @@
             w_rope_key.T,
             w_key_up,
             w_value_up,
-            w_out,
         )
     )
 
-    collected = [own]
-    for step in (1, 3, 2):
-        collected.append(
-            lax.ppermute(own, "tp", [(i, (i + 2 * step) % groups) for i in range(groups)])
-        )
-    near = jnp.stack(collected)
-    far = lax.ppermute(near, "tp", [(i, i ^ 1) for i in range(groups)])
+    near = along(own, "tp", 2)
+    far = swap(near)
+    columns = along(w_out, "kv_0", 1)
+    near_out = along(columns, "tp", 2)
+    far_out = swap(near_out)
 
     got = exchange(sent, ALL)
     powers = np.arange(0, rope, 2, dtype=np.float64) / rope
@@ -344,9 +381,12 @@
     sent = pl.pallas_call(
         functools.partial(attend_kernel, factor=factor, nope=nope),
         out_shape=jax.ShapeDtypeStruct((kv_size, groups * local + local, value), BF16),
-        in_specs=[in_vmem()] * 6 + [in_hbm()] * 2,
+        in_specs=[in_vmem()] * 3 + [in_hbm()] * 5,
         out_specs=in_vmem(),
         scratch_shapes=[
+            pltpu.VMEM((1, seqs), jnp.int32),
+            pltpu.VMEM((1, rope), F32),
+            pltpu.VMEM((1, latent_width), F32),
             pltpu.VMEM((local, positions, latent_width), BF16),
             pltpu.VMEM((local, rope, positions), BF16),
             pltpu.VMEM((groups, local, 256), F32),
@@ -355,38 +395,38 @@
             pltpu.VMEM((local * groups, positions + 128), F32),
             pltpu.VMEM((local * groups, positions), BF16),
             pltpu.VMEM((local, groups, latent_width), F32),
-            pltpu.SemaphoreType.DMA((2 * local,)),
+            pltpu.SemaphoreType.DMA((2 * local + 3,)),
         ],
         compiler_params=params(24),
         name="attend",
     )(
         got,
-        lengths[None],
-        frequencies,
         near,
         far,
-        latent_gain[None],
-        *keep_in_hbm(cache_latent, cache_rope.transpose(0, 2, 1)),
+        *keep_in_hbm(
+            lengths[None],
+            frequencies,
+            latent_gain[None],
+            cache_latent,
+            cache_rope.transpose(0, 2, 1),
+        ),
     )
     got = exchange(sent, KV)
 
+    fewer = lax.axis_size(LAST)
     sent = pl.pallas_call(
-        functools.partial(
-            combine_kernel,
-            kv_size=kv_size,
-            groups=groups,
-            local=local,
-            first=2 * latent_width,
-        ),
-        out_shape=jax.ShapeDtypeStruct((everyone, local, w_out.shape[1]), BF16),
+        functools.partial(combine_kernel, kv_size=kv_size, groups=groups, local=local),
+        out_shape=jax.ShapeDtypeStruct((fewer, 2 * local, w_out.shape[1]), BF16),
         in_specs=[in_vmem()] * 3,
         out_specs=in_vmem(),
         compiler_params=params(8),
         name="combine",
-    )(got, near, far)
-    got = exchange(sent, ALL)
+    )(got, near_out, far_out)
+    got = exchange(sent, LAST)
     return pl.pallas_call(
-        functools.partial(finish_kernel, kv_size=kv_size, groups=groups, local=local),
+        functools.partial(
+            finish_kernel, groups=groups, local=local, model_width=width * kv_size
+        ),
         out_shape=jax.ShapeDtypeStruct((seqs, w_out.shape[1]), BF16),
         in_specs=[in_vmem(), in_vmem()],
         out_specs=in_vmem(),

time: 76.7 us -> 84 us (1.095)
  blocking collectives: 50.9 us -> 10.9 us
  starting transfers between devices: 5.5 us -> 31.8 us
  waiting for transfers between devices: 11.7 us -> 28.9 us
  Pallas kernels: 7.35 us -> 9.99 us
    all_to_all x3 -> x1, blocking collectives: 50.9 us -> 10.9 us  [exchange(): return lax.all_to_all(value, axes, split_axis=0, concat_axis=0, tiled=True)]
    all_to_all x0 -> x2, starting transfers between devices: none -> 15.6 us  [exchange(): return lax.all_to_all(value, axes, split_axis=0, concat_axis=0, tiled=True)]
    ppermute x4 -> x11, starting transfers between devices: 5.5 us -> 16.2 us  [the longest x9 16 us: along(): collected.append(lax.ppermute(own, axis, pairs))]
    all_to_all x0 -> x2, waiting for transfers between devices: none -> 9.61 us  [exchange(): return lax.all_to_all(value, axes, split_axis=0, concat_axis=0, tiled=True)]
    ppermute x4 -> x11, waiting for transfers between devices: 11.7 us -> 19.3 us  [the longest x9 19.3 us: along(): collected.append(lax.ppermute(own, axis, pairs))]
    pallas_call x1, Pallas kernels: 0.48 us -> 1.71 us  [on_device(): pl.pallas_call(functools.partial(combine_kernel, kv_size=kv_size, groups=...]
  transfers between devices with their start and end apart: 4 -> 13, of which waited for: 2 -> 6; matrix products, arithmetic and copies ran while one was open for 0% -> 1% of each run, Pallas kernels for 0% -> 6%
where the time goes in v7:
time: 84 us; the launch traced here: 82.6 us
  starting transfers between devices  31.8 us (38%)
  waiting for transfers between devices  28.9 us (34%)
  blocking collectives  10.9 us (13%)
  Pallas kernels  9.99 us (12%)
  other arithmetic  0.98 us (1%)
    ppermute x9, waiting for transfers between devices, along(): collected.append(lax.ppermute(own, axis, pairs))  19.3 us
    ppermute x9, starting transfers between devices, along(): collected.append(lax.ppermute(own, axis, pairs))  16 us
    all_to_all x2, starting transfers between devices, exchange(): return lax.all_to_all(value, axes, split_axis=0, concat_axis=0, tiled=True)  15.6 us
    all_to_all x1, blocking collectives, exchange(): return lax.all_to_all(value, axes, split_axis=0, concat_axis=0, tiled=True)  10.9 us
    all_to_all x2, waiting for transfers between devices, exchange(): return lax.all_to_all(value, axes, split_axis=0, concat_axis=0, tiled=True)  9.61 us
    pallas_call x1, Pallas kernels, on_device(): pl.pallas_call(functools.partial(attend_kernel, factor=factor, nope=nope)...  5.07 us
    pallas_call x1, Pallas kernels, on_device(): pl.pallas_call(project_kernel, out_shape=(jax.ShapeDtypeStruct((everyone,...  2.51 us
    pallas_call x1, Pallas kernels, on_device(): pl.pallas_call(functools.partial(combine_kernel, kv_size=kv_size, groups=...  1.71 us
  transfers between devices with their start and end apart: 13, of which 6 were waited for; matrix products, arithmetic and copies ran while one was open for 1% of the time, Pallas kernels for 6%

profile of v7, /device:TPU:0, one launch (start us, length us, event | category | flops | bytes accessed | tf_op | source)
XLA Modules:
  0.0 82.6 jit_solution(6777965984166099070)
XLA Ops:
  0.0 2.5 %project.1 = (bf16[128,8,256]{2,1,0:T(8,128)(2,1)}, bf16[1024,128]{1,0:T(8,128)(2,1)S(1)}) custom-call(bf16[64,128]{1,0:T(8,128)(2,1)} %tokens.1, f32[1,128]{1,0:T(1,128)} %bitcast.36, bf16[192,128]{1,0:T(8,128)(2,1)} %bitcast.29, bf16[128,512]{1,0:T(8,128)(2,1)} %wd.1, bf16[64,128]{1,0:T(8,128)(2,1)} %bitcast.34, bf16[1,512,128]{2,1,0:T(8,128)(2,1)} %wk.1, ...), custom_call_target="tpu_custom_call" | custom-call | tf_op jit(solution)/shard_map/project/pallas_call | solution.py:342
  2.5 3.4 %collective-permute-start.2 = (bf16[1024,128]{1,0:T(8,128)(2,1)S(1)}, bf16[1024,128]{1,0:T(8,128)(2,1)S(1)}, u32[]{:S(2)}, u32[]{:S(2)}) collective-permute-start(bf16[1024,128]{1,0:T(8,128)(2,1)S(1)} %get-tuple-element.8), channel_id=1, source_target_pairs={{0,4},{1,5},{2,6},{3,7},{4,0},{5,1},{6,2},{7,3},{8,12},{9,13},{10,... | collective-permute-start | bytes 786440 | tf_op jit(solution)/shard_map/ppermute | solution.py:313
  5.9 1.1 %collective-permute-start.1 = (bf16[1024,128]{1,0:T(8,128)(2,1)S(1)}, bf16[1024,128]{1,0:T(8,128)(2,1)S(1)}, u32[]{:S(2)}, u32[]{:S(2)}) collective-permute-start(bf16[1024,128]{1,0:T(8,128)(2,1)S(1)} %get-tuple-element.8), channel_id=1, source_target_pairs={{0,6},{1,7},{2,0},{3,1},{4,2},{5,3},{6,4},{7,5},{8,14},{9,15},{10,... | collective-permute-start | bytes 786440 | tf_op jit(solution)/shard_map/ppermute | solution.py:313
  7.0 1.0 %collective-permute-start = (bf16[1024,128]{1,0:T(8,128)(2,1)S(1)}, bf16[1024,128]{1,0:T(8,128)(2,1)S(1)}, u32[]{:S(2)}, u32[]{:S(2)}) collective-permute-start(bf16[1024,128]{1,0:T(8,128)(2,1)S(1)} %get-tuple-element.8), channel_id=1, source_target_pairs={{0,2},{1,3},{2,4},{3,5},{4,6},{5,7},{6,0},{7,1},{8,10},{9,11},{10,... | collective-permute-start | bytes 786440 | tf_op jit(solution)/shard_map/ppermute | solution.py:313
  7.9 5.3 %collective-permute-done.2 = bf16[1024,128]{1,0:T(8,128)(2,1)S(1)} collective-permute-done((bf16[1024,128]{1,0:T(8,128)(2,1)S(1)}, bf16[1024,128]{1,0:T(8,128)(2,1)S(1)}, u32[]{:S(2)}, u32[]{:S(2)}) %collective-permute-start.2) | collective-permute-done | bytes 262176 | tf_op jit(solution)/shard_map/ppermute | solution.py:313
  13.3 5.0 %collective-permute-done.1 = bf16[1024,128]{1,0:T(8,128)(2,1)S(1)} collective-permute-done((bf16[1024,128]{1,0:T(8,128)(2,1)S(1)}, bf16[1024,128]{1,0:T(8,128)(2,1)S(1)}, u32[]{:S(2)}, u32[]{:S(2)}) %collective-permute-start.1) | collective-permute-done | bytes 262176 | tf_op jit(solution)/shard_map/ppermute | solution.py:313
  18.3 0.0 collective-permute-done
  18.3 0.1 pad_maximum_fusion.near
  18.4 0.1 collective-permute-start.3
  18.5 4.0 %collective-permute-start.6 = (bf16[128,128]{1,0:T(8,128)(2,1)}, bf16[128,128]{1,0:T(8,128)(2,1)S(1)}, u32[]{:S(2)}, u32[]{:S(2)}) collective-permute-start(bf16[128,128]{1,0:T(8,128)(2,1)} %param.22), channel_id=1, source_target_pairs={{0,64},{32,96},{64,0},{96,32},{1,65},{33,97},{65,1},{97,33},{2,66}... | collective-permute-start | bytes 98312 | tf_op jit(solution)/shard_map/ppermute | solution.py:313
  22.5 0.7 collective-permute-start.5
  23.2 1.3 %collective-permute-start.4 = (bf16[128,128]{1,0:T(8,128)(2,1)}, bf16[128,128]{1,0:T(8,128)(2,1)S(1)}, u32[]{:S(2)}, u32[]{:S(2)}) collective-permute-start(bf16[128,128]{1,0:T(8,128)(2,1)} %param.22), channel_id=1, source_target_pairs={{0,32},{32,64},{64,96},{96,0},{1,33},{33,65},{65,97},{97,1},{2,34}... | collective-permute-start | bytes 98312 | tf_op jit(solution)/shard_map/ppermute | solution.py:313
  24.5 8.6 %all-to-all-start = ((bf16[128,8,256]{2,1,0:T(8,128)(2,1)}), bf16[128,8,256]{2,1,0:T(8,128)(2,1)S(1)}, u32[]{:S(2)}, u32[]{:S(2)}) async-start(bf16[128,8,256]{2,1,0:T(8,128)(2,1)} %get-tuple-element.7), calls=%async_computation | async-start | bytes 1048576 | tf_op jit(solution)/shard_map/all_to_all | solution.py:301
  33.0 0.0 collective-permute-done.6
  33.1 0.0 collective-permute-done.5
  33.1 0.0 collective-permute-done.4
  33.1 0.8 fusion
  33.9 2.5 %collective-permute-start.9 = (bf16[4,128,128]{2,1,0:T(8,128)(2,1)S(1)}, bf16[4,128,128]{2,1,0:T(8,128)(2,1)S(1)}, u32[]{:S(2)}, u32[]{:S(2)}) collective-permute-start(bf16[4,128,128]{2,1,0:T(8,128)(2,1)S(1)} %get-tuple-element.10), channel_id=1, source_target_pairs={{0,4},{1,5},{2,6},{3,7},{4,0},{5,1},{6,2},{7,3},{8,12},{9,13},{10,... | collective-permute-start | bytes 393224 | tf_op jit(solution)/shard_map/ppermute | solution.py:313
  36.4 1.2 %collective-permute-start.8 = (bf16[4,128,128]{2,1,0:T(8,128)(2,1)S(1)}, bf16[4,128,128]{2,1,0:T(8,128)(2,1)S(1)}, u32[]{:S(2)}, u32[]{:S(2)}) collective-permute-start(bf16[4,128,128]{2,1,0:T(8,128)(2,1)S(1)} %get-tuple-element.10), channel_id=1, source_target_pairs={{0,6},{1,7},{2,0},{3,1},{4,2},{5,3},{6,4},{7,5},{8,14},{9,15},{10,... | collective-permute-start | bytes 393224 | tf_op jit(solution)/shard_map/ppermute | solution.py:313
  37.6 0.9 %collective-permute-start.7 = (bf16[4,128,128]{2,1,0:T(8,128)(2,1)S(1)}, bf16[4,128,128]{2,1,0:T(8,128)(2,1)S(1)}, u32[]{:S(2)}, u32[]{:S(2)}) collective-permute-start(bf16[4,128,128]{2,1,0:T(8,128)(2,1)S(1)} %get-tuple-element.10), channel_id=1, source_target_pairs={{0,2},{1,3},{2,4},{3,5},{4,6},{5,7},{6,0},{7,1},{8,10},{9,11},{10,... | collective-permute-start | bytes 393224 | tf_op jit(solution)/shard_map/ppermute | solution.py:313
  38.4 6.5 %collective-permute-done.9 = bf16[4,128,128]{2,1,0:T(8,128)(2,1)S(1)} collective-permute-done((bf16[4,128,128]{2,1,0:T(8,128)(2,1)S(1)}, bf16[4,128,128]{2,1,0:T(8,128)(2,1)S(1)}, u32[]{:S(2)}, u32[]{:S(2)}) %collective-permute-start.9) | collective-permute-done | bytes 131104 | tf_op jit(solution)/shard_map/ppermute | solution.py:313
  45.0 1.5 %collective-permute-done.8 = bf16[4,128,128]{2,1,0:T(8,128)(2,1)S(1)} collective-permute-done((bf16[4,128,128]{2,1,0:T(8,128)(2,1)S(1)}, bf16[4,128,128]{2,1,0:T(8,128)(2,1)S(1)}, u32[]{:S(2)}, u32[]{:S(2)}) %collective-permute-start.8) | collective-permute-done | bytes 131104 | tf_op jit(solution)/shard_map/ppermute | solution.py:313
  46.5 0.9 %collective-permute-done.7 = bf16[4,128,128]{2,1,0:T(8,128)(2,1)S(1)} collective-permute-done((bf16[4,128,128]{2,1,0:T(8,128)(2,1)S(1)}, bf16[4,128,128]{2,1,0:T(8,128)(2,1)S(1)}, u32[]{:S(2)}, u32[]{:S(2)}) %collective-permute-start.7) | collective-permute-done | bytes 131104 | tf_op jit(solution)/shard_map/ppermute | solution.py:313
  47.4 0.1 pad_maximum_fusion.1.near
  47.4 0.1 collective-permute-start.10
  47.6 0.0 all-to-all-done.got
  47.6 0.0 collective-permute-done.3.far
  47.6 0.0 copy-start
  47.6 5.1 %attend.1 = bf16[16,72,128]{2,1,0:T(8,128)(2,1)} custom-call(bf16[128,8,256]{2,1,0:T(8,128)(2,1)S(1)} %all-to-all-done.got, bf16[4,1024,128]{2,1,0:T(8,128)(2,1)S(1)} %pad_maximum_fusion.near, bf16[4,1024,128]{2,1,0:T(8,128)(2,1)S(1)} %collective-permute-done.3.far, s32[1,64]{1,0:T(1,128)} %bitcast.37, f32[1,64]{1,0:T(1,128)} %constant.2.clone.frequencies_, ...), custom_call_target="tpu_custom_call" | custom-call | tf_op jit(solution)/shard_map/attend/pallas_call | solution.py:381
  52.6 7.0 %all-to-all-start.1 = ((bf16[16,72,128]{2,1,0:T(8,128)(2,1)}), bf16[16,72,128]{2,1,0:T(8,128)(2,1)S(1)}, u32[]{:S(2)}, u32[]{:S(2)}) async-start(bf16[16,72,128]{2,1,0:T(8,128)(2,1)} %attend.1), calls=%async_computation.1 | async-start | bytes 589824 | tf_op jit(solution)/shard_map/all_to_all | solution.py:301
  59.7 0.0 collective-permute-done.10.far
  59.7 9.6 %all-to-all-done.1.got = bf16[16,72,128]{2,1,0:T(8,128)(2,1)S(1)} async-done(((bf16[16,72,128]{2,1,0:T(8,128)(2,1)}), bf16[16,72,128]{2,1,0:T(8,128)(2,1)S(1)}, u32[]{:S(2)}, u32[]{:S(2)}) %all-to-all-start.1) | async-done | bytes 294944 | tf_op jit(solution)/shard_map/all_to_all | solution.py:301
  69.3 1.7 %combine.1 = bf16[32,16,128]{2,1,0:T(8,128)(2,1)S(1)} custom-call(bf16[16,72,128]{2,1,0:T(8,128)(2,1)S(1)} %all-to-all-done.1.got, bf16[4,4,128,128]{3,2,1,0:T(8,128)(2,1)S(1)} %pad_maximum_fusion.1.near, bf16[4,4,128,128]{3,2,1,0:T(8,128)(2,1)} %collective-permute-done.10.far), custom_call_target="tpu_custom_call" | custom-call | tf_op jit(solution)/shard_map/combine/pallas_call | solution.py:417
  71.0 10.9 %all_to_all.15.got = bf16[32,16,128]{2,1,0:T(8,128)(2,1)S(1)} all-to-all(bf16[32,16,128]{2,1,0:T(8,128)(2,1)S(1)} %combine.1), channel_id=1, replica_groups=mesh['kv_0'=4,'kv_1'=4,'tp'=8] {'kv_1','tp'}, dimensions={0} | all-to-all | bytes 262144 | tf_op jit(solution)/shard_map/all_to_all | solution.py:301
  81.9 0.0 copy-done
  81.9 0.7 finish.1
Async XLA Ops:
  2.5 10.8 %collective-permute-start.2 = (bf16[1024,128]{1,0:T(8,128)(2,1)S(1)}, bf16[1024,128]{1,0:T(8,128)(2,1)S(1)}, u32[]{:S(2)}, u32[]{:S(2)}) collective-permute-start(bf16[1024,128]{1,0:T(8,128)(2,1)S(1)} %get-tuple-element.8), channel_id=1, source_target_pairs={{0,4},{1,5},{2,6},{3,7},{4,0},{5,1},{6,2},{7,3},{8,12},{9,13},{10,... | collective-permute-start | bytes 786440 | tf_op jit(solution)/shard_map/ppermute | solution.py:313
  5.9 12.4 %collective-permute-start.1 = (bf16[1024,128]{1,0:T(8,128)(2,1)S(1)}, bf16[1024,128]{1,0:T(8,128)(2,1)S(1)}, u32[]{:S(2)}, u32[]{:S(2)}) collective-permute-start(bf16[1024,128]{1,0:T(8,128)(2,1)S(1)} %get-tuple-element.8), channel_id=1, source_target_pairs={{0,6},{1,7},{2,0},{3,1},{4,2},{5,3},{6,4},{7,5},{8,14},{9,15},{10,... | collective-permute-start | bytes 786440 | tf_op jit(solution)/shard_map/ppermute | solution.py:313
  7.0 11.3 %collective-permute-start = (bf16[1024,128]{1,0:T(8,128)(2,1)S(1)}, bf16[1024,128]{1,0:T(8,128)(2,1)S(1)}, u32[]{:S(2)}, u32[]{:S(2)}) collective-permute-start(bf16[1024,128]{1,0:T(8,128)(2,1)S(1)} %get-tuple-element.8), channel_id=1, source_target_pairs={{0,2},{1,3},{2,4},{3,5},{4,6},{5,7},{6,0},{7,1},{8,10},{9,11},{10,... | collective-permute-start | bytes 786440 | tf_op jit(solution)/shard_map/ppermute | solution.py:313
  18.4 29.2 %collective-permute-start.3 = (bf16[4,1024,128]{2,1,0:T(8,128)(2,1)S(1)}, bf16[4,1024,128]{2,1,0:T(8,128)(2,1)S(1)}, u32[]{:S(2)}, u32[]{:S(2)}) collective-permute-start(bf16[4,1024,128]{2,1,0:T(8,128)(2,1)S(1)} %pad_maximum_fusion.near), channel_id=1, source_target_pairs={{0,1},{1,0},{2,3},{3,2},{4,5},{5,4},{6,7},{7,6},{8,9},{9,8},{10,11... | collective-permute-start | bytes 3145736 | tf_op jit(solution)/shard_map/ppermute | solution.py:305
  18.5 14.6 %collective-permute-start.6 = (bf16[128,128]{1,0:T(8,128)(2,1)}, bf16[128,128]{1,0:T(8,128)(2,1)S(1)}, u32[]{:S(2)}, u32[]{:S(2)}) collective-permute-start(bf16[128,128]{1,0:T(8,128)(2,1)} %param.22), channel_id=1, source_target_pairs={{0,64},{32,96},{64,0},{96,32},{1,65},{33,97},{65,1},{97,33},{2,66}... | collective-permute-start | bytes 98312 | tf_op jit(solution)/shard_map/ppermute | solution.py:313
  22.5 10.6 %collective-permute-start.5 = (bf16[128,128]{1,0:T(8,128)(2,1)}, bf16[128,128]{1,0:T(8,128)(2,1)S(1)}, u32[]{:S(2)}, u32[]{:S(2)}) collective-permute-start(bf16[128,128]{1,0:T(8,128)(2,1)} %param.22), channel_id=1, source_target_pairs={{0,96},{32,0},{64,32},{96,64},{1,97},{33,1},{65,33},{97,65},{2,98}... | collective-permute-start | bytes 98312 | tf_op jit(solution)/shard_map/ppermute | solution.py:313
  23.2 9.9 %collective-permute-start.4 = (bf16[128,128]{1,0:T(8,128)(2,1)}, bf16[128,128]{1,0:T(8,128)(2,1)S(1)}, u32[]{:S(2)}, u32[]{:S(2)}) collective-permute-start(bf16[128,128]{1,0:T(8,128)(2,1)} %param.22), channel_id=1, source_target_pairs={{0,32},{32,64},{64,96},{96,0},{1,33},{33,65},{65,97},{97,1},{2,34}... | collective-permute-start | bytes 98312 | tf_op jit(solution)/shard_map/ppermute | solution.py:313
  24.5 23.1 %all-to-all-start = ((bf16[128,8,256]{2,1,0:T(8,128)(2,1)}), bf16[128,8,256]{2,1,0:T(8,128)(2,1)S(1)}, u32[]{:S(2)}, u32[]{:S(2)}) async-start(bf16[128,8,256]{2,1,0:T(8,128)(2,1)} %get-tuple-element.7), calls=%async_computation | async-start | bytes 1048576 | tf_op jit(solution)/shard_map/all_to_all | solution.py:301
  33.9 11.1 %collective-permute-start.9 = (bf16[4,128,128]{2,1,0:T(8,128)(2,1)S(1)}, bf16[4,128,128]{2,1,0:T(8,128)(2,1)S(1)}, u32[]{:S(2)}, u32[]{:S(2)}) collective-permute-start(bf16[4,128,128]{2,1,0:T(8,128)(2,1)S(1)} %get-tuple-element.10), channel_id=1, source_target_pairs={{0,4},{1,5},{2,6},{3,7},{4,0},{5,1},{6,2},{7,3},{8,12},{9,13},{10,... | collective-permute-start | bytes 393224 | tf_op jit(solution)/shard_map/ppermute | solution.py:313
  36.4 10.1 %collective-permute-start.8 = (bf16[4,128,128]{2,1,0:T(8,128)(2,1)S(1)}, bf16[4,128,128]{2,1,0:T(8,128)(2,1)S(1)}, u32[]{:S(2)}, u32[]{:S(2)}) collective-permute-start(bf16[4,128,128]{2,1,0:T(8,128)(2,1)S(1)} %get-tuple-element.10), channel_id=1, source_target_pairs={{0,6},{1,7},{2,0},{3,1},{4,2},{5,3},{6,4},{7,5},{8,14},{9,15},{10,... | collective-permute-start | bytes 393224 | tf_op jit(solution)/shard_map/ppermute | solution.py:313
  37.6 9.8 %collective-permute-start.7 = (bf16[4,128,128]{2,1,0:T(8,128)(2,1)S(1)}, bf16[4,128,128]{2,1,0:T(8,128)(2,1)S(1)}, u32[]{:S(2)}, u32[]{:S(2)}) collective-permute-start(bf16[4,128,128]{2,1,0:T(8,128)(2,1)S(1)} %get-tuple-element.10), channel_id=1, source_target_pairs={{0,2},{1,3},{2,4},{3,5},{4,6},{5,7},{6,0},{7,1},{8,10},{9,11},{10,... | collective-permute-start | bytes 393224 | tf_op jit(solution)/shard_map/ppermute | solution.py:313
  47.4 12.2 %collective-permute-start.10 = (bf16[4,4,128,128]{3,2,1,0:T(8,128)(2,1)S(1)}, bf16[4,4,128,128]{3,2,1,0:T(8,128)(2,1)}, u32[]{:S(2)}, u32[]{:S(2)}) collective-permute-start(bf16[4,4,128,128]{3,2,1,0:T(8,128)(2,1)S(1)} %pad_maximum_fusion.1.near), channel_id=1, source_target_pairs={{0,1},{1,0},{2,3},{3,2},{4,5},{5,4},{6,7},{7,6},{8,9},{9,8},{10,11... | collective-permute-start | bytes 1572872 | tf_op jit(solution)/shard_map/ppermute | solution.py:305
  47.6 34.3 %copy-start = (f32[128]{0:T(128)S(1)}, f32[128]{0:T(128)}, u32[]{:S(2)}) copy-start(f32[128]{0:T(128)} %param.23) | copy-start | bytes 1540
  52.6 16.7 %all-to-all-start.1 = ((bf16[16,72,128]{2,1,0:T(8,128)(2,1)}), bf16[16,72,128]{2,1,0:T(8,128)(2,1)S(1)}, u32[]{:S(2)}, u32[]{:S(2)}) async-start(bf16[16,72,128]{2,1,0:T(8,128)(2,1)} %attend.1), calls=%async_computation.1 | async-start | bytes 589824 | tf_op jit(solution)/shard_map/all_to_all | solution.py:301

commit v8 on v6

--- a/solution.py
+++ b/solution.py
@@ -49,59 +49,57 @@
     return lax.broadcasted_iota(jnp.int32, shape, 0)
 
 
-def project_kernel(
-    tokens, gain, wq, wd, wr, wk, wv, wo, out, own, tokens_, gain_, wq_, wd_, wr_, sems
+def collect_kernel(
+    tokens_, gain_, wd_, wr_, wk, wv, wo, tokens, gain, wd, wr, own, sems
 ):
-    tp = lax.axis_index("tp")
-    groups = lax.axis_size("tp")
-    kv_size = lax.axis_size(KV)
     deep = wk.shape[1]
     pairs = (
-        (tokens, tokens_),
-        (gain, gain_),
-        (wq, wq_),
-        (wd, wd_),
-        (wr, wr_),
         (wk.at[0], own.at[pl.ds(0, deep)]),
         (wv.at[0], own.at[pl.ds(deep, deep)]),
         (wo, own.at[pl.ds(2 * deep, wo.shape[0])]),
+        (tokens_, tokens),
+        (gain_, gain),
+        (wd_, wd),
+        (wr_, wr),
     )
     copies = [pltpu.make_async_copy(x, y, sems.at[n]) for n, (x, y) in enumerate(pairs)]
     for copy in copies:
         copy.start()
-    for copy in copies[:5]:
+    for copy in copies:
         copy.wait()
-    scaled = (tokens_[...].astype(F32) * gain_[...]).astype(BF16)
-    query = dot(scaled, wq_[...], NT)
-    latent = dot(scaled, wd_[...], NN)
-    rope = dot(scaled, wr_[...], NT)
-    seqs = scaled.shape[0]
-    local = seqs // groups
-    chunk = latent.shape[1] // groups
-    part = latent[:, :chunk]
-    for g in range(1, groups):
-        part = jnp.where(tp == g, latent[:, g * chunk : (g + 1) * chunk], part)
-    width = rope.shape[1]
-    rope = jnp.where(lanes(rope.shape) // (width // groups) == tp, rope, 0.0)
-    blank = jnp.zeros((seqs, 128 - width), F32)
-    part = jnp.concatenate([blank, part], axis=1)
-    rope = jnp.concatenate([blank, rope], axis=1)
-    first = query[:, :128].astype(BF16)
-    second = jnp.concatenate([query[:, 128:], blank], axis=1)
-    row = rows((local, 128))
-    for t in range(groups):
-        top = first[t * local : (t + 1) * local]
-        low = second[t * local : (t + 1) * local]
-        for j in range(local):
-            r = t * local + j
-            new = jnp.where(row == 0, part[r : r + 1], 0.0) + jnp.where(row == 1, rope[r : r + 1], 0.0)
-            tile = (low + new).astype(BF16)
-            for c in range(kv_size // local):
-                b = (c * local + j) * groups + t
-                out[b, :, :128] = top
-                out[b, :, 128:] = tile
-    for copy in copies[5:]:
-        copy.wait()
+
+
+def project_kernel(tokens, gain, near, far, wd, wr, out, news):
+    tp = lax.axis_index("tp")
+    groups = lax.axis_size("tp")
+    local = tokens.shape[0] // groups
+    half = groups // 2
+    width = wr.shape[0]
+    mine = tokens[pl.ds(pl.multiple_of(tp * local, local), local), :]
+    scaled = (mine.astype(F32) * gain[...]).astype(BF16)
+    latent = dot(scaled, wd[...], NN)
+    rope = dot(scaled, wr[...], NT)
+    pieces = latent.shape[1] // 128
+    for n in range(pieces):
+        news[n] = latent[:, n * 128 : (n + 1) * 128]
+    news[pieces] = jnp.concatenate([rope, jnp.zeros((local, 128 - width), F32)], axis=1)
+    for n in range(pieces + 1, local):
+        news[n] = jnp.zeros((local, 128), F32)
+    queries = [
+        dot(scaled, (near if i < half else far)[i % half], NT) for i in range(groups)
+    ]
+    tiles = [q[:, :128].astype(BF16) for q in queries] + [
+        jnp.concatenate([queries[i][:, 128:], queries[i + half][:, 128:]], axis=1).astype(BF16)
+        for i in range(half)
+    ]
+    copies = out.shape[0] // local
+    for j in range(local):
+        new = news[:, j, :].astype(BF16)
+        for c in range(copies):
+            k = c * local + j
+            for n, tile in enumerate(tiles):
+                out[k, n * local : (n + 1) * local, :] = tile
+            out[k, len(tiles) * local :, :] = new
 
 
 def rotate(values, cosine, sine):
@@ -111,8 +109,9 @@
 
 
 def attend_kernel(
-    got, lengths, frequencies, near, far, gain, latents, ropes,
-    out, cache, cache_rope, sums, lifted, turned, scored, weights, means, sems,
+    got, near, far, lengths_, frequencies_, gain_, latents, ropes,
+    out, lengths, frequencies, gain, cache, cache_rope,
+    lifted, turned, scored, weights, means, sems,
     *, factor, nope,
 ):
     kv = lax.axis_index(KV)
@@ -121,6 +120,12 @@
     groups = lax.axis_size("tp")
     local, positions, latent_width = cache.shape
     width = cache_rope.shape[1]
+    small = []
+    for n, (a, b) in enumerate(
+        ((lengths_, lengths), (frequencies_, frequencies), (gain_, gain))
+    ):
+        small.append(pltpu.make_async_copy(a, b, sems.at[2 * local + n]))
+        small[n].start()
     copies = []
     for s in range(local):
         a = pltpu.make_async_copy(latents.at[s], cache.at[s], sems.at[s])
@@ -128,11 +133,15 @@
         a.start()
         b.start()
         copies.append((a, b))
-    for h in range(groups):
-        total = got[h].astype(F32)
+    def total(n):
+        rows_of = slice(n * local, (n + 1) * local)
+        result = got[0, rows_of, :].astype(F32)
         for k in range(1, kv_size):
-            total = total + got[k * groups + h].astype(F32)
-        sums[h] = total
+            result = result + got[k, rows_of, :].astype(F32)
+        return result
+
+    for copy in small:
+        copy.wait()
     shape = (local, lengths.shape[1])
     length = jnp.sum(
         jnp.where(lanes(shape) == rows(shape) + tp * local, lengths[...], 0), axis=1, keepdims=True
@@ -143,19 +152,17 @@
     sine = jnp.sin(angles)
     sine = jnp.where(lane < width // 2, -sine, sine)
     half = groups // 2
-    y = tp // 2
-    core = lax.rem(tp, 2)
     for i in range(groups):
-        step = (0, half - 1, 1, 2)[i % half]
-        head = 2 * lax.rem(y + step, half) + (core if i < half else 1 - core)
-        q = sums[head]
         w = near if i < half else far
-        lifted[i] = dot(q[:, :nope].astype(BF16), w[i % half, :latent_width, :], NT)
-        turned[i] = rotate(q[:, nope : nope + width].astype(BF16).astype(F32), cosine, sine)
-    raw = jnp.concatenate([sums[h][0:1, nope + width :] for h in range(groups)], axis=1)
-    rope_raw = sums[0][1:2, nope + width :]
-    for h in range(1, groups):
-        rope_raw = rope_raw + sums[h][1:2, nope + width :]
+        lifted[i] = dot(total(i).astype(BF16), w[i % half, :latent_width, :], NT)
+    for i in range(half):
+        both = total(groups + i).astype(BF16).astype(F32)
+        turned[i] = rotate(both[:, :width], cosine, sine)
+        turned[i + half] = rotate(both[:, width:], cosine, sine)
+    fresh = total(groups + half)
+    pieces = latent_width // nope
+    raw = jnp.concatenate([fresh[n : n + 1] for n in range(pieces)], axis=1)
+    rope_raw = fresh[pieces : pieces + 1, :width]
     square = jnp.sum(raw * raw, axis=1, keepdims=True) / latent_width
     new_latent = (raw * lax.rsqrt(square + EPSILON) * gain[...]).astype(BF16).astype(F32)
     new_seq = lax.rem(kv, local)
@@ -274,6 +281,19 @@
     return lax.all_to_all(value, axes, split_axis=0, concat_axis=0, tiled=True)
 
 
+def swap(value):
+    return lax.ppermute(value, "tp", [(i, i ^ 1) for i in range(lax.axis_size("tp"))])
+
+
+def along(own):
+    size = lax.axis_size("tp")
+    collected = [own]
+    for step in (1, 3, 2):
+        pairs = [(i, (i + 2 * step) % size) for i in range(size)]
+        collected.append(lax.ppermute(own, "tp", pairs))
+    return jnp.stack(collected)
+
+
 def on_device(
     tokens,
     token_gain,
@@ -299,29 +319,26 @@
     value = w_value_up.shape[2]
     factor = (nope + rope) ** (-0.5)
 
-    sent, own = pl.pallas_call(
-        project_kernel,
+    near_query = along(w_query.T)
+    far_query = swap(near_query)
+    tokens, gain, w_down, w_rope, own = pl.pallas_call(
+        collect_kernel,
         out_shape=(
-            jax.ShapeDtypeStruct((everyone, local, 256), BF16),
+            jax.ShapeDtypeStruct(tokens.shape, BF16),
+            jax.ShapeDtypeStruct((1, width), F32),
+            jax.ShapeDtypeStruct(w_down_kv.shape, BF16),
+            jax.ShapeDtypeStruct((rope, width), BF16),
             jax.ShapeDtypeStruct((2 * latent_width + value, nope), BF16),
         ),
-        in_specs=[in_hbm()] * 8,
-        out_specs=(in_vmem(),) * 2,
-        scratch_shapes=[
-            pltpu.VMEM((seqs, width), BF16),
-            pltpu.VMEM((1, width), F32),
-            pltpu.VMEM((nope + rope, width), BF16),
-            pltpu.VMEM((width, latent_width), BF16),
-            pltpu.VMEM((rope, width), BF16),
-            pltpu.SemaphoreType.DMA((8,)),
-        ],
+        in_specs=[in_hbm()] * 7,
+        out_specs=(in_vmem(),) * 5,
+        scratch_shapes=[pltpu.SemaphoreType.DMA((7,))],
         compiler_params=params(8),
-        name="project",
+        name="collect",
     )(
         *keep_in_hbm(
             tokens,
             token_gain[None],
-            w_query.T,
             w_down_kv,
             w_rope_key.T,
             w_key_up,
@@ -329,44 +346,53 @@
             w_out,
         )
     )
-
-    collected = [own]
-    for step in (1, 3, 2):
-        collected.append(
-            lax.ppermute(own, "tp", [(i, (i + 2 * step) % groups) for i in range(groups)])
-        )
-    near = jnp.stack(collected)
-    far = lax.ppermute(near, "tp", [(i, i ^ 1) for i in range(groups)])
-
-    got = exchange(sent, ALL)
+    near = along(own)
+    far = swap(near)
+
+    sent_rows = (groups + groups // 2 + 1) * local
+    sent = pl.pallas_call(
+        project_kernel,
+        out_shape=jax.ShapeDtypeStruct((kv_size, sent_rows, 128), BF16),
+        in_specs=[in_vmem()] * 6,
+        out_specs=in_vmem(),
+        scratch_shapes=[pltpu.VMEM((local, local, 128), F32)],
+        compiler_params=params(8),
+        name="project",
+    )(tokens, gain, near_query, far_query, w_down, w_rope)
+    got = exchange(sent, KV)
     powers = np.arange(0, rope, 2, dtype=np.float64) / rope
     frequencies = np.tile(1.0 / 10000.0**powers, 2)[None].astype(np.float32)
     sent = pl.pallas_call(
         functools.partial(attend_kernel, factor=factor, nope=nope),
         out_shape=jax.ShapeDtypeStruct((kv_size, groups * local + local, value), BF16),
-        in_specs=[in_vmem()] * 6 + [in_hbm()] * 2,
+        in_specs=[in_vmem()] * 3 + [in_hbm()] * 5,
         out_specs=in_vmem(),
         scratch_shapes=[
+            pltpu.VMEM((1, seqs), jnp.int32),
+            pltpu.VMEM((1, rope), F32),
+            pltpu.VMEM((1, latent_width), F32),
             pltpu.VMEM((local, positions, latent_width), BF16),
             pltpu.VMEM((local, rope, positions), BF16),
-            pltpu.VMEM((groups, local, 256), F32),
             pltpu.VMEM((groups, local, latent_width), F32),
             pltpu.VMEM((groups, local, rope), F32),
             pltpu.VMEM((local * groups, positions + 128), F32),
             pltpu.VMEM((local * groups, positions), BF16),
             pltpu.VMEM((local, groups, latent_width), F32),
-            pltpu.SemaphoreType.DMA((2 * local,)),
+            pltpu.SemaphoreType.DMA((2 * local + 3,)),
         ],
         compiler_params=params(24),
         name="attend",
     )(
         got,
-        lengths[None],
-        frequencies,
         near,
         far,
-        latent_gain[None],
-        *keep_in_hbm(cache_latent, cache_rope.transpose(0, 2, 1)),
+        *keep_in_hbm(
+            lengths[None],
+            frequencies,
+            latent_gain[None],
+            cache_latent,
+            cache_rope.transpose(0, 2, 1),
+        ),
     )
     got = exchange(sent, KV)
 

time: 76.7 us -> 82.9 us (1.081)
  waiting for transfers between devices: 11.7 us -> 16.8 us
  starting transfers between devices: 5.5 us -> 10.4 us
  blocking collectives: 50.9 us -> 46.8 us
    ppermute x4 -> x8, waiting for transfers between devices: 11.7 us -> 16.8 us  [the longest x6 15.4 us: along(): collected.append(lax.ppermute(own, 'tp', pairs))]
    ppermute x4 -> x8, starting transfers between devices: 5.5 us -> 10.4 us  [the longest x6 10.2 us: along(): collected.append(lax.ppermute(own, 'tp', pairs))]
    all_to_all x3, blocking collectives: 50.9 us -> 46.8 us  [exchange(): return lax.all_to_all(value, axes, split_axis=0, concat_axis=0, tiled=True)]
    pallas_call x1 -> x2, Pallas kernels: 1.72 us -> 1.56 us  [the longest x1 1.14 us: on_device(): pl.pallas_call(collect_kernel, out_shape=(jax.ShapeDtypeStruct(tokens.sha...]
  transfers between devices with their start and end apart: 4 -> 8, of which waited for: 2 -> 4; matrix products, arithmetic and copies ran while one was open for 0% -> 0% of each run, Pallas kernels for 0% -> 1%
where the time goes in v8:
time: 82.9 us; the launch traced here: 81.9 us
  blocking collectives  46.8 us (56%)
  waiting for transfers between devices  16.8 us (20%)
  starting transfers between devices  10.4 us (13%)
  Pallas kernels  7.14 us (9%)
    all_to_all x3, blocking collectives, exchange(): return lax.all_to_all(value, axes, split_axis=0, concat_axis=0, tiled=True)  46.8 us
    ppermute x6, waiting for transfers between devices, along(): collected.append(lax.ppermute(own, 'tp', pairs))  15.4 us
    ppermute x6, starting transfers between devices, along(): collected.append(lax.ppermute(own, 'tp', pairs))  10.2 us
    pallas_call x1, Pallas kernels, on_device(): pl.pallas_call(functools.partial(attend_kernel, factor=factor, nope=nope)...  4.35 us
  transfers between devices with their start and end apart: 8, of which 4 were waited for; matrix products, arithmetic and copies ran while one was open for 0% of the time, Pallas kernels for 1%

profile of v8, /device:TPU:0, one launch (start us, length us, event | category | flops | bytes accessed | tf_op | source)
XLA Modules:
  0.0 81.9 jit_solution(11097095885123518513)
XLA Ops:
  0.0 1.1 %collect.1 = (bf16[64,128]{1,0:T(8,128)(2,1)S(1)}, f32[1,128]{1,0:T(1,128)S(1)}, bf16[128,512]{1,0:T(8,128)(2,1)S(1)}, bf16[64,128]{1,0:T(8,128)(2,1)S(1)}, bf16[1152,128]{1,0:T(8,128)(2,1)S(1)}) custom-call(bf16[64,128]{1,0:T(8,128)(2,1)} %tokens_.1, f32[1,128]{1,0:T(1,128)} %bitcast.32, bf16[128,512]{1,0:T(8,128)(2,1)} %wd_.1, bf16[64,128]{1,0:T(8,128)(2,1)} %bitcast.29, ...), custom_call_target="tpu_custom_call" | custom-call | tf_op jit(solution)/shard_map/collect/pallas_call | solution.py:324
  1.1 3.4 %collective-permute-start.6 = (bf16[1152,128]{1,0:T(8,128)(2,1)S(1)}, bf16[1152,128]{1,0:T(8,128)(2,1)S(1)}, u32[]{:S(2)}, u32[]{:S(2)}) collective-permute-start(bf16[1152,128]{1,0:T(8,128)(2,1)S(1)} %get-tuple-element.14), channel_id=1, source_target_pairs={{0,4},{1,5},{2,6},{3,7},{4,0},{5,1},{6,2},{7,3},{8,12},{9,13},{10,... | collective-permute-start | bytes 884744 | tf_op jit(solution)/shard_map/ppermute | solution.py:293
  4.5 1.1 %collective-permute-start.5 = (bf16[1152,128]{1,0:T(8,128)(2,1)S(1)}, bf16[1152,128]{1,0:T(8,128)(2,1)S(1)}, u32[]{:S(2)}, u32[]{:S(2)}) collective-permute-start(bf16[1152,128]{1,0:T(8,128)(2,1)S(1)} %get-tuple-element.14), channel_id=1, source_target_pairs={{0,6},{1,7},{2,0},{3,1},{4,2},{5,3},{6,4},{7,5},{8,14},{9,15},{10,... | collective-permute-start | bytes 884744 | tf_op jit(solution)/shard_map/ppermute | solution.py:293
  5.6 1.0 %collective-permute-start.4 = (bf16[1152,128]{1,0:T(8,128)(2,1)S(1)}, bf16[1152,128]{1,0:T(8,128)(2,1)S(1)}, u32[]{:S(2)}, u32[]{:S(2)}) collective-permute-start(bf16[1152,128]{1,0:T(8,128)(2,1)S(1)} %get-tuple-element.14), channel_id=1, source_target_pairs={{0,2},{1,3},{2,4},{3,5},{4,6},{5,7},{6,0},{7,1},{8,10},{9,11},{10,... | collective-permute-start | bytes 884744 | tf_op jit(solution)/shard_map/ppermute | solution.py:293
  6.6 6.1 %collective-permute-done.6 = bf16[1152,128]{1,0:T(8,128)(2,1)S(1)} collective-permute-done((bf16[1152,128]{1,0:T(8,128)(2,1)S(1)}, bf16[1152,128]{1,0:T(8,128)(2,1)S(1)}, u32[]{:S(2)}, u32[]{:S(2)}) %collective-permute-start.6) | collective-permute-done | bytes 294944 | tf_op jit(solution)/shard_map/ppermute | solution.py:293
  12.6 5.7 %collective-permute-done.5 = bf16[1152,128]{1,0:T(8,128)(2,1)S(1)} collective-permute-done((bf16[1152,128]{1,0:T(8,128)(2,1)S(1)}, bf16[1152,128]{1,0:T(8,128)(2,1)S(1)}, u32[]{:S(2)}, u32[]{:S(2)}) %collective-permute-start.5) | collective-permute-done | bytes 294944 | tf_op jit(solution)/shard_map/ppermute | solution.py:293
  18.3 0.0 collective-permute-done.4
  18.3 0.0 copy-start.1
  18.3 0.1 pad_maximum_fusion.near
  18.5 0.1 collective-permute-start.7
  18.5 0.6 copy-done.1
  19.1 2.6 %collective-permute-start.1 = (bf16[192,128]{1,0:T(8,128)(2,1)S(1)}, bf16[192,128]{1,0:T(8,128)(2,1)S(1)}, u32[]{:S(2)}, u32[]{:S(2)}) collective-permute-start(bf16[192,128]{1,0:T(8,128)(2,1)S(1)} %bitcast.22), channel_id=1, source_target_pairs={{0,6},{1,7},{2,0},{3,1},{4,2},{5,3},{6,4},{7,5},{8,14},{9,15},{10,... | collective-permute-start | bytes 147464 | tf_op jit(solution)/shard_map/ppermute | solution.py:293
  21.7 0.0 collective-permute-start
  21.7 2.2 %collective-permute-start.2 = (bf16[192,128]{1,0:T(8,128)(2,1)S(1)}, bf16[192,128]{1,0:T(8,128)(2,1)S(1)}, u32[]{:S(2)}, u32[]{:S(2)}) collective-permute-start(bf16[192,128]{1,0:T(8,128)(2,1)S(1)} %bitcast.24), channel_id=1, source_target_pairs={{0,4},{1,5},{2,6},{3,7},{4,0},{5,1},{6,2},{7,3},{8,12},{9,13},{10,... | collective-permute-start | bytes 147464 | tf_op jit(solution)/shard_map/ppermute | solution.py:293
  23.9 0.0 collective-permute-done.1
  23.9 3.6 %collective-permute-done = bf16[192,128]{1,0:T(8,128)(2,1)S(1)} collective-permute-done((bf16[192,128]{1,0:T(8,128)(2,1)S(1)}, bf16[192,128]{1,0:T(8,128)(2,1)S(1)}, u32[]{:S(2)}, u32[]{:S(2)}) %collective-permute-start) | collective-permute-done | bytes 49184 | tf_op jit(solution)/shard_map/ppermute | solution.py:293
  27.6 0.0 collective-permute-done.2
  27.6 0.1 collective-permute-start.3
  27.7 1.4 %collective-permute-done.3.far = bf16[4,192,128]{2,1,0:T(8,128)(2,1)S(1)} collective-permute-done((bf16[4,192,128]{2,1,0:T(8,128)(2,1)S(1)}, bf16[4,192,128]{2,1,0:T(8,128)(2,1)S(1)}, u32[]{:S(2)}, u32[]{:S(2)}) %collective-permute-start.3) | collective-permute-done | bytes 196640 | tf_op jit(solution)/shard_map/ppermute | solution.py:285
  29.1 0.4 project.1
  29.6 18.4 %all_to_all.15.got = bf16[16,104,128]{2,1,0:T(8,128)(2,1)S(1)} all-to-all(bf16[16,104,128]{2,1,0:T(8,128)(2,1)S(1)} %project.1), channel_id=1, replica_groups=mesh['kv_0'=4,'kv_1'=4,'tp'=8] {'kv_0','kv_1'}, dimensions={0} | all-to-all | bytes 851968 | tf_op jit(solution)/shard_map/all_to_all | solution.py:281
  48.0 0.0 collective-permute-done.7.far
  48.0 4.4 %attend.1 = bf16[16,72,128]{2,1,0:T(8,128)(2,1)S(1)} custom-call(bf16[16,104,128]{2,1,0:T(8,128)(2,1)S(1)} %all_to_all.15.got, bf16[4,1152,128]{2,1,0:T(8,128)(2,1)S(1)} %pad_maximum_fusion.near, bf16[4,1152,128]{2,1,0:T(8,128)(2,1)S(1)} %collective-permute-done.7.far, s32[1,64]{1,0:T(1,128)} %bitcast.31, f32[1,64]{1,0:T(1,128)} %constant.2.clone.frequencies_, ...), custom_call_target="tpu_custom_call" | custom-call | tf_op jit(solution)/shard_map/attend/pallas_call | solution.py:365
  52.3 11.8 %all_to_all.16.got = bf16[16,72,128]{2,1,0:T(8,128)(2,1)S(1)} all-to-all(bf16[16,72,128]{2,1,0:T(8,128)(2,1)S(1)} %attend.1), channel_id=1, replica_groups=mesh['kv_0'=4,'kv_1'=4,'tp'=8] {'kv_0','kv_1'}, dimensions={0} | all-to-all | bytes 589824 | tf_op jit(solution)/shard_map/all_to_all | solution.py:281
  64.1 0.0 copy-start
  64.1 0.5 combine.1
  64.6 16.5 %all_to_all.17.got = bf16[128,8,128]{2,1,0:T(8,128)(2,1)S(1)} all-to-all(bf16[128,8,128]{2,1,0:T(8,128)(2,1)S(1)} %combine.1), channel_id=1, replica_groups=mesh['kv_0'=4,'kv_1'=4,'tp'=8] {'kv_0','kv_1','tp'}, dimensions={0} | all-to-all | bytes 524288 | tf_op jit(solution)/shard_map/all_to_all | solution.py:281
  81.2 0.0 copy-done
  81.2 0.8 finish.1
  (1 shorter events, 0.0 us)
Async XLA Ops:
  1.1 11.5 %collective-permute-start.6 = (bf16[1152,128]{1,0:T(8,128)(2,1)S(1)}, bf16[1152,128]{1,0:T(8,128)(2,1)S(1)}, u32[]{:S(2)}, u32[]{:S(2)}) collective-permute-start(bf16[1152,128]{1,0:T(8,128)(2,1)S(1)} %get-tuple-element.14), channel_id=1, source_target_pairs={{0,4},{1,5},{2,6},{3,7},{4,0},{5,1},{6,2},{7,3},{8,12},{9,13},{10,... | collective-permute-start | bytes 884744 | tf_op jit(solution)/shard_map/ppermute | solution.py:293
  4.5 13.8 %collective-permute-start.5 = (bf16[1152,128]{1,0:T(8,128)(2,1)S(1)}, bf16[1152,128]{1,0:T(8,128)(2,1)S(1)}, u32[]{:S(2)}, u32[]{:S(2)}) collective-permute-start(bf16[1152,128]{1,0:T(8,128)(2,1)S(1)} %get-tuple-element.14), channel_id=1, source_target_pairs={{0,6},{1,7},{2,0},{3,1},{4,2},{5,3},{6,4},{7,5},{8,14},{9,15},{10,... | collective-permute-start | bytes 884744 | tf_op jit(solution)/shard_map/ppermute | solution.py:293
  5.6 12.7 %collective-permute-start.4 = (bf16[1152,128]{1,0:T(8,128)(2,1)S(1)}, bf16[1152,128]{1,0:T(8,128)(2,1)S(1)}, u32[]{:S(2)}, u32[]{:S(2)}) collective-permute-start(bf16[1152,128]{1,0:T(8,128)(2,1)S(1)} %get-tuple-element.14), channel_id=1, source_target_pairs={{0,2},{1,3},{2,4},{3,5},{4,6},{5,7},{6,0},{7,1},{8,10},{9,11},{10,... | collective-permute-start | bytes 884744 | tf_op jit(solution)/shard_map/ppermute | solution.py:293
  18.3 0.8 copy-start.1
  18.5 29.5 %collective-permute-start.7 = (bf16[4,1152,128]{2,1,0:T(8,128)(2,1)S(1)}, bf16[4,1152,128]{2,1,0:T(8,128)(2,1)S(1)}, u32[]{:S(2)}, u32[]{:S(2)}) collective-permute-start(bf16[4,1152,128]{2,1,0:T(8,128)(2,1)S(1)} %pad_maximum_fusion.near), channel_id=1, source_target_pairs={{0,1},{1,0},{2,3},{3,2},{4,5},{5,4},{6,7},{7,6},{8,9},{9,8},{10,11... | collective-permute-start | bytes 3538952 | tf_op jit(solution)/shard_map/ppermute | solution.py:285
  19.1 4.8 %collective-permute-start.1 = (bf16[192,128]{1,0:T(8,128)(2,1)S(1)}, bf16[192,128]{1,0:T(8,128)(2,1)S(1)}, u32[]{:S(2)}, u32[]{:S(2)}) collective-permute-start(bf16[192,128]{1,0:T(8,128)(2,1)S(1)} %bitcast.22), channel_id=1, source_target_pairs={{0,6},{1,7},{2,0},{3,1},{4,2},{5,3},{6,4},{7,5},{8,14},{9,15},{10,... | collective-permute-start | bytes 147464 | tf_op jit(solution)/shard_map/ppermute | solution.py:293
  21.7 5.8 %collective-permute-start = (bf16[192,128]{1,0:T(8,128)(2,1)S(1)}, bf16[192,128]{1,0:T(8,128)(2,1)S(1)}, u32[]{:S(2)}, u32[]{:S(2)}) collective-permute-start(bf16[192,128]{1,0:T(8,128)(2,1)S(1)} %bitcast.23), channel_id=1, source_target_pairs={{0,2},{1,3},{2,4},{3,5},{4,6},{5,7},{6,0},{7,1},{8,10},{9,11},{10,... | collective-permute-start | bytes 147464 | tf_op jit(solution)/shard_map/ppermute | solution.py:293
  21.7 5.8 %collective-permute-start.2 = (bf16[192,128]{1,0:T(8,128)(2,1)S(1)}, bf16[192,128]{1,0:T(8,128)(2,1)S(1)}, u32[]{:S(2)}, u32[]{:S(2)}) collective-permute-start(bf16[192,128]{1,0:T(8,128)(2,1)S(1)} %bitcast.24), channel_id=1, source_target_pairs={{0,4},{1,5},{2,6},{3,7},{4,0},{5,1},{6,2},{7,3},{8,12},{9,13},{10,... | collective-permute-start | bytes 147464 | tf_op jit(solution)/shard_map/ppermute | solution.py:293
  27.6 1.5 %collective-permute-start.3 = (bf16[4,192,128]{2,1,0:T(8,128)(2,1)S(1)}, bf16[4,192,128]{2,1,0:T(8,128)(2,1)S(1)}, u32[]{:S(2)}, u32[]{:S(2)}) collective-permute-start(bf16[4,192,128]{2,1,0:T(8,128)(2,1)S(1)} %pad_maximum_fusion.1.near), channel_id=1, source_target_pairs={{0,1},{1,0},{2,3},{3,2},{4,5},{5,4},{6,7},{7,6},{8,9},{9,8},{10,11... | collective-permute-start | bytes 589832 | tf_op jit(solution)/shard_map/ppermute | solution.py:285
  64.1 17.0 %copy-start = (f32[128]{0:T(128)S(1)}, f32[128]{0:T(128)}, u32[]{:S(2)}) copy-start(f32[128]{0:T(128)} %param.23) | copy-start | bytes 1540

commit v9 on v8

--- a/solution.py
+++ b/solution.py
@@ -50,7 +50,7 @@
 
 
 def collect_kernel(
-    tokens_, gain_, wd_, wr_, wk, wv, wo, tokens, gain, wd, wr, own, sems
+    tokens_, gain_, wd_, wr_, wq_, wk, wv, wo, tokens, gain, wd, wr, wq, own, sems
 ):
     deep = wk.shape[1]
     pairs = (
@@ -61,6 +61,7 @@
         (gain_, gain),
         (wd_, wd),
         (wr_, wr),
+        (wq_, wq),
     )
     copies = [pltpu.make_async_copy(x, y, sems.at[n]) for n, (x, y) in enumerate(pairs)]
     for copy in copies:
@@ -287,11 +288,11 @@
 
 def along(own):
     size = lax.axis_size("tp")
-    collected = [own]
+    collected = []
     for step in (1, 3, 2):
         pairs = [(i, (i + 2 * step) % size) for i in range(size)]
         collected.append(lax.ppermute(own, "tp", pairs))
-    return jnp.stack(collected)
+    return collected
 
 
 def on_device(
@@ -319,20 +320,20 @@
     value = w_value_up.shape[2]
     factor = (nope + rope) ** (-0.5)
 
-    near_query = along(w_query.T)
-    far_query = swap(near_query)
-    tokens, gain, w_down, w_rope, own = pl.pallas_call(
+    others = along(w_query.T)
+    tokens, gain, w_down, w_rope, own_query, own = pl.pallas_call(
         collect_kernel,
         out_shape=(
             jax.ShapeDtypeStruct(tokens.shape, BF16),
             jax.ShapeDtypeStruct((1, width), F32),
             jax.ShapeDtypeStruct(w_down_kv.shape, BF16),
             jax.ShapeDtypeStruct((rope, width), BF16),
+            jax.ShapeDtypeStruct((nope + rope, width), BF16),
             jax.ShapeDtypeStruct((2 * latent_width + value, nope), BF16),
         ),
-        in_specs=[in_hbm()] * 7,
-        out_specs=(in_vmem(),) * 5,
-        scratch_shapes=[pltpu.SemaphoreType.DMA((7,))],
+        in_specs=[in_hbm()] * 8,
+        out_specs=(in_vmem(),) * 6,
+        scratch_shapes=[pltpu.SemaphoreType.DMA((8,))],
         compiler_params=params(8),
         name="collect",
     )(
@@ -341,12 +342,15 @@
             token_gain[None],
             w_down_kv,
             w_rope_key.T,
+            w_query.T,
             w_key_up,
             w_value_up,
             w_out,
         )
     )
-    near = along(own)
+    near_query = jnp.stack([own_query] + others)
+    far_query = swap(near_query)
+    near = jnp.stack([own] + along(own))
     far = swap(near)
 
     sent_rows = (groups + groups // 2 + 1) * local

time: 82.9 us -> 81.9 us (0.988)
  blocking collectives: 46.8 us -> 44.9 us
  waiting for transfers between devices: 16.8 us -> 17.7 us
    all_to_all x3, blocking collectives: 46.8 us -> 44.9 us  [exchange(): return lax.all_to_all(value, axes, split_axis=0, concat_axis=0, tiled=True)]
    ppermute x6, waiting for transfers between devices: 15.4 us -> 16.2 us  [along(): collected.append(lax.ppermute(own, 'tp', pairs))]
  transfers between devices with their start and end apart: 8 -> 8, of which waited for: 4 -> 6; matrix products, arithmetic and copies ran while one was open for 0% -> 0% of each run, Pallas kernels for 1% -> 1%
where the time goes in v9:
time: 81.9 us; the launch traced here: 80.9 us
  blocking collectives  44.9 us (55%)
  waiting for transfers between devices  17.7 us (22%)
  starting transfers between devices  10.4 us (13%)
  Pallas kernels  7.15 us (9%)
    all_to_all x3, blocking collectives, exchange(): return lax.all_to_all(value, axes, split_axis=0, concat_axis=0, tiled=True)  44.9 us
    ppermute x6, waiting for transfers between devices, along(): collected.append(lax.ppermute(own, 'tp', pairs))  16.2 us
    ppermute x6, starting transfers between devices, along(): collected.append(lax.ppermute(own, 'tp', pairs))  10.2 us
    pallas_call x1, Pallas kernels, on_device(): pl.pallas_call(functools.partial(attend_kernel, factor=factor, nope=nope)...  4.35 us
  transfers between devices with their start and end apart: 8, of which 6 were waited for; matrix products, arithmetic and copies ran while one was open for 0% of the time, Pallas kernels for 1%

profile of v9, /device:TPU:0, one launch (start us, length us, event | category | flops | bytes accessed | tf_op | source)
XLA Modules:
  0.0 80.9 jit_solution(5392535151743322286)
XLA Ops:
  0.0 1.2 %collect.1 = (bf16[64,128]{1,0:T(8,128)(2,1)S(1)}, f32[1,128]{1,0:T(1,128)S(1)}, bf16[128,512]{1,0:T(8,128)(2,1)S(1)}, bf16[64,128]{1,0:T(8,128)(2,1)S(1)}, bf16...) custom-call(bf16[64,128]{1,0:T(8,128)(2,1)} %tokens_.1, f32[1,128]{1,0:T(1,128)} %bitcast.31, ...), custom_call_target="tpu_custom_call" | custom-call | tf_op jit(solution)/shard_map/collect/pallas_call | solution.py:324
  1.2 3.4 %collective-permute-start.6 = (bf16[1152,128]{1,0:T(8,128)(2,1)S(1)}, bf16[1152,128]{1,0:T(8,128)(2,1)S(1)}, u32[]{:S(2)}, u32[]{:S(2)}) collective-permute-start(bf16[1152,128]{1,0:T(8,128)(2,1)S(1)} %get-tuple-element.16), channel_id=1, source_target_pairs={{0,4},{1,5},{2,6},{3,7},{4,0},{5,1},{6,2},{7,3},{8,12},{9,13},{10,... | collective-permute-start | bytes 884744 | tf_op jit(solution)/shard_map/ppermute | solution.py:294
  4.5 1.1 %collective-permute-start.5 = (bf16[1152,128]{1,0:T(8,128)(2,1)S(1)}, bf16[1152,128]{1,0:T(8,128)(2,1)S(1)}, u32[]{:S(2)}, u32[]{:S(2)}) collective-permute-start(bf16[1152,128]{1,0:T(8,128)(2,1)S(1)} %get-tuple-element.16), channel_id=1, source_target_pairs={{0,6},{1,7},{2,0},{3,1},{4,2},{5,3},{6,4},{7,5},{8,14},{9,15},{10,... | collective-permute-start | bytes 884744 | tf_op jit(solution)/shard_map/ppermute | solution.py:294
  5.6 1.0 %collective-permute-start.4 = (bf16[1152,128]{1,0:T(8,128)(2,1)S(1)}, bf16[1152,128]{1,0:T(8,128)(2,1)S(1)}, u32[]{:S(2)}, u32[]{:S(2)}) collective-permute-start(bf16[1152,128]{1,0:T(8,128)(2,1)S(1)} %get-tuple-element.16), channel_id=1, source_target_pairs={{0,2},{1,3},{2,4},{3,5},{4,6},{5,7},{6,0},{7,1},{8,10},{9,11},{10,... | collective-permute-start | bytes 884744 | tf_op jit(solution)/shard_map/ppermute | solution.py:294
  6.6 6.1 %collective-permute-done.6 = bf16[1152,128]{1,0:T(8,128)(2,1)S(1)} collective-permute-done((bf16[1152,128]{1,0:T(8,128)(2,1)S(1)}, bf16[1152,128]{1,0:T(8,128)(2,1)S(1)}, u32[]{:S(2)}, u32[]{:S(2)}) %collective-permute-start.6) | collective-permute-done | bytes 294944 | tf_op jit(solution)/shard_map/ppermute | solution.py:294
  12.7 5.7 %collective-permute-done.5 = bf16[1152,128]{1,0:T(8,128)(2,1)S(1)} collective-permute-done((bf16[1152,128]{1,0:T(8,128)(2,1)S(1)}, bf16[1152,128]{1,0:T(8,128)(2,1)S(1)}, u32[]{:S(2)}, u32[]{:S(2)}) %collective-permute-start.5) | collective-permute-done | bytes 294944 | tf_op jit(solution)/shard_map/ppermute | solution.py:294
  18.3 0.0 collective-permute-done.4
  18.3 0.0 copy-start.1
  18.3 0.1 pad_maximum_fusion.near
  18.5 0.1 collective-permute-start.7
  18.6 0.6 copy-done.1
  19.1 2.8 %collective-permute-start.2 = (bf16[192,128]{1,0:T(8,128)(2,1)S(1)}, bf16[192,128]{1,0:T(8,128)(2,1)S(1)}, u32[]{:S(2)}, u32[]{:S(2)}) collective-permute-start(bf16[192,128]{1,0:T(8,128)(2,1)S(1)} %bitcast.23), channel_id=1, source_target_pairs={{0,4},{1,5},{2,6},{3,7},{4,0},{5,1},{6,2},{7,3},{8,12},{9,13},{10,... | collective-permute-start | bytes 147464 | tf_op jit(solution)/shard_map/ppermute | solution.py:294
  21.9 1.2 %collective-permute-start.1 = (bf16[192,128]{1,0:T(8,128)(2,1)S(1)}, bf16[192,128]{1,0:T(8,128)(2,1)S(1)}, u32[]{:S(2)}, u32[]{:S(2)}) collective-permute-start(bf16[192,128]{1,0:T(8,128)(2,1)S(1)} %bitcast.24), channel_id=1, source_target_pairs={{0,6},{1,7},{2,0},{3,1},{4,2},{5,3},{6,4},{7,5},{8,14},{9,15},{10,... | collective-permute-start | bytes 147464 | tf_op jit(solution)/shard_map/ppermute | solution.py:294
  23.1 0.8 %collective-permute-start = (bf16[192,128]{1,0:T(8,128)(2,1)S(1)}, bf16[192,128]{1,0:T(8,128)(2,1)S(1)}, u32[]{:S(2)}, u32[]{:S(2)}) collective-permute-start(bf16[192,128]{1,0:T(8,128)(2,1)S(1)} %bitcast.25), channel_id=1, source_target_pairs={{0,2},{1,3},{2,4},{3,5},{4,6},{5,7},{6,0},{7,1},{8,10},{9,11},{10,... | collective-permute-start | bytes 147464 | tf_op jit(solution)/shard_map/ppermute | solution.py:294
  23.9 0.8 collective-permute-done.2
  24.7 1.3 %collective-permute-done.1 = bf16[192,128]{1,0:T(8,128)(2,1)S(1)} collective-permute-done((bf16[192,128]{1,0:T(8,128)(2,1)S(1)}, bf16[192,128]{1,0:T(8,128)(2,1)S(1)}, u32[]{:S(2)}, u32[]{:S(2)}) %collective-permute-start.1) | collective-permute-done | bytes 49184 | tf_op jit(solution)/shard_map/ppermute | solution.py:294
  26.0 2.4 %collective-permute-done = bf16[192,128]{1,0:T(8,128)(2,1)S(1)} collective-permute-done((bf16[192,128]{1,0:T(8,128)(2,1)S(1)}, bf16[192,128]{1,0:T(8,128)(2,1)S(1)}, u32[]{:S(2)}, u32[]{:S(2)}) %collective-permute-start) | collective-permute-done | bytes 49184 | tf_op jit(solution)/shard_map/ppermute | solution.py:294
  28.5 0.1 collective-permute-start.3
  28.6 1.4 %collective-permute-done.3.far = bf16[4,192,128]{2,1,0:T(8,128)(2,1)S(1)} collective-permute-done((bf16[4,192,128]{2,1,0:T(8,128)(2,1)S(1)}, bf16[4,192,128]{2,1,0:T(8,128)(2,1)S(1)}, u32[]{:S(2)}, u32[]{:S(2)}) %collective-permute-start.3) | collective-permute-done | bytes 196640 | tf_op jit(solution)/shard_map/ppermute | solution.py:286
  30.0 0.4 project.1
  30.4 18.4 %all_to_all.15.got = bf16[16,104,128]{2,1,0:T(8,128)(2,1)S(1)} all-to-all(bf16[16,104,128]{2,1,0:T(8,128)(2,1)S(1)} %project.1), channel_id=1, replica_groups=mesh['kv_0'=4,'kv_1'=4,'tp'=8] {'kv_0','kv_1'}, dimensions={0} | all-to-all | bytes 851968 | tf_op jit(solution)/shard_map/all_to_all | solution.py:282
  48.8 0.0 collective-permute-done.7.far
  48.8 4.4 %attend.1 = bf16[16,72,128]{2,1,0:T(8,128)(2,1)S(1)} custom-call(bf16[16,104,128]{2,1,0:T(8,128)(2,1)S(1)} %all_to_all.15.got, bf16[4,1152,128]{2,1,0:T(8,128)(2,1)S(1)} %pad_maximum_fusion.near, bf16[4,1152,128]{2,1,0:T(8,128)(2,1)S(1)} %collective-permute-done.7.far, s32[1,64]{1,0:T(1,128)} %bitcast.32, f32[1,64]{1,0:T(1,128)} %constant.2.clone.frequencies_, ...), custom_call_target="tpu_custom_call" | custom-call | tf_op jit(solution)/shard_map/attend/pallas_call | solution.py:369
  53.2 11.8 %all_to_all.16.got = bf16[16,72,128]{2,1,0:T(8,128)(2,1)S(1)} all-to-all(bf16[16,72,128]{2,1,0:T(8,128)(2,1)S(1)} %attend.1), channel_id=1, replica_groups=mesh['kv_0'=4,'kv_1'=4,'tp'=8] {'kv_0','kv_1'}, dimensions={0} | all-to-all | bytes 589824 | tf_op jit(solution)/shard_map/all_to_all | solution.py:282
  65.0 0.0 copy-start
  65.0 0.5 combine.1
  65.5 14.7 %all_to_all.17.got = bf16[128,8,128]{2,1,0:T(8,128)(2,1)S(1)} all-to-all(bf16[128,8,128]{2,1,0:T(8,128)(2,1)S(1)} %combine.1), channel_id=1, replica_groups=mesh['kv_0'=4,'kv_1'=4,'tp'=8] {'kv_0','kv_1','tp'}, dimensions={0} | all-to-all | bytes 524288 | tf_op jit(solution)/shard_map/all_to_all | solution.py:282
  80.1 0.0 copy-done
  80.2 0.8 finish.1
  (1 shorter events, 0.0 us)
Async XLA Ops:
  1.2 11.5 %collective-permute-start.6 = (bf16[1152,128]{1,0:T(8,128)(2,1)S(1)}, bf16[1152,128]{1,0:T(8,128)(2,1)S(1)}, u32[]{:S(2)}, u32[]{:S(2)}) collective-permute-start(bf16[1152,128]{1,0:T(8,128)(2,1)S(1)} %get-tuple-element.16), channel_id=1, source_target_pairs={{0,4},{1,5},{2,6},{3,7},{4,0},{5,1},{6,2},{7,3},{8,12},{9,13},{10,... | collective-permute-start | bytes 884744 | tf_op jit(solution)/shard_map/ppermute | solution.py:294
  4.5 13.8 %collective-permute-start.5 = (bf16[1152,128]{1,0:T(8,128)(2,1)S(1)}, bf16[1152,128]{1,0:T(8,128)(2,1)S(1)}, u32[]{:S(2)}, u32[]{:S(2)}) collective-permute-start(bf16[1152,128]{1,0:T(8,128)(2,1)S(1)} %get-tuple-element.16), channel_id=1, source_target_pairs={{0,6},{1,7},{2,0},{3,1},{4,2},{5,3},{6,4},{7,5},{8,14},{9,15},{10,... | collective-permute-start | bytes 884744 | tf_op jit(solution)/shard_map/ppermute | solution.py:294
  5.6 12.7 %collective-permute-start.4 = (bf16[1152,128]{1,0:T(8,128)(2,1)S(1)}, bf16[1152,128]{1,0:T(8,128)(2,1)S(1)}, u32[]{:S(2)}, u32[]{:S(2)}) collective-permute-start(bf16[1152,128]{1,0:T(8,128)(2,1)S(1)} %get-tuple-element.16), channel_id=1, source_target_pairs={{0,2},{1,3},{2,4},{3,5},{4,6},{5,7},{6,0},{7,1},{8,10},{9,11},{10,... | collective-permute-start | bytes 884744 | tf_op jit(solution)/shard_map/ppermute | solution.py:294
  18.3 0.8 copy-start.1
  18.5 30.4 %collective-permute-start.7 = (bf16[4,1152,128]{2,1,0:T(8,128)(2,1)S(1)}, bf16[4,1152,128]{2,1,0:T(8,128)(2,1)S(1)}, u32[]{:S(2)}, u32[]{:S(2)}) collective-permute-start(bf16[4,1152,128]{2,1,0:T(8,128)(2,1)S(1)} %pad_maximum_fusion.near), channel_id=1, source_target_pairs={{0,1},{1,0},{2,3},{3,2},{4,5},{5,4},{6,7},{7,6},{8,9},{9,8},{10,11... | collective-permute-start | bytes 3538952 | tf_op jit(solution)/shard_map/ppermute | solution.py:286
  19.1 5.6 %collective-permute-start.2 = (bf16[192,128]{1,0:T(8,128)(2,1)S(1)}, bf16[192,128]{1,0:T(8,128)(2,1)S(1)}, u32[]{:S(2)}, u32[]{:S(2)}) collective-permute-start(bf16[192,128]{1,0:T(8,128)(2,1)S(1)} %bitcast.23), channel_id=1, source_target_pairs={{0,4},{1,5},{2,6},{3,7},{4,0},{5,1},{6,2},{7,3},{8,12},{9,13},{10,... | collective-permute-start | bytes 147464 | tf_op jit(solution)/shard_map/ppermute | solution.py:294
  21.9 4.1 %collective-permute-start.1 = (bf16[192,128]{1,0:T(8,128)(2,1)S(1)}, bf16[192,128]{1,0:T(8,128)(2,1)S(1)}, u32[]{:S(2)}, u32[]{:S(2)}) collective-permute-start(bf16[192,128]{1,0:T(8,128)(2,1)S(1)} %bitcast.24), channel_id=1, source_target_pairs={{0,6},{1,7},{2,0},{3,1},{4,2},{5,3},{6,4},{7,5},{8,14},{9,15},{10,... | collective-permute-start | bytes 147464 | tf_op jit(solution)/shard_map/ppermute | solution.py:294
  23.1 5.3 %collective-permute-start = (bf16[192,128]{1,0:T(8,128)(2,1)S(1)}, bf16[192,128]{1,0:T(8,128)(2,1)S(1)}, u32[]{:S(2)}, u32[]{:S(2)}) collective-permute-start(bf16[192,128]{1,0:T(8,128)(2,1)S(1)} %bitcast.25), channel_id=1, source_target_pairs={{0,2},{1,3},{2,4},{3,5},{4,6},{5,7},{6,0},{7,1},{8,10},{9,11},{10,... | collective-permute-start | bytes 147464 | tf_op jit(solution)/shard_map/ppermute | solution.py:294
  28.5 1.5 %collective-permute-start.3 = (bf16[4,192,128]{2,1,0:T(8,128)(2,1)S(1)}, bf16[4,192,128]{2,1,0:T(8,128)(2,1)S(1)}, u32[]{:S(2)}, u32[]{:S(2)}) collective-permute-start(bf16[4,192,128]{2,1,0:T(8,128)(2,1)S(1)} %pad_maximum_fusion.1.near), channel_id=1, source_target_pairs={{0,1},{1,0},{2,3},{3,2},{4,5},{5,4},{6,7},{7,6},{8,9},{9,8},{10,11... | collective-permute-start | bytes 589832 | tf_op jit(solution)/shard_map/ppermute | solution.py:286
  65.0 15.2 %copy-start = (f32[128]{0:T(128)S(1)}, f32[128]{0:T(128)}, u32[]{:S(2)}) copy-start(f32[128]{0:T(128)} %param.23) | copy-start | bytes 1540

commit v10 on v9

--- a/solution.py
+++ b/solution.py
@@ -14,6 +14,7 @@
 ALL = ("kv_0", "kv_1", "tp")
 EPSILON = 1e-06
 NEGATIVE = -1e30
+PARTS = 2
 F32 = jnp.float32
 BF16 = jnp.bfloat16
 
@@ -110,7 +111,7 @@
 
 
 def attend_kernel(
-    got, near, far, lengths_, frequencies_, gain_, latents, ropes,
+    got, near, opposite, far, far_opposite, lengths_, frequencies_, gain_, latents, ropes,
     out, lengths, frequencies, gain, cache, cache_rope,
     lifted, turned, scored, weights, means, sems,
     *, factor, nope,
@@ -154,8 +155,8 @@
     sine = jnp.where(lane < width // 2, -sine, sine)
     half = groups // 2
     for i in range(groups):
-        w = near if i < half else far
-        lifted[i] = dot(total(i).astype(BF16), w[i % half, :latent_width, :], NT)
+        w = weights_of((near, opposite, far, far_opposite), i)
+        lifted[i] = dot(total(i).astype(BF16), w[:latent_width, :], NT)
     for i in range(half):
         both = total(groups + i).astype(BF16).astype(F32)
         turned[i] = rotate(both[:, :width], cosine, sine)
@@ -174,52 +175,53 @@
         jnp.sum(jnp.where(mine, sine, 0.0), axis=0, keepdims=True),
     )
     new_rope = new_rope.astype(BF16).astype(F32)
-    pairs = local * groups
-    for s in range(local):
-        q = lifted[:, s, :].astype(BF16)
-        qr = turned[:, s, :].astype(BF16)
-        fresh = jnp.sum(q.astype(F32) * new_latent, axis=1, keepdims=True) + jnp.sum(
-            qr.astype(F32) * new_rope, axis=1, keepdims=True
-        )
-        for copy in copies[s]:
-            copy.wait()
-        r = s * groups
-        scored[r : r + groups, :positions] = dot(q, cache[s], NT) + dot(qr, cache_rope[s], NN)
-        scored[r : r + groups, positions:] = jnp.broadcast_to(fresh, (groups, 128))
-    scores = scored[:, :positions] * factor
-    row = rows((pairs, 1))
-    sequence = row // groups
-    limit = jnp.zeros((pairs, 1), jnp.int32)
-    for s in range(local):
-        limit = jnp.where(sequence == s, length[s : s + 1, :], limit)
-    is_new = jnp.logical_and(sequence == new_seq, kv < local)
-    new = jnp.where(is_new, scored[:, positions : positions + 1] * factor, NEGATIVE)
-    visible = kv * positions + lanes((pairs, positions)) < limit
-    top = jnp.max(jnp.where(visible, scores, NEGATIVE), axis=1, keepdims=True)
-    top = jnp.maximum(top, new)
-    weight = jnp.where(visible, jnp.exp(scores - top), 0.0)
-    new_weight = jnp.where(is_new, jnp.exp(new - top), 0.0)
-    total = jnp.sum(weight, axis=1, keepdims=True) + new_weight
-    weights[...] = weight.astype(BF16)
-    some = total > 0.0
-    safe = jnp.where(some, total, 1.0)
-    inverse = 1.0 / safe
-    logs = jnp.where(some, top + jnp.log(safe), NEGATIVE)
-    rounded = new_weight.astype(BF16).astype(F32)
-    for s in range(local):
-        r = slice(s * groups, (s + 1) * groups)
-        mixed = dot(weights[r, :], cache[s], NN) + rounded[r] * new_latent
-        means[s] = mixed * inverse[r]
+    table = jnp.zeros((groups, 128), F32)
+    for start in range(0, local, local // PARTS):
+        members = range(start, start + local // PARTS)
+        pairs = len(members) * groups
+        for s in members:
+            q = lifted[:, s, :].astype(BF16)
+            qr = turned[:, s, :].astype(BF16)
+            own = jnp.sum(q.astype(F32) * new_latent, axis=1, keepdims=True) + jnp.sum(
+                qr.astype(F32) * new_rope, axis=1, keepdims=True
+            )
+            for copy in copies[s]:
+                copy.wait()
+            r = slice(s * groups, (s + 1) * groups)
+            scored[r, :positions] = dot(q, cache[s], NT) + dot(qr, cache_rope[s], NN)
+            scored[r, positions:] = jnp.broadcast_to(own, (groups, 128))
+        these = slice(start * groups, start * groups + pairs)
+        scores = scored[these, :positions] * factor
+        sequence = rows((pairs, 1)) // groups + start
+        limit = jnp.zeros((pairs, 1), jnp.int32)
+        for s in members:
+            limit = jnp.where(sequence == s, length[s : s + 1, :], limit)
+        is_new = jnp.logical_and(sequence == new_seq, kv < local)
+        new = jnp.where(is_new, scored[these, positions : positions + 1] * factor, NEGATIVE)
+        visible = kv * positions + lanes((pairs, positions)) < limit
+        top = jnp.max(jnp.where(visible, scores, NEGATIVE), axis=1, keepdims=True)
+        top = jnp.maximum(top, new)
+        weight = jnp.where(visible, jnp.exp(scores - top), 0.0)
+        new_weight = jnp.where(is_new, jnp.exp(new - top), 0.0)
+        total_weight = jnp.sum(weight, axis=1, keepdims=True) + new_weight
+        weights[these, :] = weight.astype(BF16)
+        some = total_weight > 0.0
+        safe = jnp.where(some, total_weight, 1.0)
+        inverse = 1.0 / safe
+        logs = jnp.where(some, top + jnp.log(safe), NEGATIVE)
+        rounded = new_weight.astype(BF16).astype(F32)
+        for n, s in enumerate(members):
+            r = slice(n * groups, (n + 1) * groups)
+            mixed = dot(weights[s * groups : (s + 1) * groups, :], cache[s], NN)
+            means[s] = (mixed + rounded[r] * new_latent) * inverse[r]
+            table = jnp.where(lanes((groups, 128)) == s, logs[r], table)
     for i in range(groups):
-        w = near if i < half else far
+        w = weights_of((near, opposite, far, far_opposite), i)
         x = means[:, i, :].astype(BF16)
-        up = dot(x, w[i % half, latent_width : 2 * latent_width, :], NN).astype(BF16)
+        up = dot(x, w[latent_width : 2 * latent_width, :], NN).astype(BF16)
         for k in range(kv_size):
             out[k, i * local : (i + 1) * local, :] = up
     lane = lanes((local, 128))
-    table = jnp.zeros((groups, 128), F32)
-    for s in range(local):
-        table = jnp.where(lanes((groups, 128)) == s, logs[s * groups : (s + 1) * groups], table)
     table = jnp.concatenate([table, jnp.zeros((128 - groups, 128), F32)], axis=0)
     table = jnp.transpose(table)[:local]
     high = table.astype(BF16).astype(F32)
@@ -239,7 +241,14 @@
         out[k, groups * local :, :] = packed
 
 
-def combine_kernel(got, near, far, out, *, kv_size, groups, local, first):
+def weights_of(collected, i):
+    near, opposite, far, far_opposite = collected
+    places = near.shape[0] + 1
+    stacked, single = (near, opposite) if i < places else (far, far_opposite)
+    return single if i % places == places - 1 else stacked.at[i % places]
+
+
+def combine_kernel(got, near, opposite, far, far_opposite, out, *, kv_size, groups, local, first):
     logs = []
     for k in range(kv_size):
         x = got[k, groups * local :, :].astype(F32)
@@ -249,15 +258,14 @@
     total = functools.reduce(jnp.add, shares)
     inverse = 1.0 / total
     shares = [x * inverse for x in shares]
-    half = groups // 2
     mixed = jnp.zeros((local, out.shape[2]), F32)
     for i in range(groups):
         head = jnp.zeros((local, 128), F32)
         for k in range(kv_size):
             part = got[k, i * local : (i + 1) * local, :].astype(F32)
             head = head + part * shares[k][:, i : i + 1]
-        w = near if i < half else far
-        mixed = mixed + dot(head.astype(BF16), w[i % half, first:, :], NN)
+        w = weights_of((near, opposite, far, far_opposite), i)
+        mixed = mixed + dot(head.astype(BF16), w[first:, :], NN)
     mixed = mixed.astype(BF16)
     for d in range(out.shape[0]):
         out[d] = mixed
@@ -350,8 +358,11 @@
     )
     near_query = jnp.stack([own_query] + others)
     far_query = swap(near_query)
-    near = jnp.stack([own] + along(own))
+    before, after, opposite = along(own)
+    near = jnp.stack([own, before, after])
     far = swap(near)
+    far_opposite = swap(opposite)
+    collected = (near, opposite, far, far_opposite)
 
     sent_rows = (groups + groups // 2 + 1) * local
     sent = pl.pallas_call(
@@ -369,7 +380,7 @@
     sent = pl.pallas_call(
         functools.partial(attend_kernel, factor=factor, nope=nope),
         out_shape=jax.ShapeDtypeStruct((kv_size, groups * local + local, value), BF16),
-        in_specs=[in_vmem()] * 3 + [in_hbm()] * 5,
+        in_specs=[in_vmem()] * 5 + [in_hbm()] * 5,
         out_specs=in_vmem(),
         scratch_shapes=[
             pltpu.VMEM((1, seqs), jnp.int32),
@@ -388,8 +399,7 @@
         name="attend",
     )(
         got,
-        near,
-        far,
+        *collected,
         *keep_in_hbm(
             lengths[None],
             frequencies,
@@ -409,11 +419,11 @@
             first=2 * latent_width,
         ),
         out_shape=jax.ShapeDtypeStruct((everyone, local, w_out.shape[1]), BF16),
-        in_specs=[in_vmem()] * 3,
+        in_specs=[in_vmem()] * 5,
         out_specs=in_vmem(),
         compiler_params=params(8),
         name="combine",
-    )(got, near, far)
+    )(got, *collected)
     got = exchange(sent, ALL)
     return pl.pallas_call(
         functools.partial(finish_kernel, kv_size=kv_size, groups=groups, local=local),

time: 81.9 us -> 77.1 us (0.941)
  blocking collectives: 44.9 us -> 27.5 us
  waiting for transfers between devices: 17.7 us -> 26.3 us
  starting transfers between devices: 10.4 us -> 14.1 us
  Pallas kernels: 7.15 us -> 7.97 us
    all_to_all x3 -> x2, blocking collectives: 44.9 us -> 27.5 us  [exchange(): return lax.all_to_all(value, axes, split_axis=0, concat_axis=0, tiled=True)]
    all_to_all x0 -> x1, waiting for transfers between devices: none -> 8.75 us  [exchange(): return lax.all_to_all(value, axes, split_axis=0, concat_axis=0, tiled=True)]
    all_to_all x0 -> x1, starting transfers between devices: none -> 7.88 us  [exchange(): return lax.all_to_all(value, axes, split_axis=0, concat_axis=0, tiled=True)]
    ppermute x6, starting transfers between devices: 10.2 us -> 6.04 us  [along(): collected.append(lax.ppermute(own, 'tp', pairs))]
    ppermute x6, waiting for transfers between devices: 16.2 us -> 15.2 us  [along(): collected.append(lax.ppermute(own, 'tp', pairs))]
    ppermute x2 -> x3, waiting for transfers between devices: 1.43 us -> 2.35 us  [swap(): lax.ppermute(value, 'tp', [(i, i ^ 1) for i in range(lax.axis_size('tp'))])]
  transfers between devices with their start and end apart: 8 -> 10, of which waited for: 6 -> 8; matrix products, arithmetic and copies ran while one was open for 0% -> 0% of each run, Pallas kernels for 1% -> 2%
where the time goes in v10:
time: 77.1 us; the launch traced here: 76.1 us
  blocking collectives  27.5 us (36%)
  waiting for transfers between devices  26.3 us (34%)
  starting transfers between devices  14.1 us (18%)
  Pallas kernels  7.97 us (10%)
    all_to_all x2, blocking collectives, exchange(): return lax.all_to_all(value, axes, split_axis=0, concat_axis=0, tiled=True)  27.5 us
    ppermute x6, waiting for transfers between devices, along(): collected.append(lax.ppermute(own, 'tp', pairs))  15.2 us
    all_to_all x1, waiting for transfers between devices, exchange(): return lax.all_to_all(value, axes, split_axis=0, concat_axis=0, tiled=True)  8.75 us
    all_to_all x1, starting transfers between devices, exchange(): return lax.all_to_all(value, axes, split_axis=0, concat_axis=0, tiled=True)  7.88 us
    ppermute x6, starting transfers between devices, along(): collected.append(lax.ppermute(own, 'tp', pairs))  6.04 us
    pallas_call x1, Pallas kernels, on_device(): pl.pallas_call(functools.partial(attend_kernel, factor=factor, nope=nope)...  4.39 us
    ppermute x3, waiting for transfers between devices, swap(): lax.ppermute(value, 'tp', [(i, i ^ 1) for i in range(lax.axis_size('tp'))])  2.35 us
  transfers between devices with their start and end apart: 10, of which 8 were waited for; matrix products, arithmetic and copies ran while one was open for 0% of the time, Pallas kernels for 2%

profile of v10, /device:TPU:0, one launch (start us, length us, event | category | flops | bytes accessed | tf_op | source)
XLA Modules:
  0.0 76.1 jit_solution(16935567412001073388)
XLA Ops:
  0.0 1.2 %collect.1 = (bf16[64,128]{1,0:T(8,128)(2,1)S(1)}, f32[1,128]{1,0:T(1,128)S(1)}, bf16[128,512]{1,0:T(8,128)(2,1)S(1)}, bf16[64,128]{1,0:T(8,128)(2,1)S(1)}, bf16...) custom-call(bf16[64,128]{1,0:T(8,128)(2,1)} %tokens_.1, f32[1,128]{1,0:T(1,128)} %bitcast.29, ...), custom_call_target="tpu_custom_call" | custom-call | tf_op jit(solution)/shard_map/collect/pallas_call | solution.py:332
  1.2 3.2 %collective-permute-start.5 = (bf16[1152,128]{1,0:T(8,128)(2,1)S(1)}, bf16[1152,128]{1,0:T(8,128)(2,1)S(1)}, u32[]{:S(2)}, u32[]{:S(2)}) collective-permute-start(bf16[1152,128]{1,0:T(8,128)(2,1)S(1)} %get-tuple-element.16), channel_id=1, source_target_pairs={{0,6},{1,7},{2,0},{3,1},{4,2},{5,3},{6,4},{7,5},{8,14},{9,15},{10,... | collective-permute-start | bytes 884744 | tf_op jit(solution)/shard_map/ppermute | solution.py:302
  4.4 0.0 collective-permute-start.4
  4.4 6.3 %collective-permute-done.5 = bf16[1152,128]{1,0:T(8,128)(2,1)S(1)} collective-permute-done((bf16[1152,128]{1,0:T(8,128)(2,1)S(1)}, bf16[1152,128]{1,0:T(8,128)(2,1)S(1)}, u32[]{:S(2)}, u32[]{:S(2)}) %collective-permute-start.5) | collective-permute-done | bytes 294944 | tf_op jit(solution)/shard_map/ppermute | solution.py:302
  10.6 3.4 %collective-permute-done.4 = bf16[1152,128]{1,0:T(8,128)(2,1)S(1)} collective-permute-done((bf16[1152,128]{1,0:T(8,128)(2,1)S(1)}, bf16[1152,128]{1,0:T(8,128)(2,1)S(1)}, u32[]{:S(2)}, u32[]{:S(2)}) %collective-permute-start.4) | collective-permute-done | bytes 294944 | tf_op jit(solution)/shard_map/ppermute | solution.py:302
  14.0 0.1 pad_maximum_fusion.near
  14.1 0.1 collective-permute-start.7
  14.2 0.1 collective-permute-start.2
  14.3 1.7 %collective-permute-start.1 = (bf16[192,128]{1,0:T(8,128)(2,1)}, bf16[192,128]{1,0:T(8,128)(2,1)S(1)}, u32[]{:S(2)}, u32[]{:S(2)}) collective-permute-start(bf16[192,128]{1,0:T(8,128)(2,1)} %bitcast.22), channel_id=1, source_target_pairs={{0,6},{1,7},{2,0},{3,1},{4,2},{5,3},{6,4},{7,5},{8,14},{9,15},{10,... | collective-permute-start | bytes 147464 | tf_op jit(solution)/shard_map/ppermute | solution.py:302
  16.1 0.4 collective-permute-start
  16.4 3.7 %collective-permute-done.2 = bf16[192,128]{1,0:T(8,128)(2,1)S(1)} collective-permute-done((bf16[192,128]{1,0:T(8,128)(2,1)}, bf16[192,128]{1,0:T(8,128)(2,1)S(1)}, u32[]{:S(2)}, u32[]{:S(2)}) %collective-permute-start.2) | collective-permute-done | bytes 49184 | tf_op jit(solution)/shard_map/ppermute | solution.py:302
  20.1 0.0 collective-permute-done.1
  20.1 1.4 %collective-permute-done = bf16[192,128]{1,0:T(8,128)(2,1)S(1)} collective-permute-done((bf16[192,128]{1,0:T(8,128)(2,1)}, bf16[192,128]{1,0:T(8,128)(2,1)S(1)}, u32[]{:S(2)}, u32[]{:S(2)}) %collective-permute-start) | collective-permute-done | bytes 49184 | tf_op jit(solution)/shard_map/ppermute | solution.py:302
  21.6 0.1 collective-permute-start.3
  21.7 0.7 collective-permute-start.6
  22.3 0.8 %collective-permute-done.3.far = bf16[4,192,128]{2,1,0:T(8,128)(2,1)S(1)} collective-permute-done((bf16[4,192,128]{2,1,0:T(8,128)(2,1)S(1)}, bf16[4,192,128]{2,1,0:T(8,128)(2,1)S(1)}, u32[]{:S(2)}, u32[]{:S(2)}) %collective-permute-start.3) | collective-permute-done | bytes 196640 | tf_op jit(solution)/shard_map/ppermute | solution.py:294
  23.1 1.2 %project.1 = bf16[16,104,128]{2,1,0:T(8,128)(2,1)} custom-call(bf16[64,128]{1,0:T(8,128)(2,1)S(1)} %get-tuple-element.11.tokens, f32[1,128]{1,0:T(1,128)S(1)} %get-tuple-element.12.gain, bf16[4,192,128]{2,1,0:T(8,128)(2,1)S(1)} %pad_maximum_fusion.1.near, bf16[4,192,128]{2,1,0:T(8,128)(2,1)S(1)} %collective-permute-done.3.far, ...), custom_call_target="tpu_custom_call" | custom-call | tf_op jit(solution)/shard_map/project/pallas_call | solution.py:368
  24.3 7.9 %all-to-all-start = ((bf16[16,104,128]{2,1,0:T(8,128)(2,1)}), bf16[16,104,128]{2,1,0:T(8,128)(2,1)S(1)}, u32[]{:S(2)}, u32[]{:S(2)}) async-start(bf16[16,104,128]{2,1,0:T(8,128)(2,1)} %project.1), calls=%async_computation | async-start | bytes 851968 | tf_op jit(solution)/shard_map/all_to_all | solution.py:290
  32.2 0.4 collective-permute-done.6.opposite
  32.6 0.0 collective-permute-start.8
  32.6 1.6 %collective-permute-done.8.far_opposite = bf16[1152,128]{1,0:T(8,128)(2,1)S(1)} collective-permute-done((bf16[1152,128]{1,0:T(8,128)(2,1)S(1)}, bf16[1152,128]{1,0:T(8,128)(2,1)S(1)}, u32[]{:S(2)}, u32[]{:S(2)}) %collective-permute-start.8) | collective-permute-done | bytes 294944 | tf_op jit(solution)/shard_map/ppermute | solution.py:294
  34.2 8.8 %all-to-all-done.got = bf16[16,104,128]{2,1,0:T(8,128)(2,1)S(1)} async-done(((bf16[16,104,128]{2,1,0:T(8,128)(2,1)}), bf16[16,104,128]{2,1,0:T(8,128)(2,1)S(1)}, u32[]{:S(2)}, u32[]{:S(2)}) %all-to-all-start) | async-done | bytes 426016 | tf_op jit(solution)/shard_map/all_to_all | solution.py:290
  42.9 0.0 collective-permute-done.7.far
  42.9 0.0 copy-start
  42.9 4.4 %attend.1 = bf16[16,72,128]{2,1,0:T(8,128)(2,1)S(1)} custom-call(bf16[16,104,128]{2,1,0:T(8,128)(2,1)S(1)} %all-to-all-done.got, bf16[3,1152,128]{2,1,0:T(8,128)(2,1)S(1)} %pad_maximum_fusion.near, bf16[1152,128]{1,0:T(8,128)(2,1)S(1)} %collective-permute-done.6.opposite, bf16[3,1152,128]{2,1,0:T(8,128)(2,1)S(1)} %collective-permute-done.7.far, ...), custom_call_target="tpu_custom_call" | custom-call | tf_op jit(solution)/shard_map/attend/pallas_call | solution.py:380
  47.3 11.8 %all_to_all.15.got = bf16[16,72,128]{2,1,0:T(8,128)(2,1)S(1)} all-to-all(bf16[16,72,128]{2,1,0:T(8,128)(2,1)S(1)} %attend.1), channel_id=1, replica_groups=mesh['kv_0'=4,'kv_1'=4,'tp'=8] {'kv_0','kv_1'}, dimensions={0} | all-to-all | bytes 589824 | tf_op jit(solution)/shard_map/all_to_all | solution.py:290
  59.1 0.5 combine.1
  59.6 15.7 %all_to_all.16.got = bf16[128,8,128]{2,1,0:T(8,128)(2,1)S(1)} all-to-all(bf16[128,8,128]{2,1,0:T(8,128)(2,1)S(1)} %combine.1), channel_id=1, replica_groups=mesh['kv_0'=4,'kv_1'=4,'tp'=8] {'kv_0','kv_1','tp'}, dimensions={0} | all-to-all | bytes 524288 | tf_op jit(solution)/shard_map/all_to_all | solution.py:290
  75.4 0.0 copy-done
  75.4 0.8 finish.1
  (1 shorter events, 0.0 us)
Async XLA Ops:
  1.2 9.5 %collective-permute-start.5 = (bf16[1152,128]{1,0:T(8,128)(2,1)S(1)}, bf16[1152,128]{1,0:T(8,128)(2,1)S(1)}, u32[]{:S(2)}, u32[]{:S(2)}) collective-permute-start(bf16[1152,128]{1,0:T(8,128)(2,1)S(1)} %get-tuple-element.16), channel_id=1, source_target_pairs={{0,6},{1,7},{2,0},{3,1},{4,2},{5,3},{6,4},{7,5},{8,14},{9,15},{10,... | collective-permute-start | bytes 884744 | tf_op jit(solution)/shard_map/ppermute | solution.py:302
  4.4 9.7 %collective-permute-start.4 = (bf16[1152,128]{1,0:T(8,128)(2,1)S(1)}, bf16[1152,128]{1,0:T(8,128)(2,1)S(1)}, u32[]{:S(2)}, u32[]{:S(2)}) collective-permute-start(bf16[1152,128]{1,0:T(8,128)(2,1)S(1)} %get-tuple-element.16), channel_id=1, source_target_pairs={{0,2},{1,3},{2,4},{3,5},{4,6},{5,7},{6,0},{7,1},{8,10},{9,11},{10,... | collective-permute-start | bytes 884744 | tf_op jit(solution)/shard_map/ppermute | solution.py:302
  14.1 28.8 %collective-permute-start.7 = (bf16[3,1152,128]{2,1,0:T(8,128)(2,1)S(1)}, bf16[3,1152,128]{2,1,0:T(8,128)(2,1)S(1)}, u32[]{:S(2)}, u32[]{:S(2)}) collective-permute-start(bf16[3,1152,128]{2,1,0:T(8,128)(2,1)S(1)} %pad_maximum_fusion.near), channel_id=1, source_target_pairs={{0,1},{1,0},{2,3},{3,2},{4,5},{5,4},{6,7},{7,6},{8,9},{9,8},{10,11... | collective-permute-start | bytes 2654216 | tf_op jit(solution)/shard_map/ppermute | solution.py:294
  14.2 5.9 %collective-permute-start.2 = (bf16[192,128]{1,0:T(8,128)(2,1)}, bf16[192,128]{1,0:T(8,128)(2,1)S(1)}, u32[]{:S(2)}, u32[]{:S(2)}) collective-permute-start(bf16[192,128]{1,0:T(8,128)(2,1)} %bitcast.21), channel_id=1, source_target_pairs={{0,4},{1,5},{2,6},{3,7},{4,0},{5,1},{6,2},{7,3},{8,12},{9,13},{10,... | collective-permute-start | bytes 147464 | tf_op jit(solution)/shard_map/ppermute | solution.py:302
  14.3 5.8 %collective-permute-start.1 = (bf16[192,128]{1,0:T(8,128)(2,1)}, bf16[192,128]{1,0:T(8,128)(2,1)S(1)}, u32[]{:S(2)}, u32[]{:S(2)}) collective-permute-start(bf16[192,128]{1,0:T(8,128)(2,1)} %bitcast.22), channel_id=1, source_target_pairs={{0,6},{1,7},{2,0},{3,1},{4,2},{5,3},{6,4},{7,5},{8,14},{9,15},{10,... | collective-permute-start | bytes 147464 | tf_op jit(solution)/shard_map/ppermute | solution.py:302
  16.1 5.5 %collective-permute-start = (bf16[192,128]{1,0:T(8,128)(2,1)}, bf16[192,128]{1,0:T(8,128)(2,1)S(1)}, u32[]{:S(2)}, u32[]{:S(2)}) collective-permute-start(bf16[192,128]{1,0:T(8,128)(2,1)} %bitcast.23), channel_id=1, source_target_pairs={{0,2},{1,3},{2,4},{3,5},{4,6},{5,7},{6,0},{7,1},{8,10},{9,11},{10,... | collective-permute-start | bytes 147464 | tf_op jit(solution)/shard_map/ppermute | solution.py:302
  21.6 1.5 %collective-permute-start.3 = (bf16[4,192,128]{2,1,0:T(8,128)(2,1)S(1)}, bf16[4,192,128]{2,1,0:T(8,128)(2,1)S(1)}, u32[]{:S(2)}, u32[]{:S(2)}) collective-permute-start(bf16[4,192,128]{2,1,0:T(8,128)(2,1)S(1)} %pad_maximum_fusion.1.near), channel_id=1, source_target_pairs={{0,1},{1,0},{2,3},{3,2},{4,5},{5,4},{6,7},{7,6},{8,9},{9,8},{10,11... | collective-permute-start | bytes 589832 | tf_op jit(solution)/shard_map/ppermute | solution.py:294
  21.7 10.9 %collective-permute-start.6 = (bf16[1152,128]{1,0:T(8,128)(2,1)S(1)}, bf16[1152,128]{1,0:T(8,128)(2,1)S(1)}, u32[]{:S(2)}, u32[]{:S(2)}) collective-permute-start(bf16[1152,128]{1,0:T(8,128)(2,1)S(1)} %get-tuple-element.16), channel_id=1, source_target_pairs={{0,4},{1,5},{2,6},{3,7},{4,0},{5,1},{6,2},{7,3},{8,12},{9,13},{10,... | collective-permute-start | bytes 884744 | tf_op jit(solution)/shard_map/ppermute | solution.py:302
  24.3 18.6 %all-to-all-start = ((bf16[16,104,128]{2,1,0:T(8,128)(2,1)}), bf16[16,104,128]{2,1,0:T(8,128)(2,1)S(1)}, u32[]{:S(2)}, u32[]{:S(2)}) async-start(bf16[16,104,128]{2,1,0:T(8,128)(2,1)} %project.1), calls=%async_computation | async-start | bytes 851968 | tf_op jit(solution)/shard_map/all_to_all | solution.py:290
  32.6 1.6 %collective-permute-start.8 = (bf16[1152,128]{1,0:T(8,128)(2,1)S(1)}, bf16[1152,128]{1,0:T(8,128)(2,1)S(1)}, u32[]{:S(2)}, u32[]{:S(2)}) collective-permute-start(bf16[1152,128]{1,0:T(8,128)(2,1)S(1)} %collective-permute-done.6.opposite), channel_id=1, source_target_pairs={{0,1},{1,0},{2,3},{3,2},{4,5},{5,4},{6,7},{7,6},{8,9},{9,8},{10,11... | collective-permute-start | bytes 884744 | tf_op jit(solution)/shard_map/ppermute | solution.py:294
  42.9 32.4 %copy-start = (f32[128]{0:T(128)S(1)}, f32[128]{0:T(128)}, u32[]{:S(2)}) copy-start(f32[128]{0:T(128)} %param.23) | copy-start | bytes 1540

commit v11 on v10

--- a/solution.py
+++ b/solution.py
@@ -11,7 +11,9 @@
 
 
 KV = ("kv_0", "kv_1")
-ALL = ("kv_0", "kv_1", "tp")
+TP = ("y", "core")
+ALL = KV + TP
+FIRST = KV + ("core",)
 EPSILON = 1e-06
 NEGATIVE = -1e30
 PARTS = 2
@@ -71,37 +73,39 @@
         copy.wait()
 
 
-def project_kernel(tokens, gain, near, far, wd, wr, out, news):
-    tp = lax.axis_index("tp")
-    groups = lax.axis_size("tp")
-    local = tokens.shape[0] // groups
-    half = groups // 2
+def project_kernel(tokens, gain, query_0, query_1, query_2, query_3, wd, wr, out, news):
+    cores = lax.axis_size("core")
+    local = news.shape[1] // cores
+    chip = cores * local
     width = wr.shape[0]
-    mine = tokens[pl.ds(pl.multiple_of(tp * local, local), local), :]
+    start = pl.multiple_of(lax.axis_index("y") * chip, chip)
+    mine = tokens[pl.ds(start, chip), :]
     scaled = (mine.astype(F32) * gain[...]).astype(BF16)
     latent = dot(scaled, wd[...], NN)
     rope = dot(scaled, wr[...], NT)
     pieces = latent.shape[1] // 128
     for n in range(pieces):
         news[n] = latent[:, n * 128 : (n + 1) * 128]
-    news[pieces] = jnp.concatenate([rope, jnp.zeros((local, 128 - width), F32)], axis=1)
+    news[pieces] = jnp.concatenate([rope, jnp.zeros((chip, 128 - width), F32)], axis=1)
     for n in range(pieces + 1, local):
-        news[n] = jnp.zeros((local, 128), F32)
-    queries = [
-        dot(scaled, (near if i < half else far)[i % half], NT) for i in range(groups)
-    ]
-    tiles = [q[:, :128].astype(BF16) for q in queries] + [
-        jnp.concatenate([queries[i][:, 128:], queries[i + half][:, 128:]], axis=1).astype(BF16)
+        news[n] = jnp.zeros((chip, 128), F32)
+    queries = [dot(scaled, w[...], NT) for w in (query_0, query_1, query_2, query_3)]
+    half = len(queries) // 2
+    tiles = [q[:, :128] for q in queries] + [
+        jnp.concatenate([queries[i][:, 128:], queries[i + half][:, 128:]], axis=1)
         for i in range(half)
     ]
-    copies = out.shape[0] // local
+    tiles = [
+        [tile[c * local : (c + 1) * local].astype(BF16) for c in range(cores)] for tile in tiles
+    ]
     for j in range(local):
-        new = news[:, j, :].astype(BF16)
-        for c in range(copies):
-            k = c * local + j
-            for n, tile in enumerate(tiles):
-                out[k, n * local : (n + 1) * local, :] = tile
-            out[k, len(tiles) * local :, :] = new
+        for c in range(cores):
+            new = news[:, c * local + j, :].astype(BF16)
+            for copy in range(out.shape[0] // cores // local):
+                k = copy * local + j
+                for n, tile in enumerate(tiles):
+                    out[k * cores + c, n * local : (n + 1) * local, :] = tile[c]
+                out[k * cores + c, len(tiles) * local :, :] = new
 
 
 def rotate(values, cosine, sine):
@@ -117,9 +121,9 @@
     *, factor, nope,
 ):
     kv = lax.axis_index(KV)
-    tp = lax.axis_index("tp")
+    tp = lax.axis_index(TP)
     kv_size = lax.axis_size(KV)
-    groups = lax.axis_size("tp")
+    groups = lax.axis_size(TP)
     local, positions, latent_width = cache.shape
     width = cache_rope.shape[1]
     small = []
@@ -135,11 +139,15 @@
         a.start()
         b.start()
         copies.append((a, b))
-    def total(n):
+    cores = lax.axis_size("core")
+    core = lax.axis_index("core")
+    half = groups // 2
+
+    def total(source, n):
         rows_of = slice(n * local, (n + 1) * local)
-        result = got[0, rows_of, :].astype(F32)
+        result = got[source, rows_of, :].astype(F32)
         for k in range(1, kv_size):
-            result = result + got[k, rows_of, :].astype(F32)
+            result = result + got[k * cores + source, rows_of, :].astype(F32)
         return result
 
     for copy in small:
@@ -153,15 +161,18 @@
     cosine = jnp.cos(angles)
     sine = jnp.sin(angles)
     sine = jnp.where(lane < width // 2, -sine, sine)
-    half = groups // 2
     for i in range(groups):
+        source = core if i < half else 1 - core
         w = weights_of((near, opposite, far, far_opposite), i)
-        lifted[i] = dot(total(i).astype(BF16), w[:latent_width, :], NT)
-    for i in range(half):
-        both = total(groups + i).astype(BF16).astype(F32)
+        lifted[i] = dot(total(source, i % half).astype(BF16), w[:latent_width, :], NT)
+    for i in range(groups):
+        if i % half >= half // 2:
+            continue
+        source = core if i < half else 1 - core
+        both = total(source, half + i % half).astype(BF16).astype(F32)
         turned[i] = rotate(both[:, :width], cosine, sine)
-        turned[i + half] = rotate(both[:, width:], cosine, sine)
-    fresh = total(groups + half)
+        turned[i + half // 2] = rotate(both[:, width:], cosine, sine)
+    fresh = total(0, half + half // 2)
     pieces = latent_width // nope
     raw = jnp.concatenate([fresh[n : n + 1] for n in range(pieces)], axis=1)
     rope_raw = fresh[pieces : pieces + 1, :width]
@@ -291,15 +302,15 @@
 
 
 def swap(value):
-    return lax.ppermute(value, "tp", [(i, i ^ 1) for i in range(lax.axis_size("tp"))])
+    return lax.ppermute(value, TP, [(i, i ^ 1) for i in range(lax.axis_size(TP))])
 
 
 def along(own):
-    size = lax.axis_size("tp")
+    size = lax.axis_size(TP)
     collected = []
     for step in (1, 3, 2):
         pairs = [(i, (i + 2 * step) % size) for i in range(size)]
-        collected.append(lax.ppermute(own, "tp", pairs))
+        collected.append(lax.ppermute(own, TP, pairs))
     return collected
 
 
@@ -319,7 +330,7 @@
     lengths,
 ):
     kv_size = lax.axis_size(KV)
-    groups = lax.axis_size("tp")
+    groups = lax.axis_size(TP)
     everyone = kv_size * groups
     seqs, width = tokens.shape
     local, positions, latent_width = cache_latent.shape
@@ -356,25 +367,24 @@
             w_out,
         )
     )
-    near_query = jnp.stack([own_query] + others)
-    far_query = swap(near_query)
     before, after, opposite = along(own)
     near = jnp.stack([own, before, after])
     far = swap(near)
     far_opposite = swap(opposite)
     collected = (near, opposite, far, far_opposite)
 
-    sent_rows = (groups + groups // 2 + 1) * local
+    cores = lax.axis_size("core")
+    sent_rows = (groups // 2 + groups // 4 + 1) * local
     sent = pl.pallas_call(
         project_kernel,
-        out_shape=jax.ShapeDtypeStruct((kv_size, sent_rows, 128), BF16),
-        in_specs=[in_vmem()] * 6,
+        out_shape=jax.ShapeDtypeStruct((kv_size * cores, sent_rows, 128), BF16),
+        in_specs=[in_vmem()] * 8,
         out_specs=in_vmem(),
-        scratch_shapes=[pltpu.VMEM((local, local, 128), F32)],
+        scratch_shapes=[pltpu.VMEM((local, cores * local, 128), F32)],
         compiler_params=params(8),
         name="project",
-    )(tokens, gain, near_query, far_query, w_down, w_rope)
-    got = exchange(sent, KV)
+    )(tokens, gain, own_query, *others, w_down, w_rope)
+    got = exchange(sent, FIRST)
     powers = np.arange(0, rope, 2, dtype=np.float64) / rope
     frequencies = np.tile(1.0 / 10000.0**powers, 2)[None].astype(np.float32)
     sent = pl.pallas_call(
@@ -436,7 +446,7 @@
 
 
 def solution(mesh):
-    finer = Mesh(mesh.devices.reshape(4, 4, mesh.shape["tp"]), ("kv_0", "kv_1", "tp"))
+    finer = Mesh(mesh.devices.reshape(4, 4, mesh.shape["tp"] // 2, 2), ALL)
 
     return jax.shard_map(
         on_device,
@@ -444,16 +454,16 @@
         in_specs=(
             P(None, KV),
             P(KV),
-            P(KV, "tp"),
+            P(KV, TP),
             P(KV, None),
             P(KV, None),
             P(),
-            P("tp", None, None),
-            P("tp", None, None),
-            P("tp", KV),
+            P(TP, None, None),
+            P(TP, None, None),
+            P(TP, KV),
             P(KV),
-            P("tp", KV, None),
-            P("tp", KV, None),
+            P(TP, KV, None),
+            P(TP, KV, None),
             P(),
         ),
         out_specs=P(None, KV),

time: 77.1 us -> 81.5 us (1.057)
  starting transfers between devices: 14.1 us -> 17.4 us
  waiting for transfers between devices: 26.3 us -> 27.6 us
    ppermute x9 -> x8, starting transfers between devices: 6.21 us -> 9.26 us  [the longest x6 8.83 us: along(): collected.append(lax.ppermute(own, TP, pairs))]
    all_to_all x1, waiting for transfers between devices: 8.75 us -> 10.5 us  [exchange(): return lax.all_to_all(value, axes, split_axis=0, concat_axis=0, tiled=True)]
    ppermute x9 -> x8, waiting for transfers between devices: 17.6 us -> 17.1 us  [the longest x6 17.1 us: along(): collected.append(lax.ppermute(own, TP, pairs))]
  transfers between devices with their start and end apart: 10 -> 9, of which waited for: 8 -> 5; matrix products, arithmetic and copies ran while one was open for 0% -> 0% of each run, Pallas kernels for 2% -> 1%
where the time goes in v11:
time: 81.5 us; the launch traced here: 80.5 us
  waiting for transfers between devices  27.6 us (34%)
  blocking collectives  27.4 us (34%)
  starting transfers between devices  17.4 us (21%)
  Pallas kernels  7.88 us (10%)
    all_to_all x2, blocking collectives, exchange(): return lax.all_to_all(value, axes, split_axis=0, concat_axis=0, tiled=True)  27.4 us
    ppermute x6, waiting for transfers between devices, along(): collected.append(lax.ppermute(own, TP, pairs))  17.1 us
    all_to_all x1, waiting for transfers between devices, exchange(): return lax.all_to_all(value, axes, split_axis=0, concat_axis=0, tiled=True)  10.5 us
    ppermute x6, starting transfers between devices, along(): collected.append(lax.ppermute(own, TP, pairs))  8.83 us
    all_to_all x1, starting transfers between devices, exchange(): return lax.all_to_all(value, axes, split_axis=0, concat_axis=0, tiled=True)  8.16 us
    pallas_call x1, Pallas kernels, on_device(): pl.pallas_call(functools.partial(attend_kernel, factor=factor, nope=nope)...  4.39 us
  transfers between devices with their start and end apart: 9, of which 5 were waited for; matrix products, arithmetic and copies ran while one was open for 0% of the time, Pallas kernels for 1%

profile of v11, /device:TPU:0, one launch (start us, length us, event | category | flops | bytes accessed | tf_op | source)
XLA Modules:
  0.0 80.5 jit_solution(3042654688414824550)
XLA Ops:
  0.0 1.2 %collect.1 = (bf16[64,128]{1,0:T(8,128)(2,1)S(1)}, f32[1,128]{1,0:T(1,128)S(1)}, bf16[128,512]{1,0:T(8,128)(2,1)S(1)}, bf16[64,128]{1,0:T(8,128)(2,1)S(1)}, bf16...) custom-call(bf16[64,128]{1,0:T(8,128)(2,1)} %tokens_.1, f32[1,128]{1,0:T(1,128)} %bitcast.21, ...), custom_call_target="tpu_custom_call" | custom-call | tf_op jit(solution)/shard_map/collect/pallas_call | solution.py:343
  1.2 3.2 %collective-permute-start.4 = (bf16[1152,128]{1,0:T(8,128)(2,1)S(1)}, bf16[1152,128]{1,0:T(8,128)(2,1)S(1)}, u32[]{:S(2)}, u32[]{:S(2)}) collective-permute-start(bf16[1152,128]{1,0:T(8,128)(2,1)S(1)} %get-tuple-element.16), channel_id=1, source_target_pairs={{0,6},{1,7},{2,0},{3,1},{4,2},{5,3},{6,4},{7,5},{8,14},{9,15},{10,... | collective-permute-start | bytes 884744 | tf_op jit(solution)/shard_map/ppermute | solution.py:313
  4.4 0.0 collective-permute-start.3
  4.4 6.3 %collective-permute-done.4 = bf16[1152,128]{1,0:T(8,128)(2,1)S(1)} collective-permute-done((bf16[1152,128]{1,0:T(8,128)(2,1)S(1)}, bf16[1152,128]{1,0:T(8,128)(2,1)S(1)}, u32[]{:S(2)}, u32[]{:S(2)}) %collective-permute-start.4) | collective-permute-done | bytes 294944 | tf_op jit(solution)/shard_map/ppermute | solution.py:313
  10.6 3.4 %collective-permute-done.3 = bf16[1152,128]{1,0:T(8,128)(2,1)S(1)} collective-permute-done((bf16[1152,128]{1,0:T(8,128)(2,1)S(1)}, bf16[1152,128]{1,0:T(8,128)(2,1)S(1)}, u32[]{:S(2)}, u32[]{:S(2)}) %collective-permute-start.3) | collective-permute-done | bytes 294944 | tf_op jit(solution)/shard_map/ppermute | solution.py:313
  14.0 0.1 pad_maximum_fusion.near
  14.1 0.1 collective-permute-start.6
  14.2 0.1 collective-permute-start.5
  14.3 3.5 %collective-permute-start.2 = (bf16[192,128]{1,0:T(8,128)(2,1)}, bf16[192,128]{1,0:T(8,128)(2,1)S(1)}, u32[]{:S(2)}, u32[]{:S(2)}) collective-permute-start(bf16[192,128]{1,0:T(8,128)(2,1)} %bitcast.16), channel_id=1, source_target_pairs={{0,4},{1,5},{2,6},{3,7},{4,0},{5,1},{6,2},{7,3},{8,12},{9,13},{10,... | collective-permute-start | bytes 147464 | tf_op jit(solution)/shard_map/ppermute | solution.py:313
  17.8 0.3 collective-permute-start.1
  18.1 1.7 %collective-permute-start = (bf16[192,128]{1,0:T(8,128)(2,1)}, bf16[192,128]{1,0:T(8,128)(2,1)S(1)}, u32[]{:S(2)}, u32[]{:S(2)}) collective-permute-start(bf16[192,128]{1,0:T(8,128)(2,1)} %bitcast.18), channel_id=1, source_target_pairs={{0,2},{1,3},{2,4},{3,5},{4,6},{5,7},{6,0},{7,1},{8,10},{9,11},{10,... | collective-permute-start | bytes 147464 | tf_op jit(solution)/shard_map/ppermute | solution.py:313
  19.9 6.9 %collective-permute-done.2.query_3 = bf16[192,128]{1,0:T(8,128)(2,1)S(1)} collective-permute-done((bf16[192,128]{1,0:T(8,128)(2,1)}, bf16[192,128]{1,0:T(8,128)(2,1)S(1)}, u32[]{:S(2)}, u32[]{:S(2)}) %collective-permute-start.2) | collective-permute-done | bytes 49184 | tf_op jit(solution)/shard_map/ppermute | solution.py:313
  26.8 0.0 collective-permute-done.1.query_2
  26.8 0.5 collective-permute-done.query_1
  27.2 1.1 %project.1 = bf16[32,56,128]{2,1,0:T(8,128)(2,1)} custom-call(bf16[64,128]{1,0:T(8,128)(2,1)S(1)} %get-tuple-element.11.tokens, f32[1,128]{1,0:T(1,128)S(1)} %get-tuple-element.12.gain, bf16[192,128]{1,0:T(8,128)(2,1)S(1)} %get-tuple-element.13.query_0, bf16[192,128]{1,0:T(8,128)(2,1)S(1)} %collective-permute-done.query_1, ...), custom_call_target="tpu_custom_call" | custom-call | tf_op jit(solution)/shard_map/project/pallas_call | solution.py:378
  28.4 8.2 %all-to-all-start = ((bf16[32,56,128]{2,1,0:T(8,128)(2,1)}), bf16[32,56,128]{2,1,0:T(8,128)(2,1)S(1)}, u32[]{:S(2)}, u32[]{:S(2)}) async-start(bf16[32,56,128]{2,1,0:T(8,128)(2,1)} %project.1), calls=%async_computation | async-start | bytes 917504 | tf_op jit(solution)/shard_map/all_to_all | solution.py:301
  36.5 0.0 collective-permute-done.5.opposite
  36.5 0.4 collective-permute-start.7
  36.9 10.5 %all-to-all-done.got = bf16[32,56,128]{2,1,0:T(8,128)(2,1)S(1)} async-done(((bf16[32,56,128]{2,1,0:T(8,128)(2,1)}), bf16[32,56,128]{2,1,0:T(8,128)(2,1)S(1)}, u32[]{:S(2)}, u32[]{:S(2)}) %all-to-all-start) | async-done | bytes 458784 | tf_op jit(solution)/shard_map/all_to_all | solution.py:301
  47.4 0.0 collective-permute-done.7.far_opposite
  47.4 0.0 collective-permute-done.6.far
  47.4 0.0 copy-start
  47.4 4.4 %attend.1 = bf16[16,72,128]{2,1,0:T(8,128)(2,1)S(1)} custom-call(bf16[32,56,128]{2,1,0:T(8,128)(2,1)S(1)} %all-to-all-done.got, bf16[3,1152,128]{2,1,0:T(8,128)(2,1)S(1)} %pad_maximum_fusion.near, bf16[1152,128]{1,0:T(8,128)(2,1)S(1)} %collective-permute-done.5.opposite, bf16[3,1152,128]{2,1,0:T(8,128)(2,1)S(1)} %collective-permute-done.6.far, ...), custom_call_target="tpu_custom_call" | custom-call | tf_op jit(solution)/shard_map/attend/pallas_call | solution.py:390
  51.8 12.8 %all_to_all.15.got = bf16[16,72,128]{2,1,0:T(8,128)(2,1)S(1)} all-to-all(bf16[16,72,128]{2,1,0:T(8,128)(2,1)S(1)} %attend.1), channel_id=1, replica_groups=mesh['kv_0'=4,'kv_1'=4,'y'=4,'core'=2] {'kv_0','kv_1'}, dimensions={0} | all-to-all | bytes 589824 | tf_op jit(solution)/shard_map/all_to_all | solution.py:301
  64.6 0.5 combine.1
  65.1 14.7 %all_to_all.16.got = bf16[128,8,128]{2,1,0:T(8,128)(2,1)S(1)} all-to-all(bf16[128,8,128]{2,1,0:T(8,128)(2,1)S(1)} %combine.1), channel_id=1, replica_groups=mesh['kv_0'=4,'kv_1'=4,'y'=4,'core'=2] {'kv_0','kv_1','y','core'}, dimensions={0} | all-to-all | bytes 524288 | tf_op jit(solution)/shard_map/all_to_all | solution.py:301
  79.8 0.0 copy-done
  79.8 0.8 finish.1
Async XLA Ops:
  1.2 9.5 %collective-permute-start.4 = (bf16[1152,128]{1,0:T(8,128)(2,1)S(1)}, bf16[1152,128]{1,0:T(8,128)(2,1)S(1)}, u32[]{:S(2)}, u32[]{:S(2)}) collective-permute-start(bf16[1152,128]{1,0:T(8,128)(2,1)S(1)} %get-tuple-element.16), channel_id=1, source_target_pairs={{0,6},{1,7},{2,0},{3,1},{4,2},{5,3},{6,4},{7,5},{8,14},{9,15},{10,... | collective-permute-start | bytes 884744 | tf_op jit(solution)/shard_map/ppermute | solution.py:313
  4.4 9.7 %collective-permute-start.3 = (bf16[1152,128]{1,0:T(8,128)(2,1)S(1)}, bf16[1152,128]{1,0:T(8,128)(2,1)S(1)}, u32[]{:S(2)}, u32[]{:S(2)}) collective-permute-start(bf16[1152,128]{1,0:T(8,128)(2,1)S(1)} %get-tuple-element.16), channel_id=1, source_target_pairs={{0,2},{1,3},{2,4},{3,5},{4,6},{5,7},{6,0},{7,1},{8,10},{9,11},{10,... | collective-permute-start | bytes 884744 | tf_op jit(solution)/shard_map/ppermute | solution.py:313
  14.1 33.3 %collective-permute-start.6 = (bf16[3,1152,128]{2,1,0:T(8,128)(2,1)S(1)}, bf16[3,1152,128]{2,1,0:T(8,128)(2,1)S(1)}, u32[]{:S(2)}, u32[]{:S(2)}) collective-permute-start(bf16[3,1152,128]{2,1,0:T(8,128)(2,1)S(1)} %pad_maximum_fusion.near), channel_id=1, source_target_pairs={{0,1},{1,0},{2,3},{3,2},{4,5},{5,4},{6,7},{7,6},{8,9},{9,8},{10,11... | collective-permute-start | bytes 2654216 | tf_op jit(solution)/shard_map/ppermute | solution.py:305
  14.2 22.3 %collective-permute-start.5 = (bf16[1152,128]{1,0:T(8,128)(2,1)S(1)}, bf16[1152,128]{1,0:T(8,128)(2,1)S(1)}, u32[]{:S(2)}, u32[]{:S(2)}) collective-permute-start(bf16[1152,128]{1,0:T(8,128)(2,1)S(1)} %get-tuple-element.16), channel_id=1, source_target_pairs={{0,4},{1,5},{2,6},{3,7},{4,0},{5,1},{6,2},{7,3},{8,12},{9,13},{10,... | collective-permute-start | bytes 884744 | tf_op jit(solution)/shard_map/ppermute | solution.py:313
  14.3 12.4 %collective-permute-start.2 = (bf16[192,128]{1,0:T(8,128)(2,1)}, bf16[192,128]{1,0:T(8,128)(2,1)S(1)}, u32[]{:S(2)}, u32[]{:S(2)}) collective-permute-start(bf16[192,128]{1,0:T(8,128)(2,1)} %bitcast.16), channel_id=1, source_target_pairs={{0,4},{1,5},{2,6},{3,7},{4,0},{5,1},{6,2},{7,3},{8,12},{9,13},{10,... | collective-permute-start | bytes 147464 | tf_op jit(solution)/shard_map/ppermute | solution.py:313
  17.8 8.9 %collective-permute-start.1 = (bf16[192,128]{1,0:T(8,128)(2,1)}, bf16[192,128]{1,0:T(8,128)(2,1)S(1)}, u32[]{:S(2)}, u32[]{:S(2)}) collective-permute-start(bf16[192,128]{1,0:T(8,128)(2,1)} %bitcast.17), channel_id=1, source_target_pairs={{0,6},{1,7},{2,0},{3,1},{4,2},{5,3},{6,4},{7,5},{8,14},{9,15},{10,... | collective-permute-start | bytes 147464 | tf_op jit(solution)/shard_map/ppermute | solution.py:313
  18.1 9.1 %collective-permute-start = (bf16[192,128]{1,0:T(8,128)(2,1)}, bf16[192,128]{1,0:T(8,128)(2,1)S(1)}, u32[]{:S(2)}, u32[]{:S(2)}) collective-permute-start(bf16[192,128]{1,0:T(8,128)(2,1)} %bitcast.18), channel_id=1, source_target_pairs={{0,2},{1,3},{2,4},{3,5},{4,6},{5,7},{6,0},{7,1},{8,10},{9,11},{10,... | collective-permute-start | bytes 147464 | tf_op jit(solution)/shard_map/ppermute | solution.py:313
  28.4 19.1 %all-to-all-start = ((bf16[32,56,128]{2,1,0:T(8,128)(2,1)}), bf16[32,56,128]{2,1,0:T(8,128)(2,1)S(1)}, u32[]{:S(2)}, u32[]{:S(2)}) async-start(bf16[32,56,128]{2,1,0:T(8,128)(2,1)} %project.1), calls=%async_computation | async-start | bytes 917504 | tf_op jit(solution)/shard_map/all_to_all | solution.py:301
  36.5 10.9 %collective-permute-start.7 = (bf16[1152,128]{1,0:T(8,128)(2,1)S(1)}, bf16[1152,128]{1,0:T(8,128)(2,1)S(1)}, u32[]{:S(2)}, u32[]{:S(2)}) collective-permute-start(bf16[1152,128]{1,0:T(8,128)(2,1)S(1)} %collective-permute-done.5.opposite), channel_id=1, source_target_pairs={{0,1},{1,0},{2,3},{3,2},{4,5},{5,4},{6,7},{7,6},{8,9},{9,8},{10,11... | collective-permute-start | bytes 884744 | tf_op jit(solution)/shard_map/ppermute | solution.py:305
  47.4 32.3 %copy-start = (f32[128]{0:T(128)S(1)}, f32[128]{0:T(128)}, u32[]{:S(2)}) copy-start(f32[128]{0:T(128)} %param.23) | copy-start | bytes 1540

commit v12 on v11

--- a/solution.py
+++ b/solution.py
@@ -53,7 +53,7 @@
 
 
 def collect_kernel(
-    tokens_, gain_, wd_, wr_, wq_, wk, wv, wo, tokens, gain, wd, wr, wq, own, sems
+    tokens_, gain_, wd_, wr_, wq_, wk, wv, wo, tokens, gain, wd, wr, wq, own, late, sems
 ):
     deep = wk.shape[1]
     pairs = (
@@ -65,6 +65,8 @@
         (wd_, wd),
         (wr_, wr),
         (wq_, wq),
+        (wv.at[0], late.at[pl.ds(0, deep)]),
+        (wo, late.at[pl.ds(deep, wo.shape[0])]),
     )
     copies = [pltpu.make_async_copy(x, y, sems.at[n]) for n, (x, y) in enumerate(pairs)]
     for copy in copies:
@@ -115,9 +117,9 @@
 
 
 def attend_kernel(
-    got, near, opposite, far, far_opposite, lengths_, frequencies_, gain_, latents, ropes,
-    out, lengths, frequencies, gain, cache, cache_rope,
-    lifted, turned, scored, weights, means, sems,
+    got, near, key, far, far_key, lengths_, frequencies_, gain_, latents, ropes,
+    means, packed, lengths, frequencies, gain, cache, cache_rope,
+    lifted, turned, scored, weights, sems,
     *, factor, nope,
 ):
     kv = lax.axis_index(KV)
@@ -163,8 +165,8 @@
     sine = jnp.where(lane < width // 2, -sine, sine)
     for i in range(groups):
         source = core if i < half else 1 - core
-        w = weights_of((near, opposite, far, far_opposite), i)
-        lifted[i] = dot(total(source, i % half).astype(BF16), w[:latent_width, :], NT)
+        w = weights_of((near, key, far, far_key), i, 0, latent_width)
+        lifted[i] = dot(total(source, i % half).astype(BF16), w[...], NT)
     for i in range(groups):
         if i % half >= half // 2:
             continue
@@ -226,12 +228,6 @@
             mixed = dot(weights[s * groups : (s + 1) * groups, :], cache[s], NN)
             means[s] = (mixed + rounded[r] * new_latent) * inverse[r]
             table = jnp.where(lanes((groups, 128)) == s, logs[r], table)
-    for i in range(groups):
-        w = weights_of((near, opposite, far, far_opposite), i)
-        x = means[:, i, :].astype(BF16)
-        up = dot(x, w[latent_width : 2 * latent_width, :], NN).astype(BF16)
-        for k in range(kv_size):
-            out[k, i * local : (i + 1) * local, :] = up
     lane = lanes((local, 128))
     table = jnp.concatenate([table, jnp.zeros((128 - groups, 128), F32)], axis=0)
     table = jnp.transpose(table)[:local]
@@ -239,7 +235,7 @@
     rest = table - high
     middle = rest.astype(BF16).astype(F32)
     low = (rest - middle).astype(BF16).astype(F32)
-    packed = jnp.where(
+    packed[...] = jnp.where(
         lane < groups,
         high,
         jnp.where(
@@ -248,18 +244,31 @@
             jnp.where(lane < 3 * groups, pltpu.roll(low, 2 * groups, 1), 0.0),
         ),
     ).astype(BF16)
+
+
+def up_kernel(means, packed, near, late, far, far_late, out):
+    local, groups, latent_width = means.shape
+    kv_size = out.shape[0]
+    for i in range(groups):
+        w = weights_of((near, late, far, far_late), i, latent_width, latent_width)
+        x = means[:, i, :].astype(BF16)
+        up = dot(x, w[:latent_width, :], NN).astype(BF16)
+        for k in range(kv_size):
+            out[k, i * local : (i + 1) * local, :] = up
+    logs = packed[...]
     for k in range(kv_size):
-        out[k, groups * local :, :] = packed
-
-
-def weights_of(collected, i):
-    near, opposite, far, far_opposite = collected
+        out[k, groups * local :, :] = logs
+
+
+def weights_of(collected, i, first, count):
+    near, single, far, far_single = collected
     places = near.shape[0] + 1
-    stacked, single = (near, opposite) if i < places else (far, far_opposite)
-    return single if i % places == places - 1 else stacked.at[i % places]
-
-
-def combine_kernel(got, near, opposite, far, far_opposite, out, *, kv_size, groups, local, first):
+    if i % places == places - 1:
+        return single if i < places else far_single
+    return (near if i < places else far).at[i % places, pl.ds(first, count)]
+
+
+def combine_kernel(got, near, late, far, far_late, out, *, kv_size, groups, local, first):
     logs = []
     for k in range(kv_size):
         x = got[k, groups * local :, :].astype(F32)
@@ -275,8 +284,10 @@
         for k in range(kv_size):
             part = got[k, i * local : (i + 1) * local, :].astype(F32)
             head = head + part * shares[k][:, i : i + 1]
-        w = weights_of((near, opposite, far, far_opposite), i)
-        mixed = mixed + dot(head.astype(BF16), w[first:, :], NN)
+        w = weights_of((near, late, far, far_late), i, first, 128)
+        single = w.shape[0] > 128
+        rows_of = w[late.shape[0] - 128 :, :] if single else w[...]
+        mixed = mixed + dot(head.astype(BF16), rows_of, NN)
     mixed = mixed.astype(BF16)
     for d in range(out.shape[0]):
         out[d] = mixed
@@ -305,10 +316,10 @@
     return lax.ppermute(value, TP, [(i, i ^ 1) for i in range(lax.axis_size(TP))])
 
 
-def along(own):
+def along(own, steps):
     size = lax.axis_size(TP)
     collected = []
-    for step in (1, 3, 2):
+    for step in steps:
         pairs = [(i, (i + 2 * step) % size) for i in range(size)]
         collected.append(lax.ppermute(own, TP, pairs))
     return collected
@@ -339,8 +350,8 @@
     value = w_value_up.shape[2]
     factor = (nope + rope) ** (-0.5)
 
-    others = along(w_query.T)
-    tokens, gain, w_down, w_rope, own_query, own = pl.pallas_call(
+    others = along(w_query.T, (1, 3, 2))
+    tokens, gain, w_down, w_rope, own_query, own, late = pl.pallas_call(
         collect_kernel,
         out_shape=(
             jax.ShapeDtypeStruct(tokens.shape, BF16),
@@ -349,10 +360,11 @@
             jax.ShapeDtypeStruct((rope, width), BF16),
             jax.ShapeDtypeStruct((nope + rope, width), BF16),
             jax.ShapeDtypeStruct((2 * latent_width + value, nope), BF16),
+            jax.ShapeDtypeStruct((latent_width + value, nope), BF16),
         ),
         in_specs=[in_hbm()] * 8,
-        out_specs=(in_vmem(),) * 6,
-        scratch_shapes=[pltpu.SemaphoreType.DMA((8,))],
+        out_specs=(in_vmem(),) * 7,
+        scratch_shapes=[pltpu.SemaphoreType.DMA((10,))],
         compiler_params=params(8),
         name="collect",
     )(
@@ -367,11 +379,12 @@
             w_out,
         )
     )
-    before, after, opposite = along(own)
-    near = jnp.stack([own, before, after])
+    near = jnp.stack([own] + along(own, (1, 3)))
+    (key,) = along(w_key_up[0], (2,))
+    (late,) = along(late, (2,))
     far = swap(near)
-    far_opposite = swap(opposite)
-    collected = (near, opposite, far, far_opposite)
+    far_key = swap(key)
+    far_late = swap(late)
 
     cores = lax.axis_size("core")
     sent_rows = (groups // 2 + groups // 4 + 1) * local
@@ -387,11 +400,14 @@
     got = exchange(sent, FIRST)
     powers = np.arange(0, rope, 2, dtype=np.float64) / rope
     frequencies = np.tile(1.0 / 10000.0**powers, 2)[None].astype(np.float32)
-    sent = pl.pallas_call(
+    means, packed = pl.pallas_call(
         functools.partial(attend_kernel, factor=factor, nope=nope),
-        out_shape=jax.ShapeDtypeStruct((kv_size, groups * local + local, value), BF16),
+        out_shape=(
+            jax.ShapeDtypeStruct((local, groups, latent_width), F32),
+            jax.ShapeDtypeStruct((local, 128), BF16),
+        ),
         in_specs=[in_vmem()] * 5 + [in_hbm()] * 5,
-        out_specs=in_vmem(),
+        out_specs=(in_vmem(),) * 2,
         scratch_shapes=[
             pltpu.VMEM((1, seqs), jnp.int32),
             pltpu.VMEM((1, rope), F32),
@@ -402,14 +418,16 @@
             pltpu.VMEM((groups, local, rope), F32),
             pltpu.VMEM((local * groups, positions + 128), F32),
             pltpu.VMEM((local * groups, positions), BF16),
-            pltpu.VMEM((local, groups, latent_width), F32),
             pltpu.SemaphoreType.DMA((2 * local + 3,)),
         ],
         compiler_params=params(24),
         name="attend",
     )(
         got,
-        *collected,
+        near,
+        key,
+        far,
+        far_key,
         *keep_in_hbm(
             lengths[None],
             frequencies,
@@ -418,6 +436,14 @@
             cache_rope.transpose(0, 2, 1),
         ),
     )
+    sent = pl.pallas_call(
+        up_kernel,
+        out_shape=jax.ShapeDtypeStruct((kv_size, groups * local + local, value), BF16),
+        in_specs=[in_vmem()] * 6,
+        out_specs=in_vmem(),
+        compiler_params=params(8),
+        name="value_up",
+    )(means, packed, near, late, far, far_late)
     got = exchange(sent, KV)
 
     sent = pl.pallas_call(
@@ -433,7 +459,7 @@
         out_specs=in_vmem(),
         compiler_params=params(8),
         name="combine",
-    )(got, *collected)
+    )(got, near, late, far, far_late)
     got = exchange(sent, ALL)
     return pl.pallas_call(
         functools.partial(finish_kernel, kv_size=kv_size, groups=groups, local=local),

time: 81.5 us -> 80.5 us (0.988)
  waiting for transfers between devices: 27.6 us -> 19.5 us
  blocking collectives: 27.4 us -> 31.4 us
  starting transfers between devices: 17.4 us -> 20.2 us
    all_to_all x1, waiting for transfers between devices: 10.5 us -> 0.01 us  [exchange(): return lax.all_to_all(value, axes, split_axis=0, concat_axis=0, tiled=True)]
    all_to_all x2, blocking collectives: 27.4 us -> 31.4 us  [exchange(): return lax.all_to_all(value, axes, split_axis=0, concat_axis=0, tiled=True)]
    ppermute x6 -> x7, starting transfers between devices: 8.83 us -> 11.9 us  [along(): collected.append(lax.ppermute(own, TP, pairs))]
    ppermute x2 -> x3, waiting for transfers between devices: 0.01 us -> 1.35 us  [swap(): lax.ppermute(value, TP, [(i, i ^ 1) for i in range(lax.axis_size(TP))])]
    ppermute x6 -> x7, waiting for transfers between devices: 17.1 us -> 18.2 us  [along(): collected.append(lax.ppermute(own, TP, pairs))]
  transfers between devices with their start and end apart: 9 -> 11, of which waited for: 5 -> 7; matrix products, arithmetic and copies ran while one was open for 0% -> 0% of each run, Pallas kernels for 1% -> 7%
where the time goes in v12:
time: 80.5 us; the launch traced here: 79.5 us
  blocking collectives  31.4 us (39%)
  starting transfers between devices  20.2 us (25%)
  waiting for transfers between devices  19.5 us (24%)
  Pallas kernels  8.18 us (10%)
    all_to_all x2, blocking collectives, exchange(): return lax.all_to_all(value, axes, split_axis=0, concat_axis=0, tiled=True)  31.4 us
    ppermute x7, waiting for transfers between devices, along(): collected.append(lax.ppermute(own, TP, pairs))  18.2 us
    ppermute x7, starting transfers between devices, along(): collected.append(lax.ppermute(own, TP, pairs))  11.9 us
    all_to_all x1, starting transfers between devices, exchange(): return lax.all_to_all(value, axes, split_axis=0, concat_axis=0, tiled=True)  8.16 us
    pallas_call x1, Pallas kernels, on_device(): pl.pallas_call(functools.partial(attend_kernel, factor=factor, nope=nope)...  4.28 us
  transfers between devices with their start and end apart: 11, of which 7 were waited for; matrix products, arithmetic and copies ran while one was open for 0% of the time, Pallas kernels for 7%

profile of v12, /device:TPU:0, one launch (start us, length us, event | category | flops | bytes accessed | tf_op | source)
XLA Modules:
  0.0 79.5 jit_solution(18380281236614602914)
XLA Ops:
  0.0 1.3 %collect.1 = (bf16[64,128]{1,0:T(8,128)(2,1)S(1)}, f32[1,128]{1,0:T(1,128)S(1)}, bf16[128,512]{1,0:T(8,128)(2,1)S(1)}, bf16[64,128]{1,0:T(8,128)(2,1)S(1)}, bf16...) custom-call(bf16[64,128]{1,0:T(8,128)(2,1)} %tokens_.1, f32[1,128]{1,0:T(1,128)} %bitcast.23, ...), custom_call_target="tpu_custom_call" | custom-call | tf_op jit(solution)/shard_map/collect/pallas_call | solution.py:354
  1.3 1.8 %collective-permute-start.3 = (bf16[1152,128]{1,0:T(8,128)(2,1)S(1)}, bf16[1152,128]{1,0:T(8,128)(2,1)S(1)}, u32[]{:S(2)}, u32[]{:S(2)}) collective-permute-start(bf16[1152,128]{1,0:T(8,128)(2,1)S(1)} %get-tuple-element.19), channel_id=1, source_target_pairs={{0,2},{1,3},{2,4},{3,5},{4,6},{5,7},{6,0},{7,1},{8,10},{9,11},{10,... | collective-permute-start | bytes 884744 | tf_op jit(solution)/shard_map/ppermute | solution.py:324
  3.0 1.5 %collective-permute-start.4 = (bf16[1152,128]{1,0:T(8,128)(2,1)S(1)}, bf16[1152,128]{1,0:T(8,128)(2,1)S(1)}, u32[]{:S(2)}, u32[]{:S(2)}) collective-permute-start(bf16[1152,128]{1,0:T(8,128)(2,1)S(1)} %get-tuple-element.19), channel_id=1, source_target_pairs={{0,6},{1,7},{2,0},{3,1},{4,2},{5,3},{6,4},{7,5},{8,14},{9,15},{10,... | collective-permute-start | bytes 884744 | tf_op jit(solution)/shard_map/ppermute | solution.py:324
  4.6 6.9 %collective-permute-done.3 = bf16[1152,128]{1,0:T(8,128)(2,1)S(1)} collective-permute-done((bf16[1152,128]{1,0:T(8,128)(2,1)S(1)}, bf16[1152,128]{1,0:T(8,128)(2,1)S(1)}, u32[]{:S(2)}, u32[]{:S(2)}) %collective-permute-start.3) | collective-permute-done | bytes 294944 | tf_op jit(solution)/shard_map/ppermute | solution.py:324
  11.5 0.0 collective-permute-done.4
  11.5 0.1 pad_maximum_fusion.near
  11.6 0.1 collective-permute-start.6
  11.7 1.6 %collective-permute-start = (bf16[192,128]{1,0:T(8,128)(2,1)}, bf16[192,128]{1,0:T(8,128)(2,1)S(1)}, u32[]{:S(2)}, u32[]{:S(2)}) collective-permute-start(bf16[192,128]{1,0:T(8,128)(2,1)} %bitcast.18), channel_id=1, source_target_pairs={{0,2},{1,3},{2,4},{3,5},{4,6},{5,7},{6,0},{7,1},{8,10},{9,11},{10,... | collective-permute-start | bytes 147464 | tf_op jit(solution)/shard_map/ppermute | solution.py:324
  13.3 1.7 %collective-permute-start.1 = (bf16[192,128]{1,0:T(8,128)(2,1)}, bf16[192,128]{1,0:T(8,128)(2,1)S(1)}, u32[]{:S(2)}, u32[]{:S(2)}) collective-permute-start(bf16[192,128]{1,0:T(8,128)(2,1)} %bitcast.19), channel_id=1, source_target_pairs={{0,6},{1,7},{2,0},{3,1},{4,2},{5,3},{6,4},{7,5},{8,14},{9,15},{10,... | collective-permute-start | bytes 147464 | tf_op jit(solution)/shard_map/ppermute | solution.py:324
  15.0 1.7 %collective-permute-start.2 = (bf16[192,128]{1,0:T(8,128)(2,1)}, bf16[192,128]{1,0:T(8,128)(2,1)S(1)}, u32[]{:S(2)}, u32[]{:S(2)}) collective-permute-start(bf16[192,128]{1,0:T(8,128)(2,1)} %bitcast.20), channel_id=1, source_target_pairs={{0,4},{1,5},{2,6},{3,7},{4,0},{5,1},{6,2},{7,3},{8,12},{9,13},{10,... | collective-permute-start | bytes 147464 | tf_op jit(solution)/shard_map/ppermute | solution.py:324
  16.7 0.6 collective-permute-done.query_1
  17.3 0.3 collective-permute-done.1.query_2
  17.6 3.2 %collective-permute-done.2.query_3 = bf16[192,128]{1,0:T(8,128)(2,1)S(1)} collective-permute-done((bf16[192,128]{1,0:T(8,128)(2,1)}, bf16[192,128]{1,0:T(8,128)(2,1)S(1)}, u32[]{:S(2)}, u32[]{:S(2)}) %collective-permute-start.2) | collective-permute-done | bytes 49184 | tf_op jit(solution)/shard_map/ppermute | solution.py:324
  20.8 1.1 %project.1 = bf16[32,56,128]{2,1,0:T(8,128)(2,1)} custom-call(bf16[64,128]{1,0:T(8,128)(2,1)S(1)} %get-tuple-element.14.tokens, f32[1,128]{1,0:T(1,128)S(1)} %get-tuple-element.15.gain, bf16[192,128]{1,0:T(8,128)(2,1)S(1)} %get-tuple-element.16.query_0, bf16[192,128]{1,0:T(8,128)(2,1)S(1)} %collective-permute-done.query_1, ...), custom_call_target="tpu_custom_call" | custom-call | tf_op jit(solution)/shard_map/project/pallas_call | solution.py:391
  21.9 8.2 %all-to-all-start = ((bf16[32,56,128]{2,1,0:T(8,128)(2,1)}), bf16[32,56,128]{2,1,0:T(8,128)(2,1)S(1)}, u32[]{:S(2)}, u32[]{:S(2)}) async-start(bf16[32,56,128]{2,1,0:T(8,128)(2,1)} %project.1), calls=%async_computation | async-start | bytes 917504 | tf_op jit(solution)/shard_map/all_to_all | solution.py:312
  30.1 1.8 %collective-permute-start.8 = (bf16[640,128]{1,0:T(8,128)(2,1)S(1)}, bf16[640,128]{1,0:T(8,128)(2,1)S(1)}, u32[]{:S(2)}, u32[]{:S(2)}) collective-permute-start(bf16[640,128]{1,0:T(8,128)(2,1)S(1)} %get-tuple-element.22), channel_id=1, source_target_pairs={{0,4},{1,5},{2,6},{3,7},{4,0},{5,1},{6,2},{7,3},{8,12},{9,13},{10,... | collective-permute-start | bytes 491528 | tf_op jit(solution)/shard_map/ppermute | solution.py:324
  31.9 1.8 %collective-permute-start.5 = (bf16[512,128]{1,0:T(8,128)(2,1)}, bf16[512,128]{1,0:T(8,128)(2,1)S(1)}, u32[]{:S(2)}, u32[]{:S(2)}) collective-permute-start(bf16[512,128]{1,0:T(8,128)(2,1)} %bitcast.16), channel_id=1, source_target_pairs={{0,4},{1,5},{2,6},{3,7},{4,0},{5,1},{6,2},{7,3},{8,12},{9,13},{10,... | collective-permute-start | bytes 393224 | tf_op jit(solution)/shard_map/ppermute | solution.py:324
  33.7 5.0 %collective-permute-done.8.late = bf16[640,128]{1,0:T(8,128)(2,1)S(1)} collective-permute-done((bf16[640,128]{1,0:T(8,128)(2,1)S(1)}, bf16[640,128]{1,0:T(8,128)(2,1)S(1)}, u32[]{:S(2)}, u32[]{:S(2)}) %collective-permute-start.8) | collective-permute-done | bytes 163872 | tf_op jit(solution)/shard_map/ppermute | solution.py:324
  38.7 0.0 collective-permute-start.9
  38.7 2.1 %collective-permute-done.5.key = bf16[512,128]{1,0:T(8,128)(2,1)S(1)} collective-permute-done((bf16[512,128]{1,0:T(8,128)(2,1)}, bf16[512,128]{1,0:T(8,128)(2,1)S(1)}, u32[]{:S(2)}, u32[]{:S(2)}) %collective-permute-start.5) | collective-permute-done | bytes 131104 | tf_op jit(solution)/shard_map/ppermute | solution.py:324
  40.9 0.0 collective-permute-start.7
  40.9 1.3 %collective-permute-done.7.far_key = bf16[512,128]{1,0:T(8,128)(2,1)S(1)} collective-permute-done((bf16[512,128]{1,0:T(8,128)(2,1)S(1)}, bf16[512,128]{1,0:T(8,128)(2,1)S(1)}, u32[]{:S(2)}, u32[]{:S(2)}) %collective-permute-start.7) | collective-permute-done | bytes 131104 | tf_op jit(solution)/shard_map/ppermute | solution.py:316
  42.2 0.0 all-to-all-done.got
  42.2 0.0 collective-permute-done.6.far
  42.2 4.3 %attend.1 = (f32[8,8,512]{2,1,0:T(8,128)S(1)}, bf16[8,128]{1,0:T(8,128)(2,1)S(1)}) custom-call(bf16[32,56,128]{2,1,0:T(8,128)(2,1)S(1)} %all-to-all-done.got, bf16[3,1152,128]{2,1,0:T(8,128)(2,1)S(1)} %pad_maximum_fusion.near, bf16[512,128]{1,0:T(8,128)(2,1)S(1)} %collective-permute-done.5.key, bf16[3,1152,128]{2,1,0:T(8,128)(2,1)S(1)} %collective-permute-done.6.far, ...), custom_call_target="tpu_custom_call" | custom-call | tf_op jit(solution)/shard_map/attend/pallas_call | solution.py:403
  46.5 0.0 copy-start
  46.5 0.0 collective-permute-done.9.far_late
  46.5 0.3 value_up.1
  46.8 16.1 %all_to_all.15.got = bf16[16,72,128]{2,1,0:T(8,128)(2,1)S(1)} all-to-all(bf16[16,72,128]{2,1,0:T(8,128)(2,1)S(1)} %value_up.1), channel_id=1, replica_groups=mesh['kv_0'=4,'kv_1'=4,'y'=4,'core'=2] {'kv_0','kv_1'}, dimensions={0} | all-to-all | bytes 589824 | tf_op jit(solution)/shard_map/all_to_all | solution.py:312
  62.9 0.5 combine.1
  63.4 15.3 %all_to_all.16.got = bf16[128,8,128]{2,1,0:T(8,128)(2,1)S(1)} all-to-all(bf16[128,8,128]{2,1,0:T(8,128)(2,1)S(1)} %combine.1), channel_id=1, replica_groups=mesh['kv_0'=4,'kv_1'=4,'y'=4,'core'=2] {'kv_0','kv_1','y','core'}, dimensions={0} | all-to-all | bytes 524288 | tf_op jit(solution)/shard_map/all_to_all | solution.py:312
  78.8 0.0 copy-done
  78.8 0.8 finish.1
Async XLA Ops:
  1.3 10.2 %collective-permute-start.3 = (bf16[1152,128]{1,0:T(8,128)(2,1)S(1)}, bf16[1152,128]{1,0:T(8,128)(2,1)S(1)}, u32[]{:S(2)}, u32[]{:S(2)}) collective-permute-start(bf16[1152,128]{1,0:T(8,128)(2,1)S(1)} %get-tuple-element.19), channel_id=1, source_target_pairs={{0,2},{1,3},{2,4},{3,5},{4,6},{5,7},{6,0},{7,1},{8,10},{9,11},{10,... | collective-permute-start | bytes 884744 | tf_op jit(solution)/shard_map/ppermute | solution.py:324
  3.0 8.5 %collective-permute-start.4 = (bf16[1152,128]{1,0:T(8,128)(2,1)S(1)}, bf16[1152,128]{1,0:T(8,128)(2,1)S(1)}, u32[]{:S(2)}, u32[]{:S(2)}) collective-permute-start(bf16[1152,128]{1,0:T(8,128)(2,1)S(1)} %get-tuple-element.19), channel_id=1, source_target_pairs={{0,6},{1,7},{2,0},{3,1},{4,2},{5,3},{6,4},{7,5},{8,14},{9,15},{10,... | collective-permute-start | bytes 884744 | tf_op jit(solution)/shard_map/ppermute | solution.py:324
  11.6 30.6 %collective-permute-start.6 = (bf16[3,1152,128]{2,1,0:T(8,128)(2,1)S(1)}, bf16[3,1152,128]{2,1,0:T(8,128)(2,1)S(1)}, u32[]{:S(2)}, u32[]{:S(2)}) collective-permute-start(bf16[3,1152,128]{2,1,0:T(8,128)(2,1)S(1)} %pad_maximum_fusion.near), channel_id=1, source_target_pairs={{0,1},{1,0},{2,3},{3,2},{4,5},{5,4},{6,7},{7,6},{8,9},{9,8},{10,11... | collective-permute-start | bytes 2654216 | tf_op jit(solution)/shard_map/ppermute | solution.py:316
  11.7 5.6 %collective-permute-start = (bf16[192,128]{1,0:T(8,128)(2,1)}, bf16[192,128]{1,0:T(8,128)(2,1)S(1)}, u32[]{:S(2)}, u32[]{:S(2)}) collective-permute-start(bf16[192,128]{1,0:T(8,128)(2,1)} %bitcast.18), channel_id=1, source_target_pairs={{0,2},{1,3},{2,4},{3,5},{4,6},{5,7},{6,0},{7,1},{8,10},{9,11},{10,... | collective-permute-start | bytes 147464 | tf_op jit(solution)/shard_map/ppermute | solution.py:324
  13.3 4.3 %collective-permute-start.1 = (bf16[192,128]{1,0:T(8,128)(2,1)}, bf16[192,128]{1,0:T(8,128)(2,1)S(1)}, u32[]{:S(2)}, u32[]{:S(2)}) collective-permute-start(bf16[192,128]{1,0:T(8,128)(2,1)} %bitcast.19), channel_id=1, source_target_pairs={{0,6},{1,7},{2,0},{3,1},{4,2},{5,3},{6,4},{7,5},{8,14},{9,15},{10,... | collective-permute-start | bytes 147464 | tf_op jit(solution)/shard_map/ppermute | solution.py:324
  15.0 5.8 %collective-permute-start.2 = (bf16[192,128]{1,0:T(8,128)(2,1)}, bf16[192,128]{1,0:T(8,128)(2,1)S(1)}, u32[]{:S(2)}, u32[]{:S(2)}) collective-permute-start(bf16[192,128]{1,0:T(8,128)(2,1)} %bitcast.20), channel_id=1, source_target_pairs={{0,4},{1,5},{2,6},{3,7},{4,0},{5,1},{6,2},{7,3},{8,12},{9,13},{10,... | collective-permute-start | bytes 147464 | tf_op jit(solution)/shard_map/ppermute | solution.py:324
  21.9 20.3 %all-to-all-start = ((bf16[32,56,128]{2,1,0:T(8,128)(2,1)}), bf16[32,56,128]{2,1,0:T(8,128)(2,1)S(1)}, u32[]{:S(2)}, u32[]{:S(2)}) async-start(bf16[32,56,128]{2,1,0:T(8,128)(2,1)} %project.1), calls=%async_computation | async-start | bytes 917504 | tf_op jit(solution)/shard_map/all_to_all | solution.py:312
  30.1 8.7 %collective-permute-start.8 = (bf16[640,128]{1,0:T(8,128)(2,1)S(1)}, bf16[640,128]{1,0:T(8,128)(2,1)S(1)}, u32[]{:S(2)}, u32[]{:S(2)}) collective-permute-start(bf16[640,128]{1,0:T(8,128)(2,1)S(1)} %get-tuple-element.22), channel_id=1, source_target_pairs={{0,4},{1,5},{2,6},{3,7},{4,0},{5,1},{6,2},{7,3},{8,12},{9,13},{10,... | collective-permute-start | bytes 491528 | tf_op jit(solution)/shard_map/ppermute | solution.py:324
  31.9 9.0 %collective-permute-start.5 = (bf16[512,128]{1,0:T(8,128)(2,1)}, bf16[512,128]{1,0:T(8,128)(2,1)S(1)}, u32[]{:S(2)}, u32[]{:S(2)}) collective-permute-start(bf16[512,128]{1,0:T(8,128)(2,1)} %bitcast.16), channel_id=1, source_target_pairs={{0,4},{1,5},{2,6},{3,7},{4,0},{5,1},{6,2},{7,3},{8,12},{9,13},{10,... | collective-permute-start | bytes 393224 | tf_op jit(solution)/shard_map/ppermute | solution.py:324
  38.7 7.8 %collective-permute-start.9 = (bf16[640,128]{1,0:T(8,128)(2,1)S(1)}, bf16[640,128]{1,0:T(8,128)(2,1)S(1)}, u32[]{:S(2)}, u32[]{:S(2)}) collective-permute-start(bf16[640,128]{1,0:T(8,128)(2,1)S(1)} %collective-permute-done.8.late), channel_id=1, source_target_pairs={{0,1},{1,0},{2,3},{3,2},{4,5},{5,4},{6,7},{7,6},{8,9},{9,8},{10,11... | collective-permute-start | bytes 491528 | tf_op jit(solution)/shard_map/ppermute | solution.py:316
  40.9 1.3 %collective-permute-start.7 = (bf16[512,128]{1,0:T(8,128)(2,1)S(1)}, bf16[512,128]{1,0:T(8,128)(2,1)S(1)}, u32[]{:S(2)}, u32[]{:S(2)}) collective-permute-start(bf16[512,128]{1,0:T(8,128)(2,1)S(1)} %collective-permute-done.5.key), channel_id=1, source_target_pairs={{0,1},{1,0},{2,3},{3,2},{4,5},{5,4},{6,7},{7,6},{8,9},{9,8},{10,11... | collective-permute-start | bytes 393224 | tf_op jit(solution)/shard_map/ppermute | solution.py:316
  46.5 32.3 %copy-start = (f32[128]{0:T(128)S(1)}, f32[128]{0:T(128)}, u32[]{:S(2)}) copy-start(f32[128]{0:T(128)} %param.23) | copy-start | bytes 1540

commit v13 on v11

--- a/solution.py
+++ b/solution.py
@@ -13,6 +13,7 @@
 KV = ("kv_0", "kv_1")
 TP = ("y", "core")
 ALL = KV + TP
+LAST = ("core",) + KV + ("y",)
 FIRST = KV + ("core",)
 EPSILON = 1e-06
 NEGATIVE = -1e30
@@ -284,14 +285,17 @@
 
 def finish_kernel(got, gain, out, *, kv_size, groups, local):
     kv = lax.axis_index(KV)
+    cores = lax.axis_size("core")
+    places = groups // cores
     width = got.shape[2]
     for t in range(groups):
+        y, core = t // cores, t % cores
         squares = jnp.zeros((local, width), F32)
         for k in range(kv_size):
-            x = got[k * groups + t].astype(F32)
+            x = got[(core * kv_size + k) * places + y].astype(F32)
             squares = squares + x * x
         mean = jnp.sum(squares, axis=1, keepdims=True) / (width * kv_size)
-        own = got[kv * groups + t].astype(F32)
+        own = got[(core * kv_size + kv) * places + y].astype(F32)
         out[t * local : (t + 1) * local, :] = (
             own * lax.rsqrt(mean + EPSILON) * gain[...]
         ).astype(BF16)
@@ -309,7 +313,7 @@
     size = lax.axis_size(TP)
     collected = []
     for step in (1, 3, 2):
-        pairs = [(i, (i + 2 * step) % size) for i in range(size)]
+        pairs = [(i, (i + (2 - 4 * (i % 2)) * step) % size) for i in range(size)]
         collected.append(lax.ppermute(own, TP, pairs))
     return collected
 
@@ -434,7 +438,7 @@
         compiler_params=params(8),
         name="combine",
     )(got, *collected)
-    got = exchange(sent, ALL)
+    got = exchange(sent, LAST)
     return pl.pallas_call(
         functools.partial(finish_kernel, kv_size=kv_size, groups=groups, local=local),
         out_shape=jax.ShapeDtypeStruct((seqs, w_out.shape[1]), BF16),

time: 81.5 us -> 80.3 us (0.985)
  waiting for transfers between devices: 27.6 us -> 25.8 us
    ppermute x6, waiting for transfers between devices: 17.1 us -> 15.2 us  [along(): collected.append(lax.ppermute(own, TP, pairs))]
where the time goes in v13:
time: 80.3 us; the launch traced here: 79.4 us
  blocking collectives  28.1 us (35%)
  waiting for transfers between devices  25.8 us (32%)
  starting transfers between devices  17.5 us (22%)
  Pallas kernels  7.88 us (10%)
    all_to_all x2, blocking collectives, exchange(): return lax.all_to_all(value, axes, split_axis=0, concat_axis=0, tiled=True)  28.1 us
    ppermute x6, waiting for transfers between devices, along(): collected.append(lax.ppermute(own, TP, pairs))  15.2 us
    all_to_all x1, waiting for transfers between devices, exchange(): return lax.all_to_all(value, axes, split_axis=0, concat_axis=0, tiled=True)  10.5 us
    ppermute x6, starting transfers between devices, along(): collected.append(lax.ppermute(own, TP, pairs))  8.92 us
    all_to_all x1, starting transfers between devices, exchange(): return lax.all_to_all(value, axes, split_axis=0, concat_axis=0, tiled=True)  8.16 us
    pallas_call x1, Pallas kernels, on_device(): pl.pallas_call(functools.partial(attend_kernel, factor=factor, nope=nope)...  4.39 us
  transfers between devices with their start and end apart: 9, of which 5 were waited for; matrix products, arithmetic and copies ran while one was open for 0% of the time, Pallas kernels for 1%

profile of v13, /device:TPU:0, one launch (start us, length us, event | category | flops | bytes accessed | tf_op | source)
XLA Modules:
  0.0 79.4 jit_solution(5403687433784181297)
XLA Ops:
  0.0 1.2 %collect.1 = (bf16[64,128]{1,0:T(8,128)(2,1)S(1)}, f32[1,128]{1,0:T(1,128)S(1)}, bf16[128,512]{1,0:T(8,128)(2,1)S(1)}, bf16[64,128]{1,0:T(8,128)(2,1)S(1)}, bf16...) custom-call(bf16[64,128]{1,0:T(8,128)(2,1)} %tokens_.1, f32[1,128]{1,0:T(1,128)} %bitcast.21, ...), custom_call_target="tpu_custom_call" | custom-call | tf_op jit(solution)/shard_map/collect/pallas_call | solution.py:347
  1.2 3.2 %collective-permute-start.4 = (bf16[1152,128]{1,0:T(8,128)(2,1)S(1)}, bf16[1152,128]{1,0:T(8,128)(2,1)S(1)}, u32[]{:S(2)}, u32[]{:S(2)}) collective-permute-start(bf16[1152,128]{1,0:T(8,128)(2,1)S(1)} %get-tuple-element.16), channel_id=1, source_target_pairs={{0,6},{1,3},{2,0},{3,5},{4,2},{5,7},{6,4},{7,1},{8,14},{9,11},{10,... | collective-permute-start | bytes 884744 | tf_op jit(solution)/shard_map/ppermute | solution.py:317
  4.4 0.0 collective-permute-start.3
  4.4 6.5 %collective-permute-done.4 = bf16[1152,128]{1,0:T(8,128)(2,1)S(1)} collective-permute-done((bf16[1152,128]{1,0:T(8,128)(2,1)S(1)}, bf16[1152,128]{1,0:T(8,128)(2,1)S(1)}, u32[]{:S(2)}, u32[]{:S(2)}) %collective-permute-start.4) | collective-permute-done | bytes 294944 | tf_op jit(solution)/shard_map/ppermute | solution.py:317
  10.8 1.5 %collective-permute-done.3 = bf16[1152,128]{1,0:T(8,128)(2,1)S(1)} collective-permute-done((bf16[1152,128]{1,0:T(8,128)(2,1)S(1)}, bf16[1152,128]{1,0:T(8,128)(2,1)S(1)}, u32[]{:S(2)}, u32[]{:S(2)}) %collective-permute-start.3) | collective-permute-done | bytes 294944 | tf_op jit(solution)/shard_map/ppermute | solution.py:317
  12.3 0.1 pad_maximum_fusion.near
  12.4 0.1 collective-permute-start.6
  12.5 2.1 %collective-permute-start.5 = (bf16[1152,128]{1,0:T(8,128)(2,1)S(1)}, bf16[1152,128]{1,0:T(8,128)(2,1)S(1)}, u32[]{:S(2)}, u32[]{:S(2)}) collective-permute-start(bf16[1152,128]{1,0:T(8,128)(2,1)S(1)} %get-tuple-element.16), channel_id=1, source_target_pairs={{0,4},{1,5},{2,6},{3,7},{4,0},{5,1},{6,2},{7,3},{8,12},{9,13},{10,... | collective-permute-start | bytes 884744 | tf_op jit(solution)/shard_map/ppermute | solution.py:317
  14.6 1.5 %collective-permute-start.2 = (bf16[192,128]{1,0:T(8,128)(2,1)}, bf16[192,128]{1,0:T(8,128)(2,1)S(1)}, u32[]{:S(2)}, u32[]{:S(2)}) collective-permute-start(bf16[192,128]{1,0:T(8,128)(2,1)} %bitcast.16), channel_id=1, source_target_pairs={{0,4},{1,5},{2,6},{3,7},{4,0},{5,1},{6,2},{7,3},{8,12},{9,13},{10,... | collective-permute-start | bytes 147464 | tf_op jit(solution)/shard_map/ppermute | solution.py:317
  16.1 2.1 %collective-permute-start.1 = (bf16[192,128]{1,0:T(8,128)(2,1)}, bf16[192,128]{1,0:T(8,128)(2,1)S(1)}, u32[]{:S(2)}, u32[]{:S(2)}) collective-permute-start(bf16[192,128]{1,0:T(8,128)(2,1)} %bitcast.17), channel_id=1, source_target_pairs={{0,6},{1,3},{2,0},{3,5},{4,2},{5,7},{6,4},{7,1},{8,14},{9,11},{10,... | collective-permute-start | bytes 147464 | tf_op jit(solution)/shard_map/ppermute | solution.py:317
  18.2 0.0 collective-permute-start
  18.2 6.8 %collective-permute-done.2.query_3 = bf16[192,128]{1,0:T(8,128)(2,1)S(1)} collective-permute-done((bf16[192,128]{1,0:T(8,128)(2,1)}, bf16[192,128]{1,0:T(8,128)(2,1)S(1)}, u32[]{:S(2)}, u32[]{:S(2)}) %collective-permute-start.2) | collective-permute-done | bytes 49184 | tf_op jit(solution)/shard_map/ppermute | solution.py:317
  25.0 0.0 collective-permute-done.1.query_2
  25.0 0.5 collective-permute-done.query_1
  25.5 1.1 %project.1 = bf16[32,56,128]{2,1,0:T(8,128)(2,1)} custom-call(bf16[64,128]{1,0:T(8,128)(2,1)S(1)} %get-tuple-element.11.tokens, f32[1,128]{1,0:T(1,128)S(1)} %get-tuple-element.12.gain, bf16[192,128]{1,0:T(8,128)(2,1)S(1)} %get-tuple-element.13.query_0, bf16[192,128]{1,0:T(8,128)(2,1)S(1)} %collective-permute-done.query_1, ...), custom_call_target="tpu_custom_call" | custom-call | tf_op jit(solution)/shard_map/project/pallas_call | solution.py:382
  26.6 8.2 %all-to-all-start = ((bf16[32,56,128]{2,1,0:T(8,128)(2,1)}), bf16[32,56,128]{2,1,0:T(8,128)(2,1)S(1)}, u32[]{:S(2)}, u32[]{:S(2)}) async-start(bf16[32,56,128]{2,1,0:T(8,128)(2,1)} %project.1), calls=%async_computation | async-start | bytes 917504 | tf_op jit(solution)/shard_map/all_to_all | solution.py:305
  34.8 0.0 collective-permute-done.5.opposite
  34.8 0.4 collective-permute-start.7
  35.1 10.5 %all-to-all-done.got = bf16[32,56,128]{2,1,0:T(8,128)(2,1)S(1)} async-done(((bf16[32,56,128]{2,1,0:T(8,128)(2,1)}), bf16[32,56,128]{2,1,0:T(8,128)(2,1)S(1)}, u32[]{:S(2)}, u32[]{:S(2)}) %all-to-all-start) | async-done | bytes 458784 | tf_op jit(solution)/shard_map/all_to_all | solution.py:305
  45.7 0.0 collective-permute-done.7.far_opposite
  45.7 0.0 collective-permute-done.6.far
  45.7 0.0 copy-start
  45.7 4.4 %attend.1 = bf16[16,72,128]{2,1,0:T(8,128)(2,1)S(1)} custom-call(bf16[32,56,128]{2,1,0:T(8,128)(2,1)S(1)} %all-to-all-done.got, bf16[3,1152,128]{2,1,0:T(8,128)(2,1)S(1)} %pad_maximum_fusion.near, bf16[1152,128]{1,0:T(8,128)(2,1)S(1)} %collective-permute-done.5.opposite, bf16[3,1152,128]{2,1,0:T(8,128)(2,1)S(1)} %collective-permute-done.6.far, ...), custom_call_target="tpu_custom_call" | custom-call | tf_op jit(solution)/shard_map/attend/pallas_call | solution.py:394
  50.1 12.8 %all_to_all.15.got = bf16[16,72,128]{2,1,0:T(8,128)(2,1)S(1)} all-to-all(bf16[16,72,128]{2,1,0:T(8,128)(2,1)S(1)} %attend.1), channel_id=1, replica_groups=mesh['kv_0'=4,'kv_1'=4,'y'=4,'core'=2] {'kv_0','kv_1'}, dimensions={0} | all-to-all | bytes 589824 | tf_op jit(solution)/shard_map/all_to_all | solution.py:305
  62.8 0.5 combine.1
  63.3 15.3 %all_to_all.16.got = bf16[128,8,128]{2,1,0:T(8,128)(2,1)S(1)} all-to-all(bf16[128,8,128]{2,1,0:T(8,128)(2,1)S(1)} %combine.1), channel_id=1, replica_groups=mesh['kv_0'=4,'kv_1'=4,'y'=4,'core'=2] {'core','kv_0','kv_1','y'}, dimensions={0} | all-to-all | bytes 524288 | tf_op jit(solution)/shard_map/all_to_all | solution.py:305
  78.7 0.0 copy-done
  78.7 0.8 finish.1
Async XLA Ops:
  1.2 9.7 %collective-permute-start.4 = (bf16[1152,128]{1,0:T(8,128)(2,1)S(1)}, bf16[1152,128]{1,0:T(8,128)(2,1)S(1)}, u32[]{:S(2)}, u32[]{:S(2)}) collective-permute-start(bf16[1152,128]{1,0:T(8,128)(2,1)S(1)} %get-tuple-element.16), channel_id=1, source_target_pairs={{0,6},{1,3},{2,0},{3,5},{4,2},{5,7},{6,4},{7,1},{8,14},{9,11},{10,... | collective-permute-start | bytes 884744 | tf_op jit(solution)/shard_map/ppermute | solution.py:317
  4.4 7.9 %collective-permute-start.3 = (bf16[1152,128]{1,0:T(8,128)(2,1)S(1)}, bf16[1152,128]{1,0:T(8,128)(2,1)S(1)}, u32[]{:S(2)}, u32[]{:S(2)}) collective-permute-start(bf16[1152,128]{1,0:T(8,128)(2,1)S(1)} %get-tuple-element.16), channel_id=1, source_target_pairs={{0,2},{1,7},{2,4},{3,1},{4,6},{5,3},{6,0},{7,5},{8,10},{9,15},{10,... | collective-permute-start | bytes 884744 | tf_op jit(solution)/shard_map/ppermute | solution.py:317
  12.4 33.3 %collective-permute-start.6 = (bf16[3,1152,128]{2,1,0:T(8,128)(2,1)S(1)}, bf16[3,1152,128]{2,1,0:T(8,128)(2,1)S(1)}, u32[]{:S(2)}, u32[]{:S(2)}) collective-permute-start(bf16[3,1152,128]{2,1,0:T(8,128)(2,1)S(1)} %pad_maximum_fusion.near), channel_id=1, source_target_pairs={{0,1},{1,0},{2,3},{3,2},{4,5},{5,4},{6,7},{7,6},{8,9},{9,8},{10,11... | collective-permute-start | bytes 2654216 | tf_op jit(solution)/shard_map/ppermute | solution.py:309
  12.5 22.3 %collective-permute-start.5 = (bf16[1152,128]{1,0:T(8,128)(2,1)S(1)}, bf16[1152,128]{1,0:T(8,128)(2,1)S(1)}, u32[]{:S(2)}, u32[]{:S(2)}) collective-permute-start(bf16[1152,128]{1,0:T(8,128)(2,1)S(1)} %get-tuple-element.16), channel_id=1, source_target_pairs={{0,4},{1,5},{2,6},{3,7},{4,0},{5,1},{6,2},{7,3},{8,12},{9,13},{10,... | collective-permute-start | bytes 884744 | tf_op jit(solution)/shard_map/ppermute | solution.py:317
  14.6 10.5 %collective-permute-start.2 = (bf16[192,128]{1,0:T(8,128)(2,1)}, bf16[192,128]{1,0:T(8,128)(2,1)S(1)}, u32[]{:S(2)}, u32[]{:S(2)}) collective-permute-start(bf16[192,128]{1,0:T(8,128)(2,1)} %bitcast.16), channel_id=1, source_target_pairs={{0,4},{1,5},{2,6},{3,7},{4,0},{5,1},{6,2},{7,3},{8,12},{9,13},{10,... | collective-permute-start | bytes 147464 | tf_op jit(solution)/shard_map/ppermute | solution.py:317
  16.1 8.9 %collective-permute-start.1 = (bf16[192,128]{1,0:T(8,128)(2,1)}, bf16[192,128]{1,0:T(8,128)(2,1)S(1)}, u32[]{:S(2)}, u32[]{:S(2)}) collective-permute-start(bf16[192,128]{1,0:T(8,128)(2,1)} %bitcast.17), channel_id=1, source_target_pairs={{0,6},{1,3},{2,0},{3,5},{4,2},{5,7},{6,4},{7,1},{8,14},{9,11},{10,... | collective-permute-start | bytes 147464 | tf_op jit(solution)/shard_map/ppermute | solution.py:317
  18.2 7.3 %collective-permute-start = (bf16[192,128]{1,0:T(8,128)(2,1)}, bf16[192,128]{1,0:T(8,128)(2,1)S(1)}, u32[]{:S(2)}, u32[]{:S(2)}) collective-permute-start(bf16[192,128]{1,0:T(8,128)(2,1)} %bitcast.18), channel_id=1, source_target_pairs={{0,2},{1,7},{2,4},{3,1},{4,6},{5,3},{6,0},{7,5},{8,10},{9,15},{10,... | collective-permute-start | bytes 147464 | tf_op jit(solution)/shard_map/ppermute | solution.py:317
  26.6 19.1 %all-to-all-start = ((bf16[32,56,128]{2,1,0:T(8,128)(2,1)}), bf16[32,56,128]{2,1,0:T(8,128)(2,1)S(1)}, u32[]{:S(2)}, u32[]{:S(2)}) async-start(bf16[32,56,128]{2,1,0:T(8,128)(2,1)} %project.1), calls=%async_computation | async-start | bytes 917504 | tf_op jit(solution)/shard_map/all_to_all | solution.py:305
  34.8 10.9 %collective-permute-start.7 = (bf16[1152,128]{1,0:T(8,128)(2,1)S(1)}, bf16[1152,128]{1,0:T(8,128)(2,1)S(1)}, u32[]{:S(2)}, u32[]{:S(2)}) collective-permute-start(bf16[1152,128]{1,0:T(8,128)(2,1)S(1)} %collective-permute-done.5.opposite), channel_id=1, source_target_pairs={{0,1},{1,0},{2,3},{3,2},{4,5},{5,4},{6,7},{7,6},{8,9},{9,8},{10,11... | collective-permute-start | bytes 884744 | tf_op jit(solution)/shard_map/ppermute | solution.py:309
  45.7 33.0 %copy-start = (f32[128]{0:T(128)S(1)}, f32[128]{0:T(128)}, u32[]{:S(2)}) copy-start(f32[128]{0:T(128)} %param.23) | copy-start | bytes 1540

commit v14 on v6

--- a/solution.py
+++ b/solution.py
@@ -11,7 +11,9 @@
 
 
 KV = ("kv_0", "kv_1")
-ALL = ("kv_0", "kv_1", "tp")
+TP = ("y", "core")
+ALL = KV + TP
+SPREAD = ("core",) + KV + ("y",)
 EPSILON = 1e-06
 NEGATIVE = -1e30
 F32 = jnp.float32
@@ -49,11 +51,16 @@
     return lax.broadcasted_iota(jnp.int32, shape, 0)
 
 
+def block_of(kv, tp, kv_size):
+    cores = lax.axis_size("core")
+    return (tp % cores * kv_size + kv) * lax.axis_size("y") + tp // cores
+
+
 def project_kernel(
     tokens, gain, wq, wd, wr, wk, wv, wo, out, own, tokens_, gain_, wq_, wd_, wr_, sems
 ):
-    tp = lax.axis_index("tp")
-    groups = lax.axis_size("tp")
+    tp = lax.axis_index(TP)
+    groups = lax.axis_size(TP)
     kv_size = lax.axis_size(KV)
     deep = wk.shape[1]
     pairs = (
@@ -97,7 +104,7 @@
             new = jnp.where(row == 0, part[r : r + 1], 0.0) + jnp.where(row == 1, rope[r : r + 1], 0.0)
             tile = (low + new).astype(BF16)
             for c in range(kv_size // local):
-                b = (c * local + j) * groups + t
+                b = block_of(c * local + j, t, kv_size)
                 out[b, :, :128] = top
                 out[b, :, 128:] = tile
     for copy in copies[5:]:
@@ -111,16 +118,23 @@
 
 
 def attend_kernel(
-    got, lengths, frequencies, near, far, gain, latents, ropes,
-    out, cache, cache_rope, sums, lifted, turned, scored, weights, means, sems,
+    got, near, opposite, far, far_opposite, lengths_, frequencies_, gain_, latents, ropes,
+    out, lengths, frequencies, gain, cache, cache_rope,
+    sums, lifted, turned, scored, weights, means, sems,
     *, factor, nope,
 ):
     kv = lax.axis_index(KV)
-    tp = lax.axis_index("tp")
+    tp = lax.axis_index(TP)
     kv_size = lax.axis_size(KV)
-    groups = lax.axis_size("tp")
+    groups = lax.axis_size(TP)
     local, positions, latent_width = cache.shape
     width = cache_rope.shape[1]
+    small = []
+    for n, (a, b) in enumerate(
+        ((lengths_, lengths), (frequencies_, frequencies), (gain_, gain))
+    ):
+        small.append(pltpu.make_async_copy(a, b, sems.at[2 * local + n]))
+        small[n].start()
     copies = []
     for s in range(local):
         a = pltpu.make_async_copy(latents.at[s], cache.at[s], sems.at[s])
@@ -129,10 +143,12 @@
         b.start()
         copies.append((a, b))
     for h in range(groups):
-        total = got[h].astype(F32)
+        total = got[block_of(0, h, kv_size)].astype(F32)
         for k in range(1, kv_size):
-            total = total + got[k * groups + h].astype(F32)
+            total = total + got[block_of(k, h, kv_size)].astype(F32)
         sums[h] = total
+    for copy in small:
+        copy.wait()
     shape = (local, lengths.shape[1])
     length = jnp.sum(
         jnp.where(lanes(shape) == rows(shape) + tp * local, lengths[...], 0), axis=1, keepdims=True
@@ -149,8 +165,8 @@
         step = (0, half - 1, 1, 2)[i % half]
         head = 2 * lax.rem(y + step, half) + (core if i < half else 1 - core)
         q = sums[head]
-        w = near if i < half else far
-        lifted[i] = dot(q[:, :nope].astype(BF16), w[i % half, :latent_width, :], NT)
+        w = weights_of((near, opposite, far, far_opposite), i)
+        lifted[i] = dot(q[:, :nope].astype(BF16), w[:latent_width, :], NT)
         turned[i] = rotate(q[:, nope : nope + width].astype(BF16).astype(F32), cosine, sine)
     raw = jnp.concatenate([sums[h][0:1, nope + width :] for h in range(groups)], axis=1)
     rope_raw = sums[0][1:2, nope + width :]
@@ -203,9 +219,9 @@
         mixed = dot(weights[r, :], cache[s], NN) + rounded[r] * new_latent
         means[s] = mixed * inverse[r]
     for i in range(groups):
-        w = near if i < half else far
+        w = weights_of((near, opposite, far, far_opposite), i)
         x = means[:, i, :].astype(BF16)
-        up = dot(x, w[i % half, latent_width : 2 * latent_width, :], NN).astype(BF16)
+        up = dot(x, w[latent_width : 2 * latent_width, :], NN).astype(BF16)
         for k in range(kv_size):
             out[k, i * local : (i + 1) * local, :] = up
     lane = lanes((local, 128))
@@ -231,7 +247,14 @@
         out[k, groups * local :, :] = packed
 
 
-def combine_kernel(got, near, far, out, *, kv_size, groups, local, first):
+def weights_of(collected, i):
+    near, opposite, far, far_opposite = collected
+    places = near.shape[0] + 1
+    stacked, single = (near, opposite) if i < places else (far, far_opposite)
+    return single if i % places == places - 1 else stacked.at[i % places]
+
+
+def combine_kernel(got, near, opposite, far, far_opposite, out, *, kv_size, groups, local, first):
     logs = []
     for k in range(kv_size):
         x = got[k, groups * local :, :].astype(F32)
@@ -241,15 +264,14 @@
     total = functools.reduce(jnp.add, shares)
     inverse = 1.0 / total
     shares = [x * inverse for x in shares]
-    half = groups // 2
     mixed = jnp.zeros((local, out.shape[2]), F32)
     for i in range(groups):
         head = jnp.zeros((local, 128), F32)
         for k in range(kv_size):
             part = got[k, i * local : (i + 1) * local, :].astype(F32)
             head = head + part * shares[k][:, i : i + 1]
-        w = near if i < half else far
-        mixed = mixed + dot(head.astype(BF16), w[i % half, first:, :], NN)
+        w = weights_of((near, opposite, far, far_opposite), i)
+        mixed = mixed + dot(head.astype(BF16), w[first:, :], NN)
     mixed = mixed.astype(BF16)
     for d in range(out.shape[0]):
         out[d] = mixed
@@ -261,10 +283,10 @@
     for t in range(groups):
         squares = jnp.zeros((local, width), F32)
         for k in range(kv_size):
-            x = got[k * groups + t].astype(F32)
+            x = got[block_of(k, t, kv_size)].astype(F32)
             squares = squares + x * x
         mean = jnp.sum(squares, axis=1, keepdims=True) / (width * kv_size)
-        own = got[kv * groups + t].astype(F32)
+        own = got[block_of(kv, t, kv_size)].astype(F32)
         out[t * local : (t + 1) * local, :] = (
             own * lax.rsqrt(mean + EPSILON) * gain[...]
         ).astype(BF16)
@@ -272,6 +294,19 @@
 
 def exchange(value, axes):
     return lax.all_to_all(value, axes, split_axis=0, concat_axis=0, tiled=True)
+
+
+def swap(value):
+    return lax.ppermute(value, TP, [(i, i ^ 1) for i in range(lax.axis_size(TP))])
+
+
+def along(own):
+    size = lax.axis_size(TP)
+    collected = []
+    for step in (1, 3, 2):
+        pairs = [(i, (i + 2 * step) % size) for i in range(size)]
+        collected.append(lax.ppermute(own, TP, pairs))
+    return collected
 
 
 def on_device(
@@ -290,7 +325,7 @@
     lengths,
 ):
     kv_size = lax.axis_size(KV)
-    groups = lax.axis_size("tp")
+    groups = lax.axis_size(TP)
     everyone = kv_size * groups
     seqs, width = tokens.shape
     local, positions, latent_width = cache_latent.shape
@@ -330,23 +365,24 @@
         )
     )
 
-    collected = [own]
-    for step in (1, 3, 2):
-        collected.append(
-            lax.ppermute(own, "tp", [(i, (i + 2 * step) % groups) for i in range(groups)])
-        )
-    near = jnp.stack(collected)
-    far = lax.ppermute(near, "tp", [(i, i ^ 1) for i in range(groups)])
-
-    got = exchange(sent, ALL)
+    before, after, opposite = along(own)
+    near = jnp.stack([own, before, after])
+    far = swap(near)
+    far_opposite = swap(opposite)
+    collected = (near, opposite, far, far_opposite)
+
+    got = exchange(sent, SPREAD)
     powers = np.arange(0, rope, 2, dtype=np.float64) / rope
     frequencies = np.tile(1.0 / 10000.0**powers, 2)[None].astype(np.float32)
     sent = pl.pallas_call(
         functools.partial(attend_kernel, factor=factor, nope=nope),
         out_shape=jax.ShapeDtypeStruct((kv_size, groups * local + local, value), BF16),
-        in_specs=[in_vmem()] * 6 + [in_hbm()] * 2,
+        in_specs=[in_vmem()] * 5 + [in_hbm()] * 5,
         out_specs=in_vmem(),
         scratch_shapes=[
+            pltpu.VMEM((1, seqs), jnp.int32),
+            pltpu.VMEM((1, rope), F32),
+            pltpu.VMEM((1, latent_width), F32),
             pltpu.VMEM((local, positions, latent_width), BF16),
             pltpu.VMEM((local, rope, positions), BF16),
             pltpu.VMEM((groups, local, 256), F32),
@@ -355,18 +391,20 @@
             pltpu.VMEM((local * groups, positions + 128), F32),
             pltpu.VMEM((local * groups, positions), BF16),
             pltpu.VMEM((local, groups, latent_width), F32),
-            pltpu.SemaphoreType.DMA((2 * local,)),
+            pltpu.SemaphoreType.DMA((2 * local + 3,)),
         ],
         compiler_params=params(24),
         name="attend",
     )(
         got,
-        lengths[None],
-        frequencies,
-        near,
-        far,
-        latent_gain[None],
-        *keep_in_hbm(cache_latent, cache_rope.transpose(0, 2, 1)),
+        *collected,
+        *keep_in_hbm(
+            lengths[None],
+            frequencies,
+            latent_gain[None],
+            cache_latent,
+            cache_rope.transpose(0, 2, 1),
+        ),
     )
     got = exchange(sent, KV)
 
@@ -379,12 +417,12 @@
             first=2 * latent_width,
         ),
         out_shape=jax.ShapeDtypeStruct((everyone, local, w_out.shape[1]), BF16),
-        in_specs=[in_vmem()] * 3,
+        in_specs=[in_vmem()] * 5,
         out_specs=in_vmem(),
         compiler_params=params(8),
         name="combine",
-    )(got, near, far)
-    got = exchange(sent, ALL)
+    )(got, *collected)
+    got = exchange(sent, SPREAD)
     return pl.pallas_call(
         functools.partial(finish_kernel, kv_size=kv_size, groups=groups, local=local),
         out_shape=jax.ShapeDtypeStruct((seqs, w_out.shape[1]), BF16),
@@ -396,7 +434,7 @@
 
 
 def solution(mesh):
-    finer = Mesh(mesh.devices.reshape(4, 4, mesh.shape["tp"]), ("kv_0", "kv_1", "tp"))
+    finer = Mesh(mesh.devices.reshape(4, 4, mesh.shape["tp"] // 2, 2), ALL)
 
     return jax.shard_map(
         on_device,
@@ -404,16 +442,16 @@
         in_specs=(
             P(None, KV),
             P(KV),
-            P(KV, "tp"),
+            P(KV, TP),
             P(KV, None),
             P(KV, None),
             P(),
-            P("tp", None, None),
-            P("tp", None, None),
-            P("tp", KV),
+            P(TP, None, None),
+            P(TP, None, None),
+            P(TP, KV),
             P(KV),
-            P("tp", KV, None),
-            P("tp", KV, None),
+            P(TP, KV, None),
+            P(TP, KV, None),
             P(),
         ),
         out_specs=P(None, KV),

time: 76.7 us -> 74 us (0.965)
  blocking collectives: 50.9 us -> 27.4 us
  waiting for transfers between devices: 11.7 us -> 22.5 us
  starting transfers between devices: 5.5 us -> 14.8 us
  Pallas kernels: 7.35 us -> 8.12 us
    all_to_all x3 -> x2, blocking collectives: 50.9 us -> 27.4 us  [exchange(): return lax.all_to_all(value, axes, split_axis=0, concat_axis=0, tiled=True)]
    all_to_all x0 -> x1, waiting for transfers between devices: none -> 12.8 us  [exchange(): return lax.all_to_all(value, axes, split_axis=0, concat_axis=0, tiled=True)]
    all_to_all x0 -> x1, starting transfers between devices: none -> 11.4 us  [exchange(): return lax.all_to_all(value, axes, split_axis=0, concat_axis=0, tiled=True)]
    ppermute x4 -> x5, waiting for transfers between devices: 11.7 us -> 9.68 us  [the longest x3 9.68 us: along(): collected.append(lax.ppermute(own, TP, pairs))]
    ppermute x4 -> x5, starting transfers between devices: 5.5 us -> 3.45 us  [the longest x3 3.28 us: along(): collected.append(lax.ppermute(own, TP, pairs))]
    pallas_call x1, Pallas kernels: 1.72 us -> 2.53 us  [on_device(): pl.pallas_call(project_kernel, out_shape=(jax.ShapeDtypeStruct((everyone,...]
  transfers between devices with their start and end apart: 4 -> 6, of which waited for: 2 -> 3; matrix products, arithmetic and copies ran while one was open for 0% -> 0% of each run, Pallas kernels for 0% -> 0%
where the time goes in v14:
time: 74 us; the launch traced here: 73.1 us
  blocking collectives  27.4 us (37%)
  waiting for transfers between devices  22.5 us (30%)
  starting transfers between devices  14.8 us (20%)
  Pallas kernels  8.12 us (11%)
    all_to_all x2, blocking collectives, exchange(): return lax.all_to_all(value, axes, split_axis=0, concat_axis=0, tiled=True)  27.4 us
    all_to_all x1, waiting for transfers between devices, exchange(): return lax.all_to_all(value, axes, split_axis=0, concat_axis=0, tiled=True)  12.8 us
    all_to_all x1, starting transfers between devices, exchange(): return lax.all_to_all(value, axes, split_axis=0, concat_axis=0, tiled=True)  11.4 us
    ppermute x3, waiting for transfers between devices, along(): collected.append(lax.ppermute(own, TP, pairs))  9.68 us
    pallas_call x1, Pallas kernels, on_device(): pl.pallas_call(functools.partial(attend_kernel, factor=factor, nope=nope)...  4.37 us
    ppermute x3, starting transfers between devices, along(): collected.append(lax.ppermute(own, TP, pairs))  3.28 us
    pallas_call x1, Pallas kernels, on_device(): pl.pallas_call(project_kernel, out_shape=(jax.ShapeDtypeStruct((everyone,...  2.53 us
  transfers between devices with their start and end apart: 6, of which 3 were waited for; matrix products, arithmetic and copies ran while one was open for 0% of the time, Pallas kernels for 0%

profile of v14, /device:TPU:0, one launch (start us, length us, event | category | flops | bytes accessed | tf_op | source)
XLA Modules:
  0.0 73.1 jit_solution(2990225739723435998)
XLA Ops:
  0.0 2.5 %project.1 = (bf16[128,8,256]{2,1,0:T(8,128)(2,1)}, bf16[1152,128]{1,0:T(8,128)(2,1)S(1)}) custom-call(bf16[64,128]{1,0:T(8,128)(2,1)} %tokens.1, f32[1,128]{1,0:T(1,128)} %bitcast.18, bf16[192,128]{1,0:T(8,128)(2,1)} %bitcast.15, bf16[128,512]{1,0:T(8,128)(2,1)} %wd.1, bf16[64,128]{1,0:T(8,128)(2,1)} %bitcast.16, bf16[1,512,128]{2,1,0:T(8,128)(2,1)} %wk.1, ...), custom_call_target="tpu_custom_call" | custom-call | tf_op jit(solution)/shard_map/project/pallas_call | solution.py:337
  2.5 3.2 %collective-permute-start.1 = (bf16[1152,128]{1,0:T(8,128)(2,1)S(1)}, bf16[1152,128]{1,0:T(8,128)(2,1)S(1)}, u32[]{:S(2)}, u32[]{:S(2)}) collective-permute-start(bf16[1152,128]{1,0:T(8,128)(2,1)S(1)} %get-tuple-element.8), channel_id=1, source_target_pairs={{0,6},{1,7},{2,0},{3,1},{4,2},{5,3},{6,4},{7,5},{8,14},{9,15},{10,... | collective-permute-start | bytes 884744 | tf_op jit(solution)/shard_map/ppermute | solution.py:308
  5.7 0.0 collective-permute-start
  5.7 6.3 %collective-permute-done.1 = bf16[1152,128]{1,0:T(8,128)(2,1)S(1)} collective-permute-done((bf16[1152,128]{1,0:T(8,128)(2,1)S(1)}, bf16[1152,128]{1,0:T(8,128)(2,1)S(1)}, u32[]{:S(2)}, u32[]{:S(2)}) %collective-permute-start.1) | collective-permute-done | bytes 294944 | tf_op jit(solution)/shard_map/ppermute | solution.py:308
  12.0 3.4 %collective-permute-done = bf16[1152,128]{1,0:T(8,128)(2,1)S(1)} collective-permute-done((bf16[1152,128]{1,0:T(8,128)(2,1)S(1)}, bf16[1152,128]{1,0:T(8,128)(2,1)S(1)}, u32[]{:S(2)}, u32[]{:S(2)}) %collective-permute-start) | collective-permute-done | bytes 294944 | tf_op jit(solution)/shard_map/ppermute | solution.py:308
  15.4 0.1 pad_maximum_fusion.near
  15.5 0.1 collective-permute-start.3
  15.6 0.1 collective-permute-start.2
  15.7 11.4 %all-to-all-start = ((bf16[128,8,256]{2,1,0:T(8,128)(2,1)}), bf16[128,8,256]{2,1,0:T(8,128)(2,1)S(1)}, u32[]{:S(2)}, u32[]{:S(2)}) async-start(bf16[128,8,256]{2,1,0:T(8,128)(2,1)} %get-tuple-element.7), calls=%async_computation | async-start | bytes 1048576 | tf_op jit(solution)/shard_map/all_to_all | solution.py:296
  27.1 0.0 collective-permute-done.2.opposite
  27.1 0.1 collective-permute-start.4
  27.2 12.8 %all-to-all-done.got = bf16[128,8,256]{2,1,0:T(8,128)(2,1)S(1)} async-done(((bf16[128,8,256]{2,1,0:T(8,128)(2,1)}), bf16[128,8,256]{2,1,0:T(8,128)(2,1)S(1)}, u32[]{:S(2)}, u32[]{:S(2)}) %all-to-all-start) | async-done | bytes 524320 | tf_op jit(solution)/shard_map/all_to_all | solution.py:296
  40.0 0.0 collective-permute-done.4.far_opposite
  40.0 0.0 collective-permute-done.3.far
  40.0 0.0 copy-start
  40.0 4.4 %attend.1 = bf16[16,72,128]{2,1,0:T(8,128)(2,1)S(1)} custom-call(bf16[128,8,256]{2,1,0:T(8,128)(2,1)S(1)} %all-to-all-done.got, bf16[3,1152,128]{2,1,0:T(8,128)(2,1)S(1)} %pad_maximum_fusion.near, bf16[1152,128]{1,0:T(8,128)(2,1)S(1)} %collective-permute-done.2.opposite, bf16[3,1152,128]{2,1,0:T(8,128)(2,1)S(1)} %collective-permute-done.3.far, ...), custom_call_target="tpu_custom_call" | custom-call | tf_op jit(solution)/shard_map/attend/pallas_call | solution.py:377
  44.4 13.1 %all_to_all.15.got = bf16[16,72,128]{2,1,0:T(8,128)(2,1)S(1)} all-to-all(bf16[16,72,128]{2,1,0:T(8,128)(2,1)S(1)} %attend.1), channel_id=1, replica_groups=mesh['kv_0'=4,'kv_1'=4,'y'=4,'core'=2] {'kv_0','kv_1'}, dimensions={0} | all-to-all | bytes 589824 | tf_op jit(solution)/shard_map/all_to_all | solution.py:296
  57.5 0.5 combine.1
  58.0 14.3 %all_to_all.16.got = bf16[128,8,128]{2,1,0:T(8,128)(2,1)S(1)} all-to-all(bf16[128,8,128]{2,1,0:T(8,128)(2,1)S(1)} %combine.1), channel_id=1, replica_groups=mesh['kv_0'=4,'kv_1'=4,'y'=4,'core'=2] {'core','kv_0','kv_1','y'}, dimensions={0} | all-to-all | bytes 524288 | tf_op jit(solution)/shard_map/all_to_all | solution.py:296
  72.3 0.0 copy-done
  72.3 0.8 %finish.1 = bf16[64,128]{1,0:T(8,128)(2,1)} custom-call(bf16[128,8,128]{2,1,0:T(8,128)(2,1)S(1)} %all_to_all.16.got, f32[1,128]{1,0:T(1,128)S(1)} %bitcast.11), custom_call_target="tpu_custom_call" | custom-call | tf_op jit(solution)/shard_map/finish/pallas_call | solution.py:426
Async XLA Ops:
  2.5 9.5 %collective-permute-start.1 = (bf16[1152,128]{1,0:T(8,128)(2,1)S(1)}, bf16[1152,128]{1,0:T(8,128)(2,1)S(1)}, u32[]{:S(2)}, u32[]{:S(2)}) collective-permute-start(bf16[1152,128]{1,0:T(8,128)(2,1)S(1)} %get-tuple-element.8), channel_id=1, source_target_pairs={{0,6},{1,7},{2,0},{3,1},{4,2},{5,3},{6,4},{7,5},{8,14},{9,15},{10,... | collective-permute-start | bytes 884744 | tf_op jit(solution)/shard_map/ppermute | solution.py:308
  5.7 9.7 %collective-permute-start = (bf16[1152,128]{1,0:T(8,128)(2,1)S(1)}, bf16[1152,128]{1,0:T(8,128)(2,1)S(1)}, u32[]{:S(2)}, u32[]{:S(2)}) collective-permute-start(bf16[1152,128]{1,0:T(8,128)(2,1)S(1)} %get-tuple-element.8), channel_id=1, source_target_pairs={{0,2},{1,3},{2,4},{3,5},{4,6},{5,7},{6,0},{7,1},{8,10},{9,11},{10,... | collective-permute-start | bytes 884744 | tf_op jit(solution)/shard_map/ppermute | solution.py:308
  15.5 24.5 %collective-permute-start.3 = (bf16[3,1152,128]{2,1,0:T(8,128)(2,1)S(1)}, bf16[3,1152,128]{2,1,0:T(8,128)(2,1)S(1)}, u32[]{:S(2)}, u32[]{:S(2)}) collective-permute-start(bf16[3,1152,128]{2,1,0:T(8,128)(2,1)S(1)} %pad_maximum_fusion.near), channel_id=1, source_target_pairs={{0,1},{1,0},{2,3},{3,2},{4,5},{5,4},{6,7},{7,6},{8,9},{9,8},{10,11... | collective-permute-start | bytes 2654216 | tf_op jit(solution)/shard_map/ppermute | solution.py:300
  15.6 11.5 %collective-permute-start.2 = (bf16[1152,128]{1,0:T(8,128)(2,1)S(1)}, bf16[1152,128]{1,0:T(8,128)(2,1)S(1)}, u32[]{:S(2)}, u32[]{:S(2)}) collective-permute-start(bf16[1152,128]{1,0:T(8,128)(2,1)S(1)} %get-tuple-element.8), channel_id=1, source_target_pairs={{0,4},{1,5},{2,6},{3,7},{4,0},{5,1},{6,2},{7,3},{8,12},{9,13},{10,... | collective-permute-start | bytes 884744 | tf_op jit(solution)/shard_map/ppermute | solution.py:308
  15.7 24.3 %all-to-all-start = ((bf16[128,8,256]{2,1,0:T(8,128)(2,1)}), bf16[128,8,256]{2,1,0:T(8,128)(2,1)S(1)}, u32[]{:S(2)}, u32[]{:S(2)}) async-start(bf16[128,8,256]{2,1,0:T(8,128)(2,1)} %get-tuple-element.7), calls=%async_computation | async-start | bytes 1048576 | tf_op jit(solution)/shard_map/all_to_all | solution.py:296
  27.1 12.9 %collective-permute-start.4 = (bf16[1152,128]{1,0:T(8,128)(2,1)S(1)}, bf16[1152,128]{1,0:T(8,128)(2,1)S(1)}, u32[]{:S(2)}, u32[]{:S(2)}) collective-permute-start(bf16[1152,128]{1,0:T(8,128)(2,1)S(1)} %collective-permute-done.2.opposite), channel_id=1, source_target_pairs={{0,1},{1,0},{2,3},{3,2},{4,5},{5,4},{6,7},{7,6},{8,9},{9,8},{10,11... | collective-permute-start | bytes 884744 | tf_op jit(solution)/shard_map/ppermute | solution.py:300
  40.0 32.3 %copy-start = (f32[128]{0:T(128)S(1)}, f32[128]{0:T(128)}, u32[]{:S(2)}) copy-start(f32[128]{0:T(128)} %param.23) | copy-start | bytes 1540

commit v15 on v14

--- a/solution.py
+++ b/solution.py
@@ -111,6 +111,20 @@
         copy.wait()
 
 
+def bring_kernel(latents, lengths_, frequencies_, gain_, early, lengths, frequencies, gain, sems):
+    pairs = (
+        (latents.at[pl.ds(0, 1)], early),
+        (lengths_, lengths),
+        (frequencies_, frequencies),
+        (gain_, gain),
+    )
+    copies = [pltpu.make_async_copy(x, y, sems.at[n]) for n, (x, y) in enumerate(pairs)]
+    for copy in copies:
+        copy.start()
+    for copy in copies:
+        copy.wait()
+
+
 def rotate(values, cosine, sine):
     half = values.shape[1] // 2
     swapped = jnp.concatenate([values[:, half:], values[:, :half]], axis=1)
@@ -118,8 +132,8 @@
 
 
 def attend_kernel(
-    got, near, opposite, far, far_opposite, lengths_, frequencies_, gain_, latents, ropes,
-    out, lengths, frequencies, gain, cache, cache_rope,
+    got, near, opposite, far, far_opposite, early, lengths, frequencies, gain, latents, ropes,
+    out, cache, cache_rope,
     sums, lifted, turned, scored, weights, means, sems,
     *, factor, nope,
 ):
@@ -127,28 +141,27 @@
     tp = lax.axis_index(TP)
     kv_size = lax.axis_size(KV)
     groups = lax.axis_size(TP)
-    local, positions, latent_width = cache.shape
+    local, _, positions = cache_rope.shape
+    latent_width = cache.shape[2]
     width = cache_rope.shape[1]
-    small = []
-    for n, (a, b) in enumerate(
-        ((lengths_, lengths), (frequencies_, frequencies), (gain_, gain))
-    ):
-        small.append(pltpu.make_async_copy(a, b, sems.at[2 * local + n]))
-        small[n].start()
     copies = []
     for s in range(local):
-        a = pltpu.make_async_copy(latents.at[s], cache.at[s], sems.at[s])
         b = pltpu.make_async_copy(ropes.at[s], cache_rope.at[s], sems.at[local + s])
-        a.start()
         b.start()
-        copies.append((a, b))
+        copies.append([b])
+        if s > 0:
+            a = pltpu.make_async_copy(latents.at[s], cache.at[s - 1], sems.at[s])
+            a.start()
+            copies[s].append(a)
+
+    def cached(s):
+        return cache[s - 1] if s > 0 else early[0]
+
     for h in range(groups):
         total = got[block_of(0, h, kv_size)].astype(F32)
         for k in range(1, kv_size):
             total = total + got[block_of(k, h, kv_size)].astype(F32)
         sums[h] = total
-    for copy in small:
-        copy.wait()
     shape = (local, lengths.shape[1])
     length = jnp.sum(
         jnp.where(lanes(shape) == rows(shape) + tp * local, lengths[...], 0), axis=1, keepdims=True
@@ -192,7 +205,7 @@
         for copy in copies[s]:
             copy.wait()
         r = s * groups
-        scored[r : r + groups, :positions] = dot(q, cache[s], NT) + dot(qr, cache_rope[s], NN)
+        scored[r : r + groups, :positions] = dot(q, cached(s), NT) + dot(qr, cache_rope[s], NN)
         scored[r : r + groups, positions:] = jnp.broadcast_to(fresh, (groups, 128))
     scores = scored[:, :positions] * factor
     row = rows((pairs, 1))
@@ -216,7 +229,7 @@
     rounded = new_weight.astype(BF16).astype(F32)
     for s in range(local):
         r = slice(s * groups, (s + 1) * groups)
-        mixed = dot(weights[r, :], cache[s], NN) + rounded[r] * new_latent
+        mixed = dot(weights[r, :], cached(s), NN) + rounded[r] * new_latent
         means[s] = mixed * inverse[r]
     for i in range(groups):
         w = weights_of((near, opposite, far, far_opposite), i)
@@ -374,16 +387,27 @@
     got = exchange(sent, SPREAD)
     powers = np.arange(0, rope, 2, dtype=np.float64) / rope
     frequencies = np.tile(1.0 / 10000.0**powers, 2)[None].astype(np.float32)
+    brought = pl.pallas_call(
+        bring_kernel,
+        out_shape=(
+            jax.ShapeDtypeStruct((1, positions, latent_width), BF16),
+            jax.ShapeDtypeStruct((1, seqs), jnp.int32),
+            jax.ShapeDtypeStruct((1, rope), F32),
+            jax.ShapeDtypeStruct((1, latent_width), F32),
+        ),
+        in_specs=[in_hbm()] * 4,
+        out_specs=(in_vmem(),) * 4,
+        scratch_shapes=[pltpu.SemaphoreType.DMA((4,))],
+        compiler_params=params(8),
+        name="bring",
+    )(*keep_in_hbm(cache_latent, lengths[None], frequencies, latent_gain[None]))
     sent = pl.pallas_call(
         functools.partial(attend_kernel, factor=factor, nope=nope),
         out_shape=jax.ShapeDtypeStruct((kv_size, groups * local + local, value), BF16),
-        in_specs=[in_vmem()] * 5 + [in_hbm()] * 5,
+        in_specs=[in_vmem()] * 9 + [in_hbm()] * 2,
         out_specs=in_vmem(),
         scratch_shapes=[
-            pltpu.VMEM((1, seqs), jnp.int32),
-            pltpu.VMEM((1, rope), F32),
-            pltpu.VMEM((1, latent_width), F32),
-            pltpu.VMEM((local, positions, latent_width), BF16),
+            pltpu.VMEM((local - 1, positions, latent_width), BF16),
             pltpu.VMEM((local, rope, positions), BF16),
             pltpu.VMEM((groups, local, 256), F32),
             pltpu.VMEM((groups, local, latent_width), F32),
@@ -391,20 +415,15 @@
             pltpu.VMEM((local * groups, positions + 128), F32),
             pltpu.VMEM((local * groups, positions), BF16),
             pltpu.VMEM((local, groups, latent_width), F32),
-            pltpu.SemaphoreType.DMA((2 * local + 3,)),
+            pltpu.SemaphoreType.DMA((2 * local,)),
         ],
         compiler_params=params(24),
         name="attend",
     )(
         got,
         *collected,
-        *keep_in_hbm(
-            lengths[None],
-            frequencies,
-            latent_gain[None],
-            cache_latent,
-            cache_rope.transpose(0, 2, 1),
-        ),
+        *brought,
+        *keep_in_hbm(cache_latent, cache_rope.transpose(0, 2, 1)),
     )
     got = exchange(sent, KV)
 

time: 74 us -> 73.8 us (level)
  waiting for transfers between devices: 22.5 us -> 21.4 us
  Pallas kernels: 8.12 us -> 9.06 us
    all_to_all x1, waiting for transfers between devices: 12.8 us -> 11.7 us  [exchange(): return lax.all_to_all(value, axes, split_axis=0, concat_axis=0, tiled=True)]
    pallas_call x0 -> x1, Pallas kernels: none -> 1.09 us  [on_device(): pl.pallas_call(bring_kernel, out_shape=(jax.ShapeDtypeStruct((1, position...]
  transfers between devices with their start and end apart: 6 -> 6, of which waited for: 3 -> 3; matrix products, arithmetic and copies ran while one was open for 0% -> 0% of each run, Pallas kernels for 0% -> 1%
where the time goes in v15:
time: 73.8 us; the launch traced here: 72.9 us
  blocking collectives  27.4 us (37%)
  waiting for transfers between devices  21.4 us (29%)
  starting transfers between devices  14.8 us (20%)
  Pallas kernels  9.06 us (12%)
    all_to_all x2, blocking collectives, exchange(): return lax.all_to_all(value, axes, split_axis=0, concat_axis=0, tiled=True)  27.4 us
    all_to_all x1, waiting for transfers between devices, exchange(): return lax.all_to_all(value, axes, split_axis=0, concat_axis=0, tiled=True)  11.7 us
    all_to_all x1, starting transfers between devices, exchange(): return lax.all_to_all(value, axes, split_axis=0, concat_axis=0, tiled=True)  11.4 us
    ppermute x3, waiting for transfers between devices, along(): collected.append(lax.ppermute(own, TP, pairs))  9.68 us
    pallas_call x1, Pallas kernels, on_device(): pl.pallas_call(functools.partial(attend_kernel, factor=factor, nope=nope)...  4.22 us
    ppermute x3, starting transfers between devices, along(): collected.append(lax.ppermute(own, TP, pairs))  3.28 us
    pallas_call x1, Pallas kernels, on_device(): pl.pallas_call(project_kernel, out_shape=(jax.ShapeDtypeStruct((everyone,...  2.52 us
  transfers between devices with their start and end apart: 6, of which 3 were waited for; matrix products, arithmetic and copies ran while one was open for 0% of the time, Pallas kernels for 1%

profile of v15, /device:TPU:0, one launch (start us, length us, event | category | flops | bytes accessed | tf_op | source)
XLA Modules:
  0.0 72.9 jit_solution(13660569140320463408)
XLA Ops:
  0.0 2.5 %project.1 = (bf16[128,8,256]{2,1,0:T(8,128)(2,1)}, bf16[1152,128]{1,0:T(8,128)(2,1)S(1)}) custom-call(bf16[64,128]{1,0:T(8,128)(2,1)} %tokens.1, f32[1,128]{1,0:T(1,128)} %bitcast.18, bf16[192,128]{1,0:T(8,128)(2,1)} %bitcast.15, bf16[128,512]{1,0:T(8,128)(2,1)} %wd.1, bf16[64,128]{1,0:T(8,128)(2,1)} %bitcast.16, bf16[1,512,128]{2,1,0:T(8,128)(2,1)} %wk.1, ...), custom_call_target="tpu_custom_call" | custom-call | tf_op jit(solution)/shard_map/project/pallas_call | solution.py:350
  2.5 3.2 %collective-permute-start.1 = (bf16[1152,128]{1,0:T(8,128)(2,1)S(1)}, bf16[1152,128]{1,0:T(8,128)(2,1)S(1)}, u32[]{:S(2)}, u32[]{:S(2)}) collective-permute-start(bf16[1152,128]{1,0:T(8,128)(2,1)S(1)} %get-tuple-element.12), channel_id=1, source_target_pairs={{0,6},{1,7},{2,0},{3,1},{4,2},{5,3},{6,4},{7,5},{8,14},{9,15},{10,... | collective-permute-start | bytes 884744 | tf_op jit(solution)/shard_map/ppermute | solution.py:321
  5.7 0.0 collective-permute-start
  5.7 6.3 %collective-permute-done.1 = bf16[1152,128]{1,0:T(8,128)(2,1)S(1)} collective-permute-done((bf16[1152,128]{1,0:T(8,128)(2,1)S(1)}, bf16[1152,128]{1,0:T(8,128)(2,1)S(1)}, u32[]{:S(2)}, u32[]{:S(2)}) %collective-permute-start.1) | collective-permute-done | bytes 294944 | tf_op jit(solution)/shard_map/ppermute | solution.py:321
  12.0 3.4 %collective-permute-done = bf16[1152,128]{1,0:T(8,128)(2,1)S(1)} collective-permute-done((bf16[1152,128]{1,0:T(8,128)(2,1)S(1)}, bf16[1152,128]{1,0:T(8,128)(2,1)S(1)}, u32[]{:S(2)}, u32[]{:S(2)}) %collective-permute-start) | collective-permute-done | bytes 294944 | tf_op jit(solution)/shard_map/ppermute | solution.py:321
  15.4 0.1 pad_maximum_fusion.near
  15.5 0.1 collective-permute-start.3
  15.6 0.1 collective-permute-start.2
  15.7 11.4 %all-to-all-start = ((bf16[128,8,256]{2,1,0:T(8,128)(2,1)}), bf16[128,8,256]{2,1,0:T(8,128)(2,1)S(1)}, u32[]{:S(2)}, u32[]{:S(2)}) async-start(bf16[128,8,256]{2,1,0:T(8,128)(2,1)} %get-tuple-element.11), calls=%async_computation | async-start | bytes 1048576 | tf_op jit(solution)/shard_map/all_to_all | solution.py:309
  27.1 0.0 collective-permute-done.2.opposite
  27.1 0.1 collective-permute-start.4
  27.2 1.1 %bring.1 = (bf16[1,512,512]{2,1,0:T(8,128)(2,1)S(1)}, s32[1,64]{1,0:T(1,128)S(1)}, f32[1,64]{1,0:T(1,128)S(1)}, f32[1,512]{1,0:T(1,128)S(1)}) custom-call(bf16[8,512,512]{2,1,0:T(8,128)(2,1)} %latents.3, s32[1,64]{1,0:T(1,128)} %bitcast.19, f32[1,64]{1,0:T(1,128)} %constant.2.clone.frequencies_, f32[1,512]{1,0:T(1,128)} %bitcast.17), custom_call_target="tpu_custom_call" | custom-call | tf_op jit(solution)/shard_map/bring/pallas_call | solution.py:390
  28.3 11.7 %all-to-all-done.got = bf16[128,8,256]{2,1,0:T(8,128)(2,1)S(1)} async-done(((bf16[128,8,256]{2,1,0:T(8,128)(2,1)}), bf16[128,8,256]{2,1,0:T(8,128)(2,1)S(1)}, u32[]{:S(2)}, u32[]{:S(2)}) %all-to-all-start) | async-done | bytes 524320 | tf_op jit(solution)/shard_map/all_to_all | solution.py:309
  40.0 0.0 collective-permute-done.4.far_opposite
  40.0 0.0 collective-permute-done.3.far
  40.0 0.0 copy-start
  40.0 4.2 %attend.1 = bf16[16,72,128]{2,1,0:T(8,128)(2,1)S(1)} custom-call(bf16[128,8,256]{2,1,0:T(8,128)(2,1)S(1)} %all-to-all-done.got, bf16[3,1152,128]{2,1,0:T(8,128)(2,1)S(1)} %pad_maximum_fusion.near, bf16[1152,128]{1,0:T(8,128)(2,1)S(1)} %collective-permute-done.2.opposite, bf16[3,1152,128]{2,1,0:T(8,128)(2,1)S(1)} %collective-permute-done.3.far, ...), custom_call_target="tpu_custom_call" | custom-call | tf_op jit(solution)/shard_map/attend/pallas_call | solution.py:404
  44.3 13.1 %all_to_all.15.got = bf16[16,72,128]{2,1,0:T(8,128)(2,1)S(1)} all-to-all(bf16[16,72,128]{2,1,0:T(8,128)(2,1)S(1)} %attend.1), channel_id=1, replica_groups=mesh['kv_0'=4,'kv_1'=4,'y'=4,'core'=2] {'kv_0','kv_1'}, dimensions={0} | all-to-all | bytes 589824 | tf_op jit(solution)/shard_map/all_to_all | solution.py:309
  57.3 0.5 combine.1
  57.8 14.3 %all_to_all.16.got = bf16[128,8,128]{2,1,0:T(8,128)(2,1)S(1)} all-to-all(bf16[128,8,128]{2,1,0:T(8,128)(2,1)S(1)} %combine.1), channel_id=1, replica_groups=mesh['kv_0'=4,'kv_1'=4,'y'=4,'core'=2] {'core','kv_0','kv_1','y'}, dimensions={0} | all-to-all | bytes 524288 | tf_op jit(solution)/shard_map/all_to_all | solution.py:309
  72.2 0.0 copy-done
  72.2 0.8 %finish.1 = bf16[64,128]{1,0:T(8,128)(2,1)} custom-call(bf16[128,8,128]{2,1,0:T(8,128)(2,1)S(1)} %all_to_all.16.got, f32[1,128]{1,0:T(1,128)S(1)} %bitcast.11), custom_call_target="tpu_custom_call" | custom-call | tf_op jit(solution)/shard_map/finish/pallas_call | solution.py:445
Async XLA Ops:
  2.5 9.5 %collective-permute-start.1 = (bf16[1152,128]{1,0:T(8,128)(2,1)S(1)}, bf16[1152,128]{1,0:T(8,128)(2,1)S(1)}, u32[]{:S(2)}, u32[]{:S(2)}) collective-permute-start(bf16[1152,128]{1,0:T(8,128)(2,1)S(1)} %get-tuple-element.12), channel_id=1, source_target_pairs={{0,6},{1,7},{2,0},{3,1},{4,2},{5,3},{6,4},{7,5},{8,14},{9,15},{10,... | collective-permute-start | bytes 884744 | tf_op jit(solution)/shard_map/ppermute | solution.py:321
  5.7 9.7 %collective-permute-start = (bf16[1152,128]{1,0:T(8,128)(2,1)S(1)}, bf16[1152,128]{1,0:T(8,128)(2,1)S(1)}, u32[]{:S(2)}, u32[]{:S(2)}) collective-permute-start(bf16[1152,128]{1,0:T(8,128)(2,1)S(1)} %get-tuple-element.12), channel_id=1, source_target_pairs={{0,2},{1,3},{2,4},{3,5},{4,6},{5,7},{6,0},{7,1},{8,10},{9,11},{10,... | collective-permute-start | bytes 884744 | tf_op jit(solution)/shard_map/ppermute | solution.py:321
  15.5 24.5 %collective-permute-start.3 = (bf16[3,1152,128]{2,1,0:T(8,128)(2,1)S(1)}, bf16[3,1152,128]{2,1,0:T(8,128)(2,1)S(1)}, u32[]{:S(2)}, u32[]{:S(2)}) collective-permute-start(bf16[3,1152,128]{2,1,0:T(8,128)(2,1)S(1)} %pad_maximum_fusion.near), channel_id=1, source_target_pairs={{0,1},{1,0},{2,3},{3,2},{4,5},{5,4},{6,7},{7,6},{8,9},{9,8},{10,11... | collective-permute-start | bytes 2654216 | tf_op jit(solution)/shard_map/ppermute | solution.py:313
  15.6 11.5 %collective-permute-start.2 = (bf16[1152,128]{1,0:T(8,128)(2,1)S(1)}, bf16[1152,128]{1,0:T(8,128)(2,1)S(1)}, u32[]{:S(2)}, u32[]{:S(2)}) collective-permute-start(bf16[1152,128]{1,0:T(8,128)(2,1)S(1)} %get-tuple-element.12), channel_id=1, source_target_pairs={{0,4},{1,5},{2,6},{3,7},{4,0},{5,1},{6,2},{7,3},{8,12},{9,13},{10,... | collective-permute-start | bytes 884744 | tf_op jit(solution)/shard_map/ppermute | solution.py:321
  15.7 24.3 %all-to-all-start = ((bf16[128,8,256]{2,1,0:T(8,128)(2,1)}), bf16[128,8,256]{2,1,0:T(8,128)(2,1)S(1)}, u32[]{:S(2)}, u32[]{:S(2)}) async-start(bf16[128,8,256]{2,1,0:T(8,128)(2,1)} %get-tuple-element.11), calls=%async_computation | async-start | bytes 1048576 | tf_op jit(solution)/shard_map/all_to_all | solution.py:309
  27.1 12.9 %collective-permute-start.4 = (bf16[1152,128]{1,0:T(8,128)(2,1)S(1)}, bf16[1152,128]{1,0:T(8,128)(2,1)S(1)}, u32[]{:S(2)}, u32[]{:S(2)}) collective-permute-start(bf16[1152,128]{1,0:T(8,128)(2,1)S(1)} %collective-permute-done.2.opposite), channel_id=1, source_target_pairs={{0,1},{1,0},{2,3},{3,2},{4,5},{5,4},{6,7},{7,6},{8,9},{9,8},{10,11... | collective-permute-start | bytes 884744 | tf_op jit(solution)/shard_map/ppermute | solution.py:313
  40.0 32.2 %copy-start = (f32[128]{0:T(128)S(1)}, f32[128]{0:T(128)}, u32[]{:S(2)}) copy-start(f32[128]{0:T(128)} %param.23) | copy-start | bytes 1540

commit v16 on v15

--- a/solution.py
+++ b/solution.py
@@ -132,7 +132,7 @@
 
 
 def attend_kernel(
-    got, near, opposite, far, far_opposite, early, lengths, frequencies, gain, latents, ropes,
+    got, near, last, far, far_last, early, lengths, frequencies, gain, latents, ropes,
     out, cache, cache_rope,
     sums, lifted, turned, scored, weights, means, sems,
     *, factor, nope,
@@ -175,10 +175,10 @@
     y = tp // 2
     core = lax.rem(tp, 2)
     for i in range(groups):
-        step = (0, half - 1, 1, 2)[i % half]
+        step = (0, 2, half - 1, 1)[i % half]
         head = 2 * lax.rem(y + step, half) + (core if i < half else 1 - core)
         q = sums[head]
-        w = weights_of((near, opposite, far, far_opposite), i)
+        w = weights_of((near, last, far, far_last), i)
         lifted[i] = dot(q[:, :nope].astype(BF16), w[:latent_width, :], NT)
         turned[i] = rotate(q[:, nope : nope + width].astype(BF16).astype(F32), cosine, sine)
     raw = jnp.concatenate([sums[h][0:1, nope + width :] for h in range(groups)], axis=1)
@@ -232,7 +232,7 @@
         mixed = dot(weights[r, :], cached(s), NN) + rounded[r] * new_latent
         means[s] = mixed * inverse[r]
     for i in range(groups):
-        w = weights_of((near, opposite, far, far_opposite), i)
+        w = weights_of((near, last, far, far_last), i)
         x = means[:, i, :].astype(BF16)
         up = dot(x, w[latent_width : 2 * latent_width, :], NN).astype(BF16)
         for k in range(kv_size):
@@ -261,13 +261,13 @@
 
 
 def weights_of(collected, i):
-    near, opposite, far, far_opposite = collected
+    near, last, far, far_last = collected
     places = near.shape[0] + 1
-    stacked, single = (near, opposite) if i < places else (far, far_opposite)
+    stacked, single = (near, last) if i < places else (far, far_last)
     return single if i % places == places - 1 else stacked.at[i % places]
 
 
-def combine_kernel(got, near, opposite, far, far_opposite, out, *, kv_size, groups, local, first):
+def combine_kernel(got, near, last, far, far_last, out, *, kv_size, groups, local, first):
     logs = []
     for k in range(kv_size):
         x = got[k, groups * local :, :].astype(F32)
@@ -283,7 +283,7 @@
         for k in range(kv_size):
             part = got[k, i * local : (i + 1) * local, :].astype(F32)
             head = head + part * shares[k][:, i : i + 1]
-        w = weights_of((near, opposite, far, far_opposite), i)
+        w = weights_of((near, last, far, far_last), i)
         mixed = mixed + dot(head.astype(BF16), w[first:, :], NN)
     mixed = mixed.astype(BF16)
     for d in range(out.shape[0]):
@@ -379,10 +379,10 @@
     )
 
     before, after, opposite = along(own)
-    near = jnp.stack([own, before, after])
+    near = jnp.stack([own, opposite, before])
     far = swap(near)
-    far_opposite = swap(opposite)
-    collected = (near, opposite, far, far_opposite)
+    far_last = swap(after)
+    collected = (near, after, far, far_last)
 
     got = exchange(sent, SPREAD)
     powers = np.arange(0, rope, 2, dtype=np.float64) / rope

time: 73.8 us -> 77.2 us (1.046)
  waiting for transfers between devices: 21.4 us -> 24.8 us
    ppermute x3, waiting for transfers between devices: 9.68 us -> 13 us  [along(): collected.append(lax.ppermute(own, TP, pairs))]
    all_to_all x1, starting transfers between devices: 11.4 us -> 9.88 us  [exchange(): return lax.all_to_all(value, axes, split_axis=0, concat_axis=0, tiled=True)]
    ppermute x3, starting transfers between devices: 3.28 us -> 4.73 us  [along(): collected.append(lax.ppermute(own, TP, pairs))]
where the time goes in v16:
time: 77.2 us; the launch traced here: 76.2 us
  blocking collectives  27.4 us (35%)
  waiting for transfers between devices  24.8 us (32%)
  starting transfers between devices  14.8 us (19%)
  Pallas kernels  9.06 us (12%)
    all_to_all x2, blocking collectives, exchange(): return lax.all_to_all(value, axes, split_axis=0, concat_axis=0, tiled=True)  27.4 us
    ppermute x3, waiting for transfers between devices, along(): collected.append(lax.ppermute(own, TP, pairs))  13 us
    all_to_all x1, waiting for transfers between devices, exchange(): return lax.all_to_all(value, axes, split_axis=0, concat_axis=0, tiled=True)  11.7 us
    all_to_all x1, starting transfers between devices, exchange(): return lax.all_to_all(value, axes, split_axis=0, concat_axis=0, tiled=True)  9.88 us
    ppermute x3, starting transfers between devices, along(): collected.append(lax.ppermute(own, TP, pairs))  4.73 us
    pallas_call x1, Pallas kernels, on_device(): pl.pallas_call(functools.partial(attend_kernel, factor=factor, nope=nope)...  4.22 us
    pallas_call x1, Pallas kernels, on_device(): pl.pallas_call(project_kernel, out_shape=(jax.ShapeDtypeStruct((everyone,...  2.52 us
  transfers between devices with their start and end apart: 6, of which 3 were waited for; matrix products, arithmetic and copies ran while one was open for 0% of the time, Pallas kernels for 1%

profile of v16, /device:TPU:0, one launch (start us, length us, event | category | flops | bytes accessed | tf_op | source)
XLA Modules:
  0.0 76.2 jit_solution(13446156284609292175)
XLA Ops:
  0.0 2.5 %project.1 = (bf16[128,8,256]{2,1,0:T(8,128)(2,1)}, bf16[1152,128]{1,0:T(8,128)(2,1)S(1)}) custom-call(bf16[64,128]{1,0:T(8,128)(2,1)} %tokens.1, f32[1,128]{1,0:T(1,128)} %bitcast.18, bf16[192,128]{1,0:T(8,128)(2,1)} %bitcast.15, bf16[128,512]{1,0:T(8,128)(2,1)} %wd.1, bf16[64,128]{1,0:T(8,128)(2,1)} %bitcast.16, bf16[1,512,128]{2,1,0:T(8,128)(2,1)} %wk.1, ...), custom_call_target="tpu_custom_call" | custom-call | tf_op jit(solution)/shard_map/project/pallas_call | solution.py:350
  2.5 1.8 %collective-permute-start.1 = (bf16[1152,128]{1,0:T(8,128)(2,1)S(1)}, bf16[1152,128]{1,0:T(8,128)(2,1)S(1)}, u32[]{:S(2)}, u32[]{:S(2)}) collective-permute-start(bf16[1152,128]{1,0:T(8,128)(2,1)S(1)} %get-tuple-element.12), channel_id=1, source_target_pairs={{0,2},{1,3},{2,4},{3,5},{4,6},{5,7},{6,0},{7,1},{8,10},{9,11},{10,... | collective-permute-start | bytes 884744 | tf_op jit(solution)/shard_map/ppermute | solution.py:321
  4.3 2.9 %collective-permute-start = (bf16[1152,128]{1,0:T(8,128)(2,1)S(1)}, bf16[1152,128]{1,0:T(8,128)(2,1)S(1)}, u32[]{:S(2)}, u32[]{:S(2)}) collective-permute-start(bf16[1152,128]{1,0:T(8,128)(2,1)S(1)} %get-tuple-element.12), channel_id=1, source_target_pairs={{0,4},{1,5},{2,6},{3,7},{4,0},{5,1},{6,2},{7,3},{8,12},{9,13},{10,... | collective-permute-start | bytes 884744 | tf_op jit(solution)/shard_map/ppermute | solution.py:321
  7.2 5.5 %collective-permute-done.1 = bf16[1152,128]{1,0:T(8,128)(2,1)S(1)} collective-permute-done((bf16[1152,128]{1,0:T(8,128)(2,1)S(1)}, bf16[1152,128]{1,0:T(8,128)(2,1)S(1)}, u32[]{:S(2)}, u32[]{:S(2)}) %collective-permute-start.1) | collective-permute-done | bytes 294944 | tf_op jit(solution)/shard_map/ppermute | solution.py:321
  12.7 7.5 %collective-permute-done = bf16[1152,128]{1,0:T(8,128)(2,1)S(1)} collective-permute-done((bf16[1152,128]{1,0:T(8,128)(2,1)S(1)}, bf16[1152,128]{1,0:T(8,128)(2,1)S(1)}, u32[]{:S(2)}, u32[]{:S(2)}) %collective-permute-start) | collective-permute-done | bytes 294944 | tf_op jit(solution)/shard_map/ppermute | solution.py:321
  20.2 0.1 pad_maximum_fusion.near
  20.3 0.1 collective-permute-start.3
  20.4 0.1 collective-permute-start.2
  20.5 9.9 %all-to-all-start = ((bf16[128,8,256]{2,1,0:T(8,128)(2,1)}), bf16[128,8,256]{2,1,0:T(8,128)(2,1)S(1)}, u32[]{:S(2)}, u32[]{:S(2)}) async-start(bf16[128,8,256]{2,1,0:T(8,128)(2,1)} %get-tuple-element.11), calls=%async_computation | async-start | bytes 1048576 | tf_op jit(solution)/shard_map/all_to_all | solution.py:309
  30.4 0.0 collective-permute-done.2.last
  30.4 0.1 collective-permute-start.4
  30.5 1.1 %bring.1 = (bf16[1,512,512]{2,1,0:T(8,128)(2,1)S(1)}, s32[1,64]{1,0:T(1,128)S(1)}, f32[1,64]{1,0:T(1,128)S(1)}, f32[1,512]{1,0:T(1,128)S(1)}) custom-call(bf16[8,512,512]{2,1,0:T(8,128)(2,1)} %latents.3, s32[1,64]{1,0:T(1,128)} %bitcast.19, f32[1,64]{1,0:T(1,128)} %constant.2.clone.frequencies_, f32[1,512]{1,0:T(1,128)} %bitcast.17), custom_call_target="tpu_custom_call" | custom-call | tf_op jit(solution)/shard_map/bring/pallas_call | solution.py:390
  31.6 11.7 %all-to-all-done.got = bf16[128,8,256]{2,1,0:T(8,128)(2,1)S(1)} async-done(((bf16[128,8,256]{2,1,0:T(8,128)(2,1)}), bf16[128,8,256]{2,1,0:T(8,128)(2,1)S(1)}, u32[]{:S(2)}, u32[]{:S(2)}) %all-to-all-start) | async-done | bytes 524320 | tf_op jit(solution)/shard_map/all_to_all | solution.py:309
  43.3 0.0 collective-permute-done.4.far_last
  43.3 0.0 collective-permute-done.3.far
  43.3 0.0 copy-start
  43.3 4.2 %attend.1 = bf16[16,72,128]{2,1,0:T(8,128)(2,1)S(1)} custom-call(bf16[128,8,256]{2,1,0:T(8,128)(2,1)S(1)} %all-to-all-done.got, bf16[3,1152,128]{2,1,0:T(8,128)(2,1)S(1)} %pad_maximum_fusion.near, bf16[1152,128]{1,0:T(8,128)(2,1)S(1)} %collective-permute-done.2.last, bf16[3,1152,128]{2,1,0:T(8,128)(2,1)S(1)} %collective-permute-done.3.far, ...), custom_call_target="tpu_custom_call" | custom-call | tf_op jit(solution)/shard_map/attend/pallas_call | solution.py:404
  47.6 13.1 %all_to_all.15.got = bf16[16,72,128]{2,1,0:T(8,128)(2,1)S(1)} all-to-all(bf16[16,72,128]{2,1,0:T(8,128)(2,1)S(1)} %attend.1), channel_id=1, replica_groups=mesh['kv_0'=4,'kv_1'=4,'y'=4,'core'=2] {'kv_0','kv_1'}, dimensions={0} | all-to-all | bytes 589824 | tf_op jit(solution)/shard_map/all_to_all | solution.py:309
  60.7 0.5 combine.1
  61.1 14.3 %all_to_all.16.got = bf16[128,8,128]{2,1,0:T(8,128)(2,1)S(1)} all-to-all(bf16[128,8,128]{2,1,0:T(8,128)(2,1)S(1)} %combine.1), channel_id=1, replica_groups=mesh['kv_0'=4,'kv_1'=4,'y'=4,'core'=2] {'core','kv_0','kv_1','y'}, dimensions={0} | all-to-all | bytes 524288 | tf_op jit(solution)/shard_map/all_to_all | solution.py:309
  75.5 0.0 copy-done
  75.5 0.8 finish.1
Async XLA Ops:
  2.5 10.2 %collective-permute-start.1 = (bf16[1152,128]{1,0:T(8,128)(2,1)S(1)}, bf16[1152,128]{1,0:T(8,128)(2,1)S(1)}, u32[]{:S(2)}, u32[]{:S(2)}) collective-permute-start(bf16[1152,128]{1,0:T(8,128)(2,1)S(1)} %get-tuple-element.12), channel_id=1, source_target_pairs={{0,2},{1,3},{2,4},{3,5},{4,6},{5,7},{6,0},{7,1},{8,10},{9,11},{10,... | collective-permute-start | bytes 884744 | tf_op jit(solution)/shard_map/ppermute | solution.py:321
  4.3 15.9 %collective-permute-start = (bf16[1152,128]{1,0:T(8,128)(2,1)S(1)}, bf16[1152,128]{1,0:T(8,128)(2,1)S(1)}, u32[]{:S(2)}, u32[]{:S(2)}) collective-permute-start(bf16[1152,128]{1,0:T(8,128)(2,1)S(1)} %get-tuple-element.12), channel_id=1, source_target_pairs={{0,4},{1,5},{2,6},{3,7},{4,0},{5,1},{6,2},{7,3},{8,12},{9,13},{10,... | collective-permute-start | bytes 884744 | tf_op jit(solution)/shard_map/ppermute | solution.py:321
  20.3 23.0 %collective-permute-start.3 = (bf16[3,1152,128]{2,1,0:T(8,128)(2,1)S(1)}, bf16[3,1152,128]{2,1,0:T(8,128)(2,1)S(1)}, u32[]{:S(2)}, u32[]{:S(2)}) collective-permute-start(bf16[3,1152,128]{2,1,0:T(8,128)(2,1)S(1)} %pad_maximum_fusion.near), channel_id=1, source_target_pairs={{0,1},{1,0},{2,3},{3,2},{4,5},{5,4},{6,7},{7,6},{8,9},{9,8},{10,11... | collective-permute-start | bytes 2654216 | tf_op jit(solution)/shard_map/ppermute | solution.py:313
  20.4 10.0 %collective-permute-start.2 = (bf16[1152,128]{1,0:T(8,128)(2,1)S(1)}, bf16[1152,128]{1,0:T(8,128)(2,1)S(1)}, u32[]{:S(2)}, u32[]{:S(2)}) collective-permute-start(bf16[1152,128]{1,0:T(8,128)(2,1)S(1)} %get-tuple-element.12), channel_id=1, source_target_pairs={{0,6},{1,7},{2,0},{3,1},{4,2},{5,3},{6,4},{7,5},{8,14},{9,15},{10,... | collective-permute-start | bytes 884744 | tf_op jit(solution)/shard_map/ppermute | solution.py:321
  20.5 22.8 %all-to-all-start = ((bf16[128,8,256]{2,1,0:T(8,128)(2,1)}), bf16[128,8,256]{2,1,0:T(8,128)(2,1)S(1)}, u32[]{:S(2)}, u32[]{:S(2)}) async-start(bf16[128,8,256]{2,1,0:T(8,128)(2,1)} %get-tuple-element.11), calls=%async_computation | async-start | bytes 1048576 | tf_op jit(solution)/shard_map/all_to_all | solution.py:309
  30.4 12.9 %collective-permute-start.4 = (bf16[1152,128]{1,0:T(8,128)(2,1)S(1)}, bf16[1152,128]{1,0:T(8,128)(2,1)S(1)}, u32[]{:S(2)}, u32[]{:S(2)}) collective-permute-start(bf16[1152,128]{1,0:T(8,128)(2,1)S(1)} %collective-permute-done.2.last), channel_id=1, source_target_pairs={{0,1},{1,0},{2,3},{3,2},{4,5},{5,4},{6,7},{7,6},{8,9},{9,8},{10,11... | collective-permute-start | bytes 884744 | tf_op jit(solution)/shard_map/ppermute | solution.py:313
  43.3 32.2 %copy-start = (f32[128]{0:T(128)S(1)}, f32[128]{0:T(128)}, u32[]{:S(2)}) copy-start(f32[128]{0:T(128)} %param.23) | copy-start | bytes 1540

commit v17 on v15

--- a/solution.py
+++ b/solution.py
@@ -175,8 +175,9 @@
     y = tp // 2
     core = lax.rem(tp, 2)
     for i in range(groups):
-        step = (0, half - 1, 1, 2)[i % half]
-        head = 2 * lax.rem(y + step, half) + (core if i < half else 1 - core)
+        source = core if i < half else 1 - core
+        step = (0, -1, 1, 2)[i % half] * (1 - 2 * source)
+        head = 2 * lax.rem(y + half + step, half) + source
         q = sums[head]
         w = weights_of((near, opposite, far, far_opposite), i)
         lifted[i] = dot(q[:, :nope].astype(BF16), w[:latent_width, :], NT)
@@ -317,7 +318,7 @@
     size = lax.axis_size(TP)
     collected = []
     for step in (1, 3, 2):
-        pairs = [(i, (i + 2 * step) % size) for i in range(size)]
+        pairs = [(i, (i + (2 - 4 * (i % 2)) * step) % size) for i in range(size)]
         collected.append(lax.ppermute(own, TP, pairs))
     return collected
 

time: 73.8 us -> 72.1 us (0.977)
  waiting for transfers between devices: 21.4 us -> 19.7 us
    ppermute x3, starting transfers between devices: 3.28 us -> 5.28 us  [along(): collected.append(lax.ppermute(own, TP, pairs))]
    all_to_all x1, starting transfers between devices: 11.4 us -> 9.39 us  [exchange(): return lax.all_to_all(value, axes, split_axis=0, concat_axis=0, tiled=True)]
    ppermute x3, waiting for transfers between devices: 9.68 us -> 7.93 us  [along(): collected.append(lax.ppermute(own, TP, pairs))]
  transfers between devices with their start and end apart: 6 -> 6, of which waited for: 3 -> 3; matrix products, arithmetic and copies ran while one was open for 0% -> 0% of each run, Pallas kernels for 1% -> 2%
where the time goes in v17:
time: 72.1 us; the launch traced here: 71.2 us
  blocking collectives  27.4 us (38%)
  waiting for transfers between devices  19.7 us (27%)
  starting transfers between devices  14.8 us (21%)
  Pallas kernels  9.06 us (13%)
    all_to_all x2, blocking collectives, exchange(): return lax.all_to_all(value, axes, split_axis=0, concat_axis=0, tiled=True)  27.4 us
    all_to_all x1, waiting for transfers between devices, exchange(): return lax.all_to_all(value, axes, split_axis=0, concat_axis=0, tiled=True)  11.7 us
    all_to_all x1, starting transfers between devices, exchange(): return lax.all_to_all(value, axes, split_axis=0, concat_axis=0, tiled=True)  9.39 us
    ppermute x3, waiting for transfers between devices, along(): collected.append(lax.ppermute(own, TP, pairs))  7.93 us
    ppermute x3, starting transfers between devices, along(): collected.append(lax.ppermute(own, TP, pairs))  5.28 us
    pallas_call x1, Pallas kernels, on_device(): pl.pallas_call(functools.partial(attend_kernel, factor=factor, nope=nope)...  4.22 us
    pallas_call x1, Pallas kernels, on_device(): pl.pallas_call(project_kernel, out_shape=(jax.ShapeDtypeStruct((everyone,...  2.52 us
  transfers between devices with their start and end apart: 6, of which 3 were waited for; matrix products, arithmetic and copies ran while one was open for 0% of the time, Pallas kernels for 2%

profile of v17, /device:TPU:0, one launch (start us, length us, event | category | flops | bytes accessed | tf_op | source)
XLA Modules:
  0.0 71.2 jit_solution(14455639960215620568)
XLA Ops:
  0.0 2.5 %project.1 = (bf16[128,8,256]{2,1,0:T(8,128)(2,1)}, bf16[1152,128]{1,0:T(8,128)(2,1)S(1)}) custom-call(bf16[64,128]{1,0:T(8,128)(2,1)} %tokens.1, f32[1,128]{1,0:T(1,128)} %bitcast.18, bf16[192,128]{1,0:T(8,128)(2,1)} %bitcast.15, bf16[128,512]{1,0:T(8,128)(2,1)} %wd.1, bf16[64,128]{1,0:T(8,128)(2,1)} %bitcast.16, bf16[1,512,128]{2,1,0:T(8,128)(2,1)} %wk.1, ...), custom_call_target="tpu_custom_call" | custom-call | tf_op jit(solution)/shard_map/project/pallas_call | solution.py:351
  2.5 3.2 %collective-permute-start.1 = (bf16[1152,128]{1,0:T(8,128)(2,1)S(1)}, bf16[1152,128]{1,0:T(8,128)(2,1)S(1)}, u32[]{:S(2)}, u32[]{:S(2)}) collective-permute-start(bf16[1152,128]{1,0:T(8,128)(2,1)S(1)} %get-tuple-element.12), channel_id=1, source_target_pairs={{0,6},{1,3},{2,0},{3,5},{4,2},{5,7},{6,4},{7,1},{8,14},{9,11},{10,... | collective-permute-start | bytes 884744 | tf_op jit(solution)/shard_map/ppermute | solution.py:322
  5.7 0.0 collective-permute-start
  5.7 6.5 %collective-permute-done.1 = bf16[1152,128]{1,0:T(8,128)(2,1)S(1)} collective-permute-done((bf16[1152,128]{1,0:T(8,128)(2,1)S(1)}, bf16[1152,128]{1,0:T(8,128)(2,1)S(1)}, u32[]{:S(2)}, u32[]{:S(2)}) %collective-permute-start.1) | collective-permute-done | bytes 294944 | tf_op jit(solution)/shard_map/ppermute | solution.py:322
  12.2 1.5 %collective-permute-done = bf16[1152,128]{1,0:T(8,128)(2,1)S(1)} collective-permute-done((bf16[1152,128]{1,0:T(8,128)(2,1)S(1)}, bf16[1152,128]{1,0:T(8,128)(2,1)S(1)}, u32[]{:S(2)}, u32[]{:S(2)}) %collective-permute-start) | collective-permute-done | bytes 294944 | tf_op jit(solution)/shard_map/ppermute | solution.py:322
  13.7 0.1 pad_maximum_fusion.near
  13.8 0.1 collective-permute-start.3
  13.9 2.1 %collective-permute-start.2 = (bf16[1152,128]{1,0:T(8,128)(2,1)S(1)}, bf16[1152,128]{1,0:T(8,128)(2,1)S(1)}, u32[]{:S(2)}, u32[]{:S(2)}) collective-permute-start(bf16[1152,128]{1,0:T(8,128)(2,1)S(1)} %get-tuple-element.12), channel_id=1, source_target_pairs={{0,4},{1,5},{2,6},{3,7},{4,0},{5,1},{6,2},{7,3},{8,12},{9,13},{10,... | collective-permute-start | bytes 884744 | tf_op jit(solution)/shard_map/ppermute | solution.py:322
  15.9 9.4 %all-to-all-start = ((bf16[128,8,256]{2,1,0:T(8,128)(2,1)}), bf16[128,8,256]{2,1,0:T(8,128)(2,1)S(1)}, u32[]{:S(2)}, u32[]{:S(2)}) async-start(bf16[128,8,256]{2,1,0:T(8,128)(2,1)} %get-tuple-element.11), calls=%async_computation | async-start | bytes 1048576 | tf_op jit(solution)/shard_map/all_to_all | solution.py:310
  25.3 0.0 collective-permute-done.2.opposite
  25.3 0.1 collective-permute-start.4
  25.4 1.1 %bring.1 = (bf16[1,512,512]{2,1,0:T(8,128)(2,1)S(1)}, s32[1,64]{1,0:T(1,128)S(1)}, f32[1,64]{1,0:T(1,128)S(1)}, f32[1,512]{1,0:T(1,128)S(1)}) custom-call(bf16[8,512,512]{2,1,0:T(8,128)(2,1)} %latents.3, s32[1,64]{1,0:T(1,128)} %bitcast.19, f32[1,64]{1,0:T(1,128)} %constant.2.clone.frequencies_, f32[1,512]{1,0:T(1,128)} %bitcast.17), custom_call_target="tpu_custom_call" | custom-call | tf_op jit(solution)/shard_map/bring/pallas_call | solution.py:391
  26.5 11.7 %all-to-all-done.got = bf16[128,8,256]{2,1,0:T(8,128)(2,1)S(1)} async-done(((bf16[128,8,256]{2,1,0:T(8,128)(2,1)}), bf16[128,8,256]{2,1,0:T(8,128)(2,1)S(1)}, u32[]{:S(2)}, u32[]{:S(2)}) %all-to-all-start) | async-done | bytes 524320 | tf_op jit(solution)/shard_map/all_to_all | solution.py:310
  38.3 0.0 collective-permute-done.4.far_opposite
  38.3 0.0 collective-permute-done.3.far
  38.3 0.0 copy-start
  38.3 4.2 %attend.1 = bf16[16,72,128]{2,1,0:T(8,128)(2,1)S(1)} custom-call(bf16[128,8,256]{2,1,0:T(8,128)(2,1)S(1)} %all-to-all-done.got, bf16[3,1152,128]{2,1,0:T(8,128)(2,1)S(1)} %pad_maximum_fusion.near, bf16[1152,128]{1,0:T(8,128)(2,1)S(1)} %collective-permute-done.2.opposite, bf16[3,1152,128]{2,1,0:T(8,128)(2,1)S(1)} %collective-permute-done.3.far, ...), custom_call_target="tpu_custom_call" | custom-call | tf_op jit(solution)/shard_map/attend/pallas_call | solution.py:405
  42.5 13.1 %all_to_all.15.got = bf16[16,72,128]{2,1,0:T(8,128)(2,1)S(1)} all-to-all(bf16[16,72,128]{2,1,0:T(8,128)(2,1)S(1)} %attend.1), channel_id=1, replica_groups=mesh['kv_0'=4,'kv_1'=4,'y'=4,'core'=2] {'kv_0','kv_1'}, dimensions={0} | all-to-all | bytes 589824 | tf_op jit(solution)/shard_map/all_to_all | solution.py:310
  55.6 0.5 combine.1
  56.1 14.3 %all_to_all.16.got = bf16[128,8,128]{2,1,0:T(8,128)(2,1)S(1)} all-to-all(bf16[128,8,128]{2,1,0:T(8,128)(2,1)S(1)} %combine.1), channel_id=1, replica_groups=mesh['kv_0'=4,'kv_1'=4,'y'=4,'core'=2] {'core','kv_0','kv_1','y'}, dimensions={0} | all-to-all | bytes 524288 | tf_op jit(solution)/shard_map/all_to_all | solution.py:310
  70.4 0.0 copy-done
  70.4 0.8 %finish.1 = bf16[64,128]{1,0:T(8,128)(2,1)} custom-call(bf16[128,8,128]{2,1,0:T(8,128)(2,1)S(1)} %all_to_all.16.got, f32[1,128]{1,0:T(1,128)S(1)} %bitcast.11), custom_call_target="tpu_custom_call" | custom-call | tf_op jit(solution)/shard_map/finish/pallas_call | solution.py:446
Async XLA Ops:
  2.5 9.7 %collective-permute-start.1 = (bf16[1152,128]{1,0:T(8,128)(2,1)S(1)}, bf16[1152,128]{1,0:T(8,128)(2,1)S(1)}, u32[]{:S(2)}, u32[]{:S(2)}) collective-permute-start(bf16[1152,128]{1,0:T(8,128)(2,1)S(1)} %get-tuple-element.12), channel_id=1, source_target_pairs={{0,6},{1,3},{2,0},{3,5},{4,2},{5,7},{6,4},{7,1},{8,14},{9,11},{10,... | collective-permute-start | bytes 884744 | tf_op jit(solution)/shard_map/ppermute | solution.py:322
  5.7 7.9 %collective-permute-start = (bf16[1152,128]{1,0:T(8,128)(2,1)S(1)}, bf16[1152,128]{1,0:T(8,128)(2,1)S(1)}, u32[]{:S(2)}, u32[]{:S(2)}) collective-permute-start(bf16[1152,128]{1,0:T(8,128)(2,1)S(1)} %get-tuple-element.12), channel_id=1, source_target_pairs={{0,2},{1,7},{2,4},{3,1},{4,6},{5,3},{6,0},{7,5},{8,10},{9,15},{10,... | collective-permute-start | bytes 884744 | tf_op jit(solution)/shard_map/ppermute | solution.py:322
  13.8 24.5 %collective-permute-start.3 = (bf16[3,1152,128]{2,1,0:T(8,128)(2,1)S(1)}, bf16[3,1152,128]{2,1,0:T(8,128)(2,1)S(1)}, u32[]{:S(2)}, u32[]{:S(2)}) collective-permute-start(bf16[3,1152,128]{2,1,0:T(8,128)(2,1)S(1)} %pad_maximum_fusion.near), channel_id=1, source_target_pairs={{0,1},{1,0},{2,3},{3,2},{4,5},{5,4},{6,7},{7,6},{8,9},{9,8},{10,11... | collective-permute-start | bytes 2654216 | tf_op jit(solution)/shard_map/ppermute | solution.py:314
  13.9 11.5 %collective-permute-start.2 = (bf16[1152,128]{1,0:T(8,128)(2,1)S(1)}, bf16[1152,128]{1,0:T(8,128)(2,1)S(1)}, u32[]{:S(2)}, u32[]{:S(2)}) collective-permute-start(bf16[1152,128]{1,0:T(8,128)(2,1)S(1)} %get-tuple-element.12), channel_id=1, source_target_pairs={{0,4},{1,5},{2,6},{3,7},{4,0},{5,1},{6,2},{7,3},{8,12},{9,13},{10,... | collective-permute-start | bytes 884744 | tf_op jit(solution)/shard_map/ppermute | solution.py:322
  15.9 22.3 %all-to-all-start = ((bf16[128,8,256]{2,1,0:T(8,128)(2,1)}), bf16[128,8,256]{2,1,0:T(8,128)(2,1)S(1)}, u32[]{:S(2)}, u32[]{:S(2)}) async-start(bf16[128,8,256]{2,1,0:T(8,128)(2,1)} %get-tuple-element.11), calls=%async_computation | async-start | bytes 1048576 | tf_op jit(solution)/shard_map/all_to_all | solution.py:310
  25.3 12.9 %collective-permute-start.4 = (bf16[1152,128]{1,0:T(8,128)(2,1)S(1)}, bf16[1152,128]{1,0:T(8,128)(2,1)S(1)}, u32[]{:S(2)}, u32[]{:S(2)}) collective-permute-start(bf16[1152,128]{1,0:T(8,128)(2,1)S(1)} %collective-permute-done.2.opposite), channel_id=1, source_target_pairs={{0,1},{1,0},{2,3},{3,2},{4,5},{5,4},{6,7},{7,6},{8,9},{9,8},{10,11... | collective-permute-start | bytes 884744 | tf_op jit(solution)/shard_map/ppermute | solution.py:314
  38.3 32.2 %copy-start = (f32[128]{0:T(128)S(1)}, f32[128]{0:T(128)}, u32[]{:S(2)}) copy-start(f32[128]{0:T(128)} %param.23) | copy-start | bytes 1540

commit v18 on v15

--- a/solution.py
+++ b/solution.py
@@ -90,23 +90,21 @@
         part = jnp.where(tp == g, latent[:, g * chunk : (g + 1) * chunk], part)
     width = rope.shape[1]
     rope = jnp.where(lanes(rope.shape) // (width // groups) == tp, rope, 0.0)
-    blank = jnp.zeros((seqs, 128 - width), F32)
-    part = jnp.concatenate([blank, part], axis=1)
-    rope = jnp.concatenate([blank, rope], axis=1)
     first = query[:, :128].astype(BF16)
-    second = jnp.concatenate([query[:, 128:], blank], axis=1)
-    row = rows((local, 128))
+    fresh = jnp.concatenate([part, rope], axis=1)
+    nothing = jnp.zeros((1, 128), F32)
     for t in range(groups):
-        top = first[t * local : (t + 1) * local]
-        low = second[t * local : (t + 1) * local]
+        turn = query[t * local : (t + 1) * local, 128:]
+        turn = jnp.concatenate([turn[: local // 2], turn[local // 2 :]], axis=1).astype(BF16)
+        tiles = [first[t * local + n : t * local + n + 2] for n in range(0, local, 2)]
+        tiles += [turn[n : n + 2] for n in range(0, local // 2, 2)]
         for j in range(local):
             r = t * local + j
-            new = jnp.where(row == 0, part[r : r + 1], 0.0) + jnp.where(row == 1, rope[r : r + 1], 0.0)
-            tile = (low + new).astype(BF16)
+            new = jnp.concatenate([fresh[r : r + 1], nothing], axis=0).astype(BF16)
             for c in range(kv_size // local):
                 b = block_of(c * local + j, t, kv_size)
-                out[b, :, :128] = top
-                out[b, :, 128:] = tile
+                for n, tile in enumerate(tiles + [new]):
+                    out[b, :, n * 128 : (n + 1) * 128] = tile
     for copy in copies[5:]:
         copy.wait()
 
@@ -161,7 +159,14 @@
         total = got[block_of(0, h, kv_size)].astype(F32)
         for k in range(1, kv_size):
             total = total + got[block_of(k, h, kv_size)].astype(F32)
-        sums[h] = total
+        pieces = [total[:, n * 128 : (n + 1) * 128] for n in range(7)]
+        turn = jnp.concatenate(pieces[4:6], axis=0)
+        sums[h, :, :nope] = jnp.concatenate(pieces[:4], axis=0)
+        sums[h, :, nope : nope + width] = jnp.concatenate(
+            [turn[:, :width], turn[:, width:]], axis=0
+        )
+        sums[h, 0:1, nope + width :] = pieces[6][0:1, :width]
+        sums[h, 1:2, nope + width :] = pieces[6][0:1, width:]
     shape = (local, lengths.shape[1])
     length = jnp.sum(
         jnp.where(lanes(shape) == rows(shape) + tp * local, lengths[...], 0), axis=1, keepdims=True
@@ -350,7 +355,7 @@
     sent, own = pl.pallas_call(
         project_kernel,
         out_shape=(
-            jax.ShapeDtypeStruct((everyone, local, 256), BF16),
+            jax.ShapeDtypeStruct((everyone, 2, 896), BF16),
             jax.ShapeDtypeStruct((2 * latent_width + value, nope), BF16),
         ),
         in_specs=[in_hbm()] * 8,

time: 73.8 us -> 73.3 us (level)
  transfers between devices with their start and end apart: 6 -> 6, of which waited for: 3 -> 3; matrix products, arithmetic and copies ran while one was open for 0% -> 0% of each run, Pallas kernels for 1% -> 2%
where the time goes in v18:
time: 73.3 us; the launch traced here: 72.4 us
  blocking collectives  27.4 us (37%)
  waiting for transfers between devices  20.7 us (28%)
  starting transfers between devices  14.8 us (20%)
  Pallas kernels  9.22 us (13%)
    all_to_all x2, blocking collectives, exchange(): return lax.all_to_all(value, axes, split_axis=0, concat_axis=0, tiled=True)  27.4 us
    all_to_all x1, starting transfers between devices, exchange(): return lax.all_to_all(value, axes, split_axis=0, concat_axis=0, tiled=True)  11.4 us
    all_to_all x1, waiting for transfers between devices, exchange(): return lax.all_to_all(value, axes, split_axis=0, concat_axis=0, tiled=True)  11.1 us
    ppermute x3, waiting for transfers between devices, along(): collected.append(lax.ppermute(own, TP, pairs))  9.68 us
    pallas_call x1, Pallas kernels, on_device(): pl.pallas_call(functools.partial(attend_kernel, factor=factor, nope=nope)...  4.3 us
    ppermute x3, starting transfers between devices, along(): collected.append(lax.ppermute(own, TP, pairs))  3.28 us
    pallas_call x1, Pallas kernels, on_device(): pl.pallas_call(project_kernel, out_shape=(jax.ShapeDtypeStruct((everyone,...  2.6 us
  transfers between devices with their start and end apart: 6, of which 3 were waited for; matrix products, arithmetic and copies ran while one was open for 0% of the time, Pallas kernels for 2%

profile of v18, /device:TPU:0, one launch (start us, length us, event | category | flops | bytes accessed | tf_op | source)
XLA Modules:
  0.0 72.4 jit_solution(10163783586374622827)
XLA Ops:
  0.0 2.6 %project.1 = (bf16[128,2,896]{2,1,0:T(2,128)(2,1)}, bf16[1152,128]{1,0:T(8,128)(2,1)S(1)}) custom-call(bf16[64,128]{1,0:T(8,128)(2,1)} %tokens.1, f32[1,128]{1,0:T(1,128)} %bitcast.18, bf16[192,128]{1,0:T(8,128)(2,1)} %bitcast.15, bf16[128,512]{1,0:T(8,128)(2,1)} %wd.1, bf16[64,128]{1,0:T(8,128)(2,1)} %bitcast.16, bf16[1,512,128]{2,1,0:T(8,128)(2,1)} %wk.1, ...), custom_call_target="tpu_custom_call" | custom-call | tf_op jit(solution)/shard_map/project/pallas_call | solution.py:355
  2.6 3.2 %collective-permute-start.1 = (bf16[1152,128]{1,0:T(8,128)(2,1)S(1)}, bf16[1152,128]{1,0:T(8,128)(2,1)S(1)}, u32[]{:S(2)}, u32[]{:S(2)}) collective-permute-start(bf16[1152,128]{1,0:T(8,128)(2,1)S(1)} %get-tuple-element.12), channel_id=1, source_target_pairs={{0,6},{1,7},{2,0},{3,1},{4,2},{5,3},{6,4},{7,5},{8,14},{9,15},{10,... | collective-permute-start | bytes 884744 | tf_op jit(solution)/shard_map/ppermute | solution.py:326
  5.8 0.0 collective-permute-start
  5.8 6.3 %collective-permute-done.1 = bf16[1152,128]{1,0:T(8,128)(2,1)S(1)} collective-permute-done((bf16[1152,128]{1,0:T(8,128)(2,1)S(1)}, bf16[1152,128]{1,0:T(8,128)(2,1)S(1)}, u32[]{:S(2)}, u32[]{:S(2)}) %collective-permute-start.1) | collective-permute-done | bytes 294944 | tf_op jit(solution)/shard_map/ppermute | solution.py:326
  12.1 3.4 %collective-permute-done = bf16[1152,128]{1,0:T(8,128)(2,1)S(1)} collective-permute-done((bf16[1152,128]{1,0:T(8,128)(2,1)S(1)}, bf16[1152,128]{1,0:T(8,128)(2,1)S(1)}, u32[]{:S(2)}, u32[]{:S(2)}) %collective-permute-start) | collective-permute-done | bytes 294944 | tf_op jit(solution)/shard_map/ppermute | solution.py:326
  15.5 0.1 pad_maximum_fusion.near
  15.6 0.1 collective-permute-start.3
  15.7 0.1 collective-permute-start.2
  15.8 11.4 %all-to-all-start = ((bf16[128,2,896]{2,1,0:T(2,128)(2,1)}), bf16[128,2,896]{2,1,0:T(2,128)(2,1)S(1)}, u32[]{:S(2)}, u32[]{:S(2)}) async-start(bf16[128,2,896]{2,1,0:T(2,128)(2,1)} %get-tuple-element.11), calls=%async_computation | async-start | bytes 917504 | tf_op jit(solution)/shard_map/all_to_all | solution.py:314
  27.2 0.0 collective-permute-done.2.opposite
  27.2 0.1 collective-permute-start.4
  27.3 1.1 %bring.1 = (bf16[1,512,512]{2,1,0:T(8,128)(2,1)S(1)}, s32[1,64]{1,0:T(1,128)S(1)}, f32[1,64]{1,0:T(1,128)S(1)}, f32[1,512]{1,0:T(1,128)S(1)}) custom-call(bf16[8,512,512]{2,1,0:T(8,128)(2,1)} %latents.3, s32[1,64]{1,0:T(1,128)} %bitcast.19, f32[1,64]{1,0:T(1,128)} %constant.2.clone.frequencies_, f32[1,512]{1,0:T(1,128)} %bitcast.17), custom_call_target="tpu_custom_call" | custom-call | tf_op jit(solution)/shard_map/bring/pallas_call | solution.py:395
  28.4 11.1 %all-to-all-done.got = bf16[128,2,896]{2,1,0:T(2,128)(2,1)S(1)} async-done(((bf16[128,2,896]{2,1,0:T(2,128)(2,1)}), bf16[128,2,896]{2,1,0:T(2,128)(2,1)S(1)}, u32[]{:S(2)}, u32[]{:S(2)}) %all-to-all-start) | async-done | bytes 458784 | tf_op jit(solution)/shard_map/all_to_all | solution.py:314
  39.4 0.0 collective-permute-done.4.far_opposite
  39.4 0.0 collective-permute-done.3.far
  39.4 0.0 copy-start
  39.4 4.3 %attend.1 = bf16[16,72,128]{2,1,0:T(8,128)(2,1)S(1)} custom-call(bf16[128,2,896]{2,1,0:T(2,128)(2,1)S(1)} %all-to-all-done.got, bf16[3,1152,128]{2,1,0:T(8,128)(2,1)S(1)} %pad_maximum_fusion.near, bf16[1152,128]{1,0:T(8,128)(2,1)S(1)} %collective-permute-done.2.opposite, bf16[3,1152,128]{2,1,0:T(8,128)(2,1)S(1)} %collective-permute-done.3.far, ...), custom_call_target="tpu_custom_call" | custom-call | tf_op jit(solution)/shard_map/attend/pallas_call | solution.py:409
  43.7 13.1 %all_to_all.15.got = bf16[16,72,128]{2,1,0:T(8,128)(2,1)S(1)} all-to-all(bf16[16,72,128]{2,1,0:T(8,128)(2,1)S(1)} %attend.1), channel_id=1, replica_groups=mesh['kv_0'=4,'kv_1'=4,'y'=4,'core'=2] {'kv_0','kv_1'}, dimensions={0} | all-to-all | bytes 589824 | tf_op jit(solution)/shard_map/all_to_all | solution.py:314
  56.8 0.5 combine.1
  57.3 14.3 %all_to_all.16.got = bf16[128,8,128]{2,1,0:T(8,128)(2,1)S(1)} all-to-all(bf16[128,8,128]{2,1,0:T(8,128)(2,1)S(1)} %combine.1), channel_id=1, replica_groups=mesh['kv_0'=4,'kv_1'=4,'y'=4,'core'=2] {'core','kv_0','kv_1','y'}, dimensions={0} | all-to-all | bytes 524288 | tf_op jit(solution)/shard_map/all_to_all | solution.py:314
  71.6 0.0 copy-done
  71.6 0.8 %finish.1 = bf16[64,128]{1,0:T(8,128)(2,1)} custom-call(bf16[128,8,128]{2,1,0:T(8,128)(2,1)S(1)} %all_to_all.16.got, f32[1,128]{1,0:T(1,128)S(1)} %bitcast.11), custom_call_target="tpu_custom_call" | custom-call | tf_op jit(solution)/shard_map/finish/pallas_call | solution.py:450
Async XLA Ops:
  2.6 9.5 %collective-permute-start.1 = (bf16[1152,128]{1,0:T(8,128)(2,1)S(1)}, bf16[1152,128]{1,0:T(8,128)(2,1)S(1)}, u32[]{:S(2)}, u32[]{:S(2)}) collective-permute-start(bf16[1152,128]{1,0:T(8,128)(2,1)S(1)} %get-tuple-element.12), channel_id=1, source_target_pairs={{0,6},{1,7},{2,0},{3,1},{4,2},{5,3},{6,4},{7,5},{8,14},{9,15},{10,... | collective-permute-start | bytes 884744 | tf_op jit(solution)/shard_map/ppermute | solution.py:326
  5.8 9.7 %collective-permute-start = (bf16[1152,128]{1,0:T(8,128)(2,1)S(1)}, bf16[1152,128]{1,0:T(8,128)(2,1)S(1)}, u32[]{:S(2)}, u32[]{:S(2)}) collective-permute-start(bf16[1152,128]{1,0:T(8,128)(2,1)S(1)} %get-tuple-element.12), channel_id=1, source_target_pairs={{0,2},{1,3},{2,4},{3,5},{4,6},{5,7},{6,0},{7,1},{8,10},{9,11},{10,... | collective-permute-start | bytes 884744 | tf_op jit(solution)/shard_map/ppermute | solution.py:326
  15.6 23.8 %collective-permute-start.3 = (bf16[3,1152,128]{2,1,0:T(8,128)(2,1)S(1)}, bf16[3,1152,128]{2,1,0:T(8,128)(2,1)S(1)}, u32[]{:S(2)}, u32[]{:S(2)}) collective-permute-start(bf16[3,1152,128]{2,1,0:T(8,128)(2,1)S(1)} %pad_maximum_fusion.near), channel_id=1, source_target_pairs={{0,1},{1,0},{2,3},{3,2},{4,5},{5,4},{6,7},{7,6},{8,9},{9,8},{10,11... | collective-permute-start | bytes 2654216 | tf_op jit(solution)/shard_map/ppermute | solution.py:318
  15.7 11.5 %collective-permute-start.2 = (bf16[1152,128]{1,0:T(8,128)(2,1)S(1)}, bf16[1152,128]{1,0:T(8,128)(2,1)S(1)}, u32[]{:S(2)}, u32[]{:S(2)}) collective-permute-start(bf16[1152,128]{1,0:T(8,128)(2,1)S(1)} %get-tuple-element.12), channel_id=1, source_target_pairs={{0,4},{1,5},{2,6},{3,7},{4,0},{5,1},{6,2},{7,3},{8,12},{9,13},{10,... | collective-permute-start | bytes 884744 | tf_op jit(solution)/shard_map/ppermute | solution.py:326
  15.8 23.6 %all-to-all-start = ((bf16[128,2,896]{2,1,0:T(2,128)(2,1)}), bf16[128,2,896]{2,1,0:T(2,128)(2,1)S(1)}, u32[]{:S(2)}, u32[]{:S(2)}) async-start(bf16[128,2,896]{2,1,0:T(2,128)(2,1)} %get-tuple-element.11), calls=%async_computation | async-start | bytes 917504 | tf_op jit(solution)/shard_map/all_to_all | solution.py:314
  27.2 12.2 %collective-permute-start.4 = (bf16[1152,128]{1,0:T(8,128)(2,1)S(1)}, bf16[1152,128]{1,0:T(8,128)(2,1)S(1)}, u32[]{:S(2)}, u32[]{:S(2)}) collective-permute-start(bf16[1152,128]{1,0:T(8,128)(2,1)S(1)} %collective-permute-done.2.opposite), channel_id=1, source_target_pairs={{0,1},{1,0},{2,3},{3,2},{4,5},{5,4},{6,7},{7,6},{8,9},{9,8},{10,11... | collective-permute-start | bytes 884744 | tf_op jit(solution)/shard_map/ppermute | solution.py:318
  39.4 32.2 %copy-start = (f32[128]{0:T(128)S(1)}, f32[128]{0:T(128)}, u32[]{:S(2)}) copy-start(f32[128]{0:T(128)} %param.23) | copy-start | bytes 1540

commit v19 on v14

--- a/solution.py
+++ b/solution.py
@@ -90,23 +90,21 @@
         part = jnp.where(tp == g, latent[:, g * chunk : (g + 1) * chunk], part)
     width = rope.shape[1]
     rope = jnp.where(lanes(rope.shape) // (width // groups) == tp, rope, 0.0)
-    blank = jnp.zeros((seqs, 128 - width), F32)
-    part = jnp.concatenate([blank, part], axis=1)
-    rope = jnp.concatenate([blank, rope], axis=1)
     first = query[:, :128].astype(BF16)
-    second = jnp.concatenate([query[:, 128:], blank], axis=1)
-    row = rows((local, 128))
+    fresh = jnp.concatenate([part, rope], axis=1)
+    nothing = jnp.zeros((1, 128), F32)
     for t in range(groups):
-        top = first[t * local : (t + 1) * local]
-        low = second[t * local : (t + 1) * local]
+        turn = query[t * local : (t + 1) * local, 128:]
+        turn = jnp.concatenate([turn[: local // 2], turn[local // 2 :]], axis=1).astype(BF16)
+        tiles = [first[t * local + n : t * local + n + 2] for n in range(0, local, 2)]
+        tiles += [turn[n : n + 2] for n in range(0, local // 2, 2)]
         for j in range(local):
             r = t * local + j
-            new = jnp.where(row == 0, part[r : r + 1], 0.0) + jnp.where(row == 1, rope[r : r + 1], 0.0)
-            tile = (low + new).astype(BF16)
+            new = jnp.concatenate([fresh[r : r + 1], nothing], axis=0).astype(BF16)
             for c in range(kv_size // local):
                 b = block_of(c * local + j, t, kv_size)
-                out[b, :, :128] = top
-                out[b, :, 128:] = tile
+                for n, tile in enumerate(tiles + [new]):
+                    out[b, :, n * 128 : (n + 1) * 128] = tile
     for copy in copies[5:]:
         copy.wait()
 
@@ -146,7 +144,14 @@
         total = got[block_of(0, h, kv_size)].astype(F32)
         for k in range(1, kv_size):
             total = total + got[block_of(k, h, kv_size)].astype(F32)
-        sums[h] = total
+        pieces = [total[:, n * 128 : (n + 1) * 128] for n in range(7)]
+        turn = jnp.concatenate(pieces[4:6], axis=0)
+        sums[h, :, :nope] = jnp.concatenate(pieces[:4], axis=0)
+        sums[h, :, nope : nope + width] = jnp.concatenate(
+            [turn[:, :width], turn[:, width:]], axis=0
+        )
+        sums[h, 0:1, nope + width :] = pieces[6][0:1, :width]
+        sums[h, 1:2, nope + width :] = pieces[6][0:1, width:]
     for copy in small:
         copy.wait()
     shape = (local, lengths.shape[1])
@@ -337,7 +342,7 @@
     sent, own = pl.pallas_call(
         project_kernel,
         out_shape=(
-            jax.ShapeDtypeStruct((everyone, local, 256), BF16),
+            jax.ShapeDtypeStruct((everyone, 2, 896), BF16),
             jax.ShapeDtypeStruct((2 * latent_width + value, nope), BF16),
         ),
         in_specs=[in_hbm()] * 8,

time: 74 us -> 73.4 us (level)
  no operation moved by 1% of the time
where the time goes in v19:
time: 73.4 us; the launch traced here: 72.5 us
  blocking collectives  27.4 us (37%)
  waiting for transfers between devices  21.8 us (30%)
  starting transfers between devices  14.8 us (20%)
  Pallas kernels  8.25 us (11%)
    all_to_all x2, blocking collectives, exchange(): return lax.all_to_all(value, axes, split_axis=0, concat_axis=0, tiled=True)  27.4 us
    all_to_all x1, waiting for transfers between devices, exchange(): return lax.all_to_all(value, axes, split_axis=0, concat_axis=0, tiled=True)  12.2 us
    all_to_all x1, starting transfers between devices, exchange(): return lax.all_to_all(value, axes, split_axis=0, concat_axis=0, tiled=True)  11.4 us
    ppermute x3, waiting for transfers between devices, along(): collected.append(lax.ppermute(own, TP, pairs))  9.68 us
    pallas_call x1, Pallas kernels, on_device(): pl.pallas_call(functools.partial(attend_kernel, factor=factor, nope=nope)...  4.41 us
    ppermute x3, starting transfers between devices, along(): collected.append(lax.ppermute(own, TP, pairs))  3.28 us
    pallas_call x1, Pallas kernels, on_device(): pl.pallas_call(project_kernel, out_shape=(jax.ShapeDtypeStruct((everyone,...  2.61 us
  transfers between devices with their start and end apart: 6, of which 3 were waited for; matrix products, arithmetic and copies ran while one was open for 0% of the time, Pallas kernels for 0%

profile of v19, /device:TPU:0, one launch (start us, length us, event | category | flops | bytes accessed | tf_op | source)
XLA Modules:
  0.0 72.5 jit_solution(15186169751005868318)
XLA Ops:
  0.0 2.6 %project.1 = (bf16[128,2,896]{2,1,0:T(2,128)(2,1)}, bf16[1152,128]{1,0:T(8,128)(2,1)S(1)}) custom-call(bf16[64,128]{1,0:T(8,128)(2,1)} %tokens.1, f32[1,128]{1,0:T(1,128)} %bitcast.18, bf16[192,128]{1,0:T(8,128)(2,1)} %bitcast.15, bf16[128,512]{1,0:T(8,128)(2,1)} %wd.1, bf16[64,128]{1,0:T(8,128)(2,1)} %bitcast.16, bf16[1,512,128]{2,1,0:T(8,128)(2,1)} %wk.1, ...), custom_call_target="tpu_custom_call" | custom-call | tf_op jit(solution)/shard_map/project/pallas_call | solution.py:342
  2.6 3.2 %collective-permute-start.1 = (bf16[1152,128]{1,0:T(8,128)(2,1)S(1)}, bf16[1152,128]{1,0:T(8,128)(2,1)S(1)}, u32[]{:S(2)}, u32[]{:S(2)}) collective-permute-start(bf16[1152,128]{1,0:T(8,128)(2,1)S(1)} %get-tuple-element.8), channel_id=1, source_target_pairs={{0,6},{1,7},{2,0},{3,1},{4,2},{5,3},{6,4},{7,5},{8,14},{9,15},{10,... | collective-permute-start | bytes 884744 | tf_op jit(solution)/shard_map/ppermute | solution.py:313
  5.8 0.0 collective-permute-start
  5.8 6.3 %collective-permute-done.1 = bf16[1152,128]{1,0:T(8,128)(2,1)S(1)} collective-permute-done((bf16[1152,128]{1,0:T(8,128)(2,1)S(1)}, bf16[1152,128]{1,0:T(8,128)(2,1)S(1)}, u32[]{:S(2)}, u32[]{:S(2)}) %collective-permute-start.1) | collective-permute-done | bytes 294944 | tf_op jit(solution)/shard_map/ppermute | solution.py:313
  12.1 3.4 %collective-permute-done = bf16[1152,128]{1,0:T(8,128)(2,1)S(1)} collective-permute-done((bf16[1152,128]{1,0:T(8,128)(2,1)S(1)}, bf16[1152,128]{1,0:T(8,128)(2,1)S(1)}, u32[]{:S(2)}, u32[]{:S(2)}) %collective-permute-start) | collective-permute-done | bytes 294944 | tf_op jit(solution)/shard_map/ppermute | solution.py:313
  15.5 0.1 pad_maximum_fusion.near
  15.6 0.1 collective-permute-start.3
  15.7 0.1 collective-permute-start.2
  15.8 11.4 %all-to-all-start = ((bf16[128,2,896]{2,1,0:T(2,128)(2,1)}), bf16[128,2,896]{2,1,0:T(2,128)(2,1)S(1)}, u32[]{:S(2)}, u32[]{:S(2)}) async-start(bf16[128,2,896]{2,1,0:T(2,128)(2,1)} %get-tuple-element.7), calls=%async_computation | async-start | bytes 917504 | tf_op jit(solution)/shard_map/all_to_all | solution.py:301
  27.2 0.0 collective-permute-done.2.opposite
  27.2 0.1 collective-permute-start.4
  27.3 12.2 %all-to-all-done.got = bf16[128,2,896]{2,1,0:T(2,128)(2,1)S(1)} async-done(((bf16[128,2,896]{2,1,0:T(2,128)(2,1)}), bf16[128,2,896]{2,1,0:T(2,128)(2,1)S(1)}, u32[]{:S(2)}, u32[]{:S(2)}) %all-to-all-start) | async-done | bytes 458784 | tf_op jit(solution)/shard_map/all_to_all | solution.py:301
  39.4 0.0 collective-permute-done.4.far_opposite
  39.4 0.0 collective-permute-done.3.far
  39.4 0.0 copy-start
  39.4 4.4 %attend.1 = bf16[16,72,128]{2,1,0:T(8,128)(2,1)S(1)} custom-call(bf16[128,2,896]{2,1,0:T(2,128)(2,1)S(1)} %all-to-all-done.got, bf16[3,1152,128]{2,1,0:T(8,128)(2,1)S(1)} %pad_maximum_fusion.near, bf16[1152,128]{1,0:T(8,128)(2,1)S(1)} %collective-permute-done.2.opposite, bf16[3,1152,128]{2,1,0:T(8,128)(2,1)S(1)} %collective-permute-done.3.far, ...), custom_call_target="tpu_custom_call" | custom-call | tf_op jit(solution)/shard_map/attend/pallas_call | solution.py:382
  43.9 13.1 %all_to_all.15.got = bf16[16,72,128]{2,1,0:T(8,128)(2,1)S(1)} all-to-all(bf16[16,72,128]{2,1,0:T(8,128)(2,1)S(1)} %attend.1), channel_id=1, replica_groups=mesh['kv_0'=4,'kv_1'=4,'y'=4,'core'=2] {'kv_0','kv_1'}, dimensions={0} | all-to-all | bytes 589824 | tf_op jit(solution)/shard_map/all_to_all | solution.py:301
  56.9 0.5 combine.1
  57.4 14.3 %all_to_all.16.got = bf16[128,8,128]{2,1,0:T(8,128)(2,1)S(1)} all-to-all(bf16[128,8,128]{2,1,0:T(8,128)(2,1)S(1)} %combine.1), channel_id=1, replica_groups=mesh['kv_0'=4,'kv_1'=4,'y'=4,'core'=2] {'core','kv_0','kv_1','y'}, dimensions={0} | all-to-all | bytes 524288 | tf_op jit(solution)/shard_map/all_to_all | solution.py:301
  71.7 0.0 copy-done
  71.7 0.8 %finish.1 = bf16[64,128]{1,0:T(8,128)(2,1)} custom-call(bf16[128,8,128]{2,1,0:T(8,128)(2,1)S(1)} %all_to_all.16.got, f32[1,128]{1,0:T(1,128)S(1)} %bitcast.11), custom_call_target="tpu_custom_call" | custom-call | tf_op jit(solution)/shard_map/finish/pallas_call | solution.py:431
Async XLA Ops:
  2.6 9.5 %collective-permute-start.1 = (bf16[1152,128]{1,0:T(8,128)(2,1)S(1)}, bf16[1152,128]{1,0:T(8,128)(2,1)S(1)}, u32[]{:S(2)}, u32[]{:S(2)}) collective-permute-start(bf16[1152,128]{1,0:T(8,128)(2,1)S(1)} %get-tuple-element.8), channel_id=1, source_target_pairs={{0,6},{1,7},{2,0},{3,1},{4,2},{5,3},{6,4},{7,5},{8,14},{9,15},{10,... | collective-permute-start | bytes 884744 | tf_op jit(solution)/shard_map/ppermute | solution.py:313
  5.8 9.7 %collective-permute-start = (bf16[1152,128]{1,0:T(8,128)(2,1)S(1)}, bf16[1152,128]{1,0:T(8,128)(2,1)S(1)}, u32[]{:S(2)}, u32[]{:S(2)}) collective-permute-start(bf16[1152,128]{1,0:T(8,128)(2,1)S(1)} %get-tuple-element.8), channel_id=1, source_target_pairs={{0,2},{1,3},{2,4},{3,5},{4,6},{5,7},{6,0},{7,1},{8,10},{9,11},{10,... | collective-permute-start | bytes 884744 | tf_op jit(solution)/shard_map/ppermute | solution.py:313
  15.6 23.8 %collective-permute-start.3 = (bf16[3,1152,128]{2,1,0:T(8,128)(2,1)S(1)}, bf16[3,1152,128]{2,1,0:T(8,128)(2,1)S(1)}, u32[]{:S(2)}, u32[]{:S(2)}) collective-permute-start(bf16[3,1152,128]{2,1,0:T(8,128)(2,1)S(1)} %pad_maximum_fusion.near), channel_id=1, source_target_pairs={{0,1},{1,0},{2,3},{3,2},{4,5},{5,4},{6,7},{7,6},{8,9},{9,8},{10,11... | collective-permute-start | bytes 2654216 | tf_op jit(solution)/shard_map/ppermute | solution.py:305
  15.7 11.5 %collective-permute-start.2 = (bf16[1152,128]{1,0:T(8,128)(2,1)S(1)}, bf16[1152,128]{1,0:T(8,128)(2,1)S(1)}, u32[]{:S(2)}, u32[]{:S(2)}) collective-permute-start(bf16[1152,128]{1,0:T(8,128)(2,1)S(1)} %get-tuple-element.8), channel_id=1, source_target_pairs={{0,4},{1,5},{2,6},{3,7},{4,0},{5,1},{6,2},{7,3},{8,12},{9,13},{10,... | collective-permute-start | bytes 884744 | tf_op jit(solution)/shard_map/ppermute | solution.py:313
  15.8 23.6 %all-to-all-start = ((bf16[128,2,896]{2,1,0:T(2,128)(2,1)}), bf16[128,2,896]{2,1,0:T(2,128)(2,1)S(1)}, u32[]{:S(2)}, u32[]{:S(2)}) async-start(bf16[128,2,896]{2,1,0:T(2,128)(2,1)} %get-tuple-element.7), calls=%async_computation | async-start | bytes 917504 | tf_op jit(solution)/shard_map/all_to_all | solution.py:301
  27.2 12.2 %collective-permute-start.4 = (bf16[1152,128]{1,0:T(8,128)(2,1)S(1)}, bf16[1152,128]{1,0:T(8,128)(2,1)S(1)}, u32[]{:S(2)}, u32[]{:S(2)}) collective-permute-start(bf16[1152,128]{1,0:T(8,128)(2,1)S(1)} %collective-permute-done.2.opposite), channel_id=1, source_target_pairs={{0,1},{1,0},{2,3},{3,2},{4,5},{5,4},{6,7},{7,6},{8,9},{9,8},{10,11... | collective-permute-start | bytes 884744 | tf_op jit(solution)/shard_map/ppermute | solution.py:305
  39.4 32.3 %copy-start = (f32[128]{0:T(128)S(1)}, f32[128]{0:T(128)}, u32[]{:S(2)}) copy-start(f32[128]{0:T(128)} %param.23) | copy-start | bytes 1540

commit v20 on v19

--- a/solution.py
+++ b/solution.py
@@ -116,7 +116,7 @@
 
 
 def attend_kernel(
-    got, near, opposite, far, far_opposite, lengths_, frequencies_, gain_, latents, ropes,
+    got, near, last, far, far_last, lengths_, frequencies_, gain_, latents, ropes,
     out, lengths, frequencies, gain, cache, cache_rope,
     sums, lifted, turned, scored, weights, means, sems,
     *, factor, nope,
@@ -167,10 +167,10 @@
     y = tp // 2
     core = lax.rem(tp, 2)
     for i in range(groups):
-        step = (0, half - 1, 1, 2)[i % half]
+        step = (0, half - 1, 2, 1)[i % half]
         head = 2 * lax.rem(y + step, half) + (core if i < half else 1 - core)
         q = sums[head]
-        w = weights_of((near, opposite, far, far_opposite), i)
+        w = weights_of((near, last, far, far_last), i)
         lifted[i] = dot(q[:, :nope].astype(BF16), w[:latent_width, :], NT)
         turned[i] = rotate(q[:, nope : nope + width].astype(BF16).astype(F32), cosine, sine)
     raw = jnp.concatenate([sums[h][0:1, nope + width :] for h in range(groups)], axis=1)
@@ -224,7 +224,7 @@
         mixed = dot(weights[r, :], cache[s], NN) + rounded[r] * new_latent
         means[s] = mixed * inverse[r]
     for i in range(groups):
-        w = weights_of((near, opposite, far, far_opposite), i)
+        w = weights_of((near, last, far, far_last), i)
         x = means[:, i, :].astype(BF16)
         up = dot(x, w[latent_width : 2 * latent_width, :], NN).astype(BF16)
         for k in range(kv_size):
@@ -253,13 +253,13 @@
 
 
 def weights_of(collected, i):
-    near, opposite, far, far_opposite = collected
+    near, last, far, far_last = collected
     places = near.shape[0] + 1
-    stacked, single = (near, opposite) if i < places else (far, far_opposite)
+    stacked, single = (near, last) if i < places else (far, far_last)
     return single if i % places == places - 1 else stacked.at[i % places]
 
 
-def combine_kernel(got, near, opposite, far, far_opposite, out, *, kv_size, groups, local, first):
+def combine_kernel(got, near, last, far, far_last, out, *, kv_size, groups, local, first):
     logs = []
     for k in range(kv_size):
         x = got[k, groups * local :, :].astype(F32)
@@ -275,7 +275,7 @@
         for k in range(kv_size):
             part = got[k, i * local : (i + 1) * local, :].astype(F32)
             head = head + part * shares[k][:, i : i + 1]
-        w = weights_of((near, opposite, far, far_opposite), i)
+        w = weights_of((near, last, far, far_last), i)
         mixed = mixed + dot(head.astype(BF16), w[first:, :], NN)
     mixed = mixed.astype(BF16)
     for d in range(out.shape[0]):
@@ -371,10 +371,10 @@
     )
 
     before, after, opposite = along(own)
-    near = jnp.stack([own, before, after])
+    near = jnp.stack([own, before, opposite])
     far = swap(near)
-    far_opposite = swap(opposite)
-    collected = (near, opposite, far, far_opposite)
+    far_last = swap(after)
+    collected = (near, after, far, far_last)
 
     got = exchange(sent, SPREAD)
     powers = np.arange(0, rope, 2, dtype=np.float64) / rope

time: 73.4 us -> 77.6 us (1.057)
  waiting for transfers between devices: 21.8 us -> 24.8 us
  starting transfers between devices: 14.8 us -> 16 us
    ppermute x3, waiting for transfers between devices: 9.68 us -> 12.7 us  [along(): collected.append(lax.ppermute(own, TP, pairs))]
    ppermute x3, starting transfers between devices: 3.28 us -> 4.73 us  [along(): collected.append(lax.ppermute(own, TP, pairs))]
where the time goes in v20:
time: 77.6 us; the launch traced here: 76.7 us
  blocking collectives  27.4 us (35%)
  waiting for transfers between devices  24.8 us (32%)
  starting transfers between devices  16 us (21%)
  Pallas kernels  8.25 us (11%)
    all_to_all x2, blocking collectives, exchange(): return lax.all_to_all(value, axes, split_axis=0, concat_axis=0, tiled=True)  27.4 us
    ppermute x3, waiting for transfers between devices, along(): collected.append(lax.ppermute(own, TP, pairs))  12.7 us
    all_to_all x1, waiting for transfers between devices, exchange(): return lax.all_to_all(value, axes, split_axis=0, concat_axis=0, tiled=True)  12.2 us
    all_to_all x1, starting transfers between devices, exchange(): return lax.all_to_all(value, axes, split_axis=0, concat_axis=0, tiled=True)  11.1 us
    ppermute x3, starting transfers between devices, along(): collected.append(lax.ppermute(own, TP, pairs))  4.73 us
    pallas_call x1, Pallas kernels, on_device(): pl.pallas_call(functools.partial(attend_kernel, factor=factor, nope=nope)...  4.41 us
    pallas_call x1, Pallas kernels, on_device(): pl.pallas_call(project_kernel, out_shape=(jax.ShapeDtypeStruct((everyone,...  2.61 us
  transfers between devices with their start and end apart: 6, of which 3 were waited for; matrix products, arithmetic and copies ran while one was open for 0% of the time, Pallas kernels for 0%

profile of v20, /device:TPU:0, one launch (start us, length us, event | category | flops | bytes accessed | tf_op | source)
XLA Modules:
  0.0 76.7 jit_solution(676041627913316990)
XLA Ops:
  0.0 2.6 %project.1 = (bf16[128,2,896]{2,1,0:T(2,128)(2,1)}, bf16[1152,128]{1,0:T(8,128)(2,1)S(1)}) custom-call(bf16[64,128]{1,0:T(8,128)(2,1)} %tokens.1, f32[1,128]{1,0:T(1,128)} %bitcast.18, bf16[192,128]{1,0:T(8,128)(2,1)} %bitcast.15, bf16[128,512]{1,0:T(8,128)(2,1)} %wd.1, bf16[64,128]{1,0:T(8,128)(2,1)} %bitcast.16, bf16[1,512,128]{2,1,0:T(8,128)(2,1)} %wk.1, ...), custom_call_target="tpu_custom_call" | custom-call | tf_op jit(solution)/shard_map/project/pallas_call | solution.py:342
  2.6 3.4 %collective-permute-start.1 = (bf16[1152,128]{1,0:T(8,128)(2,1)S(1)}, bf16[1152,128]{1,0:T(8,128)(2,1)S(1)}, u32[]{:S(2)}, u32[]{:S(2)}) collective-permute-start(bf16[1152,128]{1,0:T(8,128)(2,1)S(1)} %get-tuple-element.8), channel_id=1, source_target_pairs={{0,4},{1,5},{2,6},{3,7},{4,0},{5,1},{6,2},{7,3},{8,12},{9,13},{10,... | collective-permute-start | bytes 884744 | tf_op jit(solution)/shard_map/ppermute | solution.py:313
  6.0 0.7 collective-permute-start
  6.7 7.4 %collective-permute-done.1 = bf16[1152,128]{1,0:T(8,128)(2,1)S(1)} collective-permute-done((bf16[1152,128]{1,0:T(8,128)(2,1)S(1)}, bf16[1152,128]{1,0:T(8,128)(2,1)S(1)}, u32[]{:S(2)}, u32[]{:S(2)}) %collective-permute-start.1) | collective-permute-done | bytes 294944 | tf_op jit(solution)/shard_map/ppermute | solution.py:313
  14.1 5.2 %collective-permute-done = bf16[1152,128]{1,0:T(8,128)(2,1)S(1)} collective-permute-done((bf16[1152,128]{1,0:T(8,128)(2,1)S(1)}, bf16[1152,128]{1,0:T(8,128)(2,1)S(1)}, u32[]{:S(2)}, u32[]{:S(2)}) %collective-permute-start) | collective-permute-done | bytes 294944 | tf_op jit(solution)/shard_map/ppermute | solution.py:313
  19.3 0.1 pad_maximum_fusion.near
  19.4 0.1 collective-permute-start.3
  19.5 0.7 collective-permute-start.2
  20.2 11.1 %all-to-all-start = ((bf16[128,2,896]{2,1,0:T(2,128)(2,1)}), bf16[128,2,896]{2,1,0:T(2,128)(2,1)S(1)}, u32[]{:S(2)}, u32[]{:S(2)}) async-start(bf16[128,2,896]{2,1,0:T(2,128)(2,1)} %get-tuple-element.7), calls=%async_computation | async-start | bytes 917504 | tf_op jit(solution)/shard_map/all_to_all | solution.py:301
  31.3 0.0 collective-permute-done.2.last
  31.3 0.1 collective-permute-start.4
  31.4 12.2 %all-to-all-done.got = bf16[128,2,896]{2,1,0:T(2,128)(2,1)S(1)} async-done(((bf16[128,2,896]{2,1,0:T(2,128)(2,1)}), bf16[128,2,896]{2,1,0:T(2,128)(2,1)S(1)}, u32[]{:S(2)}, u32[]{:S(2)}) %all-to-all-start) | async-done | bytes 458784 | tf_op jit(solution)/shard_map/all_to_all | solution.py:301
  43.6 0.0 collective-permute-done.4.far_last
  43.6 0.0 collective-permute-done.3.far
  43.6 0.0 copy-start
  43.6 4.4 %attend.1 = bf16[16,72,128]{2,1,0:T(8,128)(2,1)S(1)} custom-call(bf16[128,2,896]{2,1,0:T(2,128)(2,1)S(1)} %all-to-all-done.got, bf16[3,1152,128]{2,1,0:T(8,128)(2,1)S(1)} %pad_maximum_fusion.near, bf16[1152,128]{1,0:T(8,128)(2,1)S(1)} %collective-permute-done.2.last, bf16[3,1152,128]{2,1,0:T(8,128)(2,1)S(1)} %collective-permute-done.3.far, ...), custom_call_target="tpu_custom_call" | custom-call | tf_op jit(solution)/shard_map/attend/pallas_call | solution.py:382
  48.0 13.1 %all_to_all.15.got = bf16[16,72,128]{2,1,0:T(8,128)(2,1)S(1)} all-to-all(bf16[16,72,128]{2,1,0:T(8,128)(2,1)S(1)} %attend.1), channel_id=1, replica_groups=mesh['kv_0'=4,'kv_1'=4,'y'=4,'core'=2] {'kv_0','kv_1'}, dimensions={0} | all-to-all | bytes 589824 | tf_op jit(solution)/shard_map/all_to_all | solution.py:301
  61.1 0.5 combine.1
  61.6 14.3 %all_to_all.16.got = bf16[128,8,128]{2,1,0:T(8,128)(2,1)S(1)} all-to-all(bf16[128,8,128]{2,1,0:T(8,128)(2,1)S(1)} %combine.1), channel_id=1, replica_groups=mesh['kv_0'=4,'kv_1'=4,'y'=4,'core'=2] {'core','kv_0','kv_1','y'}, dimensions={0} | all-to-all | bytes 524288 | tf_op jit(solution)/shard_map/all_to_all | solution.py:301
  75.9 0.0 copy-done
  75.9 0.8 finish.1
Async XLA Ops:
  2.6 11.5 %collective-permute-start.1 = (bf16[1152,128]{1,0:T(8,128)(2,1)S(1)}, bf16[1152,128]{1,0:T(8,128)(2,1)S(1)}, u32[]{:S(2)}, u32[]{:S(2)}) collective-permute-start(bf16[1152,128]{1,0:T(8,128)(2,1)S(1)} %get-tuple-element.8), channel_id=1, source_target_pairs={{0,4},{1,5},{2,6},{3,7},{4,0},{5,1},{6,2},{7,3},{8,12},{9,13},{10,... | collective-permute-start | bytes 884744 | tf_op jit(solution)/shard_map/ppermute | solution.py:313
  6.0 13.3 %collective-permute-start = (bf16[1152,128]{1,0:T(8,128)(2,1)S(1)}, bf16[1152,128]{1,0:T(8,128)(2,1)S(1)}, u32[]{:S(2)}, u32[]{:S(2)}) collective-permute-start(bf16[1152,128]{1,0:T(8,128)(2,1)S(1)} %get-tuple-element.8), channel_id=1, source_target_pairs={{0,2},{1,3},{2,4},{3,5},{4,6},{5,7},{6,0},{7,1},{8,10},{9,11},{10,... | collective-permute-start | bytes 884744 | tf_op jit(solution)/shard_map/ppermute | solution.py:313
  19.4 24.1 %collective-permute-start.3 = (bf16[3,1152,128]{2,1,0:T(8,128)(2,1)S(1)}, bf16[3,1152,128]{2,1,0:T(8,128)(2,1)S(1)}, u32[]{:S(2)}, u32[]{:S(2)}) collective-permute-start(bf16[3,1152,128]{2,1,0:T(8,128)(2,1)S(1)} %pad_maximum_fusion.near), channel_id=1, source_target_pairs={{0,1},{1,0},{2,3},{3,2},{4,5},{5,4},{6,7},{7,6},{8,9},{9,8},{10,11... | collective-permute-start | bytes 2654216 | tf_op jit(solution)/shard_map/ppermute | solution.py:305
  19.5 11.8 %collective-permute-start.2 = (bf16[1152,128]{1,0:T(8,128)(2,1)S(1)}, bf16[1152,128]{1,0:T(8,128)(2,1)S(1)}, u32[]{:S(2)}, u32[]{:S(2)}) collective-permute-start(bf16[1152,128]{1,0:T(8,128)(2,1)S(1)} %get-tuple-element.8), channel_id=1, source_target_pairs={{0,6},{1,7},{2,0},{3,1},{4,2},{5,3},{6,4},{7,5},{8,14},{9,15},{10,... | collective-permute-start | bytes 884744 | tf_op jit(solution)/shard_map/ppermute | solution.py:313
  20.2 23.4 %all-to-all-start = ((bf16[128,2,896]{2,1,0:T(2,128)(2,1)}), bf16[128,2,896]{2,1,0:T(2,128)(2,1)S(1)}, u32[]{:S(2)}, u32[]{:S(2)}) async-start(bf16[128,2,896]{2,1,0:T(2,128)(2,1)} %get-tuple-element.7), calls=%async_computation | async-start | bytes 917504 | tf_op jit(solution)/shard_map/all_to_all | solution.py:301
  31.3 12.2 %collective-permute-start.4 = (bf16[1152,128]{1,0:T(8,128)(2,1)S(1)}, bf16[1152,128]{1,0:T(8,128)(2,1)S(1)}, u32[]{:S(2)}, u32[]{:S(2)}) collective-permute-start(bf16[1152,128]{1,0:T(8,128)(2,1)S(1)} %collective-permute-done.2.last), channel_id=1, source_target_pairs={{0,1},{1,0},{2,3},{3,2},{4,5},{5,4},{6,7},{7,6},{8,9},{9,8},{10,11... | collective-permute-start | bytes 884744 | tf_op jit(solution)/shard_map/ppermute | solution.py:305
  43.6 32.3 %copy-start = (f32[128]{0:T(128)S(1)}, f32[128]{0:T(128)}, u32[]{:S(2)}) copy-start(f32[128]{0:T(128)} %param.23) | copy-start | bytes 1540

commit v21 on v19

--- a/solution.py
+++ b/solution.py
@@ -13,7 +13,7 @@
 KV = ("kv_0", "kv_1")
 TP = ("y", "core")
 ALL = KV + TP
-SPREAD = ("core",) + KV + ("y",)
+SPREAD = ("core", "kv_0", "y", "kv_1")
 EPSILON = 1e-06
 NEGATIVE = -1e30
 F32 = jnp.float32
@@ -51,9 +51,11 @@
     return lax.broadcasted_iota(jnp.int32, shape, 0)
 
 
-def block_of(kv, tp, kv_size):
+def block_of(kv, tp):
     cores = lax.axis_size("core")
-    return (tp % cores * kv_size + kv) * lax.axis_size("y") + tp // cores
+    inner = lax.axis_size("kv_1")
+    outer = tp % cores * lax.axis_size("kv_0") + kv // inner
+    return (outer * lax.axis_size("y") + tp // cores) * inner + kv % inner
 
 
 def project_kernel(
@@ -102,7 +104,7 @@
             r = t * local + j
             new = jnp.concatenate([fresh[r : r + 1], nothing], axis=0).astype(BF16)
             for c in range(kv_size // local):
-                b = block_of(c * local + j, t, kv_size)
+                b = block_of(c * local + j, t)
                 for n, tile in enumerate(tiles + [new]):
                     out[b, :, n * 128 : (n + 1) * 128] = tile
     for copy in copies[5:]:
@@ -141,9 +143,9 @@
         b.start()
         copies.append((a, b))
     for h in range(groups):
-        total = got[block_of(0, h, kv_size)].astype(F32)
+        total = got[block_of(0, h)].astype(F32)
         for k in range(1, kv_size):
-            total = total + got[block_of(k, h, kv_size)].astype(F32)
+            total = total + got[block_of(k, h)].astype(F32)
         pieces = [total[:, n * 128 : (n + 1) * 128] for n in range(7)]
         turn = jnp.concatenate(pieces[4:6], axis=0)
         sums[h, :, :nope] = jnp.concatenate(pieces[:4], axis=0)
@@ -288,10 +290,10 @@
     for t in range(groups):
         squares = jnp.zeros((local, width), F32)
         for k in range(kv_size):
-            x = got[block_of(k, t, kv_size)].astype(F32)
+            x = got[block_of(k, t)].astype(F32)
             squares = squares + x * x
         mean = jnp.sum(squares, axis=1, keepdims=True) / (width * kv_size)
-        own = got[block_of(kv, t, kv_size)].astype(F32)
+        own = got[block_of(kv, t)].astype(F32)
         out[t * local : (t + 1) * local, :] = (
             own * lax.rsqrt(mean + EPSILON) * gain[...]
         ).astype(BF16)

time: 73.4 us -> 73.6 us (level)
  no operation moved by 1% of the time
where the time goes in v21:
time: 73.6 us; the launch traced here: 72.6 us
  blocking collectives  27.3 us (37%)
  waiting for transfers between devices  22.1 us (30%)
  starting transfers between devices  14.8 us (20%)
  Pallas kernels  8.25 us (11%)
    all_to_all x2, blocking collectives, exchange(): return lax.all_to_all(value, axes, split_axis=0, concat_axis=0, tiled=True)  27.3 us
    all_to_all x1, waiting for transfers between devices, exchange(): return lax.all_to_all(value, axes, split_axis=0, concat_axis=0, tiled=True)  12.4 us
    all_to_all x1, starting transfers between devices, exchange(): return lax.all_to_all(value, axes, split_axis=0, concat_axis=0, tiled=True)  11.4 us
    ppermute x3, waiting for transfers between devices, along(): collected.append(lax.ppermute(own, TP, pairs))  9.68 us
    pallas_call x1, Pallas kernels, on_device(): pl.pallas_call(functools.partial(attend_kernel, factor=factor, nope=nope)...  4.41 us
    ppermute x3, starting transfers between devices, along(): collected.append(lax.ppermute(own, TP, pairs))  3.28 us
    pallas_call x1, Pallas kernels, on_device(): pl.pallas_call(project_kernel, out_shape=(jax.ShapeDtypeStruct((everyone,...  2.61 us
  transfers between devices with their start and end apart: 6, of which 3 were waited for; matrix products, arithmetic and copies ran while one was open for 0% of the time, Pallas kernels for 0%

profile of v21, /device:TPU:0, one launch (start us, length us, event | category | flops | bytes accessed | tf_op | source)
XLA Modules:
  0.0 72.6 jit_solution(8010532159874613874)
XLA Ops:
  0.0 2.6 %project.1 = (bf16[128,2,896]{2,1,0:T(2,128)(2,1)}, bf16[1152,128]{1,0:T(8,128)(2,1)S(1)}) custom-call(bf16[64,128]{1,0:T(8,128)(2,1)} %tokens.1, f32[1,128]{1,0:T(1,128)} %bitcast.18, bf16[192,128]{1,0:T(8,128)(2,1)} %bitcast.15, bf16[128,512]{1,0:T(8,128)(2,1)} %wd.1, bf16[64,128]{1,0:T(8,128)(2,1)} %bitcast.16, bf16[1,512,128]{2,1,0:T(8,128)(2,1)} %wk.1, ...), custom_call_target="tpu_custom_call" | custom-call | tf_op jit(solution)/shard_map/project/pallas_call | solution.py:344
  2.6 3.2 %collective-permute-start.1 = (bf16[1152,128]{1,0:T(8,128)(2,1)S(1)}, bf16[1152,128]{1,0:T(8,128)(2,1)S(1)}, u32[]{:S(2)}, u32[]{:S(2)}) collective-permute-start(bf16[1152,128]{1,0:T(8,128)(2,1)S(1)} %get-tuple-element.8), channel_id=1, source_target_pairs={{0,6},{1,7},{2,0},{3,1},{4,2},{5,3},{6,4},{7,5},{8,14},{9,15},{10,... | collective-permute-start | bytes 884744 | tf_op jit(solution)/shard_map/ppermute | solution.py:315
  5.8 0.0 collective-permute-start
  5.8 6.3 %collective-permute-done.1 = bf16[1152,128]{1,0:T(8,128)(2,1)S(1)} collective-permute-done((bf16[1152,128]{1,0:T(8,128)(2,1)S(1)}, bf16[1152,128]{1,0:T(8,128)(2,1)S(1)}, u32[]{:S(2)}, u32[]{:S(2)}) %collective-permute-start.1) | collective-permute-done | bytes 294944 | tf_op jit(solution)/shard_map/ppermute | solution.py:315
  12.1 3.4 %collective-permute-done = bf16[1152,128]{1,0:T(8,128)(2,1)S(1)} collective-permute-done((bf16[1152,128]{1,0:T(8,128)(2,1)S(1)}, bf16[1152,128]{1,0:T(8,128)(2,1)S(1)}, u32[]{:S(2)}, u32[]{:S(2)}) %collective-permute-start) | collective-permute-done | bytes 294944 | tf_op jit(solution)/shard_map/ppermute | solution.py:315
  15.5 0.1 pad_maximum_fusion.near
  15.6 0.1 collective-permute-start.3
  15.7 0.1 collective-permute-start.2
  15.8 11.4 %all-to-all-start = ((bf16[128,2,896]{2,1,0:T(2,128)(2,1)}), bf16[128,2,896]{2,1,0:T(2,128)(2,1)S(1)}, u32[]{:S(2)}, u32[]{:S(2)}) async-start(bf16[128,2,896]{2,1,0:T(2,128)(2,1)} %get-tuple-element.7), calls=%async_computation | async-start | bytes 917504 | tf_op jit(solution)/shard_map/all_to_all | solution.py:303
  27.2 0.0 collective-permute-done.2.opposite
  27.2 0.1 collective-permute-start.4
  27.3 12.4 %all-to-all-done.got = bf16[128,2,896]{2,1,0:T(2,128)(2,1)S(1)} async-done(((bf16[128,2,896]{2,1,0:T(2,128)(2,1)}), bf16[128,2,896]{2,1,0:T(2,128)(2,1)S(1)}, u32[]{:S(2)}, u32[]{:S(2)}) %all-to-all-start) | async-done | bytes 458784 | tf_op jit(solution)/shard_map/all_to_all | solution.py:303
  39.7 0.0 collective-permute-done.4.far_opposite
  39.7 0.0 collective-permute-done.3.far
  39.7 0.0 copy-start
  39.7 4.4 %attend.1 = bf16[16,72,128]{2,1,0:T(8,128)(2,1)S(1)} custom-call(bf16[128,2,896]{2,1,0:T(2,128)(2,1)S(1)} %all-to-all-done.got, bf16[3,1152,128]{2,1,0:T(8,128)(2,1)S(1)} %pad_maximum_fusion.near, bf16[1152,128]{1,0:T(8,128)(2,1)S(1)} %collective-permute-done.2.opposite, bf16[3,1152,128]{2,1,0:T(8,128)(2,1)S(1)} %collective-permute-done.3.far, ...), custom_call_target="tpu_custom_call" | custom-call | tf_op jit(solution)/shard_map/attend/pallas_call | solution.py:384
  44.1 12.7 %all_to_all.15.got = bf16[16,72,128]{2,1,0:T(8,128)(2,1)S(1)} all-to-all(bf16[16,72,128]{2,1,0:T(8,128)(2,1)S(1)} %attend.1), channel_id=1, replica_groups=mesh['kv_0'=4,'kv_1'=4,'y'=4,'core'=2] {'kv_0','kv_1'}, dimensions={0} | all-to-all | bytes 589824 | tf_op jit(solution)/shard_map/all_to_all | solution.py:303
  56.9 0.5 combine.1
  57.4 14.5 %all_to_all.16.got = bf16[128,8,128]{2,1,0:T(8,128)(2,1)S(1)} all-to-all(bf16[128,8,128]{2,1,0:T(8,128)(2,1)S(1)} %combine.1), channel_id=1, replica_groups=mesh['kv_0'=4,'kv_1'=4,'y'=4,'core'=2] {'core','kv_0','y','kv_1'}, dimensions={0} | all-to-all | bytes 524288 | tf_op jit(solution)/shard_map/all_to_all | solution.py:303
  71.9 0.0 copy-done
  71.9 0.8 %finish.1 = bf16[64,128]{1,0:T(8,128)(2,1)} custom-call(bf16[128,8,128]{2,1,0:T(8,128)(2,1)S(1)} %all_to_all.16.got, f32[1,128]{1,0:T(1,128)S(1)} %bitcast.11), custom_call_target="tpu_custom_call" | custom-call | tf_op jit(solution)/shard_map/finish/pallas_call | solution.py:433
Async XLA Ops:
  2.6 9.5 %collective-permute-start.1 = (bf16[1152,128]{1,0:T(8,128)(2,1)S(1)}, bf16[1152,128]{1,0:T(8,128)(2,1)S(1)}, u32[]{:S(2)}, u32[]{:S(2)}) collective-permute-start(bf16[1152,128]{1,0:T(8,128)(2,1)S(1)} %get-tuple-element.8), channel_id=1, source_target_pairs={{0,6},{1,7},{2,0},{3,1},{4,2},{5,3},{6,4},{7,5},{8,14},{9,15},{10,... | collective-permute-start | bytes 884744 | tf_op jit(solution)/shard_map/ppermute | solution.py:315
  5.8 9.7 %collective-permute-start = (bf16[1152,128]{1,0:T(8,128)(2,1)S(1)}, bf16[1152,128]{1,0:T(8,128)(2,1)S(1)}, u32[]{:S(2)}, u32[]{:S(2)}) collective-permute-start(bf16[1152,128]{1,0:T(8,128)(2,1)S(1)} %get-tuple-element.8), channel_id=1, source_target_pairs={{0,2},{1,3},{2,4},{3,5},{4,6},{5,7},{6,0},{7,1},{8,10},{9,11},{10,... | collective-permute-start | bytes 884744 | tf_op jit(solution)/shard_map/ppermute | solution.py:315
  15.6 24.1 %collective-permute-start.3 = (bf16[3,1152,128]{2,1,0:T(8,128)(2,1)S(1)}, bf16[3,1152,128]{2,1,0:T(8,128)(2,1)S(1)}, u32[]{:S(2)}, u32[]{:S(2)}) collective-permute-start(bf16[3,1152,128]{2,1,0:T(8,128)(2,1)S(1)} %pad_maximum_fusion.near), channel_id=1, source_target_pairs={{0,1},{1,0},{2,3},{3,2},{4,5},{5,4},{6,7},{7,6},{8,9},{9,8},{10,11... | collective-permute-start | bytes 2654216 | tf_op jit(solution)/shard_map/ppermute | solution.py:307
  15.7 11.5 %collective-permute-start.2 = (bf16[1152,128]{1,0:T(8,128)(2,1)S(1)}, bf16[1152,128]{1,0:T(8,128)(2,1)S(1)}, u32[]{:S(2)}, u32[]{:S(2)}) collective-permute-start(bf16[1152,128]{1,0:T(8,128)(2,1)S(1)} %get-tuple-element.8), channel_id=1, source_target_pairs={{0,4},{1,5},{2,6},{3,7},{4,0},{5,1},{6,2},{7,3},{8,12},{9,13},{10,... | collective-permute-start | bytes 884744 | tf_op jit(solution)/shard_map/ppermute | solution.py:315
  15.8 23.9 %all-to-all-start = ((bf16[128,2,896]{2,1,0:T(2,128)(2,1)}), bf16[128,2,896]{2,1,0:T(2,128)(2,1)S(1)}, u32[]{:S(2)}, u32[]{:S(2)}) async-start(bf16[128,2,896]{2,1,0:T(2,128)(2,1)} %get-tuple-element.7), calls=%async_computation | async-start | bytes 917504 | tf_op jit(solution)/shard_map/all_to_all | solution.py:303
  27.2 12.5 %collective-permute-start.4 = (bf16[1152,128]{1,0:T(8,128)(2,1)S(1)}, bf16[1152,128]{1,0:T(8,128)(2,1)S(1)}, u32[]{:S(2)}, u32[]{:S(2)}) collective-permute-start(bf16[1152,128]{1,0:T(8,128)(2,1)S(1)} %collective-permute-done.2.opposite), channel_id=1, source_target_pairs={{0,1},{1,0},{2,3},{3,2},{4,5},{5,4},{6,7},{7,6},{8,9},{9,8},{10,11... | collective-permute-start | bytes 884744 | tf_op jit(solution)/shard_map/ppermute | solution.py:307
  39.7 32.2 %copy-start = (f32[128]{0:T(128)S(1)}, f32[128]{0:T(128)}, u32[]{:S(2)}) copy-start(f32[128]{0:T(128)} %param.23) | copy-start | bytes 1540
